TPU v7x, 512 devices: a whole 4x4x16 slice. The times are simulated.
512 devices in a mesh: ep: 16 (over y, x), tp: 32 (over z, core).
Axes of the slice: x: 4, y: 4, z: 16, core: 2. Of those that a mesh axis runs over, the one named last changes fastest.
Arguments:
- tokens: bfloat16 [3072, 4096], P('ep', 'tp'), may hold values from -6 to 6
- cotangent: bfloat16 [3072, 4096], P('ep', 'tp'), may hold values from -4 to 4
- routes: int32 [3072, 2], P('ep'), may hold values from 0 to 31, all different within a row; in each aligned block of 192 rows (0 to 191, 192 to 383, ...) at most 18 rows name the same one
- gate_weights: bfloat16 [3072, 2], P('ep'), may hold values from 0.099609375 to 2.5
- expert_gate: bfloat16 [32, 4096, 1024], P('ep', 'tp'), may hold values from -0.09375 to 0.09375
- expert_up: bfloat16 [32, 4096, 1024], P('ep', 'tp'), may hold values from -0.09375 to 0.09375
- expert_down: bfloat16 [32, 4096, 1024], P('ep', 'tp'), may hold values from -0.1875 to 0.1875
- shared_gate: bfloat16 [4096, 1024], P('tp'), may hold values from -0.09375 to 0.09375
- shared_up: bfloat16 [4096, 1024], P('tp'), may hold values from -0.09375 to 0.09375
- shared_down: bfloat16 [4096, 1024], P('tp'), may hold values from -0.1875 to 0.1875
Outputs:
- token_grad: bfloat16 [3072, 4096], P('ep', 'tp')
- gate_grad: bfloat16 [3072, 2], P('ep')
- expert_grads: bfloat16 [3, 32, 4096, 1024], P(None, 'ep', 'tp')
- shared_grads: float32 [3, 4096, 1024], P(None, 'tp', 'ep')
- expert_norms: float32 [3, 32, 1024], P(None, 'ep')
- shared_norms: float32 [3, 1024], P(None, 'ep')
Inputs may be any that keep to these rules, and one draw needn't show every extreme that they name: `routes`: each row names 2 different experts. In each aligned block of 192 rows no expert is named by more than 18 rows, a bound that some block reaches.
All inputs are finite; a program needn't handle non-finite values.
Results may differ from a plain program's by a relative error of at most 0.0069.
Values may be sent and summed in bfloat16 or wider, within the bound.
No kernel may reach another device: no remote copies, remote signals or barrier semaphores. Data moves between devices by JAX's collectives and lax.ppermute only.
A program may use at most 64 MiB of HBM per device.

v0:
```python
import math

import jax
import jax.numpy as jnp
from jax import lax
from jax.sharding import PartitionSpec as P


def side_by_side(arrays, axis, split_dim, concat_dim, along):
    widths = [math.prod(a.shape[along:]) for a in arrays]
    both = jnp.concatenate(
        [a.reshape(*a.shape[:along], w) for a, w in zip(arrays, widths)], axis=along
    )
    filled = lax.all_to_all(both, axis, split_axis=split_dim, concat_axis=concat_dim, tiled=True)
    parts = jnp.split(filled, [sum(widths[:k]) for k in range(1, len(widths))], axis=along)
    return tuple(
        (b.reshape(*filled.shape[:along], *a.shape[along:]) for a, b in zip(arrays, parts))
    )


def side_by_side_2(arrays, axis, dim, along):
    columns = [a.reshape(*a.shape[:along], -1) for a in arrays]
    both = jnp.concatenate(columns, axis=along)
    filled, at, outs = (lax.all_gather(both, axis, axis=dim, tiled=True), 0, [])
    for a, column in zip(arrays, columns):
        share = filled[..., at : at + column.shape[along]]
        outs.append(share.reshape(*share.shape[:along], *a.shape[along:]))
        at += column.shape[along]
    return tuple(outs)


def split_up(x, dim, count):
    before, after = (x.shape[:dim], x.shape[dim + 1 :])
    return jnp.moveaxis(x.reshape(*before, count, -1, *after), dim, 0)


def sum_at_owner(x, axis, dim):
    count = lax.axis_size(axis)
    parts = lax.all_to_all(split_up(x, dim, count), axis, 0, 0, tiled=True)
    return jnp.sum(parts, axis=0)


def copy_for_each(x, axis):
    count = lax.axis_size(axis)
    return lax.all_to_all(jnp.broadcast_to(x[None], (count, *x.shape)), axis, 0, 0, tiled=True)


def over_copies(x, axis):
    everything = copy_for_each(x, axis)
    return jnp.sum(everything, axis=0)


def packed_total(arrays, axis):
    line, at, outs = (jnp.concatenate([a.reshape(-1) for a in arrays]), 0, [])
    so_far = over_copies(line, axis)
    for a in arrays:
        outs.append(so_far[at : at + a.size].reshape(a.shape))
        at += a.size
    return tuple(outs)


def row_backward(summed, weights):
    hidden = summed.shape[1] // 3
    pre_gate = summed[:, :hidden]
    pre_up = summed[:, hidden : 2 * hidden]
    back_act = summed[:, 2 * hidden :]
    sigmoid_gate = jax.nn.sigmoid(pre_gate)
    silu_gate = pre_gate * sigmoid_gate
    activation = silu_gate * pre_up
    act_grad = weights[:, None] * back_act
    grad_up = (act_grad * silu_gate).astype(jnp.bfloat16)
    grad_gate = (act_grad * pre_up * sigmoid_gate * (1.0 + pre_gate * (1.0 - sigmoid_gate))).astype(
        jnp.bfloat16
    )
    scaled_act = (weights[:, None] * activation).astype(jnp.bfloat16)
    weight_grad = jnp.sum(activation * back_act, axis=1).astype(jnp.bfloat16)
    return (grad_gate, grad_up, scaled_act, weight_grad)


def body(
    tokens,
    cotangent,
    routes,
    gate_weights,
    expert_gate,
    expert_up,
    expert_down,
    shared_gate,
    shared_up,
    shared_down,
):
    groups = lax.axis_size("ep")
    tp_lanes = lax.axis_size("tp")
    rows_here, feat_width = tokens.shape
    choose = routes.shape[1]
    local_experts = expert_gate.shape[0]
    hidden = expert_gate.shape[2]
    experts = local_experts * groups
    capacity = 3 * rows_here * choose // (2 * experts)
    total_slots = experts * capacity
    flat_expert = routes.reshape(-1)
    onehot = (flat_expert[:, None] == jnp.arange(experts, dtype=jnp.int32)[None, :]).astype(
        jnp.int32
    )
    position = jnp.sum((jnp.cumsum(onehot, axis=0) - onehot) * onehot, axis=1)
    slot_index = flat_expert * capacity + position
    owner_row = jnp.arange(rows_here * choose, dtype=jnp.int32) // choose
    slot_token = jnp.zeros((total_slots,), jnp.int32).at[slot_index].set(owner_row)
    slot_live = (
        jnp.zeros((total_slots,), jnp.bfloat16)
        .at[slot_index]
        .set(jnp.ones((rows_here * choose,), jnp.bfloat16))
    )
    slot_weight = (
        jnp.zeros((total_slots,), jnp.bfloat16).at[slot_index].set(gate_weights.reshape(-1))
    )
    send_tokens = (tokens[slot_token] * slot_live[:, None]).reshape(
        groups, local_experts * capacity, feat_width
    )
    send_cotan = (cotangent[slot_token] * slot_live[:, None]).reshape(
        groups, local_experts * capacity, feat_width
    )
    recv_tokens, recv_cotan, recv_weight = side_by_side(
        (send_tokens, send_cotan, slot_weight.reshape(groups, local_experts * capacity)),
        "ep",
        0,
        0,
        2,
    )
    in_tokens = recv_tokens.reshape(groups, local_experts, capacity, feat_width)
    in_cotan = recv_cotan.reshape(groups, local_experts, capacity, feat_width)

    def project(row_block, weight):
        return jnp.einsum(
            "secd,edf->secf", row_block, weight, preferred_element_type=jnp.float32
        ).reshape(total_slots, hidden)

    pre_gate = jnp.concatenate(
        [
            project(in_tokens, expert_gate),
            jnp.dot(tokens, shared_gate, preferred_element_type=jnp.float32),
        ],
        axis=0,
    )
    pre_up = jnp.concatenate(
        [
            project(in_tokens, expert_up),
            jnp.dot(tokens, shared_up, preferred_element_type=jnp.float32),
        ],
        axis=0,
    )
    pre_back = jnp.concatenate(
        [
            project(in_cotan, expert_down),
            jnp.dot(cotangent, shared_down, preferred_element_type=jnp.float32),
        ],
        axis=0,
    )
    partials = jnp.concatenate([pre_gate, pre_up, pre_back], axis=1).astype(jnp.bfloat16)
    all_rows = partials.shape[0]
    piece = all_rows // tp_lanes
    weights = jnp.concatenate(
        [recv_weight.reshape(-1).astype(jnp.float32), jnp.ones((rows_here,), jnp.float32)]
    )
    arrived = lax.all_to_all(
        partials.reshape(tp_lanes, piece, 3 * hidden), "tp", split_axis=0, concat_axis=0, tiled=True
    )
    share = jnp.sum(arrived.astype(jnp.float32), axis=0)
    own_weights = lax.dynamic_slice_in_dim(weights, lax.axis_index("tp") * piece, piece)
    part_gate, part_up, part_scaled, part_weight = row_backward(share, own_weights)
    grad_gate, grad_up, scaled_act, weight_grad = side_by_side_2(
        (part_gate, part_up, part_scaled, part_weight), "tp", 0, 1
    )
    routed_gate = grad_gate[:total_slots].reshape(groups, local_experts, capacity, hidden)
    routed_up = grad_up[:total_slots].reshape(groups, local_experts, capacity, hidden)
    routed_scaled = scaled_act[:total_slots].reshape(groups, local_experts, capacity, hidden)
    slot_grad = (
        jnp.einsum("secf,edf->secd", routed_gate, expert_gate, preferred_element_type=jnp.float32)
        + jnp.einsum("secf,edf->secd", routed_up, expert_up, preferred_element_type=jnp.float32)
    ).astype(jnp.bfloat16)
    back_rows, back_weight = side_by_side(
        (
            slot_grad.reshape(groups, local_experts * capacity, feat_width),
            weight_grad[:total_slots].reshape(groups, local_experts * capacity),
        ),
        "ep",
        0,
        0,
        2,
    )
    routed_sum = jnp.sum(
        back_rows.reshape(total_slots, feat_width)[slot_index]
        .astype(jnp.float32)
        .reshape(rows_here, choose, feat_width),
        axis=1,
    )
    shared_gg = grad_gate[total_slots:]
    shared_gu = grad_up[total_slots:]
    shared_sa = scaled_act[total_slots:]
    shared_part = jnp.einsum(
        "tf,df->td", shared_gg, shared_gate, preferred_element_type=jnp.float32
    ) + jnp.einsum("tf,df->td", shared_gu, shared_up, preferred_element_type=jnp.float32)
    token_grad = (routed_sum + shared_part).astype(jnp.bfloat16)
    gate_grad = back_weight.reshape(-1)[slot_index].reshape(rows_here, choose)
    expert_stack = jnp.stack(
        [
            jnp.einsum(
                "secd,secf->edf", in_tokens, routed_gate, preferred_element_type=jnp.float32
            ),
            jnp.einsum("secd,secf->edf", in_tokens, routed_up, preferred_element_type=jnp.float32),
            jnp.einsum(
                "secd,secf->edf", in_cotan, routed_scaled, preferred_element_type=jnp.float32
            ),
        ]
    )
    shared_stack = jnp.stack(
        [
            jnp.einsum("td,tf->df", tokens, shared_gg, preferred_element_type=jnp.float32),
            jnp.einsum("td,tf->df", tokens, shared_gu, preferred_element_type=jnp.float32),
            jnp.einsum("td,tf->df", cotangent, shared_sa, preferred_element_type=jnp.float32),
        ]
    )
    shared_summed = sum_at_owner(shared_stack, "ep", 2)
    expert_sq = jnp.sum(expert_stack * expert_stack, axis=2)
    shared_sq = jnp.sum(shared_summed * shared_summed, axis=1)
    expert_norms, shared_norms = packed_total((expert_sq, shared_sq), "tp")
    inverse_width = 1.0 / (feat_width * tp_lanes)
    return (
        token_grad,
        gate_grad,
        expert_stack.astype(jnp.bfloat16),
        shared_summed,
        expert_norms * inverse_width,
        shared_norms * inverse_width,
    )


def solution(mesh):
    return jax.shard_map(
        body,
        mesh=mesh,
        in_specs=(
            P("ep", "tp"),
            P("ep", "tp"),
            P("ep", None),
            P("ep", None),
            P("ep", "tp", None),
            P("ep", "tp", None),
            P("ep", "tp", None),
            P("tp", None),
            P("tp", None),
            P("tp", None),
        ),
        out_specs=(
            P("ep", "tp"),
            P("ep", None),
            P(None, "ep", "tp", None),
            P(None, "tp", "ep"),
            P(None, "ep", None),
            P(None, "ep"),
        ),
        check_vma=False,
    )
```

profile of v0, /device:TPU:1, one launch (start us, length us, event | category | flops | bytes accessed | tf_op | source)
XLA Modules:
  0.0 467.0 jit_solution(5999173458967010335)
XLA Ops:
  11.6 3.0 scatter_custom_fusion.2
  14.6 3.0 scatter_custom_fusion.1
  17.6 2.9 scatter_custom_fusion
  20.6 1.9 gather_fusion.1
  22.6 1.9 gather_fusion
  25.9 7.6 %all-to-all-start = ((bf16[16,36,257]{2,1,0:T(8,128)(2,1)}), bf16[16,36,257]{2,1,0:T(8,128)(2,1)S(1)}, u32[]{:S(2)}, u32[]{:S(2)}) async-start(bf16[16,36,257]{2,1,0:T(8,128)(2,1)} %pad_maximum_fusion.5), calls=%async_computation | async-start | bytes 983040 | tf_op jit(solution)/shard_map/all_to_all | solution.py:14
  33.5 1.0 convolution_convert_fusion.3
  34.8 1.0 convolution_convert_fusion.4
  35.8 6.5 %all-to-all-done = bf16[16,36,257]{2,1,0:T(8,128)(2,1)S(1)} async-done(((bf16[16,36,257]{2,1,0:T(8,128)(2,1)}), bf16[16,36,257]{2,1,0:T(8,128)(2,1)S(1)}, u32[]{:S(2)}, u32[]{:S(2)}) %all-to-all-start) | async-done | bytes 296096 | tf_op jit(solution)/shard_map/all_to_all | solution.py:14
  43.1 1.2 reshape.176
  45.0 1.2 reshape.174
  46.3 1.6 fusion.5
  48.1 1.2 reshape.173
  49.3 1.6 pad_maximum_fusion.4
  51.2 1.1 copy-done.7
  52.5 2.4 pad_maximum_fusion
  54.8 18.6 %all-to-all-start.1 = ((bf16[32,24,3072]{2,1,0:T(8,128)(2,1)}), bf16[32,24,3072]{2,1,0:T(8,128)(2,1)}, u32[]{:S(2)}, u32[]{:S(2)}) async-start(bf16[32,24,3072]{2,1,0:T(8,128)(2,1)} %pad_maximum_fusion), calls=%async_computation.1 | async-start | bytes 9437184 | tf_op jit(solution)/shard_map/all_to_all | solution.py:165
  73.9 204.3 %all-to-all-done.1 = bf16[32,24,3072]{2,1,0:T(8,128)(2,1)} async-done(((bf16[32,24,3072]{2,1,0:T(8,128)(2,1)}), bf16[32,24,3072]{2,1,0:T(8,128)(2,1)}, u32[]{:S(2)}, u32[]{:S(2)}) %all-to-all-start.1) | async-done | bytes 4718624 | tf_op jit(solution)/shard_map/all_to_all | solution.py:165
  278.2 3.2 convert_reduce_fusion
  282.4 71.1 %all-gather.2.cloned.1.call-done = bf16[768,3073]{1,0:T(8,128)(2,1)} async-done(((bf16[24,3073]{1,0:T(8,128)(2,1)}), bf16[768,3073]{1,0:T(8,128)(2,1)}) %all-gather.2.cloned.1.call-update) | async-done | bytes 4720144 | tf_op jit(solution)/shard_map/all_gather | solution.py:24
  353.5 1.3 fusion.27
  354.8 1.3 fusion.32
  356.2 1.3 fusion.29
  357.5 1.3 maximum_bitcast_fusion
  358.8 6.5 %all-to-all-start.3 = ((f32[16,3,128,64]{2,3,1,0:T(8,128)}), f32[16,3,128,64]{2,3,1,0:T(8,128)}, u32[]{:S(2)}, u32[]{:S(2)}) async-start(f32[16,3,128,64]{2,3,1,0:T(8,128)} %maximum_bitcast_fusion), calls=%async_computation.3 | async-start | bytes 3145728 | tf_op jit(solution)/shard_map/all_to_all | solution.py:39
  365.3 3.9 fusion.54
  369.1 1.4 reshape.178
  370.6 1.4 fusion.1
  372.0 1.1 slice_reduce_fusion.2
  373.2 0.9 copy.116
  374.1 2.5 reshape.182
  376.6 2.4 reshape.177
  379.0 2.1 fusion.17
  381.1 0.9 convolution_bitcast_fusion.1
  386.0 1.2 reshape.261
  387.2 2.6 all-to-all-done.3
  389.8 3.9 all-to-all-start.2
  393.7 1.5 reduce_sum.79
  395.4 5.3 %all-to-all-done.2 = bf16[16,2,2322]{2,1,0:T(2,128)(2,1)S(1)} async-done(((bf16[16,2,2322]{2,1,0:T(2,128)(2,1)}), bf16[16,2,2322]{2,1,0:T(2,128)(2,1)S(1)}, u32[]{:S(2)}, u32[]{:S(2)}) %all-to-all-start.2) | async-done | bytes 148640 | tf_op jit(solution)/shard_map/all_to_all | solution.py:14
  400.7 1.3 broadcast_in_dim.8
  402.0 10.4 %all-to-all-start.4 = ((f32[32,1,6336]{2,1,0:T(1,128)}), f32[32,1,6336]{2,1,0:T(1,128)S(1)}, u32[]{:S(2)}, u32[]{:S(2)}) async-start(f32[32,1,6336]{2,1,0:T(1,128)} %broadcast_in_dim.8), calls=%async_computation.4 | async-start | bytes 1638400 | tf_op jit(solution)/shard_map/all_to_all | solution.py:45
  412.4 2.8 fusion
  415.2 1.3 fusion.34
  416.5 1.3 reshape.262
  418.1 1.4 gather_fusion.2
  419.6 2.8 gather_fusion.3
  423.5 1.9 fusion.21
  425.4 33.0 %all-to-all-done.4 = f32[32,1,6336]{2,1,0:T(1,128)S(1)} async-done(((f32[32,1,6336]{2,1,0:T(1,128)}), f32[32,1,6336]{2,1,0:T(1,128)S(1)}, u32[]{:S(2)}, u32[]{:S(2)}) %all-to-all-start.4) | async-done | bytes 811040 | tf_op jit(solution)/shard_map/all_to_all | solution.py:45
  (105 shorter events, 17.0 us)
Async XLA Ops:
  7.2 37.2 %copy-start = (bf16[2,128,1024]{2,1,0:T(8,128)(2,1)S(1)}, bf16[2,128,1024]{2,1,0:T(8,128)(2,1)}, u32[]{:S(2)}) copy-start(bf16[2,128,1024]{2,1,0:T(8,128)(2,1)} %param.15) | copy-start | bytes 1572868
  7.2 13.4 %copy-start.2 = (bf16[192,128]{1,0:T(8,128)(2,1)S(1)}, bf16[192,128]{1,0:T(8,128)(2,1)}, u32[]{:S(2)}) copy-start(bf16[192,128]{1,0:T(8,128)(2,1)} %param.11) | copy-start | bytes 147460
  7.2 15.4 %copy-start.1 = (bf16[192,128]{1,0:T(8,128)(2,1)S(1)}, bf16[192,128]{1,0:T(8,128)(2,1)}, u32[]{:S(2)}) copy-start(bf16[192,128]{1,0:T(8,128)(2,1)} %param.10) | copy-start | bytes 147460
  24.5 8.9 %copy-start.18 = (bf16[128,1024]{1,0:T(8,128)(2,1)S(1)}, bf16[128,1024]{1,0:T(8,128)(2,1)}, u32[]{:S(2)}) copy-start(bf16[128,1024]{1,0:T(8,128)(2,1)} %param.19) | copy-start | bytes 786436
  24.8 9.7 %copy-start.9 = (bf16[128,1024]{1,0:T(8,128)(2,1)S(1)}, bf16[128,1024]{1,0:T(8,128)(2,1)}, u32[]{:S(2)}) copy-start(bf16[128,1024]{1,0:T(8,128)(2,1)} %param.17) | copy-start | bytes 786436
  25.0 9.8 %copy-start.11 = (bf16[128,1024]{1,0:T(8,128)(2,1)S(1)}, bf16[128,1024]{1,0:T(8,128)(2,1)}, u32[]{:S(2)}) copy-start(bf16[128,1024]{1,0:T(8,128)(2,1)} %param.18) | copy-start | bytes 786436
  25.9 16.4 %all-to-all-start = ((bf16[16,36,257]{2,1,0:T(8,128)(2,1)}), bf16[16,36,257]{2,1,0:T(8,128)(2,1)S(1)}, u32[]{:S(2)}, u32[]{:S(2)}) async-start(bf16[16,36,257]{2,1,0:T(8,128)(2,1)} %pad_maximum_fusion.5), calls=%async_computation | async-start | bytes 983040 | tf_op jit(solution)/shard_map/all_to_all | solution.py:14
  33.5 8.9 %copy-start.15 = (bf16[2,128,1024]{2,1,0:T(8,128)(2,1)S(1)}, bf16[2,128,1024]{2,1,0:T(8,128)(2,1)}, u32[]{:S(2)}) copy-start(bf16[2,128,1024]{2,1,0:T(8,128)(2,1)} %param.16) | copy-start | bytes 1572868
  49.3 1.7 copy-start.6
  49.3 1.8 copy-start.8
  51.1 1.3 copy-start.7
  54.8 223.3 %all-to-all-start.1 = ((bf16[32,24,3072]{2,1,0:T(8,128)(2,1)}), bf16[32,24,3072]{2,1,0:T(8,128)(2,1)}, u32[]{:S(2)}, u32[]{:S(2)}) async-start(bf16[32,24,3072]{2,1,0:T(8,128)(2,1)} %pad_maximum_fusion), calls=%async_computation.1 | async-start | bytes 9437184 | tf_op jit(solution)/shard_map/all_to_all | solution.py:165
  73.5 280.0 %all-gather.2.cloned.1.call-start = ((), (), s32[]{:S(2)}) async-start(), calls=%async_computation.5 | async-start | bytes 5068800 | tf_op jit(solution)/shard_map/all_gather | solution.py:24
  358.8 31.1 %all-to-all-start.3 = ((f32[16,3,128,64]{2,3,1,0:T(8,128)}), f32[16,3,128,64]{2,3,1,0:T(8,128)}, u32[]{:S(2)}, u32[]{:S(2)}) async-start(f32[16,3,128,64]{2,3,1,0:T(8,128)} %maximum_bitcast_fusion), calls=%async_computation.3 | async-start | bytes 3145728 | tf_op jit(solution)/shard_map/all_to_all | solution.py:39
  376.6 2.4 copy-start.16
  381.1 1.4 copy-start.5
  382.5 1.4 copy-start.4
  384.8 1.1 copy-start.3
  384.8 1.1 copy-start.14
  389.8 10.9 %all-to-all-start.2 = ((bf16[16,2,2322]{2,1,0:T(2,128)(2,1)}), bf16[16,2,2322]{2,1,0:T(2,128)(2,1)S(1)}, u32[]{:S(2)}, u32[]{:S(2)}) async-start(bf16[16,2,2322]{2,1,0:T(2,128)(2,1)} %reshape.261), calls=%async_computation.2 | async-start | bytes 311296 | tf_op jit(solution)/shard_map/all_to_all | solution.py:14
  395.2 20.0 %copy-start.17 = (f32[3,128,64]{1,2,0:T(8,128)}, f32[3,128,64]{1,2,0:T(8,128)S(1)}, u32[]{:S(2)}) copy-start(f32[3,128,64]{1,2,0:T(8,128)S(1)} %reduce_sum.79) | copy-start | bytes 294916
  400.7 1.3 copy-start.13
  402.0 56.4 %all-to-all-start.4 = ((f32[32,1,6336]{2,1,0:T(1,128)}), f32[32,1,6336]{2,1,0:T(1,128)S(1)}, u32[]{:S(2)}, u32[]{:S(2)}) async-start(f32[32,1,6336]{2,1,0:T(1,128)} %broadcast_in_dim.8), calls=%async_computation.4 | async-start | bytes 1638400 | tf_op jit(solution)/shard_map/all_to_all | solution.py:45
  412.4 2.8 copy-start.10
  417.7 5.7 %copy-start.12 = (bf16[128,1024]{1,0:T(8,128)(2,1)S(1)}, bf16[128,1024]{1,0:T(8,128)(2,1)}, u32[]{:S(2)}) copy-start(bf16[128,1024]{1,0:T(8,128)(2,1)} %param.18) | copy-start | bytes 786436
Sparse Core Ops, SparseCore 0:
  282.5 70.9 all-gather.1
where the time goes:
time: 468 us; the launch traced here: 467 us
  waiting for transfers between devices  323 us (69%)
  starting transfers between devices  47 us (10%)
  local copies, waits for them, and re-layouts  46.3 us (10%)
  matrix products  18.3 us (4%)
  other arithmetic  18 us (4%)
  between operations  14.6 us (3%)
    all_to_all x1, waiting for transfers between devices, body(): lax.all_to_all(partials.reshape(tp_lanes, piece, 3 * hidden), 'tp', split...  204 us
    all_gather x1, waiting for transfers between devices, side_by_side_2(): filled, at, outs = (lax.all_gather(both, axis, axis=dim, tiled=True), 0, [])  71.1 us
    all_to_all x1, waiting for transfers between devices, copy_for_each(): lax.all_to_all(jnp.broadcast_to(x[None], (count, *x.shape)), axis, 0, 0,...  33 us
    all_to_all x1, starting transfers between devices, body(): lax.all_to_all(partials.reshape(tp_lanes, piece, 3 * hidden), 'tp', split...  18.6 us
    all_to_all x2, waiting for transfers between devices, side_by_side(): lax.all_to_all(both, axis, split_axis=split_dim, concat_axis=concat_dim,...  11.8 us
    all_to_all x2, starting transfers between devices, side_by_side(): lax.all_to_all(both, axis, split_axis=split_dim, concat_axis=concat_dim,...  11.5 us
    all_to_all x1, starting transfers between devices, copy_for_each(): lax.all_to_all(jnp.broadcast_to(x[None], (count, *x.shape)), axis, 0, 0,...  10.4 us
  transfers between devices with their start and end apart: 6, of which 6 were waited for; matrix products, arithmetic and copies ran while one was open for 8% of the time, Pallas kernels for 0%

commit v1 on v0

v1 whole, which is shorter than its diff:
```python
import jax
import jax.numpy as jnp
from jax import lax
from jax.sharding import PartitionSpec as P

BF = jnp.bfloat16
F32 = jnp.float32


def mm(a, b, dims=((1,), (0,)), precision=None):
    return lax.dot_general(a, b, (dims, ((), ())), precision=precision, preferred_element_type=F32)


def hot(a, b):
    return (a == b).astype(BF)


def row_backward(summed, weights):
    hidden = summed.shape[1] // 3
    pre_gate = summed[:, :hidden]
    pre_up = summed[:, hidden : 2 * hidden]
    back_act = summed[:, 2 * hidden :]
    sigmoid_gate = jax.nn.sigmoid(pre_gate)
    silu_gate = pre_gate * sigmoid_gate
    activation = silu_gate * pre_up
    act_grad = weights * back_act
    grad_up = (act_grad * silu_gate).astype(BF)
    grad_gate = (act_grad * pre_up * sigmoid_gate * (1.0 + pre_gate * (1.0 - sigmoid_gate))).astype(BF)
    scaled_act = (weights * activation).astype(BF)
    weight_grad = jnp.sum(activation * back_act, axis=1, keepdims=True).astype(BF)
    return grad_gate, grad_up, scaled_act, weight_grad


def body(tokens, cotangent, routes, gate_weights, e_gate, e_up, e_down, s_gate, s_up, s_down):
    n_ep, n_tp = lax.axis_size("ep"), lax.axis_size("tp")
    nz = n_tp // 2
    rows, width = tokens.shape
    top = routes.shape[1]
    le, _, hidden = e_gate.shape
    experts = le * n_ep
    cap = 3 * rows * top // (2 * experts)
    ls = le * cap
    bl = (ls + 8) // 8 * 8
    slots = n_ep * ls
    total = slots + rows
    half = total // 2
    piece = total // n_tp
    tp = lax.axis_index("tp")
    z, c = tp // 2, tp % 2
    cw = [(i, (i + 2) % n_tp) for i in range(n_tp)]
    ccw = [(i, (i - 2) % n_tp) for i in range(n_tp)]
    swap = [(i, i ^ 1) for i in range(n_tp)]

    ids = jnp.arange(experts, dtype=jnp.int32)
    on = [hot(routes[:, k : k + 1], ids[None, :]) for k in range(top)]
    tri = (jnp.arange(rows)[:, None] > jnp.arange(rows)[None, :]).astype(BF)
    before = mm(tri, sum(on))
    dest, within = [], []
    for k in range(top):
        pos = jnp.sum(on[k].astype(F32) * before, axis=1).astype(jnp.int32)
        dest.append(routes[:, k] // le)
        within.append(routes[:, k] % le * cap + pos)
    blk = jnp.arange(n_ep * bl, dtype=jnp.int32)
    spread = sum(hot(blk[:, None], (dest[k] * bl + within[k])[None, :]) for k in range(top))
    tail = hot(blk[:, None], (jnp.arange(n_ep, dtype=jnp.int32) * bl + ls)[None, :])
    groups = jnp.arange(n_ep, dtype=jnp.int32)
    lanes = jnp.arange(2 * width, dtype=jnp.int32)
    w_block = sum(
        mm(hot(groups[:, None], dest[k][None, :]) * gate_weights[:, k][None, :], hot(within[k][:, None], lanes[None, :]))
        for k in range(top)
    ).astype(BF)
    both = jnp.concatenate([tokens, cotangent], axis=1)
    sent = mm(jnp.concatenate([spread, tail], 1), jnp.concatenate([both, w_block], 0)).astype(BF)
    got = lax.all_to_all(sent.reshape(n_ep, bl, 2 * width), "ep", 0, 0, tiled=True)

    r = jnp.arange(total, dtype=jnp.int32)
    place = piece * (2 * ((z + r % half // piece) % nz) + (c ^ (r // half))) + r % piece
    kind = jnp.where(place < slots, place % ls // cap, le)
    src = jnp.where(place < slots, place // ls * bl + place % ls, n_ep * bl + place - slots)
    pick = hot(src[:, None], jnp.arange(n_ep * bl + rows, dtype=jnp.int32)[None, :])
    mine = mm(pick, jnp.concatenate([got.reshape(n_ep * bl, 2 * width), both], 0)).astype(BF)
    masks = [(kind == e)[:, None] for e in range(le + 1)]
    x_rows = jnp.concatenate([jnp.where(m, mine[:, :width], 0) for m in masks], 1)
    g_rows = jnp.concatenate([jnp.where(m, mine[:, width:], 0) for m in masks], 1)
    w_gate = jnp.concatenate([e_gate.reshape(le * width, hidden), s_gate], 0)
    w_up = jnp.concatenate([e_up.reshape(le * width, hidden), s_up], 0)
    w_down = jnp.concatenate([e_down.reshape(le * width, hidden), s_down], 0)
    part = jnp.concatenate([mm(x_rows, w_gate), mm(x_rows, w_up), mm(g_rows, w_down)], 1).astype(BF)
    own = part[:half].reshape(nz, piece, 3 * hidden)
    other = lax.ppermute(part[half:], "tp", swap).reshape(nz, piece, 3 * hidden)

    def local(j):
        return own[j % nz].astype(F32) + other[j % nz].astype(F32)

    hops, back_hops = nz // 2, nz - nz // 2 - 1
    right, left = local(hops).astype(BF), local(-back_hops).astype(BF)
    for t in range(hops):
        right = lax.ppermute(right, "tp", cw)
        if t < hops - 1:
            right = (right.astype(F32) + local(hops - 1 - t)).astype(BF)
        if t < back_hops:
            left = lax.ppermute(left, "tp", ccw)
        if t < back_hops - 1:
            left = (left.astype(F32) + local(t + 1 - back_hops)).astype(BF)
    summed = right.astype(F32) + left.astype(F32) + local(0)

    q = tp * piece + jnp.arange(piece, dtype=jnp.int32)
    w_rows = mm(hot((q // ls)[:, None], groups[None, :]), got[:, ls, :])
    own_w = jnp.sum(jnp.where((q % ls)[:, None] == lanes[None, :], w_rows, 0.0), axis=1)
    own_w = jnp.where(q < slots, own_w, 1.0)[:, None]
    gg, gu, sa, wg = row_backward(summed, own_w)
    block = jnp.concatenate([gg, gu, sa, jnp.broadcast_to(wg, (piece, 128))], 1)

    ring = [None] * nz
    ring[0] = right = left = block
    for t in range(1, hops + 1):
        right = lax.ppermute(right, "tp", cw)
        ring[-t % nz] = right
        if t <= back_hops:
            left = lax.ppermute(left, "tp", ccw)
            ring[t] = left
    kept = jnp.concatenate(ring, 0)
    grads = jnp.concatenate([kept, lax.ppermute(kept, "tp", swap)], 0)
    gg, gu, sa, wg = grads[:, :hidden], grads[:, hidden : 2 * hidden], grads[:, 2 * hidden : 3 * hidden], grads[:, 3 * hidden :]

    first = ((0,), (0,))
    stack = jnp.stack(
        [mm(a[:, : le * width], b, first).reshape(le, width, hidden) for a, b in ((x_rows, gg), (x_rows, gu), (g_rows, sa))]
    )
    e_sq = jnp.sum(stack * stack, axis=2)
    piece_sq = e_sq.reshape(n_tp, -1)
    piece_sq = jnp.sum(lax.all_to_all(piece_sq, "tp", 0, 0, tiled=True), axis=0)

    last = ((1,), (1,))
    slot = mm(gg, w_gate, last) + mm(gu, w_up, last)
    slot = sum(jnp.where(m, slot[:, e * width : (e + 1) * width], 0.0) for e, m in enumerate(masks))
    routed = pick[:, : n_ep * bl]
    lane1 = jnp.arange(width, dtype=jnp.int32)
    wg_block = mm(
        hot(groups[:, None], jnp.where(place < slots, place // ls, -1)[None, :]) * wg[:, 0][None, :],
        hot((place % ls)[:, None], lane1[None, :]),
    ).astype(BF)
    back = mm(routed, slot.astype(BF), first) + mm(tail, wg_block)
    shared_part = mm(pick[:, n_ep * bl :].astype(F32), slot, first, lax.Precision.HIGHEST)
    x_sh, g_sh = x_rows[:, le * width :], g_rows[:, le * width :]
    sh = jnp.stack([mm(gg, x_sh, first), mm(gu, x_sh, first), mm(sa, g_sh, first)]).astype(BF)
    cols = hidden // n_ep
    sh = jnp.moveaxis(sh.reshape(3, n_ep, cols, width), 1, 0).reshape(n_ep, 3 * cols, width)
    out = jnp.concatenate([back.astype(BF).reshape(n_ep, bl, width), sh], axis=1)
    home = lax.all_to_all(out, "ep", 0, 0, tiled=True)
    rows_home = home[:, :bl].reshape(n_ep * bl, width)
    token_grad = (mm(spread, rows_home, first) + shared_part).astype(BF)
    wg_home = home[:, ls]
    gate_grad = []
    for k in range(top):
        line = mm(hot(dest[k][:, None], groups[None, :]), wg_home)
        gate_grad.append(jnp.sum(jnp.where(within[k][:, None] == lane1[None, :], line, 0.0), axis=1))
    gate_grad = jnp.stack(gate_grad, 1).astype(BF)
    shared = jnp.sum(home[:, bl:].astype(F32), axis=0).reshape(3, cols, width)
    s_sq = jnp.sum(shared * shared, axis=2).reshape(-1)
    line = jnp.concatenate([piece_sq, s_sq])
    lines = lax.all_to_all(jnp.broadcast_to(line[None], (n_tp, line.size)), "tp", 0, 0, tiled=True)
    scale = 1.0 / (width * n_tp)
    n_e = piece_sq.size
    return (
        token_grad,
        gate_grad,
        stack.astype(BF),
        jnp.swapaxes(shared, 1, 2),
        lines[:, :n_e].reshape(3, le, hidden) * scale,
        jnp.sum(lines[:, n_e:], axis=0).reshape(3, cols) * scale,
    )


def solution(mesh):
    return jax.shard_map(
        body,
        mesh=mesh,
        in_specs=(
            P("ep", "tp"),
            P("ep", "tp"),
            P("ep", None),
            P("ep", None),
            P("ep", "tp", None),
            P("ep", "tp", None),
            P("ep", "tp", None),
            P("tp", None),
            P("tp", None),
            P("tp", None),
        ),
        out_specs=(
            P("ep", "tp"),
            P("ep", None),
            P(None, "ep", "tp", None),
            P(None, "tp", "ep"),
            P(None, "ep", None),
            P(None, "ep"),
        ),
        check_vma=False,
    )
```

time: 468 us -> 291 us (0.62)
  waiting for transfers between devices: 323 us -> 96.2 us
  starting transfers between devices: 47 us -> 140 us
  local copies, waits for them, and re-layouts: 46.3 us -> 11.8 us
  between operations: 14.6 us -> 1.66 us
  matrix products: 18.3 us -> 24 us
    all_to_all x5 -> x4, waiting for transfers between devices: 252 us -> 29.3 us  [the longest x1 12.5 us: body(): home = lax.all_to_all(out, 'ep', 0, 0, tiled=True)]
    ppermute x0 -> x32, starting transfers between devices: none -> 111 us  [the longest x14 45 us: body(): left = lax.ppermute(left, 'tp', ccw)]
    all_gather x1 -> x0, waiting for transfers between devices: 71.1 us -> none  [side_by_side_2(): filled, at, outs = (lax.all_gather(both, axis, axis=dim, tiled=True), 0, [])]
    ppermute x0 -> x32, waiting for transfers between devices: none -> 66.9 us  [the longest x16 47.7 us: body(): right = lax.ppermute(right, 'tp', cw)]
    all_to_all x5 -> x4, starting transfers between devices: 46.9 us -> 28.3 us  [the longest x1 10.8 us: body(): lax.all_to_all(jnp.broadcast_to(line[None], (n_tp, line.size)), 'tp', 0,...]
    reshape x10 -> x0, local copies, waits for them, and re-layouts: 10.4 us -> none  [the longest x3 3.67 us: project(): return jnp.einsum('secd,edf->secf', row_block, weight, preferred_element_...]
    scatter x3 -> x0, local copies, waits for them, and re-layouts: 8.82 us -> none  [the longest x1 2.95 us: body(): jnp.zeros((total_slots,), jnp.bfloat16).at[slot_index]]
    gather x6 -> x0, local copies, waits for them, and re-layouts: 8.2 us -> none  [the longest x1 2.81 us: body(): gate_grad = back_weight.reshape(-1)[slot_index].reshape(rows_here, choose)]
  transfers between devices with their start and end apart: 6 -> 36, of which waited for: 6 -> 35; matrix products, arithmetic and copies ran while one was open for 8% -> 7% of each run, Pallas kernels for 0% -> 0%
where the time goes in v1:
time: 291 us; the launch traced here: 289 us
  starting transfers between devices  140 us (48%)
  waiting for transfers between devices  96.2 us (33%)
  matrix products  24 us (8%)
  other arithmetic  15.5 us (5%)
  local copies, waits for them, and re-layouts  11.8 us (4%)
    ppermute x16, waiting for transfers between devices, body(): right = lax.ppermute(right, 'tp', cw)  47.7 us
    ppermute x14, starting transfers between devices, body(): left = lax.ppermute(left, 'tp', ccw)  45 us
    ppermute x16, starting transfers between devices, body(): right = lax.ppermute(right, 'tp', cw)  38.9 us
    dot_general x23, matrix products, mm(): lax.dot_general(a, b, (dims, ((), ())), precision=precision, preferred_el...  24 us
    ppermute x1, starting transfers between devices, body(): grads = jnp.concatenate([kept, lax.ppermute(kept, 'tp', swap)], 0)  21.7 us
    all_to_all x1, waiting for transfers between devices, body(): home = lax.all_to_all(out, 'ep', 0, 0, tiled=True)  12.5 us
    ppermute x14, waiting for transfers between devices, body(): left = lax.ppermute(left, 'tp', ccw)  12.3 us
    all_to_all x1, starting transfers between devices, body(): lax.all_to_all(jnp.broadcast_to(line[None], (n_tp, line.size)), 'tp', 0,...  10.8 us
  transfers between devices with their start and end apart: 36, of which 35 were waited for; matrix products, arithmetic and copies ran while one was open for 7% of the time, Pallas kernels for 0%

profile of v1, /device:TPU:1, one launch (start us, length us, event | category | flops | bytes accessed | tf_op | source)
XLA Modules:
  0.0 288.9 jit_solution(5234338517317224261)
XLA Ops:
  7.0 7.7 %all-to-all-start = ((bf16[16,40,256]{2,1,0:T(8,128)(2,1)}), bf16[16,40,256]{2,1,0:T(8,128)(2,1)S(1)}, u32[]{:S(2)}, u32[]{:S(2)}) async-start(bf16[16,40,256]{2,1,0:T(8,128)(2,1)} %bitcast.6), calls=%async_computation | async-start | bytes 655360 | tf_op jit(solution)/shard_map/all_to_all | solution.py:74
  14.9 7.7 %all-to-all-done = bf16[16,40,256]{2,1,0:T(8,128)(2,1)S(1)} async-done(((bf16[16,40,256]{2,1,0:T(8,128)(2,1)}), bf16[16,40,256]{2,1,0:T(8,128)(2,1)S(1)}, u32[]{:S(2)}, u32[]{:S(2)}) %all-to-all-start) | async-done | bytes 327712 | tf_op jit(solution)/shard_map/all_to_all | solution.py:74
  27.8 5.8 %collective-permute-start = (bf16[384,3072]{1,0:T(8,128)(2,1)S(1)}, bf16[384,3072]{1,0:T(8,128)(2,1)S(1)}, u32[]{:S(2)}, u32[]{:S(2)}) collective-permute-start(bf16[384,3072]{1,0:T(8,128)(2,1)S(1)} %slice.296), channel_id=1, source_target_pairs={{0,1},{1,0},{2,3},{3,2},{4,5},{5,4},{6,7},{7,6},{8,9},{9,8},{10,11... | collective-permute-start | bytes 7077896 | tf_op jit(solution)/shard_map/ppermute | solution.py:90
  33.6 4.1 %collective-permute-done = bf16[384,3072]{1,0:T(8,128)(2,1)S(1)} collective-permute-done((bf16[384,3072]{1,0:T(8,128)(2,1)S(1)}, bf16[384,3072]{1,0:T(8,128)(2,1)S(1)}, u32[]{:S(2)}, u32[]{:S(2)}) %collective-permute-start) | collective-permute-done | bytes 2359328 | tf_op jit(solution)/shard_map/ppermute | solution.py:90
  37.8 2.1 collective-permute-start.1
  39.9 11.4 %collective-permute-done.1 = bf16[24,3072]{1,0:T(8,128)(2,1)S(1)} collective-permute-done((bf16[24,3072]{1,0:T(8,128)(2,1)S(1)}, bf16[24,3072]{1,0:T(8,128)(2,1)S(1)}, u32[]{:S(2)}, u32[]{:S(2)}) %collective-permute-start.1) | collective-permute-done | bytes 147488 | tf_op jit(solution)/shard_map/ppermute | solution.py:98
  51.4 1.9 collective-permute-start.2
  53.3 4.6 %collective-permute-start.9 = (bf16[24,3072]{1,0:T(8,128)(2,1)S(1)}, bf16[24,3072]{1,0:T(8,128)(2,1)S(1)}, u32[]{:S(2)}, u32[]{:S(2)}) collective-permute-start(bf16[24,3072]{1,0:T(8,128)(2,1)S(1)} %get-tuple-element.31), channel_id=1, source_target_pairs={{0,30},{1,31},{2,0},{3,1},{4,2},{5,3},{6,4},{7,5},{8,6},{9,7},{10,... | collective-permute-start | bytes 442376 | tf_op jit(solution)/shard_map/ppermute | solution.py:102
  60.1 5.0 %collective-permute-start.10 = (bf16[24,3072]{1,0:T(8,128)(2,1)S(1)}, bf16[24,3072]{1,0:T(8,128)(2,1)S(1)}, u32[]{:S(2)}, u32[]{:S(2)}) collective-permute-start(bf16[24,3072]{1,0:T(8,128)(2,1)S(1)} %get-tuple-element.29), channel_id=1, source_target_pairs={{0,30},{1,31},{2,0},{3,1},{4,2},{5,3},{6,4},{7,5},{8,6},{9,7},{10,... | collective-permute-start | bytes 442376 | tf_op jit(solution)/shard_map/ppermute | solution.py:102
  65.1 1.9 collective-permute-start.3
  67.2 5.0 %collective-permute-done.3 = bf16[24,3072]{1,0:T(8,128)(2,1)S(1)} collective-permute-done((bf16[24,3072]{1,0:T(8,128)(2,1)S(1)}, bf16[24,3072]{1,0:T(8,128)(2,1)S(1)}, u32[]{:S(2)}, u32[]{:S(2)}) %collective-permute-start.3) | collective-permute-done | bytes 147488 | tf_op jit(solution)/shard_map/ppermute | solution.py:98
  72.3 1.9 collective-permute-start.11
  74.2 3.4 %collective-permute-start.4 = (bf16[24,3072]{1,0:T(8,128)(2,1)S(1)}, bf16[24,3072]{1,0:T(8,128)(2,1)S(1)}, u32[]{:S(2)}, u32[]{:S(2)}) collective-permute-start(bf16[24,3072]{1,0:T(8,128)(2,1)S(1)} %get-tuple-element.26), channel_id=1, source_target_pairs={{0,2},{1,3},{2,4},{3,5},{4,6},{5,7},{6,8},{7,9},{8,10},{9,11},{10,... | collective-permute-start | bytes 442376 | tf_op jit(solution)/shard_map/ppermute | solution.py:98
  78.2 3.1 %collective-permute-done.4 = bf16[24,3072]{1,0:T(8,128)(2,1)S(1)} collective-permute-done((bf16[24,3072]{1,0:T(8,128)(2,1)S(1)}, bf16[24,3072]{1,0:T(8,128)(2,1)S(1)}, u32[]{:S(2)}, u32[]{:S(2)}) %collective-permute-start.4) | collective-permute-done | bytes 147488 | tf_op jit(solution)/shard_map/ppermute | solution.py:98
  81.4 1.9 collective-permute-start.12
  83.4 3.4 %collective-permute-start.5 = (bf16[24,3072]{1,0:T(8,128)(2,1)S(1)}, bf16[24,3072]{1,0:T(8,128)(2,1)S(1)}, u32[]{:S(2)}, u32[]{:S(2)}) collective-permute-start(bf16[24,3072]{1,0:T(8,128)(2,1)S(1)} %get-tuple-element.24), channel_id=1, source_target_pairs={{0,2},{1,3},{2,4},{3,5},{4,6},{5,7},{6,8},{7,9},{8,10},{9,11},{10,... | collective-permute-start | bytes 442376 | tf_op jit(solution)/shard_map/ppermute | solution.py:98
  87.3 3.1 %collective-permute-done.5 = bf16[24,3072]{1,0:T(8,128)(2,1)S(1)} collective-permute-done((bf16[24,3072]{1,0:T(8,128)(2,1)S(1)}, bf16[24,3072]{1,0:T(8,128)(2,1)S(1)}, u32[]{:S(2)}, u32[]{:S(2)}) %collective-permute-start.5) | collective-permute-done | bytes 147488 | tf_op jit(solution)/shard_map/ppermute | solution.py:98
  91.3 2.6 collective-permute-start.13
  93.9 2.7 collective-permute-start.6
  97.5 3.8 %collective-permute-done.6 = bf16[24,3072]{1,0:T(8,128)(2,1)} collective-permute-done((bf16[24,3072]{1,0:T(8,128)(2,1)}, bf16[24,3072]{1,0:T(8,128)(2,1)}, u32[]{:S(2)}, u32[]{:S(2)}) %collective-permute-start.6) | collective-permute-done | bytes 147488 | tf_op jit(solution)/shard_map/ppermute | solution.py:98
  102.6 2.2 collective-permute-start.14
  104.8 3.1 %collective-permute-start.7 = (bf16[24,3072]{1,0:T(8,128)(2,1)S(1)}, bf16[24,3072]{1,0:T(8,128)(2,1)S(1)}, u32[]{:S(2)}, u32[]{:S(2)}) collective-permute-start(bf16[24,3072]{1,0:T(8,128)(2,1)S(1)} %get-tuple-element.20), channel_id=1, source_target_pairs={{0,2},{1,3},{2,4},{3,5},{4,6},{5,7},{6,8},{7,9},{8,10},{9,11},{10,... | collective-permute-start | bytes 442376 | tf_op jit(solution)/shard_map/ppermute | solution.py:98
  108.9 3.0 %collective-permute-done.7 = bf16[24,3072]{1,0:T(8,128)(2,1)S(1)} collective-permute-done((bf16[24,3072]{1,0:T(8,128)(2,1)S(1)}, bf16[24,3072]{1,0:T(8,128)(2,1)S(1)}, u32[]{:S(2)}, u32[]{:S(2)}) %collective-permute-start.7) | collective-permute-done | bytes 147488 | tf_op jit(solution)/shard_map/ppermute | solution.py:98
  112.9 1.9 collective-permute-start.15
  114.9 3.4 %collective-permute-start.8 = (bf16[24,3072]{1,0:T(8,128)(2,1)S(1)}, bf16[24,3072]{1,0:T(8,128)(2,1)S(1)}, u32[]{:S(2)}, u32[]{:S(2)}) collective-permute-start(bf16[24,3072]{1,0:T(8,128)(2,1)S(1)} %get-tuple-element.18), channel_id=1, source_target_pairs={{0,2},{1,3},{2,4},{3,5},{4,6},{5,7},{6,8},{7,9},{8,10},{9,11},{10,... | collective-permute-start | bytes 442376 | tf_op jit(solution)/shard_map/ppermute | solution.py:98
  118.8 3.7 %collective-permute-done.8 = bf16[24,3072]{1,0:T(8,128)(2,1)S(1)} collective-permute-done((bf16[24,3072]{1,0:T(8,128)(2,1)S(1)}, bf16[24,3072]{1,0:T(8,128)(2,1)S(1)}, u32[]{:S(2)}, u32[]{:S(2)}) %collective-permute-start.8) | collective-permute-done | bytes 147488 | tf_op jit(solution)/shard_map/ppermute | solution.py:98
  123.8 1.9 collective-permute-start.16
  125.7 3.4 %collective-permute-start.23 = (bf16[24,3200]{1,0:T(8,128)(2,1)S(1)}, bf16[24,3200]{1,0:T(8,128)(2,1)S(1)}, u32[]{:S(2)}, u32[]{:S(2)}) collective-permute-start(bf16[24,3200]{1,0:T(8,128)(2,1)S(1)} %get-tuple-element.78), channel_id=1, source_target_pairs={{0,2},{1,3},{2,4},{3,5},{4,6},{5,7},{6,8},{7,9},{8,10},{9,11},{10,... | collective-permute-start | bytes 460808 | tf_op jit(solution)/shard_map/ppermute | solution.py:117
  129.1 2.5 collective-permute-done.16
  131.6 2.5 collective-permute-start.17
  134.7 2.2 collective-permute-start.24
  137.6 3.8 %collective-permute-start.18 = (bf16[24,3200]{1,0:T(8,128)(2,1)S(1)}, bf16[24,3200]{1,0:T(8,128)(2,1)S(1)}, u32[]{:S(2)}, u32[]{:S(2)}) collective-permute-start(bf16[24,3200]{1,0:T(8,128)(2,1)S(1)} %collective-permute-done.17), channel_id=1, source_target_pairs={{0,30},{1,31},{2,0},{3,1},{4,2},{5,3},{6,4},{7,5},{8,6},{9,7},{10,... | collective-permute-start | bytes 460808 | tf_op jit(solution)/shard_map/ppermute | solution.py:120
  144.7 3.8 %collective-permute-start.19 = (bf16[24,3200]{1,0:T(8,128)(2,1)S(1)}, bf16[24,3200]{1,0:T(8,128)(2,1)S(1)}, u32[]{:S(2)}, u32[]{:S(2)}) collective-permute-start(bf16[24,3200]{1,0:T(8,128)(2,1)S(1)} %collective-permute-done.18), channel_id=1, source_target_pairs={{0,30},{1,31},{2,0},{3,1},{4,2},{5,3},{6,4},{7,5},{8,6},{9,7},{10,... | collective-permute-start | bytes 460808 | tf_op jit(solution)/shard_map/ppermute | solution.py:120
  152.5 3.1 %collective-permute-start.20 = (bf16[24,3200]{1,0:T(8,128)(2,1)S(1)}, bf16[24,3200]{1,0:T(8,128)(2,1)S(1)}, u32[]{:S(2)}, u32[]{:S(2)}) collective-permute-start(bf16[24,3200]{1,0:T(8,128)(2,1)S(1)} %collective-permute-done.19), channel_id=1, source_target_pairs={{0,30},{1,31},{2,0},{3,1},{4,2},{5,3},{6,4},{7,5},{8,6},{9,7},{10,... | collective-permute-start | bytes 460808 | tf_op jit(solution)/shard_map/ppermute | solution.py:120
  159.4 4.4 %collective-permute-start.21 = (bf16[24,3200]{1,0:T(8,128)(2,1)S(1)}, bf16[24,3200]{1,0:T(8,128)(2,1)S(1)}, u32[]{:S(2)}, u32[]{:S(2)}) collective-permute-start(bf16[24,3200]{1,0:T(8,128)(2,1)S(1)} %collective-permute-done.20), channel_id=1, source_target_pairs={{0,30},{1,31},{2,0},{3,1},{4,2},{5,3},{6,4},{7,5},{8,6},{9,7},{10,... | collective-permute-start | bytes 460808 | tf_op jit(solution)/shard_map/ppermute | solution.py:120
  167.1 5.3 %collective-permute-start.22 = (bf16[24,3200]{1,0:T(8,128)(2,1)S(1)}, bf16[24,3200]{1,0:T(8,128)(2,1)S(1)}, u32[]{:S(2)}, u32[]{:S(2)}) collective-permute-start(bf16[24,3200]{1,0:T(8,128)(2,1)S(1)} %collective-permute-done.21), channel_id=1, source_target_pairs={{0,30},{1,31},{2,0},{3,1},{4,2},{5,3},{6,4},{7,5},{8,6},{9,7},{10,... | collective-permute-start | bytes 460808 | tf_op jit(solution)/shard_map/ppermute | solution.py:120
  174.6 5.7 %collective-permute-done.29 = bf16[24,3200]{1,0:T(8,128)(2,1)S(1)} collective-permute-done((bf16[24,3200]{1,0:T(8,128)(2,1)S(1)}, bf16[24,3200]{1,0:T(8,128)(2,1)S(1)}, u32[]{:S(2)}, u32[]{:S(2)}) %collective-permute-start.29) | collective-permute-done | bytes 153632 | tf_op jit(solution)/shard_map/ppermute | solution.py:117
  182.3 5.2 %collective-permute-done.30 = bf16[24,3200]{1,0:T(8,128)(2,1)S(1)} collective-permute-done((bf16[24,3200]{1,0:T(8,128)(2,1)S(1)}, bf16[24,3200]{1,0:T(8,128)(2,1)S(1)}, u32[]{:S(2)}, u32[]{:S(2)}) %collective-permute-start.30) | collective-permute-done | bytes 153632 | tf_op jit(solution)/shard_map/ppermute | solution.py:117
  187.8 21.7 %collective-permute-start.31 = (bf16[384,3200]{1,0:T(8,128)(2,1)S(1)}, bf16[384,3200]{1,0:T(8,128)(2,1)S(1)}, u32[]{:S(2)}, u32[]{:S(2)}) collective-permute-start(bf16[384,3200]{1,0:T(8,128)(2,1)S(1)} %get-tuple-element.46), channel_id=1, source_target_pairs={{0,1},{1,0},{2,3},{3,2},{4,5},{5,4},{6,7},{7,6},{8,9},{9,8},{10,11... | collective-permute-start | bytes 7372808 | tf_op jit(solution)/shard_map/ppermute | solution.py:123
  210.8 2.8 collective-permute-done.31
  225.4 5.4 %all-to-all-start.2 = ((f32[32,1,192]{2,1,0:T(1,128)}), f32[32,1,192]{2,1,0:T(1,128)}, u32[]{:S(2)}, u32[]{:S(2)}) async-start(f32[32,1,192]{2,1,0:T(1,128)} %all_to_all.20), calls=%async_computation.2 | async-start | bytes 65536 | tf_op jit(solution)/shard_map/all_to_all | solution.py:132
  230.9 2.7 convolution_add_fusion
  239.5 3.4 %all-to-all-done.2 = f32[32,1,192]{2,1,0:T(1,128)} async-done(((f32[32,1,192]{2,1,0:T(1,128)}), f32[32,1,192]{2,1,0:T(1,128)}, u32[]{:S(2)}, u32[]{:S(2)}) %all-to-all-start.2) | async-done | bytes 24608 | tf_op jit(solution)/shard_map/all_to_all | solution.py:132
  242.9 4.3 %all-to-all-start.1 = ((bf16[16,232,128]{2,1,0:T(8,128)(2,1)}), bf16[16,232,128]{2,1,0:T(8,128)(2,1)}, u32[]{:S(2)}, u32[]{:S(2)}) async-start(bf16[16,232,128]{2,1,0:T(8,128)(2,1)} %pad_maximum_fusion.2), calls=%async_computation.1 | async-start | bytes 1900544 | tf_op jit(solution)/shard_map/all_to_all | solution.py:150
  249.6 12.5 %all-to-all-done.1 = bf16[16,232,128]{2,1,0:T(8,128)(2,1)} async-done(((bf16[16,232,128]{2,1,0:T(8,128)(2,1)}), bf16[16,232,128]{2,1,0:T(8,128)(2,1)}, u32[]{:S(2)}, u32[]{:S(2)}) %all-to-all-start.1) | async-done | bytes 950304 | tf_op jit(solution)/shard_map/all_to_all | solution.py:150
  264.2 10.8 %all-to-all-start.3 = ((f32[32,1,384]{2,1,0:T(1,128)}), f32[32,1,384]{2,1,0:T(1,128)S(1)}, u32[]{:S(2)}, u32[]{:S(2)}) async-start(f32[32,1,384]{2,1,0:T(1,128)} %broadcast_in_dim.131), calls=%async_computation.3 | async-start | bytes 98304 | tf_op jit(solution)/shard_map/all_to_all | solution.py:162
  279.7 2.0 fusion.18
  281.7 5.7 %all-to-all-done.3 = f32[32,1,384]{2,1,0:T(1,128)S(1)} async-done(((f32[32,1,384]{2,1,0:T(1,128)}), f32[32,1,384]{2,1,0:T(1,128)S(1)}, u32[]{:S(2)}, u32[]{:S(2)}) %all-to-all-start.3) | async-done | bytes 49184 | tf_op jit(solution)/shard_map/all_to_all | solution.py:162
  (193 shorter events, 71.5 us)
Async XLA Ops:
  7.0 16.7 %copy-start.31 = (bf16[2,128,1024]{2,1,0:T(8,128)(2,1)S(1)}, bf16[2,128,1024]{2,1,0:T(8,128)(2,1)}, u32[]{:S(2)}) copy-start(bf16[2,128,1024]{2,1,0:T(8,128)(2,1)} %param.14) | copy-start | bytes 1572868
  7.0 16.7 %copy-start.35 = (bf16[128,1024]{1,0:T(8,128)(2,1)S(1)}, bf16[128,1024]{1,0:T(8,128)(2,1)}, u32[]{:S(2)}) copy-start(bf16[128,1024]{1,0:T(8,128)(2,1)} %param.17) | copy-start | bytes 786436
  7.0 15.6 %all-to-all-start = ((bf16[16,40,256]{2,1,0:T(8,128)(2,1)}), bf16[16,40,256]{2,1,0:T(8,128)(2,1)S(1)}, u32[]{:S(2)}, u32[]{:S(2)}) async-start(bf16[16,40,256]{2,1,0:T(8,128)(2,1)} %bitcast.6), calls=%async_computation | async-start | bytes 655360 | tf_op jit(solution)/shard_map/all_to_all | solution.py:74
  14.8 9.9 %copy-start.17 = (pred[768]{0:T(1024)(128)(4,1)}, pred[768]{0:T(1024)(128)(4,1)S(1)}, u32[]{:S(2)}) copy-start(pred[768]{0:T(1024)(128)(4,1)S(1)} %broadcast_compare_fusion.3) | copy-start | bytes 2308
  27.2 63.2 %copy-start = (bf16[768,1024]{1,0:T(8,128)(2,1)}, bf16[768,1024]{1,0:T(8,128)(2,1)S(1)}, u32[]{:S(2)}) copy-start(bf16[768,1024]{1,0:T(8,128)(2,1)S(1)} %convolution_convert_fusion) | copy-start | bytes 4718596
  27.8 10.0 %collective-permute-start = (bf16[384,3072]{1,0:T(8,128)(2,1)S(1)}, bf16[384,3072]{1,0:T(8,128)(2,1)S(1)}, u32[]{:S(2)}, u32[]{:S(2)}) collective-permute-start(bf16[384,3072]{1,0:T(8,128)(2,1)S(1)} %slice.296), channel_id=1, source_target_pairs={{0,1},{1,0},{2,3},{3,2},{4,5},{5,4},{6,7},{7,6},{8,9},{9,8},{10,11... | collective-permute-start | bytes 7077896 | tf_op jit(solution)/shard_map/ppermute | solution.py:90
  37.7 52.7 %copy-start.2 = (bf16[384,3072]{1,0:T(8,128)(2,1)}, bf16[384,3072]{1,0:T(8,128)(2,1)S(1)}, u32[]{:S(2)}) copy-start(bf16[384,3072]{1,0:T(8,128)(2,1)S(1)} %collective-permute-done) | copy-start | bytes 7077892
  37.8 13.5 %collective-permute-start.1 = (bf16[24,3072]{1,0:T(8,128)(2,1)S(1)}, bf16[24,3072]{1,0:T(8,128)(2,1)S(1)}, u32[]{:S(2)}, u32[]{:S(2)}) collective-permute-start(bf16[24,3072]{1,0:T(8,128)(2,1)S(1)} %add_convert_fusion.14), channel_id=1, source_target_pairs={{0,2},{1,3},{2,4},{3,5},{4,6},{5,7},{6,8},{7,9},{8,10},{9,11},{10,... | collective-permute-start | bytes 442376 | tf_op jit(solution)/shard_map/ppermute | solution.py:98
  51.4 7.6 %collective-permute-start.2 = (bf16[24,3072]{1,0:T(8,128)(2,1)S(1)}, bf16[24,3072]{1,0:T(8,128)(2,1)S(1)}, u32[]{:S(2)}, u32[]{:S(2)}) collective-permute-start(bf16[24,3072]{1,0:T(8,128)(2,1)S(1)} %get-tuple-element.30), channel_id=1, source_target_pairs={{0,2},{1,3},{2,4},{3,5},{4,6},{5,7},{6,8},{7,9},{8,10},{9,11},{10,... | collective-permute-start | bytes 442376 | tf_op jit(solution)/shard_map/ppermute | solution.py:98
  53.3 6.7 %collective-permute-start.9 = (bf16[24,3072]{1,0:T(8,128)(2,1)S(1)}, bf16[24,3072]{1,0:T(8,128)(2,1)S(1)}, u32[]{:S(2)}, u32[]{:S(2)}) collective-permute-start(bf16[24,3072]{1,0:T(8,128)(2,1)S(1)} %get-tuple-element.31), channel_id=1, source_target_pairs={{0,30},{1,31},{2,0},{3,1},{4,2},{5,3},{6,4},{7,5},{8,6},{9,7},{10,... | collective-permute-start | bytes 442376 | tf_op jit(solution)/shard_map/ppermute | solution.py:102
  60.1 7.1 %collective-permute-start.10 = (bf16[24,3072]{1,0:T(8,128)(2,1)S(1)}, bf16[24,3072]{1,0:T(8,128)(2,1)S(1)}, u32[]{:S(2)}, u32[]{:S(2)}) collective-permute-start(bf16[24,3072]{1,0:T(8,128)(2,1)S(1)} %get-tuple-element.29), channel_id=1, source_target_pairs={{0,30},{1,31},{2,0},{3,1},{4,2},{5,3},{6,4},{7,5},{8,6},{9,7},{10,... | collective-permute-start | bytes 442376 | tf_op jit(solution)/shard_map/ppermute | solution.py:102
  65.1 7.1 %collective-permute-start.3 = (bf16[24,3072]{1,0:T(8,128)(2,1)S(1)}, bf16[24,3072]{1,0:T(8,128)(2,1)S(1)}, u32[]{:S(2)}, u32[]{:S(2)}) collective-permute-start(bf16[24,3072]{1,0:T(8,128)(2,1)S(1)} %get-tuple-element.28), channel_id=1, source_target_pairs={{0,2},{1,3},{2,4},{3,5},{4,6},{5,7},{6,8},{7,9},{8,10},{9,11},{10,... | collective-permute-start | bytes 442376 | tf_op jit(solution)/shard_map/ppermute | solution.py:98
  72.3 5.9 %collective-permute-start.11 = (bf16[24,3072]{1,0:T(8,128)(2,1)S(1)}, bf16[24,3072]{1,0:T(8,128)(2,1)S(1)}, u32[]{:S(2)}, u32[]{:S(2)}) collective-permute-start(bf16[24,3072]{1,0:T(8,128)(2,1)S(1)} %get-tuple-element.27), channel_id=1, source_target_pairs={{0,30},{1,31},{2,0},{3,1},{4,2},{5,3},{6,4},{7,5},{8,6},{9,7},{10,... | collective-permute-start | bytes 442376 | tf_op jit(solution)/shard_map/ppermute | solution.py:102
  74.2 7.1 %collective-permute-start.4 = (bf16[24,3072]{1,0:T(8,128)(2,1)S(1)}, bf16[24,3072]{1,0:T(8,128)(2,1)S(1)}, u32[]{:S(2)}, u32[]{:S(2)}) collective-permute-start(bf16[24,3072]{1,0:T(8,128)(2,1)S(1)} %get-tuple-element.26), channel_id=1, source_target_pairs={{0,2},{1,3},{2,4},{3,5},{4,6},{5,7},{6,8},{7,9},{8,10},{9,11},{10,... | collective-permute-start | bytes 442376 | tf_op jit(solution)/shard_map/ppermute | solution.py:98
  81.4 5.9 %collective-permute-start.12 = (bf16[24,3072]{1,0:T(8,128)(2,1)S(1)}, bf16[24,3072]{1,0:T(8,128)(2,1)S(1)}, u32[]{:S(2)}, u32[]{:S(2)}) collective-permute-start(bf16[24,3072]{1,0:T(8,128)(2,1)S(1)} %get-tuple-element.25), channel_id=1, source_target_pairs={{0,30},{1,31},{2,0},{3,1},{4,2},{5,3},{6,4},{7,5},{8,6},{9,7},{10,... | collective-permute-start | bytes 442376 | tf_op jit(solution)/shard_map/ppermute | solution.py:102
  83.4 7.1 %collective-permute-start.5 = (bf16[24,3072]{1,0:T(8,128)(2,1)S(1)}, bf16[24,3072]{1,0:T(8,128)(2,1)S(1)}, u32[]{:S(2)}, u32[]{:S(2)}) collective-permute-start(bf16[24,3072]{1,0:T(8,128)(2,1)S(1)} %get-tuple-element.24), channel_id=1, source_target_pairs={{0,2},{1,3},{2,4},{3,5},{4,6},{5,7},{6,8},{7,9},{8,10},{9,11},{10,... | collective-permute-start | bytes 442376 | tf_op jit(solution)/shard_map/ppermute | solution.py:98
  91.3 6.2 %collective-permute-start.13 = (bf16[24,3072]{1,0:T(8,128)(2,1)}, bf16[24,3072]{1,0:T(8,128)(2,1)}, u32[]{:S(2)}, u32[]{:S(2)}) collective-permute-start(bf16[24,3072]{1,0:T(8,128)(2,1)} %get-tuple-element.23), channel_id=1, source_target_pairs={{0,30},{1,31},{2,0},{3,1},{4,2},{5,3},{6,4},{7,5},{8,6},{9,7},{10,... | collective-permute-start | bytes 442376 | tf_op jit(solution)/shard_map/ppermute | solution.py:102
  93.9 7.4 %collective-permute-start.6 = (bf16[24,3072]{1,0:T(8,128)(2,1)}, bf16[24,3072]{1,0:T(8,128)(2,1)}, u32[]{:S(2)}, u32[]{:S(2)}) collective-permute-start(bf16[24,3072]{1,0:T(8,128)(2,1)} %get-tuple-element.22), channel_id=1, source_target_pairs={{0,2},{1,3},{2,4},{3,5},{4,6},{5,7},{6,8},{7,9},{8,10},{9,11},{10,... | collective-permute-start | bytes 442376 | tf_op jit(solution)/shard_map/ppermute | solution.py:98
  96.6 15.2 %copy-start.1 = (bf16[768,1024]{1,0:T(8,128)(2,1)S(1)}, bf16[768,1024]{1,0:T(8,128)(2,1)}, u32[]{:S(2)}) copy-start(bf16[768,1024]{1,0:T(8,128)(2,1)} %copy-done) | copy-start | bytes 4718596
  102.6 6.3 %collective-permute-start.14 = (bf16[24,3072]{1,0:T(8,128)(2,1)S(1)}, bf16[24,3072]{1,0:T(8,128)(2,1)S(1)}, u32[]{:S(2)}, u32[]{:S(2)}) collective-permute-start(bf16[24,3072]{1,0:T(8,128)(2,1)S(1)} %get-tuple-element.21), channel_id=1, source_target_pairs={{0,30},{1,31},{2,0},{3,1},{4,2},{5,3},{6,4},{7,5},{8,6},{9,7},{10,... | collective-permute-start | bytes 442376 | tf_op jit(solution)/shard_map/ppermute | solution.py:102
  104.8 7.1 %collective-permute-start.7 = (bf16[24,3072]{1,0:T(8,128)(2,1)S(1)}, bf16[24,3072]{1,0:T(8,128)(2,1)S(1)}, u32[]{:S(2)}, u32[]{:S(2)}) collective-permute-start(bf16[24,3072]{1,0:T(8,128)(2,1)S(1)} %get-tuple-element.20), channel_id=1, source_target_pairs={{0,2},{1,3},{2,4},{3,5},{4,6},{5,7},{6,8},{7,9},{8,10},{9,11},{10,... | collective-permute-start | bytes 442376 | tf_op jit(solution)/shard_map/ppermute | solution.py:98
  112.9 5.9 %collective-permute-start.15 = (bf16[24,3072]{1,0:T(8,128)(2,1)S(1)}, bf16[24,3072]{1,0:T(8,128)(2,1)S(1)}, u32[]{:S(2)}, u32[]{:S(2)}) collective-permute-start(bf16[24,3072]{1,0:T(8,128)(2,1)S(1)} %get-tuple-element.19), channel_id=1, source_target_pairs={{0,30},{1,31},{2,0},{3,1},{4,2},{5,3},{6,4},{7,5},{8,6},{9,7},{10,... | collective-permute-start | bytes 442376 | tf_op jit(solution)/shard_map/ppermute | solution.py:102
  114.9 7.7 %collective-permute-start.8 = (bf16[24,3072]{1,0:T(8,128)(2,1)S(1)}, bf16[24,3072]{1,0:T(8,128)(2,1)S(1)}, u32[]{:S(2)}, u32[]{:S(2)}) collective-permute-start(bf16[24,3072]{1,0:T(8,128)(2,1)S(1)} %get-tuple-element.18), channel_id=1, source_target_pairs={{0,2},{1,3},{2,4},{3,5},{4,6},{5,7},{6,8},{7,9},{8,10},{9,11},{10,... | collective-permute-start | bytes 442376 | tf_op jit(solution)/shard_map/ppermute | solution.py:98
  123.8 7.8 %collective-permute-start.16 = (bf16[24,3200]{1,0:T(8,128)(2,1)S(1)}, bf16[24,3200]{1,0:T(8,128)(2,1)S(1)}, u32[]{:S(2)}, u32[]{:S(2)}) collective-permute-start(bf16[24,3200]{1,0:T(8,128)(2,1)S(1)} %get-tuple-element.78), channel_id=1, source_target_pairs={{0,30},{1,31},{2,0},{3,1},{4,2},{5,3},{6,4},{7,5},{8,6},{9,7},{10,... | collective-permute-start | bytes 460808 | tf_op jit(solution)/shard_map/ppermute | solution.py:120
  125.7 8.9 %collective-permute-start.23 = (bf16[24,3200]{1,0:T(8,128)(2,1)S(1)}, bf16[24,3200]{1,0:T(8,128)(2,1)S(1)}, u32[]{:S(2)}, u32[]{:S(2)}) collective-permute-start(bf16[24,3200]{1,0:T(8,128)(2,1)S(1)} %get-tuple-element.78), channel_id=1, source_target_pairs={{0,2},{1,3},{2,4},{3,5},{4,6},{5,7},{6,8},{7,9},{8,10},{9,11},{10,... | collective-permute-start | bytes 460808 | tf_op jit(solution)/shard_map/ppermute | solution.py:117
  131.6 5.9 %collective-permute-start.17 = (bf16[24,3200]{1,0:T(8,128)(2,1)S(1)}, bf16[24,3200]{1,0:T(8,128)(2,1)S(1)}, u32[]{:S(2)}, u32[]{:S(2)}) collective-permute-start(bf16[24,3200]{1,0:T(8,128)(2,1)S(1)} %collective-permute-done.16), channel_id=1, source_target_pairs={{0,30},{1,31},{2,0},{3,1},{4,2},{5,3},{6,4},{7,5},{8,6},{9,7},{10,... | collective-permute-start | bytes 460808 | tf_op jit(solution)/shard_map/ppermute | solution.py:120
  134.7 7.2 %collective-permute-start.24 = (bf16[24,3200]{1,0:T(8,128)(2,1)S(1)}, bf16[24,3200]{1,0:T(8,128)(2,1)S(1)}, u32[]{:S(2)}, u32[]{:S(2)}) collective-permute-start(bf16[24,3200]{1,0:T(8,128)(2,1)S(1)} %collective-permute-done.23), channel_id=1, source_target_pairs={{0,2},{1,3},{2,4},{3,5},{4,6},{5,7},{6,8},{7,9},{8,10},{9,11},{10,... | collective-permute-start | bytes 460808 | tf_op jit(solution)/shard_map/ppermute | solution.py:117
  137.6 7.1 %collective-permute-start.18 = (bf16[24,3200]{1,0:T(8,128)(2,1)S(1)}, bf16[24,3200]{1,0:T(8,128)(2,1)S(1)}, u32[]{:S(2)}, u32[]{:S(2)}) collective-permute-start(bf16[24,3200]{1,0:T(8,128)(2,1)S(1)} %collective-permute-done.17), channel_id=1, source_target_pairs={{0,30},{1,31},{2,0},{3,1},{4,2},{5,3},{6,4},{7,5},{8,6},{9,7},{10,... | collective-permute-start | bytes 460808 | tf_op jit(solution)/shard_map/ppermute | solution.py:120
  141.8 7.2 %collective-permute-start.25 = (bf16[24,3200]{1,0:T(8,128)(2,1)S(1)}, bf16[24,3200]{1,0:T(8,128)(2,1)S(1)}, u32[]{:S(2)}, u32[]{:S(2)}) collective-permute-start(bf16[24,3200]{1,0:T(8,128)(2,1)S(1)} %collective-permute-done.24), channel_id=1, source_target_pairs={{0,2},{1,3},{2,4},{3,5},{4,6},{5,7},{6,8},{7,9},{8,10},{9,11},{10,... | collective-permute-start | bytes 460808 | tf_op jit(solution)/shard_map/ppermute | solution.py:117
  144.7 7.8 %collective-permute-start.19 = (bf16[24,3200]{1,0:T(8,128)(2,1)S(1)}, bf16[24,3200]{1,0:T(8,128)(2,1)S(1)}, u32[]{:S(2)}, u32[]{:S(2)}) collective-permute-start(bf16[24,3200]{1,0:T(8,128)(2,1)S(1)} %collective-permute-done.18), channel_id=1, source_target_pairs={{0,30},{1,31},{2,0},{3,1},{4,2},{5,3},{6,4},{7,5},{8,6},{9,7},{10,... | collective-permute-start | bytes 460808 | tf_op jit(solution)/shard_map/ppermute | solution.py:120
  149.0 7.2 %collective-permute-start.26 = (bf16[24,3200]{1,0:T(8,128)(2,1)S(1)}, bf16[24,3200]{1,0:T(8,128)(2,1)S(1)}, u32[]{:S(2)}, u32[]{:S(2)}) collective-permute-start(bf16[24,3200]{1,0:T(8,128)(2,1)S(1)} %collective-permute-done.25), channel_id=1, source_target_pairs={{0,2},{1,3},{2,4},{3,5},{4,6},{5,7},{6,8},{7,9},{8,10},{9,11},{10,... | collective-permute-start | bytes 460808 | tf_op jit(solution)/shard_map/ppermute | solution.py:117
  152.5 6.9 %collective-permute-start.20 = (bf16[24,3200]{1,0:T(8,128)(2,1)S(1)}, bf16[24,3200]{1,0:T(8,128)(2,1)S(1)}, u32[]{:S(2)}, u32[]{:S(2)}) collective-permute-start(bf16[24,3200]{1,0:T(8,128)(2,1)S(1)} %collective-permute-done.19), channel_id=1, source_target_pairs={{0,30},{1,31},{2,0},{3,1},{4,2},{5,3},{6,4},{7,5},{8,6},{9,7},{10,... | collective-permute-start | bytes 460808 | tf_op jit(solution)/shard_map/ppermute | solution.py:120
  156.1 8.0 %collective-permute-start.27 = (bf16[24,3200]{1,0:T(8,128)(2,1)S(1)}, bf16[24,3200]{1,0:T(8,128)(2,1)S(1)}, u32[]{:S(2)}, u32[]{:S(2)}) collective-permute-start(bf16[24,3200]{1,0:T(8,128)(2,1)S(1)} %collective-permute-done.26), channel_id=1, source_target_pairs={{0,2},{1,3},{2,4},{3,5},{4,6},{5,7},{6,8},{7,9},{8,10},{9,11},{10,... | collective-permute-start | bytes 460808 | tf_op jit(solution)/shard_map/ppermute | solution.py:117
  159.4 7.6 %collective-permute-start.21 = (bf16[24,3200]{1,0:T(8,128)(2,1)S(1)}, bf16[24,3200]{1,0:T(8,128)(2,1)S(1)}, u32[]{:S(2)}, u32[]{:S(2)}) collective-permute-start(bf16[24,3200]{1,0:T(8,128)(2,1)S(1)} %collective-permute-done.20), channel_id=1, source_target_pairs={{0,30},{1,31},{2,0},{3,1},{4,2},{5,3},{6,4},{7,5},{8,6},{9,7},{10,... | collective-permute-start | bytes 460808 | tf_op jit(solution)/shard_map/ppermute | solution.py:120
  164.1 8.5 %collective-permute-start.28 = (bf16[24,3200]{1,0:T(8,128)(2,1)S(1)}, bf16[24,3200]{1,0:T(8,128)(2,1)S(1)}, u32[]{:S(2)}, u32[]{:S(2)}) collective-permute-start(bf16[24,3200]{1,0:T(8,128)(2,1)S(1)} %collective-permute-done.27), channel_id=1, source_target_pairs={{0,2},{1,3},{2,4},{3,5},{4,6},{5,7},{6,8},{7,9},{8,10},{9,11},{10,... | collective-permute-start | bytes 460808 | tf_op jit(solution)/shard_map/ppermute | solution.py:117
  167.1 15.2 %collective-permute-start.22 = (bf16[24,3200]{1,0:T(8,128)(2,1)S(1)}, bf16[24,3200]{1,0:T(8,128)(2,1)S(1)}, u32[]{:S(2)}, u32[]{:S(2)}) collective-permute-start(bf16[24,3200]{1,0:T(8,128)(2,1)S(1)} %collective-permute-done.21), channel_id=1, source_target_pairs={{0,30},{1,31},{2,0},{3,1},{4,2},{5,3},{6,4},{7,5},{8,6},{9,7},{10,... | collective-permute-start | bytes 460808 | tf_op jit(solution)/shard_map/ppermute | solution.py:120
  172.7 7.7 %collective-permute-start.29 = (bf16[24,3200]{1,0:T(8,128)(2,1)S(1)}, bf16[24,3200]{1,0:T(8,128)(2,1)S(1)}, u32[]{:S(2)}, u32[]{:S(2)}) collective-permute-start(bf16[24,3200]{1,0:T(8,128)(2,1)S(1)} %collective-permute-done.28), channel_id=1, source_target_pairs={{0,2},{1,3},{2,4},{3,5},{4,6},{5,7},{6,8},{7,9},{8,10},{9,11},{10,... | collective-permute-start | bytes 460808 | tf_op jit(solution)/shard_map/ppermute | solution.py:117
  180.3 7.2 %collective-permute-start.30 = (bf16[24,3200]{1,0:T(8,128)(2,1)S(1)}, bf16[24,3200]{1,0:T(8,128)(2,1)S(1)}, u32[]{:S(2)}, u32[]{:S(2)}) collective-permute-start(bf16[24,3200]{1,0:T(8,128)(2,1)S(1)} %collective-permute-done.29), channel_id=1, source_target_pairs={{0,2},{1,3},{2,4},{3,5},{4,6},{5,7},{6,8},{7,9},{8,10},{9,11},{10,... | collective-permute-start | bytes 460808 | tf_op jit(solution)/shard_map/ppermute | solution.py:117
  187.8 25.8 %collective-permute-start.31 = (bf16[384,3200]{1,0:T(8,128)(2,1)S(1)}, bf16[384,3200]{1,0:T(8,128)(2,1)S(1)}, u32[]{:S(2)}, u32[]{:S(2)}) collective-permute-start(bf16[384,3200]{1,0:T(8,128)(2,1)S(1)} %get-tuple-element.46), channel_id=1, source_target_pairs={{0,1},{1,0},{2,3},{3,2},{4,5},{5,4},{6,7},{7,6},{8,9},{9,8},{10,11... | collective-permute-start | bytes 7372808 | tf_op jit(solution)/shard_map/ppermute | solution.py:123
  214.6 8.4 %copy-start.16 = (bf16[768,3200]{1,0:T(8,128)(2,1)}, bf16[768,3200]{1,0:T(8,128)(2,1)S(1)}, u32[]{:S(2)}) copy-start(bf16[768,3200]{1,0:T(8,128)(2,1)S(1)} %constant_dynamic-update-slice_fusion.18) | copy-start | bytes 14745604
  225.4 17.5 %all-to-all-start.2 = ((f32[32,1,192]{2,1,0:T(1,128)}), f32[32,1,192]{2,1,0:T(1,128)}, u32[]{:S(2)}, u32[]{:S(2)}) async-start(f32[32,1,192]{2,1,0:T(1,128)} %all_to_all.20), calls=%async_computation.2 | async-start | bytes 65536 | tf_op jit(solution)/shard_map/all_to_all | solution.py:132
  242.9 19.1 %all-to-all-start.1 = ((bf16[16,232,128]{2,1,0:T(8,128)(2,1)}), bf16[16,232,128]{2,1,0:T(8,128)(2,1)}, u32[]{:S(2)}, u32[]{:S(2)}) async-start(bf16[16,232,128]{2,1,0:T(8,128)(2,1)} %pad_maximum_fusion.2), calls=%async_computation.1 | async-start | bytes 1900544 | tf_op jit(solution)/shard_map/all_to_all | solution.py:150
  247.3 28.5 %copy-start.27 = (s32[192,1]{0,1:T(1,128)S(1)}, s32[192,1]{0,1:T(1,128)}, u32[]{:S(2)}) copy-start(s32[192,1]{0,1:T(1,128)} %copy-done.26) | copy-start | bytes 2308
  247.3 29.5 %copy-start.25 = (s32[192,1]{0,1:T(1,128)S(1)}, s32[192,1]{0,1:T(1,128)}, u32[]{:S(2)}) copy-start(s32[192,1]{0,1:T(1,128)} %copy-done.24) | copy-start | bytes 2308
  247.3 31.5 %copy-start.20 = (s32[192]{0:T(256)S(1)}, s32[192]{0:T(256)}, u32[]{:S(2)}) copy-start(s32[192]{0:T(256)} %copy-done.19) | copy-start | bytes 2308
  247.3 31.5 %copy-start.22 = (s32[192]{0:T(256)S(1)}, s32[192]{0:T(256)}, u32[]{:S(2)}) copy-start(s32[192]{0:T(256)} %copy-done.21) | copy-start | bytes 2308
  263.3 25.6 %copy-start.3 = (f32[192,128]{1,0:T(8,128)}, f32[192,128]{1,0:T(8,128)S(1)}, u32[]{:S(2)}) copy-start(f32[192,128]{1,0:T(8,128)S(1)} %convert_reduce_fusion) | copy-start | bytes 294916
  264.2 23.2 %all-to-all-start.3 = ((f32[32,1,384]{2,1,0:T(1,128)}), f32[32,1,384]{2,1,0:T(1,128)S(1)}, u32[]{:S(2)}, u32[]{:S(2)}) async-start(f32[32,1,384]{2,1,0:T(1,128)} %broadcast_in_dim.131), calls=%async_computation.3 | async-start | bytes 98304 | tf_op jit(solution)/shard_map/all_to_all | solution.py:162
  (25 other events, 53.3 us)

commit v2 on v1

v2 whole, which is shorter than its diff:
```python
import jax
import jax.numpy as jnp
from jax import lax
from jax.experimental import pallas as pl
from jax.experimental.pallas import tpu as pltpu
from jax.sharding import PartitionSpec as P

BF = jnp.bfloat16
F32 = jnp.float32
VM = pl.BlockSpec(memory_space=pltpu.VMEM)


def mm(a, b, dims=((1,), (0,))):
    return lax.dot_general(a, b, (dims, ((), ())), preferred_element_type=F32)


NT = ((1,), (1,))


def hot(a, b):
    return (a == b).astype(BF)


def call(kernel, outs, *args):
    return pl.pallas_call(
        kernel,
        out_shape=[jax.ShapeDtypeStruct(s, d) for s, d in outs],
        in_specs=[VM] * len(args),
        out_specs=[VM] * len(outs),
    )(*args)


def project(pick, got, both, kind, eg, eu, ed, sg, su, sd, own_r, own_l, out_r, out_l, mine_ref):
    le, width, hidden = eg.shape
    nb = got.shape[0]
    mine = mm(pick[:, :nb], got[...]) + mm(pick[:, nb:], both[...])
    mine_ref[...] = mine.astype(BF)
    kd = kind[...]
    part = [jnp.where(kd == e, mine, 0.0).astype(BF) for e in range(le + 1)]
    x = jnp.concatenate([p[:, :width] for p in part[:le]], 1)
    g = jnp.concatenate([p[:, width:] for p in part[:le]], 1)
    nr, nl = own_r.shape[0], own_l.shape[0]
    half = nr + nl
    todo = ((x, part[le][:, :width], eg, sg), (x, part[le][:, :width], eu, su), (g, part[le][:, width:], ed, sd))
    for t, (xe, xs, we, ws) in enumerate(todo):
        cols = slice(t * hidden, (t + 1) * hidden)
        p = mm(xe, we[...].reshape(le * width, hidden)) + mm(xs, ws[...])
        own_r[:, cols] = p[:nr]
        own_l[:, cols] = p[nr:half]
        out_r[:, cols] = p[half : half + nr].astype(BF)
        out_l[:, cols] = p[half + nr :].astype(BF)


def shared_grads(kept, other, xt, gt, out):
    half = kept.shape[0]
    n_ep, rows, width = out.shape
    cols = rows // 3
    hidden = cols * n_ep
    for t, lhs in enumerate((xt, xt, gt)):
        part = slice(t * hidden, (t + 1) * hidden)
        r = mm(lhs[:, :half], kept[:, part]) + mm(lhs[:, half:], other[:, part])
        out[:, t * cols : (t + 1) * cols, :] = r.T.astype(BF).reshape(n_ep, cols, width)


def expert_grads(kept, other, xt, gt, eg, eu, sg, su, kind, pick_t, tail_t, lane_hot, stack, sq, back, shared):
    le, width, hidden = eg.shape
    half = kept.shape[0]
    nb = back.shape[0]
    slots = []
    for h, src in enumerate((kept, other)):
        gg, gu = src[:, :hidden], src[:, hidden : 2 * hidden]
        se = mm(gg, eg[...].reshape(le * width, hidden), NT) + mm(gu, eu[...].reshape(le * width, hidden), NT)
        ss = mm(gg, sg[...], NT) + mm(gu, su[...], NT)
        kd = kind[h * half : (h + 1) * half, :]
        s = jnp.where(kd == le, ss, 0.0)
        for e in range(le):
            s = s + jnp.where(kd == e, se[:, e * width : (e + 1) * width], 0.0)
        slots.append(s)
    slot = jnp.concatenate(slots, 0)
    hi = slot.astype(BF)
    rest = slot - hi.astype(F32)
    mid = rest.astype(BF)
    low = (rest - mid.astype(F32)).astype(BF)
    wg = jnp.concatenate([kept[:, 3 * hidden :], other[:, 3 * hidden :]], 0).astype(F32)
    wg = (wg * lane_hot[...].astype(F32)).astype(BF)
    back[...] = (mm(pick_t[:nb, :], hi) + mm(tail_t[...], wg)).astype(BF)
    ps = pick_t[nb:, :]
    shared[...] = mm(ps, hi) + mm(ps, mid) + mm(ps, low)
    for t, lhs in enumerate((xt, xt, gt)):
        part = slice(t * hidden, (t + 1) * hidden)
        r = mm(lhs[:, :half], kept[:, part]) + mm(lhs[:, half:], other[:, part])
        r = r.reshape(le, width, hidden)
        stack[t] = r.astype(BF)
        sq[t] = jnp.sum(r * r, axis=1)


def row_backward(summed, weights):
    hidden = summed.shape[1] // 3
    pre_gate = summed[:, :hidden]
    pre_up = summed[:, hidden : 2 * hidden]
    back_act = summed[:, 2 * hidden :]
    sigmoid_gate = jax.nn.sigmoid(pre_gate)
    silu_gate = pre_gate * sigmoid_gate
    activation = silu_gate * pre_up
    act_grad = weights * back_act
    grad_up = (act_grad * silu_gate).astype(BF)
    grad_gate = (act_grad * pre_up * sigmoid_gate * (1.0 + pre_gate * (1.0 - sigmoid_gate))).astype(BF)
    scaled_act = (weights * activation).astype(BF)
    weight_grad = jnp.sum(activation * back_act, axis=1, keepdims=True).astype(BF)
    return grad_gate, grad_up, scaled_act, weight_grad


def body(tokens, cotangent, routes, gate_weights, e_gate, e_up, e_down, s_gate, s_up, s_down):
    n_ep, n_tp = lax.axis_size("ep"), lax.axis_size("tp")
    nz = n_tp // 2
    rows, width = tokens.shape
    top = routes.shape[1]
    le, _, hidden = e_gate.shape
    experts = le * n_ep
    cap = 3 * rows * top // (2 * experts)
    ls = le * cap
    bl = (ls + 8) // 8 * 8
    slots = n_ep * ls
    total = slots + rows
    half = total // 2
    piece = total // n_tp
    tp = lax.axis_index("tp")
    z, c = tp // 2, tp % 2
    fwd = [(i, (i + 2 - 4 * (i % 2)) % n_tp) for i in range(n_tp)]
    bwd = [(i, (i - 2 + 4 * (i % 2)) % n_tp) for i in range(n_tp)]
    swap = [(i, i ^ 1) for i in range(n_tp)]

    ids = jnp.arange(experts, dtype=jnp.int32)
    on = [hot(routes[:, k : k + 1], ids[None, :]) for k in range(top)]
    tri = (jnp.arange(rows)[:, None] > jnp.arange(rows)[None, :]).astype(BF)
    before = mm(tri, sum(on))
    dest, within = [], []
    for k in range(top):
        pos = jnp.sum(on[k].astype(F32) * before, axis=1).astype(jnp.int32)
        dest.append(routes[:, k] // le)
        within.append(routes[:, k] % le * cap + pos)
    blk = jnp.arange(n_ep * bl, dtype=jnp.int32)
    spread = sum(hot(blk[:, None], (dest[k] * bl + within[k])[None, :]) for k in range(top))
    tail = hot(blk[:, None], (jnp.arange(n_ep, dtype=jnp.int32) * bl + ls)[None, :])
    groups = jnp.arange(n_ep, dtype=jnp.int32)
    lanes = jnp.arange(2 * width, dtype=jnp.int32)
    w_block = sum(
        mm(hot(groups[:, None], dest[k][None, :]) * gate_weights[:, k][None, :], hot(within[k][:, None], lanes[None, :]))
        for k in range(top)
    ).astype(BF)
    both = jnp.concatenate([tokens, cotangent], axis=1)
    sent = mm(jnp.concatenate([spread, tail], 1), jnp.concatenate([both, w_block], 0)).astype(BF)
    got = lax.all_to_all(sent.reshape(n_ep, bl, 2 * width), "ep", 0, 0, tiled=True)

    r = jnp.arange(total, dtype=jnp.int32)
    h = r // half
    turn = (1 - 2 * c) * (1 - 2 * h) * (r % half // piece)
    place = piece * (2 * ((z + turn) % nz) + (c ^ h)) + r % piece
    kind = jnp.where(place < slots, place % ls // cap, le)
    src = jnp.where(place < slots, place // ls * bl + place % ls, n_ep * bl + place - slots)
    column = jnp.arange(n_ep * bl + rows, dtype=jnp.int32)
    pick = hot(src[:, None], column[None, :])
    hops, back_hops = nz // 2, nz - nz // 2 - 1
    nr, nl = (hops + 1) * piece, back_hops * piece
    width3 = 3 * hidden
    own_r, own_l, out_r, out_l, mine = call(
        project,
        [((nr, width3), F32), ((nl, width3), F32), ((nr, width3), BF), ((nl, width3), BF), ((total, 2 * width), BF)],
        pick, got.reshape(n_ep * bl, 2 * width), both, kind[:, None], e_gate, e_up, e_down, s_gate, s_up, s_down,
    )
    oth_r = lax.ppermute(out_r, "tp", swap)
    oth_l = lax.ppermute(out_l, "tp", swap)

    def at_r(j):
        rows_j = slice(j * piece, (j + 1) * piece)
        return own_r[rows_j] + oth_r[rows_j].astype(F32)

    def at_l(j):
        rows_j = slice((back_hops - j) * piece, (back_hops - j + 1) * piece)
        return own_l[rows_j] + oth_l[rows_j].astype(F32)

    right, left = at_r(hops).astype(BF), at_l(back_hops).astype(BF)
    for t in range(hops):
        right = lax.ppermute(right, "tp", fwd)
        if t < hops - 1:
            right = right.astype(F32) + at_r(hops - 1 - t)
            right = right if t == hops - 2 else right.astype(BF)
        if t < back_hops:
            left = lax.ppermute(left, "tp", bwd)
        if t < back_hops - 1:
            left = left.astype(F32) + at_l(back_hops - 1 - t)
            left = left if t == back_hops - 2 else left.astype(BF)
    summed = right.astype(F32) + left.astype(F32) + at_r(0)

    q = tp * piece + jnp.arange(piece, dtype=jnp.int32)
    w_rows = mm(hot((q // ls)[:, None], groups[None, :]), got[:, ls, :])
    own_w = jnp.sum(jnp.where((q % ls)[:, None] == lanes[None, :], w_rows, 0.0), axis=1)
    own_w = jnp.where(q < slots, own_w, 1.0)[:, None]
    gg, gu, sa, wg = row_backward(summed, own_w)
    block = jnp.concatenate([gg, gu, sa, jnp.broadcast_to(wg, (piece, 128))], 1)

    ring = [None] * nz
    ring[0] = right = left = block
    for t in range(1, hops + 1):
        right = lax.ppermute(right, "tp", fwd)
        ring[-t % nz] = right
        if t <= back_hops:
            left = lax.ppermute(left, "tp", bwd)
            ring[t] = left
    kept = jnp.concatenate(ring, 0)
    other = lax.ppermute(kept, "tp", swap)

    kind_row = kind[None, :]
    mine_t = mine.T
    x_t = [jnp.where(kind_row == e, mine_t[:width], 0) for e in range(le + 1)]
    g_t = [jnp.where(kind_row == e, mine_t[width:], 0) for e in range(le + 1)]
    cols = hidden // n_ep
    (sh,) = call(shared_grads, [((n_ep, 3 * cols, width), BF)], kept, other, x_t[le], g_t[le])
    sh_home = lax.all_to_all(sh, "ep", 0, 0, tiled=True)

    lane1 = jnp.arange(width, dtype=jnp.int32)
    pick_t = hot(column[:, None], src[None, :])
    tail_t = hot(blk[:, None], jnp.where(place < slots, place // ls * bl + ls, -1)[None, :])
    lane_hot = hot((place % ls)[:, None], lane1[None, :])
    stack, e_sq, back, shared_part = call(
        expert_grads,
        [((3, le, width, hidden), BF), ((3, le, hidden), F32), ((n_ep * bl, width), BF), ((rows, width), F32)],
        kept, other, jnp.concatenate(x_t[:le], 0), jnp.concatenate(g_t[:le], 0),
        e_gate, e_up, s_gate, s_up, kind[:, None], pick_t, tail_t, lane_hot,
    )
    piece_sq = jnp.sum(lax.all_to_all(e_sq.reshape(n_tp, -1), "tp", 0, 0, tiled=True), axis=0)
    home = lax.all_to_all(back.reshape(n_ep, bl, width), "ep", 0, 0, tiled=True)
    rows_home = home.reshape(n_ep * bl, width)
    token_grad = (mm(spread, rows_home, ((0,), (0,))) + shared_part).astype(BF)
    wg_home = home[:, ls]
    gate_grad = []
    for k in range(top):
        line = mm(hot(dest[k][:, None], groups[None, :]), wg_home)
        gate_grad.append(jnp.sum(jnp.where(within[k][:, None] == lane1[None, :], line, 0.0), axis=1))
    gate_grad = jnp.stack(gate_grad, 1).astype(BF)
    shared = jnp.sum(sh_home.astype(F32), axis=0).reshape(3, cols, width)
    s_sq = jnp.sum(shared * shared, axis=2).reshape(-1)
    line = jnp.concatenate([piece_sq, s_sq])
    lines = lax.all_to_all(jnp.broadcast_to(line[None], (n_tp, line.size)), "tp", 0, 0, tiled=True)
    scale = 1.0 / (width * n_tp)
    n_e = piece_sq.size
    return (
        token_grad,
        gate_grad,
        stack,
        jnp.swapaxes(shared, 1, 2),
        lines[:, :n_e].reshape(3, le, hidden) * scale,
        jnp.sum(lines[:, n_e:], axis=0).reshape(3, cols) * scale,
    )


def solution(mesh):
    return jax.shard_map(
        body,
        mesh=mesh,
        in_specs=(
            P("ep", "tp"),
            P("ep", "tp"),
            P("ep", None),
            P("ep", None),
            P("ep", "tp", None),
            P("ep", "tp", None),
            P("ep", "tp", None),
            P("tp", None),
            P("tp", None),
            P("tp", None),
        ),
        out_specs=(
            P("ep", "tp"),
            P("ep", None),
            P(None, "ep", "tp", None),
            P(None, "tp", "ep"),
            P(None, "ep", None),
            P(None, "ep"),
        ),
        check_vma=False,
    )
```

time: 291 us -> 288 us (0.990)
  waiting for transfers between devices: 96.2 us -> 44.7 us
  blocking collectives: 0 us -> 24.2 us
  Pallas kernels: 0 us -> 23.1 us
  matrix products: 24 us -> 2.9 us
  other arithmetic: 15.5 us -> 28.6 us
  starting transfers between devices: 140 us -> 153 us
  local copies, waits for them, and re-layouts: 11.8 us -> 7.59 us
    ppermute x32 -> x33, waiting for transfers between devices: 66.9 us -> 14.9 us  [the longest x16 11.2 us: body(): right = lax.ppermute(right, 'tp', fwd)]
    all_to_all x0 -> x1, blocking collectives: none -> 24.2 us  [body(): lax.all_to_all(e_sq.reshape(n_tp, -1), 'tp', 0, 0, tiled=True)]
    pallas_call x0 -> x3, Pallas kernels: none -> 23.1 us  [call(): pl.pallas_call(kernel, out_shape=[jax.ShapeDtypeStruct(s, d) for s, d in...]
    dot_general x23 -> x8, matrix products: 24 us -> 2.9 us  [mm(): return lax.dot_general(a, b, (dims, ((), ())), preferred_element_type=F32)]
    ppermute x32 -> x33, starting transfers between devices: 111 us -> 132 us  [the longest x16 82.3 us: body(): right = lax.ppermute(right, 'tp', fwd)]
    convert_element_type x9 -> x14, other arithmetic: 5.17 us -> 13.6 us  [the longest x6 5.87 us: body(): right = right if t == hops - 2 else right.astype(BF)]
    all_to_all x1, waiting for transfers between devices: 5.7 us -> 11.9 us  [body(): lax.all_to_all(jnp.broadcast_to(line[None], (n_tp, line.size)), 'tp', 0,...]
    convert_element_type x1 -> x5, other arithmetic: 0.05 us -> 5.1 us  [hot(): return (a == b).astype(BF)]
  transfers between devices with their start and end apart: 36 -> 37, of which waited for: 35 -> 16; matrix products, arithmetic and copies ran while one was open for 7% -> 10% of each run, Pallas kernels for 0% -> 2%
where the time goes in v2:
time: 288 us; the launch traced here: 286 us
  starting transfers between devices  153 us (53%)
  waiting for transfers between devices  44.7 us (16%)
  other arithmetic  28.6 us (10%)
  blocking collectives  24.2 us (8%)
  Pallas kernels  23.1 us (8%)
  local copies, waits for them, and re-layouts  7.59 us (3%)
  matrix products  2.9 us (1%)
    ppermute x16, starting transfers between devices, body(): right = lax.ppermute(right, 'tp', fwd)  82.3 us
    ppermute x14, starting transfers between devices, body(): left = lax.ppermute(left, 'tp', bwd)  26.8 us
    all_to_all x1, blocking collectives, body(): lax.all_to_all(e_sq.reshape(n_tp, -1), 'tp', 0, 0, tiled=True)  24.2 us
    pallas_call x3, Pallas kernels, call(): pl.pallas_call(kernel, out_shape=[jax.ShapeDtypeStruct(s, d) for s, d in...  23.1 us
    ppermute x1, starting transfers between devices, body(): other = lax.ppermute(kept, 'tp', swap)  14.8 us
    all_to_all x1, waiting for transfers between devices, body(): lax.all_to_all(jnp.broadcast_to(line[None], (n_tp, line.size)), 'tp', 0,...  11.9 us
    ppermute x16, waiting for transfers between devices, body(): right = lax.ppermute(right, 'tp', fwd)  11.2 us
    all_to_all x1, waiting for transfers between devices, body(): sh_home = lax.all_to_all(sh, 'ep', 0, 0, tiled=True)  11 us
  transfers between devices with their start and end apart: 37, of which 16 were waited for; matrix products, arithmetic and copies ran while one was open for 10% of the time, Pallas kernels for 2%

profile of v2, /device:TPU:1, one launch (start us, length us, event | category | flops | bytes accessed | tf_op | source)
XLA Modules:
  0.0 285.7 jit_solution(16426175670418535633)
XLA Ops:
  5.8 7.6 %all-to-all-start = ((bf16[16,40,256]{2,1,0:T(8,128)(2,1)}), bf16[16,40,256]{2,1,0:T(8,128)(2,1)S(1)}, u32[]{:S(2)}, u32[]{:S(2)}) async-start(bf16[16,40,256]{2,1,0:T(8,128)(2,1)} %bitcast.6), calls=%async_computation | async-start | bytes 655360 | tf_op jit(solution)/shard_map/all_to_all | solution.py:153
  14.8 2.2 fusion.22.kind
  17.0 4.2 %all-to-all-done = bf16[16,40,256]{2,1,0:T(8,128)(2,1)S(1)} async-done(((bf16[16,40,256]{2,1,0:T(8,128)(2,1)}), bf16[16,40,256]{2,1,0:T(8,128)(2,1)S(1)}, u32[]{:S(2)}, u32[]{:S(2)}) %all-to-all-start) | async-done | bytes 327712 | tf_op jit(solution)/shard_map/all_to_all | solution.py:153
  22.0 8.9 %shard_map.145 = (f32[216,3072]{1,0:T(8,128)}, f32[168,3072]{1,0:T(8,128)}, bf16[216,3072]{1,0:T(8,128)(2,1)}, bf16[168,3072]{1,0:T(8,128)(2,1)}, bf16[768,256]{1,0:T(8,128)(2,1)}) custom-call(bf16[768,832]{1,0:T(8,128)(2,1)} %fusion.pick, bf16[640,256]{1,0:T(8,128)(2,1)} %bitcast.29, bf16[192,256]{1,0:T(8,128)(2,1)} %copy-done.6, s32[768,1]{1,0:T(8,128)} %fusion.22.kind, ...), custom_call_target="tpu_custom_call" | custom-call | tf_op jit(solution)/shard_map/pallas_call | solution.py:25
  30.9 6.1 %collective-permute-start = (bf16[216,3072]{1,0:T(8,128)(2,1)}, bf16[216,3072]{1,0:T(8,128)(2,1)}, u32[]{:S(2)}, u32[]{:S(2)}) collective-permute-start(bf16[216,3072]{1,0:T(8,128)(2,1)} %get-tuple-element.16), channel_id=1, source_target_pairs={{0,1},{1,0},{2,3},{3,2},{4,5},{5,4},{6,7},{7,6},{8,9},{9,8},{10,11... | collective-permute-start | bytes 3981320 | tf_op jit(solution)/shard_map/ppermute | solution.py:171
  37.0 1.9 collective-permute-start.9
  41.0 9.6 %collective-permute-start.1 = (bf16[24,3072]{1,0:T(8,128)(2,1)S(1)}, bf16[24,3072]{1,0:T(8,128)(2,1)S(1)}, u32[]{:S(2)}, u32[]{:S(2)}) collective-permute-start(bf16[24,3072]{1,0:T(8,128)(2,1)S(1)} %add_convert_fusion.12), channel_id=1, source_target_pairs={{0,2},{1,31},{2,4},{3,1},{4,6},{5,3},{6,8},{7,5},{8,10},{9,7},{10,... | collective-permute-start | bytes 442376 | tf_op jit(solution)/shard_map/ppermute | solution.py:184
  51.7 1.9 collective-permute-start.10
  54.7 4.6 %collective-permute-start.2 = (bf16[24,3072]{1,0:T(8,128)(2,1)S(1)}, bf16[24,3072]{1,0:T(8,128)(2,1)S(1)}, u32[]{:S(2)}, u32[]{:S(2)}) collective-permute-start(bf16[24,3072]{1,0:T(8,128)(2,1)S(1)} %add_convert_fusion.11), channel_id=1, source_target_pairs={{0,2},{1,31},{2,4},{3,1},{4,6},{5,3},{6,8},{7,5},{8,10},{9,7},{10,... | collective-permute-start | bytes 442376 | tf_op jit(solution)/shard_map/ppermute | solution.py:184
  60.3 1.9 collective-permute-start.11
  63.3 4.6 %collective-permute-start.3 = (bf16[24,3072]{1,0:T(8,128)(2,1)S(1)}, bf16[24,3072]{1,0:T(8,128)(2,1)S(1)}, u32[]{:S(2)}, u32[]{:S(2)}) collective-permute-start(bf16[24,3072]{1,0:T(8,128)(2,1)S(1)} %add_convert_fusion.10), channel_id=1, source_target_pairs={{0,2},{1,31},{2,4},{3,1},{4,6},{5,3},{6,8},{7,5},{8,10},{9,7},{10,... | collective-permute-start | bytes 442376 | tf_op jit(solution)/shard_map/ppermute | solution.py:184
  68.9 1.9 collective-permute-start.12
  71.8 4.6 %collective-permute-start.4 = (bf16[24,3072]{1,0:T(8,128)(2,1)S(1)}, bf16[24,3072]{1,0:T(8,128)(2,1)S(1)}, u32[]{:S(2)}, u32[]{:S(2)}) collective-permute-start(bf16[24,3072]{1,0:T(8,128)(2,1)S(1)} %add_convert_fusion.9), channel_id=1, source_target_pairs={{0,2},{1,31},{2,4},{3,1},{4,6},{5,3},{6,8},{7,5},{8,10},{9,7},{10,... | collective-permute-start | bytes 442376 | tf_op jit(solution)/shard_map/ppermute | solution.py:184
  77.4 1.9 collective-permute-start.13
  80.3 4.6 %collective-permute-start.5 = (bf16[24,3072]{1,0:T(8,128)(2,1)S(1)}, bf16[24,3072]{1,0:T(8,128)(2,1)S(1)}, u32[]{:S(2)}, u32[]{:S(2)}) collective-permute-start(bf16[24,3072]{1,0:T(8,128)(2,1)S(1)} %add_convert_fusion.8), channel_id=1, source_target_pairs={{0,2},{1,31},{2,4},{3,1},{4,6},{5,3},{6,8},{7,5},{8,10},{9,7},{10,... | collective-permute-start | bytes 442376 | tf_op jit(solution)/shard_map/ppermute | solution.py:184
  85.8 1.9 collective-permute-start.14
  88.8 4.6 %collective-permute-start.6 = (bf16[24,3072]{1,0:T(8,128)(2,1)S(1)}, bf16[24,3072]{1,0:T(8,128)(2,1)S(1)}, u32[]{:S(2)}, u32[]{:S(2)}) collective-permute-start(bf16[24,3072]{1,0:T(8,128)(2,1)S(1)} %add_convert_fusion.7), channel_id=1, source_target_pairs={{0,2},{1,31},{2,4},{3,1},{4,6},{5,3},{6,8},{7,5},{8,10},{9,7},{10,... | collective-permute-start | bytes 442376 | tf_op jit(solution)/shard_map/ppermute | solution.py:184
  94.3 1.9 collective-permute-start.15
  97.2 4.6 %collective-permute-start.7 = (bf16[24,3072]{1,0:T(8,128)(2,1)S(1)}, bf16[24,3072]{1,0:T(8,128)(2,1)S(1)}, u32[]{:S(2)}, u32[]{:S(2)}) collective-permute-start(bf16[24,3072]{1,0:T(8,128)(2,1)S(1)} %add_convert_fusion.6), channel_id=1, source_target_pairs={{0,2},{1,31},{2,4},{3,1},{4,6},{5,3},{6,8},{7,5},{8,10},{9,7},{10,... | collective-permute-start | bytes 442376 | tf_op jit(solution)/shard_map/ppermute | solution.py:184
  102.8 1.9 collective-permute-start.16
  105.7 4.8 %collective-permute-start.8 = (f32[24,3072]{1,0:T(8,128)S(1)}, f32[24,3072]{1,0:T(8,128)S(1)}, u32[]{:S(2)}, u32[]{:S(2)}) collective-permute-start(f32[24,3072]{1,0:T(8,128)S(1)} %add_add_fusion.2), channel_id=1, source_target_pairs={{0,2},{1,31},{2,4},{3,1},{4,6},{5,3},{6,8},{7,5},{8,10},{9,7},{10,... | collective-permute-start | bytes 884744 | tf_op jit(solution)/shard_map/ppermute | solution.py:184
  112.5 4.6 %collective-permute-done.8 = f32[24,3072]{1,0:T(8,128)S(1)} collective-permute-done((f32[24,3072]{1,0:T(8,128)S(1)}, f32[24,3072]{1,0:T(8,128)S(1)}, u32[]{:S(2)}, u32[]{:S(2)}) %collective-permute-start.8) | collective-permute-done | bytes 294944 | tf_op jit(solution)/shard_map/ppermute | solution.py:184
  118.3 1.9 collective-permute-start.17
  120.3 5.3 %collective-permute-start.24 = (bf16[24,3200]{1,0:T(8,128)(2,1)S(1)}, bf16[24,3200]{1,0:T(8,128)(2,1)S(1)}, u32[]{:S(2)}, u32[]{:S(2)}) collective-permute-start(bf16[24,3200]{1,0:T(8,128)(2,1)S(1)} %get-tuple-element.50), channel_id=1, source_target_pairs={{0,2},{1,31},{2,4},{3,1},{4,6},{5,3},{6,8},{7,5},{8,10},{9,7},{10,... | collective-permute-start | bytes 460808 | tf_op jit(solution)/shard_map/ppermute | solution.py:205
  126.2 1.9 collective-permute-start.18
  129.0 5.0 %collective-permute-start.25 = (bf16[24,3200]{1,0:T(8,128)(2,1)S(1)}, bf16[24,3200]{1,0:T(8,128)(2,1)S(1)}, u32[]{:S(2)}, u32[]{:S(2)}) collective-permute-start(bf16[24,3200]{1,0:T(8,128)(2,1)S(1)} %collective-permute-done.24), channel_id=1, source_target_pairs={{0,2},{1,31},{2,4},{3,1},{4,6},{5,3},{6,8},{7,5},{8,10},{9,7},{10,... | collective-permute-start | bytes 460808 | tf_op jit(solution)/shard_map/ppermute | solution.py:205
  134.3 1.9 collective-permute-start.19
  137.0 5.3 %collective-permute-start.26 = (bf16[24,3200]{1,0:T(8,128)(2,1)S(1)}, bf16[24,3200]{1,0:T(8,128)(2,1)S(1)}, u32[]{:S(2)}, u32[]{:S(2)}) collective-permute-start(bf16[24,3200]{1,0:T(8,128)(2,1)S(1)} %collective-permute-done.25), channel_id=1, source_target_pairs={{0,2},{1,31},{2,4},{3,1},{4,6},{5,3},{6,8},{7,5},{8,10},{9,7},{10,... | collective-permute-start | bytes 460808 | tf_op jit(solution)/shard_map/ppermute | solution.py:205
  142.6 1.9 collective-permute-start.20
  144.5 4.9 %collective-permute-start.27 = (bf16[24,3200]{1,0:T(8,128)(2,1)S(1)}, bf16[24,3200]{1,0:T(8,128)(2,1)S(1)}, u32[]{:S(2)}, u32[]{:S(2)}) collective-permute-start(bf16[24,3200]{1,0:T(8,128)(2,1)S(1)} %collective-permute-done.26), channel_id=1, source_target_pairs={{0,2},{1,31},{2,4},{3,1},{4,6},{5,3},{6,8},{7,5},{8,10},{9,7},{10,... | collective-permute-start | bytes 460808 | tf_op jit(solution)/shard_map/ppermute | solution.py:205
  149.8 1.9 collective-permute-start.21
  151.7 4.9 %collective-permute-start.28 = (bf16[24,3200]{1,0:T(8,128)(2,1)S(1)}, bf16[24,3200]{1,0:T(8,128)(2,1)S(1)}, u32[]{:S(2)}, u32[]{:S(2)}) collective-permute-start(bf16[24,3200]{1,0:T(8,128)(2,1)S(1)} %collective-permute-done.27), channel_id=1, source_target_pairs={{0,2},{1,31},{2,4},{3,1},{4,6},{5,3},{6,8},{7,5},{8,10},{9,7},{10,... | collective-permute-start | bytes 460808 | tf_op jit(solution)/shard_map/ppermute | solution.py:205
  156.9 1.9 collective-permute-start.22
  158.9 4.9 %collective-permute-start.29 = (bf16[24,3200]{1,0:T(8,128)(2,1)S(1)}, bf16[24,3200]{1,0:T(8,128)(2,1)S(1)}, u32[]{:S(2)}, u32[]{:S(2)}) collective-permute-start(bf16[24,3200]{1,0:T(8,128)(2,1)S(1)} %collective-permute-done.28), channel_id=1, source_target_pairs={{0,2},{1,31},{2,4},{3,1},{4,6},{5,3},{6,8},{7,5},{8,10},{9,7},{10,... | collective-permute-start | bytes 460808 | tf_op jit(solution)/shard_map/ppermute | solution.py:205
  166.0 4.9 %collective-permute-start.30 = (bf16[24,3200]{1,0:T(8,128)(2,1)S(1)}, bf16[24,3200]{1,0:T(8,128)(2,1)S(1)}, u32[]{:S(2)}, u32[]{:S(2)}) collective-permute-start(bf16[24,3200]{1,0:T(8,128)(2,1)S(1)} %collective-permute-done.29), channel_id=1, source_target_pairs={{0,2},{1,31},{2,4},{3,1},{4,6},{5,3},{6,8},{7,5},{8,10},{9,7},{10,... | collective-permute-start | bytes 460808 | tf_op jit(solution)/shard_map/ppermute | solution.py:205
  171.0 2.1 collective-permute-done.30
  173.1 5.0 %collective-permute-start.31 = (bf16[24,3200]{1,0:T(8,128)(2,1)S(1)}, bf16[24,3200]{1,0:T(8,128)(2,1)S(1)}, u32[]{:S(2)}, u32[]{:S(2)}) collective-permute-start(bf16[24,3200]{1,0:T(8,128)(2,1)S(1)} %collective-permute-done.30), channel_id=1, source_target_pairs={{0,2},{1,31},{2,4},{3,1},{4,6},{5,3},{6,8},{7,5},{8,10},{9,7},{10,... | collective-permute-start | bytes 460808 | tf_op jit(solution)/shard_map/ppermute | solution.py:205
  178.1 2.8 collective-permute-done.31
  181.2 14.8 %collective-permute-start.32 = (bf16[384,3200]{1,0:T(8,128)(2,1)S(1)}, bf16[384,3200]{1,0:T(8,128)(2,1)}, u32[]{:S(2)}, u32[]{:S(2)}) collective-permute-start(bf16[384,3200]{1,0:T(8,128)(2,1)S(1)} %constant_dynamic-update-slice_fusion.2.kept), channel_id=1, source_target_pairs={{0,1},{1,0},{2,3},{3,2},{4,5},{5,4},{6,7},{7,6},{8,9},{9,8},{10,11... | collective-permute-start | bytes 7372808 | tf_op jit(solution)/shard_map/ppermute | solution.py:211
  202.4 9.8 %shard_map.146 = (bf16[3,2,128,1024]{3,2,1,0:T(8,128)(2,1)}, f32[3,2,1024]{2,1,0:T(2,128)}, bf16[640,128]{1,0:T(8,128)(2,1)}, f32[192,128]{1,0:T(8,128)}) custom-call(bf16[384,3200]{1,0:T(8,128)(2,1)} %copy-done, bf16[384,3200]{1,0:T(8,128)(2,1)} %collective-permute-done.32.other, bf16[256,768]{1,0:T(8,128)(2,1)} %pad_maximum_fusion.xt, ...), custom_call_target="tpu_custom_call" | custom-call | tf_op jit(solution)/shard_map/pallas_call | solution.py:25
  213.0 24.2 %all_to_all.34 = f32[32,1,192]{2,1,0:T(1,128)S(1)} all-to-all(f32[32,1,192]{2,1,0:T(1,128)S(1)} %all_to_all.28), channel_id=1, replica_groups=mesh['ep'=16,'tp'=32] {'tp'}, dimensions={0} | all-to-all | bytes 49152 | tf_op jit(solution)/shard_map/all_to_all | solution.py:231
  237.2 3.5 %all-to-all-start.1 = ((bf16[16,40,128]{2,1,0:T(8,128)(2,1)}), bf16[16,40,128]{2,1,0:T(8,128)(2,1)S(1)}, u32[]{:S(2)}, u32[]{:S(2)}) async-start(bf16[16,40,128]{2,1,0:T(8,128)(2,1)} %bitcast.33), calls=%async_computation.1 | async-start | bytes 327680 | tf_op jit(solution)/shard_map/all_to_all | solution.py:232
  240.7 4.4 %shard_map.147 = bf16[16,192,128]{2,1,0:T(8,128)(2,1)} custom-call(bf16[384,3200]{1,0:T(8,128)(2,1)} %copy-done, bf16[384,3200]{1,0:T(8,128)(2,1)} %collective-permute-done.32.other, bf16[128,768]{1,0:T(8,128)(2,1)} %get-tuple-element.37.xt, bf16[128,768]{1,0:T(8,128)(2,1)} %get-tuple-element.36.gt), custom_call_target="tpu_custom_call" | custom-call | tf_op jit(solution)/shard_map/pallas_call | solution.py:25
  245.2 2.6 all-to-all-done.1
  247.8 4.1 %all-to-all-start.2 = ((bf16[16,192,128]{2,1,0:T(8,128)(2,1)}), bf16[16,192,128]{2,1,0:T(8,128)(2,1)S(1)}, u32[]{:S(2)}, u32[]{:S(2)}) async-start(bf16[16,192,128]{2,1,0:T(8,128)(2,1)} %shard_map.147), calls=%async_computation.2 | async-start | bytes 1572864 | tf_op jit(solution)/shard_map/all_to_all | solution.py:219
  253.6 11.0 %all-to-all-done.2 = bf16[16,192,128]{2,1,0:T(8,128)(2,1)S(1)} async-done(((bf16[16,192,128]{2,1,0:T(8,128)(2,1)}), bf16[16,192,128]{2,1,0:T(8,128)(2,1)S(1)}, u32[]{:S(2)}, u32[]{:S(2)}) %all-to-all-start.2) | async-done | bytes 786464 | tf_op jit(solution)/shard_map/all_to_all | solution.py:219
  265.5 6.2 %all-to-all-start.4 = ((f32[32,1,384]{2,1,0:T(1,128)}), f32[32,1,384]{2,1,0:T(1,128)S(1)}, u32[]{:S(2)}, u32[]{:S(2)}) async-start(f32[32,1,384]{2,1,0:T(1,128)} %broadcast_in_dim.64), calls=%async_computation.4 | async-start | bytes 98304 | tf_op jit(solution)/shard_map/all_to_all | solution.py:244
  272.3 11.9 %all-to-all-done.4 = f32[32,1,384]{2,1,0:T(1,128)S(1)} async-done(((f32[32,1,384]{2,1,0:T(1,128)}), f32[32,1,384]{2,1,0:T(1,128)S(1)}, u32[]{:S(2)}, u32[]{:S(2)}) %all-to-all-start.4) | async-done | bytes 49184 | tf_op jit(solution)/shard_map/all_to_all | solution.py:244
  (131 shorter events, 44.2 us)
Async XLA Ops:
  4.3 17.0 %copy-start.6 = (bf16[192,256]{1,0:T(8,128)(2,1)}, bf16[192,256]{1,0:T(8,128)(2,1)S(1)}, u32[]{:S(2)}) copy-start(bf16[192,256]{1,0:T(8,128)(2,1)S(1)} %constant_dynamic-update-slice_fusion.both) | copy-start | bytes 294916
  5.8 15.5 %all-to-all-start = ((bf16[16,40,256]{2,1,0:T(8,128)(2,1)}), bf16[16,40,256]{2,1,0:T(8,128)(2,1)S(1)}, u32[]{:S(2)}, u32[]{:S(2)}) async-start(bf16[16,40,256]{2,1,0:T(8,128)(2,1)} %bitcast.6), calls=%async_computation | async-start | bytes 655360 | tf_op jit(solution)/shard_map/all_to_all | solution.py:153
  21.3 0.8 copy-start.3
  30.9 31.4 %copy-start.1 = (f32[216,3072]{1,0:T(8,128)S(1)}, f32[216,3072]{1,0:T(8,128)}, u32[]{:S(2)}) copy-start(f32[216,3072]{1,0:T(8,128)} %get-tuple-element.15) | copy-start | bytes 7962628
  30.9 9.1 %collective-permute-start = (bf16[216,3072]{1,0:T(8,128)(2,1)}, bf16[216,3072]{1,0:T(8,128)(2,1)}, u32[]{:S(2)}, u32[]{:S(2)}) collective-permute-start(bf16[216,3072]{1,0:T(8,128)(2,1)} %get-tuple-element.16), channel_id=1, source_target_pairs={{0,1},{1,0},{2,3},{3,2},{4,5},{5,4},{6,7},{7,6},{8,9},{9,8},{10,11... | collective-permute-start | bytes 3981320 | tf_op jit(solution)/shard_map/ppermute | solution.py:171
  37.0 13.7 %collective-permute-start.9 = (bf16[168,3072]{1,0:T(8,128)(2,1)}, bf16[168,3072]{1,0:T(8,128)(2,1)}, u32[]{:S(2)}, u32[]{:S(2)}) collective-permute-start(bf16[168,3072]{1,0:T(8,128)(2,1)} %get-tuple-element.18), channel_id=1, source_target_pairs={{0,1},{1,0},{2,3},{3,2},{4,5},{5,4},{6,7},{7,6},{8,9},{9,8},{10,11... | collective-permute-start | bytes 3096584 | tf_op jit(solution)/shard_map/ppermute | solution.py:172
  38.9 37.5 %copy-start.2 = (f32[168,3072]{1,0:T(8,128)S(1)}, f32[168,3072]{1,0:T(8,128)}, u32[]{:S(2)}) copy-start(f32[168,3072]{1,0:T(8,128)} %get-tuple-element.17) | copy-start | bytes 6193156
  41.0 12.6 %collective-permute-start.1 = (bf16[24,3072]{1,0:T(8,128)(2,1)S(1)}, bf16[24,3072]{1,0:T(8,128)(2,1)S(1)}, u32[]{:S(2)}, u32[]{:S(2)}) collective-permute-start(bf16[24,3072]{1,0:T(8,128)(2,1)S(1)} %add_convert_fusion.12), channel_id=1, source_target_pairs={{0,2},{1,31},{2,4},{3,1},{4,6},{5,3},{6,8},{7,5},{8,10},{9,7},{10,... | collective-permute-start | bytes 442376 | tf_op jit(solution)/shard_map/ppermute | solution.py:184
  51.7 7.6 %collective-permute-start.10 = (bf16[24,3072]{1,0:T(8,128)(2,1)S(1)}, bf16[24,3072]{1,0:T(8,128)(2,1)S(1)}, u32[]{:S(2)}, u32[]{:S(2)}) collective-permute-start(bf16[24,3072]{1,0:T(8,128)(2,1)S(1)} %add_convert_fusion.5), channel_id=1, source_target_pairs={{0,30},{1,3},{2,0},{3,5},{4,2},{5,7},{6,4},{7,9},{8,6},{9,11},{10,... | collective-permute-start | bytes 442376 | tf_op jit(solution)/shard_map/ppermute | solution.py:189
  54.7 7.6 %collective-permute-start.2 = (bf16[24,3072]{1,0:T(8,128)(2,1)S(1)}, bf16[24,3072]{1,0:T(8,128)(2,1)S(1)}, u32[]{:S(2)}, u32[]{:S(2)}) collective-permute-start(bf16[24,3072]{1,0:T(8,128)(2,1)S(1)} %add_convert_fusion.11), channel_id=1, source_target_pairs={{0,2},{1,31},{2,4},{3,1},{4,6},{5,3},{6,8},{7,5},{8,10},{9,7},{10,... | collective-permute-start | bytes 442376 | tf_op jit(solution)/shard_map/ppermute | solution.py:184
  60.3 7.5 %collective-permute-start.11 = (bf16[24,3072]{1,0:T(8,128)(2,1)S(1)}, bf16[24,3072]{1,0:T(8,128)(2,1)S(1)}, u32[]{:S(2)}, u32[]{:S(2)}) collective-permute-start(bf16[24,3072]{1,0:T(8,128)(2,1)S(1)} %add_convert_fusion.4), channel_id=1, source_target_pairs={{0,30},{1,3},{2,0},{3,5},{4,2},{5,7},{6,4},{7,9},{8,6},{9,11},{10,... | collective-permute-start | bytes 442376 | tf_op jit(solution)/shard_map/ppermute | solution.py:189
  63.3 7.6 %collective-permute-start.3 = (bf16[24,3072]{1,0:T(8,128)(2,1)S(1)}, bf16[24,3072]{1,0:T(8,128)(2,1)S(1)}, u32[]{:S(2)}, u32[]{:S(2)}) collective-permute-start(bf16[24,3072]{1,0:T(8,128)(2,1)S(1)} %add_convert_fusion.10), channel_id=1, source_target_pairs={{0,2},{1,31},{2,4},{3,1},{4,6},{5,3},{6,8},{7,5},{8,10},{9,7},{10,... | collective-permute-start | bytes 442376 | tf_op jit(solution)/shard_map/ppermute | solution.py:184
  68.9 7.5 %collective-permute-start.12 = (bf16[24,3072]{1,0:T(8,128)(2,1)S(1)}, bf16[24,3072]{1,0:T(8,128)(2,1)S(1)}, u32[]{:S(2)}, u32[]{:S(2)}) collective-permute-start(bf16[24,3072]{1,0:T(8,128)(2,1)S(1)} %add_convert_fusion.3), channel_id=1, source_target_pairs={{0,30},{1,3},{2,0},{3,5},{4,2},{5,7},{6,4},{7,9},{8,6},{9,11},{10,... | collective-permute-start | bytes 442376 | tf_op jit(solution)/shard_map/ppermute | solution.py:189
  71.8 7.5 %collective-permute-start.4 = (bf16[24,3072]{1,0:T(8,128)(2,1)S(1)}, bf16[24,3072]{1,0:T(8,128)(2,1)S(1)}, u32[]{:S(2)}, u32[]{:S(2)}) collective-permute-start(bf16[24,3072]{1,0:T(8,128)(2,1)S(1)} %add_convert_fusion.9), channel_id=1, source_target_pairs={{0,2},{1,31},{2,4},{3,1},{4,6},{5,3},{6,8},{7,5},{8,10},{9,7},{10,... | collective-permute-start | bytes 442376 | tf_op jit(solution)/shard_map/ppermute | solution.py:184
  77.4 7.5 %collective-permute-start.13 = (bf16[24,3072]{1,0:T(8,128)(2,1)S(1)}, bf16[24,3072]{1,0:T(8,128)(2,1)S(1)}, u32[]{:S(2)}, u32[]{:S(2)}) collective-permute-start(bf16[24,3072]{1,0:T(8,128)(2,1)S(1)} %add_convert_fusion.2), channel_id=1, source_target_pairs={{0,30},{1,3},{2,0},{3,5},{4,2},{5,7},{6,4},{7,9},{8,6},{9,11},{10,... | collective-permute-start | bytes 442376 | tf_op jit(solution)/shard_map/ppermute | solution.py:189
  80.3 7.5 %collective-permute-start.5 = (bf16[24,3072]{1,0:T(8,128)(2,1)S(1)}, bf16[24,3072]{1,0:T(8,128)(2,1)S(1)}, u32[]{:S(2)}, u32[]{:S(2)}) collective-permute-start(bf16[24,3072]{1,0:T(8,128)(2,1)S(1)} %add_convert_fusion.8), channel_id=1, source_target_pairs={{0,2},{1,31},{2,4},{3,1},{4,6},{5,3},{6,8},{7,5},{8,10},{9,7},{10,... | collective-permute-start | bytes 442376 | tf_op jit(solution)/shard_map/ppermute | solution.py:184
  85.8 7.5 %collective-permute-start.14 = (bf16[24,3072]{1,0:T(8,128)(2,1)S(1)}, bf16[24,3072]{1,0:T(8,128)(2,1)S(1)}, u32[]{:S(2)}, u32[]{:S(2)}) collective-permute-start(bf16[24,3072]{1,0:T(8,128)(2,1)S(1)} %add_convert_fusion.1), channel_id=1, source_target_pairs={{0,30},{1,3},{2,0},{3,5},{4,2},{5,7},{6,4},{7,9},{8,6},{9,11},{10,... | collective-permute-start | bytes 442376 | tf_op jit(solution)/shard_map/ppermute | solution.py:189
  88.8 7.5 %collective-permute-start.6 = (bf16[24,3072]{1,0:T(8,128)(2,1)S(1)}, bf16[24,3072]{1,0:T(8,128)(2,1)S(1)}, u32[]{:S(2)}, u32[]{:S(2)}) collective-permute-start(bf16[24,3072]{1,0:T(8,128)(2,1)S(1)} %add_convert_fusion.7), channel_id=1, source_target_pairs={{0,2},{1,31},{2,4},{3,1},{4,6},{5,3},{6,8},{7,5},{8,10},{9,7},{10,... | collective-permute-start | bytes 442376 | tf_op jit(solution)/shard_map/ppermute | solution.py:184
  94.3 7.5 %collective-permute-start.15 = (bf16[24,3072]{1,0:T(8,128)(2,1)S(1)}, bf16[24,3072]{1,0:T(8,128)(2,1)S(1)}, u32[]{:S(2)}, u32[]{:S(2)}) collective-permute-start(bf16[24,3072]{1,0:T(8,128)(2,1)S(1)} %add_convert_fusion), channel_id=1, source_target_pairs={{0,30},{1,3},{2,0},{3,5},{4,2},{5,7},{6,4},{7,9},{8,6},{9,11},{10,... | collective-permute-start | bytes 442376 | tf_op jit(solution)/shard_map/ppermute | solution.py:189
  97.2 7.5 %collective-permute-start.7 = (bf16[24,3072]{1,0:T(8,128)(2,1)S(1)}, bf16[24,3072]{1,0:T(8,128)(2,1)S(1)}, u32[]{:S(2)}, u32[]{:S(2)}) collective-permute-start(bf16[24,3072]{1,0:T(8,128)(2,1)S(1)} %add_convert_fusion.6), channel_id=1, source_target_pairs={{0,2},{1,31},{2,4},{3,1},{4,6},{5,3},{6,8},{7,5},{8,10},{9,7},{10,... | collective-permute-start | bytes 442376 | tf_op jit(solution)/shard_map/ppermute | solution.py:184
  102.8 9.7 %collective-permute-start.16 = (f32[24,3072]{1,0:T(8,128)S(1)}, f32[24,3072]{1,0:T(8,128)S(1)}, u32[]{:S(2)}, u32[]{:S(2)}) collective-permute-start(f32[24,3072]{1,0:T(8,128)S(1)} %add_add_fusion.1), channel_id=1, source_target_pairs={{0,30},{1,3},{2,0},{3,5},{4,2},{5,7},{6,4},{7,9},{8,6},{9,11},{10,... | collective-permute-start | bytes 884744 | tf_op jit(solution)/shard_map/ppermute | solution.py:189
  105.7 11.4 %collective-permute-start.8 = (f32[24,3072]{1,0:T(8,128)S(1)}, f32[24,3072]{1,0:T(8,128)S(1)}, u32[]{:S(2)}, u32[]{:S(2)}) collective-permute-start(f32[24,3072]{1,0:T(8,128)S(1)} %add_add_fusion.2), channel_id=1, source_target_pairs={{0,2},{1,31},{2,4},{3,1},{4,6},{5,3},{6,8},{7,5},{8,10},{9,7},{10,... | collective-permute-start | bytes 884744 | tf_op jit(solution)/shard_map/ppermute | solution.py:184
  118.3 7.9 %collective-permute-start.17 = (bf16[24,3200]{1,0:T(8,128)(2,1)S(1)}, bf16[24,3200]{1,0:T(8,128)(2,1)S(1)}, u32[]{:S(2)}, u32[]{:S(2)}) collective-permute-start(bf16[24,3200]{1,0:T(8,128)(2,1)S(1)} %get-tuple-element.50), channel_id=1, source_target_pairs={{0,30},{1,3},{2,0},{3,5},{4,2},{5,7},{6,4},{7,9},{8,6},{9,11},{10,... | collective-permute-start | bytes 460808 | tf_op jit(solution)/shard_map/ppermute | solution.py:208
  120.3 8.8 %collective-permute-start.24 = (bf16[24,3200]{1,0:T(8,128)(2,1)S(1)}, bf16[24,3200]{1,0:T(8,128)(2,1)S(1)}, u32[]{:S(2)}, u32[]{:S(2)}) collective-permute-start(bf16[24,3200]{1,0:T(8,128)(2,1)S(1)} %get-tuple-element.50), channel_id=1, source_target_pairs={{0,2},{1,31},{2,4},{3,1},{4,6},{5,3},{6,8},{7,5},{8,10},{9,7},{10,... | collective-permute-start | bytes 460808 | tf_op jit(solution)/shard_map/ppermute | solution.py:205
  126.2 8.1 %collective-permute-start.18 = (bf16[24,3200]{1,0:T(8,128)(2,1)S(1)}, bf16[24,3200]{1,0:T(8,128)(2,1)S(1)}, u32[]{:S(2)}, u32[]{:S(2)}) collective-permute-start(bf16[24,3200]{1,0:T(8,128)(2,1)S(1)} %collective-permute-done.17), channel_id=1, source_target_pairs={{0,30},{1,3},{2,0},{3,5},{4,2},{5,7},{6,4},{7,9},{8,6},{9,11},{10,... | collective-permute-start | bytes 460808 | tf_op jit(solution)/shard_map/ppermute | solution.py:208
  129.0 8.0 %collective-permute-start.25 = (bf16[24,3200]{1,0:T(8,128)(2,1)S(1)}, bf16[24,3200]{1,0:T(8,128)(2,1)S(1)}, u32[]{:S(2)}, u32[]{:S(2)}) collective-permute-start(bf16[24,3200]{1,0:T(8,128)(2,1)S(1)} %collective-permute-done.24), channel_id=1, source_target_pairs={{0,2},{1,31},{2,4},{3,1},{4,6},{5,3},{6,8},{7,5},{8,10},{9,7},{10,... | collective-permute-start | bytes 460808 | tf_op jit(solution)/shard_map/ppermute | solution.py:205
  134.3 8.3 %collective-permute-start.19 = (bf16[24,3200]{1,0:T(8,128)(2,1)S(1)}, bf16[24,3200]{1,0:T(8,128)(2,1)S(1)}, u32[]{:S(2)}, u32[]{:S(2)}) collective-permute-start(bf16[24,3200]{1,0:T(8,128)(2,1)S(1)} %collective-permute-done.18), channel_id=1, source_target_pairs={{0,30},{1,3},{2,0},{3,5},{4,2},{5,7},{6,4},{7,9},{8,6},{9,11},{10,... | collective-permute-start | bytes 460808 | tf_op jit(solution)/shard_map/ppermute | solution.py:208
  137.0 7.5 %collective-permute-start.26 = (bf16[24,3200]{1,0:T(8,128)(2,1)S(1)}, bf16[24,3200]{1,0:T(8,128)(2,1)S(1)}, u32[]{:S(2)}, u32[]{:S(2)}) collective-permute-start(bf16[24,3200]{1,0:T(8,128)(2,1)S(1)} %collective-permute-done.25), channel_id=1, source_target_pairs={{0,2},{1,31},{2,4},{3,1},{4,6},{5,3},{6,8},{7,5},{8,10},{9,7},{10,... | collective-permute-start | bytes 460808 | tf_op jit(solution)/shard_map/ppermute | solution.py:205
  142.6 7.2 %collective-permute-start.20 = (bf16[24,3200]{1,0:T(8,128)(2,1)S(1)}, bf16[24,3200]{1,0:T(8,128)(2,1)S(1)}, u32[]{:S(2)}, u32[]{:S(2)}) collective-permute-start(bf16[24,3200]{1,0:T(8,128)(2,1)S(1)} %collective-permute-done.19), channel_id=1, source_target_pairs={{0,30},{1,3},{2,0},{3,5},{4,2},{5,7},{6,4},{7,9},{8,6},{9,11},{10,... | collective-permute-start | bytes 460808 | tf_op jit(solution)/shard_map/ppermute | solution.py:208
  144.5 7.1 %collective-permute-start.27 = (bf16[24,3200]{1,0:T(8,128)(2,1)S(1)}, bf16[24,3200]{1,0:T(8,128)(2,1)S(1)}, u32[]{:S(2)}, u32[]{:S(2)}) collective-permute-start(bf16[24,3200]{1,0:T(8,128)(2,1)S(1)} %collective-permute-done.26), channel_id=1, source_target_pairs={{0,2},{1,31},{2,4},{3,1},{4,6},{5,3},{6,8},{7,5},{8,10},{9,7},{10,... | collective-permute-start | bytes 460808 | tf_op jit(solution)/shard_map/ppermute | solution.py:205
  149.8 7.2 %collective-permute-start.21 = (bf16[24,3200]{1,0:T(8,128)(2,1)S(1)}, bf16[24,3200]{1,0:T(8,128)(2,1)S(1)}, u32[]{:S(2)}, u32[]{:S(2)}) collective-permute-start(bf16[24,3200]{1,0:T(8,128)(2,1)S(1)} %collective-permute-done.20), channel_id=1, source_target_pairs={{0,30},{1,3},{2,0},{3,5},{4,2},{5,7},{6,4},{7,9},{8,6},{9,11},{10,... | collective-permute-start | bytes 460808 | tf_op jit(solution)/shard_map/ppermute | solution.py:208
  151.7 7.1 %collective-permute-start.28 = (bf16[24,3200]{1,0:T(8,128)(2,1)S(1)}, bf16[24,3200]{1,0:T(8,128)(2,1)S(1)}, u32[]{:S(2)}, u32[]{:S(2)}) collective-permute-start(bf16[24,3200]{1,0:T(8,128)(2,1)S(1)} %collective-permute-done.27), channel_id=1, source_target_pairs={{0,2},{1,31},{2,4},{3,1},{4,6},{5,3},{6,8},{7,5},{8,10},{9,7},{10,... | collective-permute-start | bytes 460808 | tf_op jit(solution)/shard_map/ppermute | solution.py:205
  156.9 7.2 %collective-permute-start.22 = (bf16[24,3200]{1,0:T(8,128)(2,1)S(1)}, bf16[24,3200]{1,0:T(8,128)(2,1)S(1)}, u32[]{:S(2)}, u32[]{:S(2)}) collective-permute-start(bf16[24,3200]{1,0:T(8,128)(2,1)S(1)} %collective-permute-done.21), channel_id=1, source_target_pairs={{0,30},{1,3},{2,0},{3,5},{4,2},{5,7},{6,4},{7,9},{8,6},{9,11},{10,... | collective-permute-start | bytes 460808 | tf_op jit(solution)/shard_map/ppermute | solution.py:208
  158.9 7.1 %collective-permute-start.29 = (bf16[24,3200]{1,0:T(8,128)(2,1)S(1)}, bf16[24,3200]{1,0:T(8,128)(2,1)S(1)}, u32[]{:S(2)}, u32[]{:S(2)}) collective-permute-start(bf16[24,3200]{1,0:T(8,128)(2,1)S(1)} %collective-permute-done.28), channel_id=1, source_target_pairs={{0,2},{1,31},{2,4},{3,1},{4,6},{5,3},{6,8},{7,5},{8,10},{9,7},{10,... | collective-permute-start | bytes 460808 | tf_op jit(solution)/shard_map/ppermute | solution.py:205
  164.1 14.0 %collective-permute-start.23 = (bf16[24,3200]{1,0:T(8,128)(2,1)S(1)}, bf16[24,3200]{1,0:T(8,128)(2,1)S(1)}, u32[]{:S(2)}, u32[]{:S(2)}) collective-permute-start(bf16[24,3200]{1,0:T(8,128)(2,1)S(1)} %collective-permute-done.22), channel_id=1, source_target_pairs={{0,30},{1,3},{2,0},{3,5},{4,2},{5,7},{6,4},{7,9},{8,6},{9,11},{10,... | collective-permute-start | bytes 460808 | tf_op jit(solution)/shard_map/ppermute | solution.py:208
  166.0 7.1 %collective-permute-start.30 = (bf16[24,3200]{1,0:T(8,128)(2,1)S(1)}, bf16[24,3200]{1,0:T(8,128)(2,1)S(1)}, u32[]{:S(2)}, u32[]{:S(2)}) collective-permute-start(bf16[24,3200]{1,0:T(8,128)(2,1)S(1)} %collective-permute-done.29), channel_id=1, source_target_pairs={{0,2},{1,31},{2,4},{3,1},{4,6},{5,3},{6,8},{7,5},{8,10},{9,7},{10,... | collective-permute-start | bytes 460808 | tf_op jit(solution)/shard_map/ppermute | solution.py:205
  173.1 7.9 %collective-permute-start.31 = (bf16[24,3200]{1,0:T(8,128)(2,1)S(1)}, bf16[24,3200]{1,0:T(8,128)(2,1)S(1)}, u32[]{:S(2)}, u32[]{:S(2)}) collective-permute-start(bf16[24,3200]{1,0:T(8,128)(2,1)S(1)} %collective-permute-done.30), channel_id=1, source_target_pairs={{0,2},{1,31},{2,4},{3,1},{4,6},{5,3},{6,8},{7,5},{8,10},{9,7},{10,... | collective-permute-start | bytes 460808 | tf_op jit(solution)/shard_map/ppermute | solution.py:205
  178.1 21.6 %copy-start.4 = (bf16[768,256]{1,0:T(8,128)(2,1)S(1)}, bf16[768,256]{1,0:T(8,128)(2,1)}, u32[]{:S(2)}) copy-start(bf16[768,256]{1,0:T(8,128)(2,1)} %get-tuple-element.19) | copy-start | bytes 1179652
  181.2 20.5 %copy-start = (bf16[384,3200]{1,0:T(8,128)(2,1)}, bf16[384,3200]{1,0:T(8,128)(2,1)S(1)}, u32[]{:S(2)}) copy-start(bf16[384,3200]{1,0:T(8,128)(2,1)S(1)} %constant_dynamic-update-slice_fusion.2.kept) | copy-start | bytes 7372804
  181.2 21.2 %collective-permute-start.32 = (bf16[384,3200]{1,0:T(8,128)(2,1)S(1)}, bf16[384,3200]{1,0:T(8,128)(2,1)}, u32[]{:S(2)}, u32[]{:S(2)}) collective-permute-start(bf16[384,3200]{1,0:T(8,128)(2,1)S(1)} %constant_dynamic-update-slice_fusion.2.kept), channel_id=1, source_target_pairs={{0,1},{1,0},{2,3},{3,2},{4,5},{5,4},{6,7},{7,6},{8,9},{9,8},{10,11... | collective-permute-start | bytes 7372808 | tf_op jit(solution)/shard_map/ppermute | solution.py:211
  237.2 10.6 %all-to-all-start.1 = ((bf16[16,40,128]{2,1,0:T(8,128)(2,1)}), bf16[16,40,128]{2,1,0:T(8,128)(2,1)S(1)}, u32[]{:S(2)}, u32[]{:S(2)}) async-start(bf16[16,40,128]{2,1,0:T(8,128)(2,1)} %bitcast.33), calls=%async_computation.1 | async-start | bytes 327680 | tf_op jit(solution)/shard_map/all_to_all | solution.py:232
  245.2 26.5 %copy-start.7 = (f32[192,128]{1,0:T(8,128)S(1)}, f32[192,128]{1,0:T(8,128)}, u32[]{:S(2)}) copy-start(f32[192,128]{1,0:T(8,128)} %get-tuple-element.21) | copy-start | bytes 294916
  247.8 16.7 %all-to-all-start.2 = ((bf16[16,192,128]{2,1,0:T(8,128)(2,1)}), bf16[16,192,128]{2,1,0:T(8,128)(2,1)S(1)}, u32[]{:S(2)}, u32[]{:S(2)}) async-start(bf16[16,192,128]{2,1,0:T(8,128)(2,1)} %shard_map.147), calls=%async_computation.2 | async-start | bytes 1572864 | tf_op jit(solution)/shard_map/all_to_all | solution.py:219
  264.6 21.1 %copy-start.5 = (f32[192,128]{1,0:T(8,128)}, f32[192,128]{1,0:T(8,128)S(1)}, u32[]{:S(2)}) copy-start(f32[192,128]{1,0:T(8,128)S(1)} %convert_reduce_fusion) | copy-start | bytes 294916
  265.5 18.7 %all-to-all-start.4 = ((f32[32,1,384]{2,1,0:T(1,128)}), f32[32,1,384]{2,1,0:T(1,128)S(1)}, u32[]{:S(2)}, u32[]{:S(2)}) async-start(f32[32,1,384]{2,1,0:T(1,128)} %broadcast_in_dim.64), calls=%async_computation.4 | async-start | bytes 98304 | tf_op jit(solution)/shard_map/all_to_all | solution.py:244

commit v3 on v2

--- a/solution.py
+++ b/solution.py
@@ -1,3 +1,5 @@
+import functools
+
 import jax
 import jax.numpy as jnp
 from jax import lax
@@ -5,6 +7,7 @@
 from jax.experimental.pallas import tpu as pltpu
 from jax.sharding import PartitionSpec as P
 
+
 BF = jnp.bfloat16
 F32 = jnp.float32
 VM = pl.BlockSpec(memory_space=pltpu.VMEM)
@@ -21,77 +24,137 @@
     return (a == b).astype(BF)
 
 
-def call(kernel, outs, *args):
+def call(kernel, outs, *args, smem=0, rest=0):
+    first = [pl.BlockSpec(memory_space=pltpu.SMEM)] * smem
+    last = [pl.BlockSpec(memory_space=pl.ANY)] * rest
     return pl.pallas_call(
         kernel,
         out_shape=[jax.ShapeDtypeStruct(s, d) for s, d in outs],
-        in_specs=[VM] * len(args),
+        in_specs=first + [VM] * (len(args) - smem - rest) + last,
         out_specs=[VM] * len(outs),
     )(*args)
 
 
-def project(pick, got, both, kind, eg, eu, ed, sg, su, sd, own_r, own_l, out_r, out_l, mine_ref):
+def quotient(n, by, top):
+    shift = 0
+    while (1 << shift) < by * top:
+        shift += 1
+    factor = -(-(1 << shift) // by)
+    assert factor * top < 2**31
+    return lax.shift_right_logical(n * factor, jnp.int32(shift))
+
+
+def ring_rows(r, z, c, sizes):
+    nz, piece, ls, cap, bl, slots = sizes
+    half = nz * piece
+    h = (r >= half).astype(jnp.int32)
+    inner = r - half * h
+    j = quotient(inner, piece, half)
+    turn = (1 - 2 * c) * (1 - 2 * h) * j
+    place = piece * (2 * ((z + turn) & (nz - 1)) + jnp.abs(c - h)) + inner - piece * j
+    block = quotient(place, ls, 2 * half)
+    within = place - ls * block
+    routed = place < slots
+    expert = jnp.where(routed, quotient(within, cap, ls), ls // cap)
+    src = jnp.where(routed, block * bl + within, slots // ls * bl + place - slots)
+    return src, expert, jnp.where(routed, block, -1), within
+
+
+def along(n, dim):
+    return lax.broadcasted_iota(jnp.int32, (n, 1) if dim == 0 else (1, n), dim)
+
+
+def one_hot(a, b):
+    return jnp.where(a == b, 1.0, 0.0).astype(BF)
+
+
+def project(sizes, pos, got, both, eg, eu, ed, sg, su, sd, own_r, own_l, out_r, out_l, xt_ref, gt_ref, xs_ref, gs_ref):
     le, width, hidden = eg.shape
-    nb = got.shape[0]
-    mine = mm(pick[:, :nb], got[...]) + mm(pick[:, nb:], both[...])
-    mine_ref[...] = mine.astype(BF)
-    kd = kind[...]
+    nb, rows = got.shape[0], both.shape[0]
+    nr, nl = own_r.shape[0], own_l.shape[0]
+    half = nr + nl
+    z, c = pos[0], pos[1]
+    src, kd, _, _ = ring_rows(along(2 * half, 0), z, c, sizes)
+    cols = lax.broadcasted_iota(jnp.int32, (2 * half, nb), 1)
+    mine = mm(one_hot(src, cols), got[...])
+    mine = mine + mm(one_hot(src - nb, lax.broadcasted_iota(jnp.int32, (2 * half, rows), 1)), both[...])
     part = [jnp.where(kd == e, mine, 0.0).astype(BF) for e in range(le + 1)]
     x = jnp.concatenate([p[:, :width] for p in part[:le]], 1)
     g = jnp.concatenate([p[:, width:] for p in part[:le]], 1)
-    nr, nl = own_r.shape[0], own_l.shape[0]
-    half = nr + nl
     todo = ((x, part[le][:, :width], eg, sg), (x, part[le][:, :width], eu, su), (g, part[le][:, width:], ed, sd))
     for t, (xe, xs, we, ws) in enumerate(todo):
-        cols = slice(t * hidden, (t + 1) * hidden)
+        cut = slice(t * hidden, (t + 1) * hidden)
         p = mm(xe, we[...].reshape(le * width, hidden)) + mm(xs, ws[...])
-        own_r[:, cols] = p[:nr]
-        own_l[:, cols] = p[nr:half]
-        out_r[:, cols] = p[half : half + nr].astype(BF)
-        out_l[:, cols] = p[half + nr :].astype(BF)
-
-
-def shared_grads(kept, other, xt, gt, out):
-    half = kept.shape[0]
-    n_ep, rows, width = out.shape
-    cols = rows // 3
-    hidden = cols * n_ep
+        own_r[:, cut] = p[:nr]
+        own_l[:, cut] = p[nr:half]
+        out_r[:, cut] = p[half : half + nr].astype(BF)
+        out_l[:, cut] = p[half + nr :].astype(BF)
+    _, kr, _, _ = ring_rows(along(2 * half, 1), z, c, sizes)
+    mine_t = mine.T
+    for e in range(le + 1):
+        both_t = jnp.where(kr == e, mine_t, 0.0).astype(BF)
+        to_x, to_g, at = (xt_ref, gt_ref, e * width) if e < le else (xs_ref, gs_ref, 0)
+        to_x[at : at + width, :] = both_t[:width]
+        to_g[at : at + width, :] = both_t[width:]
+
+
+def over_rows(lhs, parts, cut):
+    at, out = 0, None
+    for p in parts:
+        n = p.shape[0]
+        r = mm(lhs[:, at : at + n], p[:, cut])
+        out = r if out is None else out + r
+        at += n
+    return out
+
+
+def expert_grads(kept, other, xt, gt, stack, sq):
+    _, le, width, hidden = stack.shape
     for t, lhs in enumerate((xt, xt, gt)):
-        part = slice(t * hidden, (t + 1) * hidden)
-        r = mm(lhs[:, :half], kept[:, part]) + mm(lhs[:, half:], other[:, part])
+        r = over_rows(lhs, (kept, other), slice(t * hidden, (t + 1) * hidden)).reshape(le, width, hidden)
+        stack[t] = r.astype(BF)
+        sq[t] = jnp.sum(r * r, axis=1)
+
+
+def row_grads(sizes, pos, kept, other, eg, eu, sg, su, xs, gs, after, out, shared):
+    le, width, hidden = eg.shape
+    ls, bl = sizes[2], sizes[4]
+    n_ep, rows = out.shape[0], shared.shape[0]
+    nb = n_ep * bl
+    cols = hidden // n_ep
+    for t, lhs in enumerate((xs, xs, gs)):
+        r = over_rows(lhs, (kept, other), slice(t * hidden, (t + 1) * hidden))
         out[:, t * cols : (t + 1) * cols, :] = r.T.astype(BF).reshape(n_ep, cols, width)
-
-
-def expert_grads(kept, other, xt, gt, eg, eu, sg, su, kind, pick_t, tail_t, lane_hot, stack, sq, back, shared):
-    le, width, hidden = eg.shape
-    half = kept.shape[0]
-    nb = back.shape[0]
-    slots = []
-    for h, src in enumerate((kept, other)):
+    total = 2 * sizes[0] * sizes[1]
+    z, c = pos[0], pos[1]
+    _, kd, _, within = ring_rows(along(total, 0), z, c, sizes)
+    slots, wg, at = [], [], 0
+    for src in (kept, other):
+        n = src.shape[0]
         gg, gu = src[:, :hidden], src[:, hidden : 2 * hidden]
         se = mm(gg, eg[...].reshape(le * width, hidden), NT) + mm(gu, eu[...].reshape(le * width, hidden), NT)
         ss = mm(gg, sg[...], NT) + mm(gu, su[...], NT)
-        kd = kind[h * half : (h + 1) * half, :]
-        s = jnp.where(kd == le, ss, 0.0)
+        k = kd[at : at + n]
+        s = jnp.where(k == le, ss, 0.0)
         for e in range(le):
-            s = s + jnp.where(kd == e, se[:, e * width : (e + 1) * width], 0.0)
+            s = s + jnp.where(k == e, se[:, e * width : (e + 1) * width], 0.0)
         slots.append(s)
+        lanes = lax.broadcasted_iota(jnp.int32, (n, width), 1)
+        wg.append(jnp.where(within[at : at + n] == lanes, src[:, 3 * hidden :].astype(F32), 0.0))
+        at += n
     slot = jnp.concatenate(slots, 0)
     hi = slot.astype(BF)
     rest = slot - hi.astype(F32)
     mid = rest.astype(BF)
     low = (rest - mid.astype(F32)).astype(BF)
-    wg = jnp.concatenate([kept[:, 3 * hidden :], other[:, 3 * hidden :]], 0).astype(F32)
-    wg = (wg * lane_hot[...].astype(F32)).astype(BF)
-    back[...] = (mm(pick_t[:nb, :], hi) + mm(tail_t[...], wg)).astype(BF)
-    ps = pick_t[nb:, :]
+    src_r, _, block, _ = ring_rows(along(total, 1), z, c, sizes)
+    lines = lax.broadcasted_iota(jnp.int32, (nb, total), 0)
+    to_slot = one_hot(lines, src_r)
+    to_tail = one_hot(lines, jnp.where(block >= 0, block * bl + ls, -1))
+    back = mm(to_slot, hi) + mm(to_tail, jnp.concatenate(wg, 0).astype(BF))
+    out[:, 3 * cols :, :] = back.reshape(n_ep, bl, width).astype(BF)
+    ps = one_hot(lax.broadcasted_iota(jnp.int32, (rows, total), 0) + nb, src_r)
     shared[...] = mm(ps, hi) + mm(ps, mid) + mm(ps, low)
-    for t, lhs in enumerate((xt, xt, gt)):
-        part = slice(t * hidden, (t + 1) * hidden)
-        r = mm(lhs[:, :half], kept[:, part]) + mm(lhs[:, half:], other[:, part])
-        r = r.reshape(le, width, hidden)
-        stack[t] = r.astype(BF)
-        sq[t] = jnp.sum(r * r, axis=1)
 
 
 def row_backward(summed, weights):
@@ -122,7 +185,6 @@
     bl = (ls + 8) // 8 * 8
     slots = n_ep * ls
     total = slots + rows
-    half = total // 2
     piece = total // n_tp
     tp = lax.axis_index("tp")
     z, c = tp // 2, tp % 2
@@ -152,21 +214,17 @@
     sent = mm(jnp.concatenate([spread, tail], 1), jnp.concatenate([both, w_block], 0)).astype(BF)
     got = lax.all_to_all(sent.reshape(n_ep, bl, 2 * width), "ep", 0, 0, tiled=True)
 
-    r = jnp.arange(total, dtype=jnp.int32)
-    h = r // half
-    turn = (1 - 2 * c) * (1 - 2 * h) * (r % half // piece)
-    place = piece * (2 * ((z + turn) % nz) + (c ^ h)) + r % piece
-    kind = jnp.where(place < slots, place % ls // cap, le)
-    src = jnp.where(place < slots, place // ls * bl + place % ls, n_ep * bl + place - slots)
-    column = jnp.arange(n_ep * bl + rows, dtype=jnp.int32)
-    pick = hot(src[:, None], column[None, :])
+    sizes = (nz, piece, ls, cap, bl, slots)
+    pos = jnp.stack([z, c]).astype(jnp.int32)
     hops, back_hops = nz // 2, nz - nz // 2 - 1
     nr, nl = (hops + 1) * piece, back_hops * piece
     width3 = 3 * hidden
-    own_r, own_l, out_r, out_l, mine = call(
-        project,
-        [((nr, width3), F32), ((nl, width3), F32), ((nr, width3), BF), ((nl, width3), BF), ((total, 2 * width), BF)],
-        pick, got.reshape(n_ep * bl, 2 * width), both, kind[:, None], e_gate, e_up, e_down, s_gate, s_up, s_down,
+    own_r, own_l, out_r, out_l, xt, gt, xs, gs = call(
+        functools.partial(project, sizes),
+        [((nr, width3), F32), ((nl, width3), F32), ((nr, width3), BF), ((nl, width3), BF)]
+        + [((le * width, total), BF)] * 2
+        + [((width, total), BF)] * 2,
+        pos, got.reshape(n_ep * bl, 2 * width), both, e_gate, e_up, e_down, s_gate, s_up, s_down, smem=1,
     )
     oth_r = lax.ppermute(out_r, "tp", swap)
     oth_l = lax.ppermute(out_l, "tp", swap)
@@ -208,28 +266,27 @@
             left = lax.ppermute(left, "tp", bwd)
             ring[t] = left
     kept = jnp.concatenate(ring, 0)
-    other = lax.ppermute(kept, "tp", swap)
-
-    kind_row = kind[None, :]
-    mine_t = mine.T
-    x_t = [jnp.where(kind_row == e, mine_t[:width], 0) for e in range(le + 1)]
-    g_t = [jnp.where(kind_row == e, mine_t[width:], 0) for e in range(le + 1)]
+    grads = (kept, lax.ppermute(kept, "tp", swap))
+
     cols = hidden // n_ep
-    (sh,) = call(shared_grads, [((n_ep, 3 * cols, width), BF)], kept, other, x_t[le], g_t[le])
-    sh_home = lax.all_to_all(sh, "ep", 0, 0, tiled=True)
-
+    stack, e_sq = call(
+        expert_grads, [((3, le, width, hidden), BF), ((3, le, hidden), F32)], *grads, xt, gt
+    )
+    piece_sq = lax.all_to_all(e_sq.reshape(n_tp, -1), "tp", 0, 0, tiled=True)
+    piece_sq = jnp.sum(piece_sq, axis=0)
+    out, shared_part = call(
+        functools.partial(row_grads, sizes),
+        [((n_ep, 3 * cols + bl, width), BF), ((rows, width), F32)],
+        pos, *grads, e_gate, e_up, s_gate, s_up, xs, gs, e_sq, smem=1, rest=1,
+    )
+    home = lax.all_to_all(out, "ep", 0, 0, tiled=True)
+    sh_home, home = home[:, : 3 * cols], home[:, 3 * cols :]
     lane1 = jnp.arange(width, dtype=jnp.int32)
-    pick_t = hot(column[:, None], src[None, :])
-    tail_t = hot(blk[:, None], jnp.where(place < slots, place // ls * bl + ls, -1)[None, :])
-    lane_hot = hot((place % ls)[:, None], lane1[None, :])
-    stack, e_sq, back, shared_part = call(
-        expert_grads,
-        [((3, le, width, hidden), BF), ((3, le, hidden), F32), ((n_ep * bl, width), BF), ((rows, width), F32)],
-        kept, other, jnp.concatenate(x_t[:le], 0), jnp.concatenate(g_t[:le], 0),
-        e_gate, e_up, s_gate, s_up, kind[:, None], pick_t, tail_t, lane_hot,
-    )
-    piece_sq = jnp.sum(lax.all_to_all(e_sq.reshape(n_tp, -1), "tp", 0, 0, tiled=True), axis=0)
-    home = lax.all_to_all(back.reshape(n_ep, bl, width), "ep", 0, 0, tiled=True)
+    shared = jnp.sum(sh_home.astype(F32), axis=0).reshape(3, cols, width)
+    s_sq = jnp.sum(shared * shared, axis=2).reshape(-1)
+    line = jnp.concatenate([piece_sq, s_sq])
+    home, line = lax.optimization_barrier((home, line))
+    lines = lax.all_to_all(jnp.broadcast_to(line[None], (n_tp, line.size)), "tp", 0, 0, tiled=True)
     rows_home = home.reshape(n_ep * bl, width)
     token_grad = (mm(spread, rows_home, ((0,), (0,))) + shared_part).astype(BF)
     wg_home = home[:, ls]
@@ -238,10 +295,6 @@
         line = mm(hot(dest[k][:, None], groups[None, :]), wg_home)
         gate_grad.append(jnp.sum(jnp.where(within[k][:, None] == lane1[None, :], line, 0.0), axis=1))
     gate_grad = jnp.stack(gate_grad, 1).astype(BF)
-    shared = jnp.sum(sh_home.astype(F32), axis=0).reshape(3, cols, width)
-    s_sq = jnp.sum(shared * shared, axis=2).reshape(-1)
-    line = jnp.concatenate([piece_sq, s_sq])
-    lines = lax.all_to_all(jnp.broadcast_to(line[None], (n_tp, line.size)), "tp", 0, 0, tiled=True)
     scale = 1.0 / (width * n_tp)
     n_e = piece_sq.size
     return (

time: 288 us -> 279 us (0.969)
  blocking collectives: 24.2 us -> 0 us
  starting transfers between devices: 153 us -> 165 us
  waiting for transfers between devices: 44.7 us -> 56.7 us
  other arithmetic: 28.6 us -> 19.4 us
    all_to_all x1 -> x0, blocking collectives: 24.2 us -> none  [body(): lax.all_to_all(e_sq.reshape(n_tp, -1), 'tp', 0, 0, tiled=True)]
    all_to_all x2, starting transfers between devices: 7.63 us -> 16.2 us  [the longest x1 12.6 us: body(): piece_sq = lax.all_to_all(e_sq.reshape(n_tp, -1), 'tp', 0, 0, tiled=True)]
    all_to_all x2, waiting for transfers between devices: 13.6 us -> 19.3 us  [the longest x1 14.7 us: body(): home = lax.all_to_all(out, 'ep', 0, 0, tiled=True)]
    convert_element_type x5 -> x1, other arithmetic: 5.1 us -> 0.05 us  [hot(): return (a == b).astype(BF)]
    ppermute x1, waiting for transfers between devices: 0.01 us -> 4.28 us  [body(): grads = (kept, lax.ppermute(kept, 'tp', swap))]
    all_to_all x1, starting transfers between devices: 6.18 us -> 9.77 us  [body(): lax.all_to_all(jnp.broadcast_to(line[None], (n_tp, line.size)), 'tp', 0,...]
    select_n x4 -> x0, other arithmetic: 3.19 us -> none  [the longest x1 2.21 us: body(): kind = jnp.where(place < slots, place % ls // cap, le)]
    all_to_all x1, waiting for transfers between devices: 4.23 us -> 7.22 us  [body(): lax.all_to_all(sent.reshape(n_ep, bl, 2 * width), 'ep', 0, 0, tiled=True)]
  transfers between devices with their start and end apart: 37 -> 37, of which waited for: 16 -> 17; matrix products, arithmetic and copies ran while one was open for 10% -> 7% of each run, Pallas kernels for 2% -> 3%
where the time goes in v3:
time: 279 us; the launch traced here: 277 us
  starting transfers between devices  165 us (59%)
  waiting for transfers between devices  56.7 us (20%)
  Pallas kernels  21.8 us (8%)
  other arithmetic  19.4 us (7%)
  local copies, waits for them, and re-layouts  9.49 us (3%)
  matrix products  2.9 us (1%)
    ppermute x16, starting transfers between devices, body(): right = lax.ppermute(right, 'tp', fwd)  82.2 us
    ppermute x14, starting transfers between devices, body(): left = lax.ppermute(left, 'tp', bwd)  26.8 us
    pallas_call x3, Pallas kernels, call(): pl.pallas_call(kernel, out_shape=[jax.ShapeDtypeStruct(s, d) for s, d in...  21.8 us
    all_to_all x1, waiting for transfers between devices, body(): home = lax.all_to_all(out, 'ep', 0, 0, tiled=True)  14.7 us
    ppermute x1, starting transfers between devices, body(): grads = (kept, lax.ppermute(kept, 'tp', swap))  14.6 us
    all_to_all x1, starting transfers between devices, body(): piece_sq = lax.all_to_all(e_sq.reshape(n_tp, -1), 'tp', 0, 0, tiled=True)  12.6 us
    ppermute x16, waiting for transfers between devices, body(): right = lax.ppermute(right, 'tp', fwd)  11.2 us
    all_to_all x1, waiting for transfers between devices, body(): lax.all_to_all(jnp.broadcast_to(line[None], (n_tp, line.size)), 'tp', 0,...  10.9 us
  transfers between devices with their start and end apart: 37, of which 17 were waited for; matrix products, arithmetic and copies ran while one was open for 7% of the time, Pallas kernels for 3%

profile of v3, /device:TPU:1, one launch (start us, length us, event | category | flops | bytes accessed | tf_op | source)
XLA Modules:
  0.0 277.0 jit_solution(372080073751652075)
XLA Ops:
  5.8 7.6 %all-to-all-start = ((bf16[16,40,256]{2,1,0:T(8,128)(2,1)}), bf16[16,40,256]{2,1,0:T(8,128)(2,1)S(1)}, u32[]{:S(2)}, u32[]{:S(2)}) async-start(bf16[16,40,256]{2,1,0:T(8,128)(2,1)} %bitcast.8), calls=%async_computation | async-start | bytes 655360 | tf_op jit(solution)/shard_map/all_to_all | solution.py:215
  14.1 7.2 %all-to-all-done = bf16[16,40,256]{2,1,0:T(8,128)(2,1)S(1)} async-done(((bf16[16,40,256]{2,1,0:T(8,128)(2,1)}), bf16[16,40,256]{2,1,0:T(8,128)(2,1)S(1)}, u32[]{:S(2)}, u32[]{:S(2)}) %all-to-all-start) | async-done | bytes 327712 | tf_op jit(solution)/shard_map/all_to_all | solution.py:215
  22.0 8.9 %shard_map.145 = (f32[216,3072]{1,0:T(8,128)}, f32[168,3072]{1,0:T(8,128)}, bf16[216,3072]{1,0:T(8,128)(2,1)}, bf16[168,3072]{1,0:T(8,128)(2,1)}, bf16[256,768]{...) custom-call(s32[2]{0:T(128)} %pad_add_fusion.pos, ...), custom_call_target="tpu_custom_call" | custom-call | tf_op jit(solution)/shard_map/pallas_call | solution.py:30
  30.9 6.1 %collective-permute-start = (bf16[216,3072]{1,0:T(8,128)(2,1)}, bf16[216,3072]{1,0:T(8,128)(2,1)}, u32[]{:S(2)}, u32[]{:S(2)}) collective-permute-start(bf16[216,3072]{1,0:T(8,128)(2,1)} %get-tuple-element.21), channel_id=1, source_target_pairs={{0,1},{1,0},{2,3},{3,2},{4,5},{5,4},{6,7},{7,6},{8,9},{9,8},{10,11... | collective-permute-start | bytes 3981320 | tf_op jit(solution)/shard_map/ppermute | solution.py:229
  37.0 1.9 collective-permute-start.9
  41.0 9.6 %collective-permute-start.1 = (bf16[24,3072]{1,0:T(8,128)(2,1)S(1)}, bf16[24,3072]{1,0:T(8,128)(2,1)S(1)}, u32[]{:S(2)}, u32[]{:S(2)}) collective-permute-start(bf16[24,3072]{1,0:T(8,128)(2,1)S(1)} %add_convert_fusion.12), channel_id=1, source_target_pairs={{0,2},{1,31},{2,4},{3,1},{4,6},{5,3},{6,8},{7,5},{8,10},{9,7},{10,... | collective-permute-start | bytes 442376 | tf_op jit(solution)/shard_map/ppermute | solution.py:242
  51.7 1.9 collective-permute-start.10
  54.7 4.6 %collective-permute-start.2 = (bf16[24,3072]{1,0:T(8,128)(2,1)S(1)}, bf16[24,3072]{1,0:T(8,128)(2,1)S(1)}, u32[]{:S(2)}, u32[]{:S(2)}) collective-permute-start(bf16[24,3072]{1,0:T(8,128)(2,1)S(1)} %add_convert_fusion.11), channel_id=1, source_target_pairs={{0,2},{1,31},{2,4},{3,1},{4,6},{5,3},{6,8},{7,5},{8,10},{9,7},{10,... | collective-permute-start | bytes 442376 | tf_op jit(solution)/shard_map/ppermute | solution.py:242
  60.4 1.9 collective-permute-start.11
  63.3 4.6 %collective-permute-start.3 = (bf16[24,3072]{1,0:T(8,128)(2,1)S(1)}, bf16[24,3072]{1,0:T(8,128)(2,1)S(1)}, u32[]{:S(2)}, u32[]{:S(2)}) collective-permute-start(bf16[24,3072]{1,0:T(8,128)(2,1)S(1)} %add_convert_fusion.10), channel_id=1, source_target_pairs={{0,2},{1,31},{2,4},{3,1},{4,6},{5,3},{6,8},{7,5},{8,10},{9,7},{10,... | collective-permute-start | bytes 442376 | tf_op jit(solution)/shard_map/ppermute | solution.py:242
  68.9 1.9 collective-permute-start.12
  71.9 4.6 %collective-permute-start.4 = (bf16[24,3072]{1,0:T(8,128)(2,1)S(1)}, bf16[24,3072]{1,0:T(8,128)(2,1)S(1)}, u32[]{:S(2)}, u32[]{:S(2)}) collective-permute-start(bf16[24,3072]{1,0:T(8,128)(2,1)S(1)} %add_convert_fusion.9), channel_id=1, source_target_pairs={{0,2},{1,31},{2,4},{3,1},{4,6},{5,3},{6,8},{7,5},{8,10},{9,7},{10,... | collective-permute-start | bytes 442376 | tf_op jit(solution)/shard_map/ppermute | solution.py:242
  77.4 1.9 collective-permute-start.13
  80.3 4.6 %collective-permute-start.5 = (bf16[24,3072]{1,0:T(8,128)(2,1)S(1)}, bf16[24,3072]{1,0:T(8,128)(2,1)S(1)}, u32[]{:S(2)}, u32[]{:S(2)}) collective-permute-start(bf16[24,3072]{1,0:T(8,128)(2,1)S(1)} %add_convert_fusion.8), channel_id=1, source_target_pairs={{0,2},{1,31},{2,4},{3,1},{4,6},{5,3},{6,8},{7,5},{8,10},{9,7},{10,... | collective-permute-start | bytes 442376 | tf_op jit(solution)/shard_map/ppermute | solution.py:242
  85.9 1.9 collective-permute-start.14
  88.8 4.6 %collective-permute-start.6 = (bf16[24,3072]{1,0:T(8,128)(2,1)S(1)}, bf16[24,3072]{1,0:T(8,128)(2,1)S(1)}, u32[]{:S(2)}, u32[]{:S(2)}) collective-permute-start(bf16[24,3072]{1,0:T(8,128)(2,1)S(1)} %add_convert_fusion.7), channel_id=1, source_target_pairs={{0,2},{1,31},{2,4},{3,1},{4,6},{5,3},{6,8},{7,5},{8,10},{9,7},{10,... | collective-permute-start | bytes 442376 | tf_op jit(solution)/shard_map/ppermute | solution.py:242
  94.4 1.9 collective-permute-start.15
  97.3 4.6 %collective-permute-start.7 = (bf16[24,3072]{1,0:T(8,128)(2,1)S(1)}, bf16[24,3072]{1,0:T(8,128)(2,1)S(1)}, u32[]{:S(2)}, u32[]{:S(2)}) collective-permute-start(bf16[24,3072]{1,0:T(8,128)(2,1)S(1)} %add_convert_fusion.6), channel_id=1, source_target_pairs={{0,2},{1,31},{2,4},{3,1},{4,6},{5,3},{6,8},{7,5},{8,10},{9,7},{10,... | collective-permute-start | bytes 442376 | tf_op jit(solution)/shard_map/ppermute | solution.py:242
  102.8 1.9 collective-permute-start.16
  105.7 4.8 %collective-permute-start.8 = (f32[24,3072]{1,0:T(8,128)S(1)}, f32[24,3072]{1,0:T(8,128)S(1)}, u32[]{:S(2)}, u32[]{:S(2)}) collective-permute-start(f32[24,3072]{1,0:T(8,128)S(1)} %add_add_fusion.2), channel_id=1, source_target_pairs={{0,2},{1,31},{2,4},{3,1},{4,6},{5,3},{6,8},{7,5},{8,10},{9,7},{10,... | collective-permute-start | bytes 884744 | tf_op jit(solution)/shard_map/ppermute | solution.py:242
  112.6 4.6 %collective-permute-done.8 = f32[24,3072]{1,0:T(8,128)S(1)} collective-permute-done((f32[24,3072]{1,0:T(8,128)S(1)}, f32[24,3072]{1,0:T(8,128)S(1)}, u32[]{:S(2)}, u32[]{:S(2)}) %collective-permute-start.8) | collective-permute-done | bytes 294944 | tf_op jit(solution)/shard_map/ppermute | solution.py:242
  118.4 1.9 collective-permute-start.17
  120.3 5.3 %collective-permute-start.24 = (bf16[24,3200]{1,0:T(8,128)(2,1)S(1)}, bf16[24,3200]{1,0:T(8,128)(2,1)S(1)}, u32[]{:S(2)}, u32[]{:S(2)}) collective-permute-start(bf16[24,3200]{1,0:T(8,128)(2,1)S(1)} %get-tuple-element.50), channel_id=1, source_target_pairs={{0,2},{1,31},{2,4},{3,1},{4,6},{5,3},{6,8},{7,5},{8,10},{9,7},{10,... | collective-permute-start | bytes 460808 | tf_op jit(solution)/shard_map/ppermute | solution.py:263
  126.3 1.9 collective-permute-start.18
  129.1 5.0 %collective-permute-start.25 = (bf16[24,3200]{1,0:T(8,128)(2,1)S(1)}, bf16[24,3200]{1,0:T(8,128)(2,1)S(1)}, u32[]{:S(2)}, u32[]{:S(2)}) collective-permute-start(bf16[24,3200]{1,0:T(8,128)(2,1)S(1)} %collective-permute-done.24), channel_id=1, source_target_pairs={{0,2},{1,31},{2,4},{3,1},{4,6},{5,3},{6,8},{7,5},{8,10},{9,7},{10,... | collective-permute-start | bytes 460808 | tf_op jit(solution)/shard_map/ppermute | solution.py:263
  134.4 1.9 collective-permute-start.19
  137.1 5.3 %collective-permute-start.26 = (bf16[24,3200]{1,0:T(8,128)(2,1)S(1)}, bf16[24,3200]{1,0:T(8,128)(2,1)S(1)}, u32[]{:S(2)}, u32[]{:S(2)}) collective-permute-start(bf16[24,3200]{1,0:T(8,128)(2,1)S(1)} %collective-permute-done.25), channel_id=1, source_target_pairs={{0,2},{1,31},{2,4},{3,1},{4,6},{5,3},{6,8},{7,5},{8,10},{9,7},{10,... | collective-permute-start | bytes 460808 | tf_op jit(solution)/shard_map/ppermute | solution.py:263
  142.7 1.9 collective-permute-start.20
  144.6 4.9 %collective-permute-start.27 = (bf16[24,3200]{1,0:T(8,128)(2,1)S(1)}, bf16[24,3200]{1,0:T(8,128)(2,1)S(1)}, u32[]{:S(2)}, u32[]{:S(2)}) collective-permute-start(bf16[24,3200]{1,0:T(8,128)(2,1)S(1)} %collective-permute-done.26), channel_id=1, source_target_pairs={{0,2},{1,31},{2,4},{3,1},{4,6},{5,3},{6,8},{7,5},{8,10},{9,7},{10,... | collective-permute-start | bytes 460808 | tf_op jit(solution)/shard_map/ppermute | solution.py:263
  149.8 1.9 collective-permute-start.21
  151.8 4.9 %collective-permute-start.28 = (bf16[24,3200]{1,0:T(8,128)(2,1)S(1)}, bf16[24,3200]{1,0:T(8,128)(2,1)S(1)}, u32[]{:S(2)}, u32[]{:S(2)}) collective-permute-start(bf16[24,3200]{1,0:T(8,128)(2,1)S(1)} %collective-permute-done.27), channel_id=1, source_target_pairs={{0,2},{1,31},{2,4},{3,1},{4,6},{5,3},{6,8},{7,5},{8,10},{9,7},{10,... | collective-permute-start | bytes 460808 | tf_op jit(solution)/shard_map/ppermute | solution.py:263
  157.0 1.9 collective-permute-start.22
  158.9 4.9 %collective-permute-start.29 = (bf16[24,3200]{1,0:T(8,128)(2,1)S(1)}, bf16[24,3200]{1,0:T(8,128)(2,1)S(1)}, u32[]{:S(2)}, u32[]{:S(2)}) collective-permute-start(bf16[24,3200]{1,0:T(8,128)(2,1)S(1)} %collective-permute-done.28), channel_id=1, source_target_pairs={{0,2},{1,31},{2,4},{3,1},{4,6},{5,3},{6,8},{7,5},{8,10},{9,7},{10,... | collective-permute-start | bytes 460808 | tf_op jit(solution)/shard_map/ppermute | solution.py:263
  164.1 1.9 collective-permute-start.23
  166.1 4.9 %collective-permute-start.30 = (bf16[24,3200]{1,0:T(8,128)(2,1)S(1)}, bf16[24,3200]{1,0:T(8,128)(2,1)S(1)}, u32[]{:S(2)}, u32[]{:S(2)}) collective-permute-start(bf16[24,3200]{1,0:T(8,128)(2,1)S(1)} %collective-permute-done.29), channel_id=1, source_target_pairs={{0,2},{1,31},{2,4},{3,1},{4,6},{5,3},{6,8},{7,5},{8,10},{9,7},{10,... | collective-permute-start | bytes 460808 | tf_op jit(solution)/shard_map/ppermute | solution.py:263
  171.0 2.1 collective-permute-done.30
  173.2 5.0 %collective-permute-start.31 = (bf16[24,3200]{1,0:T(8,128)(2,1)S(1)}, bf16[24,3200]{1,0:T(8,128)(2,1)S(1)}, u32[]{:S(2)}, u32[]{:S(2)}) collective-permute-start(bf16[24,3200]{1,0:T(8,128)(2,1)S(1)} %collective-permute-done.30), channel_id=1, source_target_pairs={{0,2},{1,31},{2,4},{3,1},{4,6},{5,3},{6,8},{7,5},{8,10},{9,7},{10,... | collective-permute-start | bytes 460808 | tf_op jit(solution)/shard_map/ppermute | solution.py:263
  178.2 2.8 %collective-permute-done.31 = bf16[24,3200]{1,0:T(8,128)(2,1)S(1)} collective-permute-done((bf16[24,3200]{1,0:T(8,128)(2,1)S(1)}, bf16[24,3200]{1,0:T(8,128)(2,1)S(1)}, u32[]{:S(2)}, u32[]{:S(2)}) %collective-permute-start.31) | collective-permute-done | bytes 153632 | tf_op jit(solution)/shard_map/ppermute | solution.py:263
  181.2 14.6 %collective-permute-start.32 = (bf16[384,3200]{1,0:T(8,128)(2,1)S(1)}, bf16[384,3200]{1,0:T(8,128)(2,1)S(1)}, u32[]{:S(2)}, u32[]{:S(2)}) collective-permute-start(bf16[384,3200]{1,0:T(8,128)(2,1)S(1)} %constant_dynamic-update-slice_fusion.2.kept), channel_id=1, source_target_pairs={{0,1},{1,0},{2,3},{3,2},{4,5},{5,4},{6,7},{7,6},{8,9},{9,8},{10,11... | collective-permute-start | bytes 7372808 | tf_op jit(solution)/shard_map/ppermute | solution.py:269
  195.8 4.3 %collective-permute-done.32.other = bf16[384,3200]{1,0:T(8,128)(2,1)S(1)} collective-permute-done((bf16[384,3200]{1,0:T(8,128)(2,1)S(1)}, bf16[384,3200]{1,0:T(8,128)(2,1)S(1)}, u32[]{:S(2)}, u32[]{:S(2)}) %collective-permute-start.32) | collective-permute-done | bytes 2457632 | tf_op jit(solution)/shard_map/ppermute | solution.py:269
  201.6 5.5 %shard_map.146 = (bf16[3,2,128,1024]{3,2,1,0:T(8,128)(2,1)}, f32[3,2,1024]{2,1,0:T(2,128)}) custom-call(bf16[384,3200]{1,0:T(8,128)(2,1)} %copy-done, bf16[384,3200]{1,0:T(8,128)(2,1)} %copy-done.1, bf16[256,768]{1,0:T(8,128)(2,1)} %get-tuple-element.26.xt, bf16[256,768]{1,0:T(8,128)(2,1)} %get-tuple-element.27.gt), custom_call_target="tpu_custom_call" | custom-call | tf_op jit(solution)/shard_map/pallas_call | solution.py:30
  208.5 12.6 %all-to-all-start.2 = ((f32[32,1,192]{2,1,0:T(1,128)}), f32[32,1,192]{2,1,0:T(1,128)S(1)}, u32[]{:S(2)}, u32[]{:S(2)}) async-start(f32[32,1,192]{2,1,0:T(1,128)} %all_to_all.24), calls=%async_computation.2 | async-start | bytes 65536 | tf_op jit(solution)/shard_map/all_to_all | solution.py:275
  221.2 7.4 %shard_map.147 = (bf16[16,232,128]{2,1,0:T(8,128)(2,1)}, f32[192,128]{1,0:T(8,128)}) custom-call(s32[2]{0:T(128)} %pad_add_fusion.pos, bf16[384,3200]{1,0:T(8,128)(2,1)} %copy-done, bf16[384,3200]{1,0:T(8,128)(2,1)} %copy-done.1, bf16[2,128,1024]{2,1,0:T(8,128)(2,1)} %eg.3, bf16[2,128,1024]{2,1,0:T(8,128)(2,1)} %eu.3, bf16[128,1024]{1,0:T(8,128)(2,1)} %sg.3, ...), custom_call_target="tpu_custom_call" | custom-call | tf_op jit(solution)/shard_map/pallas_call | solution.py:30
  228.6 4.6 %all-to-all-done.2 = f32[32,1,192]{2,1,0:T(1,128)S(1)} async-done(((f32[32,1,192]{2,1,0:T(1,128)}), f32[32,1,192]{2,1,0:T(1,128)S(1)}, u32[]{:S(2)}, u32[]{:S(2)}) %all-to-all-start.2) | async-done | bytes 24608 | tf_op jit(solution)/shard_map/all_to_all | solution.py:275
  233.2 3.6 %all-to-all-start.1 = ((bf16[16,232,128]{2,1,0:T(8,128)(2,1)}), bf16[16,232,128]{2,1,0:T(8,128)(2,1)S(1)}, u32[]{:S(2)}, u32[]{:S(2)}) async-start(bf16[16,232,128]{2,1,0:T(8,128)(2,1)} %get-tuple-element.29), calls=%async_computation.1 | async-start | bytes 1900544 | tf_op jit(solution)/shard_map/all_to_all | solution.py:282
  236.9 14.7 %all-to-all-done.1 = bf16[16,232,128]{2,1,0:T(8,128)(2,1)S(1)} async-done(((bf16[16,232,128]{2,1,0:T(8,128)(2,1)}), bf16[16,232,128]{2,1,0:T(8,128)(2,1)S(1)}, u32[]{:S(2)}, u32[]{:S(2)}) %all-to-all-start.1) | async-done | bytes 950304 | tf_op jit(solution)/shard_map/all_to_all | solution.py:282
  253.3 9.8 %all-to-all-start.3 = ((f32[32,1,384]{2,1,0:T(1,128)}), f32[32,1,384]{2,1,0:T(1,128)S(1)}, u32[]{:S(2)}, u32[]{:S(2)}) async-start(f32[32,1,384]{2,1,0:T(1,128)} %broadcast_in_dim.18), calls=%async_computation.3 | async-start | bytes 98304 | tf_op jit(solution)/shard_map/all_to_all | solution.py:289
  264.6 10.9 %all-to-all-done.3 = f32[32,1,384]{2,1,0:T(1,128)S(1)} async-done(((f32[32,1,384]{2,1,0:T(1,128)}), f32[32,1,384]{2,1,0:T(1,128)S(1)}, u32[]{:S(2)}, u32[]{:S(2)}) %all-to-all-start.3) | async-done | bytes 49184 | tf_op jit(solution)/shard_map/all_to_all | solution.py:289
  (119 shorter events, 37.2 us)
Async XLA Ops:
  4.1 17.2 %copy-start.6 = (bf16[192,256]{1,0:T(8,128)(2,1)}, bf16[192,256]{1,0:T(8,128)(2,1)S(1)}, u32[]{:S(2)}) copy-start(bf16[192,256]{1,0:T(8,128)(2,1)S(1)} %constant_dynamic-update-slice_fusion.both) | copy-start | bytes 294916
  5.8 15.5 %all-to-all-start = ((bf16[16,40,256]{2,1,0:T(8,128)(2,1)}), bf16[16,40,256]{2,1,0:T(8,128)(2,1)S(1)}, u32[]{:S(2)}, u32[]{:S(2)}) async-start(bf16[16,40,256]{2,1,0:T(8,128)(2,1)} %bitcast.8), calls=%async_computation | async-start | bytes 655360 | tf_op jit(solution)/shard_map/all_to_all | solution.py:215
  21.3 0.7 copy-start.4
  30.9 31.4 %copy-start.2 = (f32[216,3072]{1,0:T(8,128)S(1)}, f32[216,3072]{1,0:T(8,128)}, u32[]{:S(2)}) copy-start(f32[216,3072]{1,0:T(8,128)} %get-tuple-element.20) | copy-start | bytes 7962628
  30.9 9.1 %collective-permute-start = (bf16[216,3072]{1,0:T(8,128)(2,1)}, bf16[216,3072]{1,0:T(8,128)(2,1)}, u32[]{:S(2)}, u32[]{:S(2)}) collective-permute-start(bf16[216,3072]{1,0:T(8,128)(2,1)} %get-tuple-element.21), channel_id=1, source_target_pairs={{0,1},{1,0},{2,3},{3,2},{4,5},{5,4},{6,7},{7,6},{8,9},{9,8},{10,11... | collective-permute-start | bytes 3981320 | tf_op jit(solution)/shard_map/ppermute | solution.py:229
  37.0 13.7 %collective-permute-start.9 = (bf16[168,3072]{1,0:T(8,128)(2,1)}, bf16[168,3072]{1,0:T(8,128)(2,1)}, u32[]{:S(2)}, u32[]{:S(2)}) collective-permute-start(bf16[168,3072]{1,0:T(8,128)(2,1)} %get-tuple-element.23), channel_id=1, source_target_pairs={{0,1},{1,0},{2,3},{3,2},{4,5},{5,4},{6,7},{7,6},{8,9},{9,8},{10,11... | collective-permute-start | bytes 3096584 | tf_op jit(solution)/shard_map/ppermute | solution.py:230
  38.9 37.5 %copy-start.3 = (f32[168,3072]{1,0:T(8,128)S(1)}, f32[168,3072]{1,0:T(8,128)}, u32[]{:S(2)}) copy-start(f32[168,3072]{1,0:T(8,128)} %get-tuple-element.22) | copy-start | bytes 6193156
  41.0 12.6 %collective-permute-start.1 = (bf16[24,3072]{1,0:T(8,128)(2,1)S(1)}, bf16[24,3072]{1,0:T(8,128)(2,1)S(1)}, u32[]{:S(2)}, u32[]{:S(2)}) collective-permute-start(bf16[24,3072]{1,0:T(8,128)(2,1)S(1)} %add_convert_fusion.12), channel_id=1, source_target_pairs={{0,2},{1,31},{2,4},{3,1},{4,6},{5,3},{6,8},{7,5},{8,10},{9,7},{10,... | collective-permute-start | bytes 442376 | tf_op jit(solution)/shard_map/ppermute | solution.py:242
  51.7 7.6 %collective-permute-start.10 = (bf16[24,3072]{1,0:T(8,128)(2,1)S(1)}, bf16[24,3072]{1,0:T(8,128)(2,1)S(1)}, u32[]{:S(2)}, u32[]{:S(2)}) collective-permute-start(bf16[24,3072]{1,0:T(8,128)(2,1)S(1)} %add_convert_fusion.5), channel_id=1, source_target_pairs={{0,30},{1,3},{2,0},{3,5},{4,2},{5,7},{6,4},{7,9},{8,6},{9,11},{10,... | collective-permute-start | bytes 442376 | tf_op jit(solution)/shard_map/ppermute | solution.py:247
  54.7 7.6 %collective-permute-start.2 = (bf16[24,3072]{1,0:T(8,128)(2,1)S(1)}, bf16[24,3072]{1,0:T(8,128)(2,1)S(1)}, u32[]{:S(2)}, u32[]{:S(2)}) collective-permute-start(bf16[24,3072]{1,0:T(8,128)(2,1)S(1)} %add_convert_fusion.11), channel_id=1, source_target_pairs={{0,2},{1,31},{2,4},{3,1},{4,6},{5,3},{6,8},{7,5},{8,10},{9,7},{10,... | collective-permute-start | bytes 442376 | tf_op jit(solution)/shard_map/ppermute | solution.py:242
  60.4 7.5 %collective-permute-start.11 = (bf16[24,3072]{1,0:T(8,128)(2,1)S(1)}, bf16[24,3072]{1,0:T(8,128)(2,1)S(1)}, u32[]{:S(2)}, u32[]{:S(2)}) collective-permute-start(bf16[24,3072]{1,0:T(8,128)(2,1)S(1)} %add_convert_fusion.4), channel_id=1, source_target_pairs={{0,30},{1,3},{2,0},{3,5},{4,2},{5,7},{6,4},{7,9},{8,6},{9,11},{10,... | collective-permute-start | bytes 442376 | tf_op jit(solution)/shard_map/ppermute | solution.py:247
  63.3 7.6 %collective-permute-start.3 = (bf16[24,3072]{1,0:T(8,128)(2,1)S(1)}, bf16[24,3072]{1,0:T(8,128)(2,1)S(1)}, u32[]{:S(2)}, u32[]{:S(2)}) collective-permute-start(bf16[24,3072]{1,0:T(8,128)(2,1)S(1)} %add_convert_fusion.10), channel_id=1, source_target_pairs={{0,2},{1,31},{2,4},{3,1},{4,6},{5,3},{6,8},{7,5},{8,10},{9,7},{10,... | collective-permute-start | bytes 442376 | tf_op jit(solution)/shard_map/ppermute | solution.py:242
  68.9 7.5 %collective-permute-start.12 = (bf16[24,3072]{1,0:T(8,128)(2,1)S(1)}, bf16[24,3072]{1,0:T(8,128)(2,1)S(1)}, u32[]{:S(2)}, u32[]{:S(2)}) collective-permute-start(bf16[24,3072]{1,0:T(8,128)(2,1)S(1)} %add_convert_fusion.3), channel_id=1, source_target_pairs={{0,30},{1,3},{2,0},{3,5},{4,2},{5,7},{6,4},{7,9},{8,6},{9,11},{10,... | collective-permute-start | bytes 442376 | tf_op jit(solution)/shard_map/ppermute | solution.py:247
  71.9 7.5 %collective-permute-start.4 = (bf16[24,3072]{1,0:T(8,128)(2,1)S(1)}, bf16[24,3072]{1,0:T(8,128)(2,1)S(1)}, u32[]{:S(2)}, u32[]{:S(2)}) collective-permute-start(bf16[24,3072]{1,0:T(8,128)(2,1)S(1)} %add_convert_fusion.9), channel_id=1, source_target_pairs={{0,2},{1,31},{2,4},{3,1},{4,6},{5,3},{6,8},{7,5},{8,10},{9,7},{10,... | collective-permute-start | bytes 442376 | tf_op jit(solution)/shard_map/ppermute | solution.py:242
  77.4 7.5 %collective-permute-start.13 = (bf16[24,3072]{1,0:T(8,128)(2,1)S(1)}, bf16[24,3072]{1,0:T(8,128)(2,1)S(1)}, u32[]{:S(2)}, u32[]{:S(2)}) collective-permute-start(bf16[24,3072]{1,0:T(8,128)(2,1)S(1)} %add_convert_fusion.2), channel_id=1, source_target_pairs={{0,30},{1,3},{2,0},{3,5},{4,2},{5,7},{6,4},{7,9},{8,6},{9,11},{10,... | collective-permute-start | bytes 442376 | tf_op jit(solution)/shard_map/ppermute | solution.py:247
  80.3 7.5 %collective-permute-start.5 = (bf16[24,3072]{1,0:T(8,128)(2,1)S(1)}, bf16[24,3072]{1,0:T(8,128)(2,1)S(1)}, u32[]{:S(2)}, u32[]{:S(2)}) collective-permute-start(bf16[24,3072]{1,0:T(8,128)(2,1)S(1)} %add_convert_fusion.8), channel_id=1, source_target_pairs={{0,2},{1,31},{2,4},{3,1},{4,6},{5,3},{6,8},{7,5},{8,10},{9,7},{10,... | collective-permute-start | bytes 442376 | tf_op jit(solution)/shard_map/ppermute | solution.py:242
  85.9 7.5 %collective-permute-start.14 = (bf16[24,3072]{1,0:T(8,128)(2,1)S(1)}, bf16[24,3072]{1,0:T(8,128)(2,1)S(1)}, u32[]{:S(2)}, u32[]{:S(2)}) collective-permute-start(bf16[24,3072]{1,0:T(8,128)(2,1)S(1)} %add_convert_fusion.1), channel_id=1, source_target_pairs={{0,30},{1,3},{2,0},{3,5},{4,2},{5,7},{6,4},{7,9},{8,6},{9,11},{10,... | collective-permute-start | bytes 442376 | tf_op jit(solution)/shard_map/ppermute | solution.py:247
  88.8 7.5 %collective-permute-start.6 = (bf16[24,3072]{1,0:T(8,128)(2,1)S(1)}, bf16[24,3072]{1,0:T(8,128)(2,1)S(1)}, u32[]{:S(2)}, u32[]{:S(2)}) collective-permute-start(bf16[24,3072]{1,0:T(8,128)(2,1)S(1)} %add_convert_fusion.7), channel_id=1, source_target_pairs={{0,2},{1,31},{2,4},{3,1},{4,6},{5,3},{6,8},{7,5},{8,10},{9,7},{10,... | collective-permute-start | bytes 442376 | tf_op jit(solution)/shard_map/ppermute | solution.py:242
  94.4 7.5 %collective-permute-start.15 = (bf16[24,3072]{1,0:T(8,128)(2,1)S(1)}, bf16[24,3072]{1,0:T(8,128)(2,1)S(1)}, u32[]{:S(2)}, u32[]{:S(2)}) collective-permute-start(bf16[24,3072]{1,0:T(8,128)(2,1)S(1)} %add_convert_fusion), channel_id=1, source_target_pairs={{0,30},{1,3},{2,0},{3,5},{4,2},{5,7},{6,4},{7,9},{8,6},{9,11},{10,... | collective-permute-start | bytes 442376 | tf_op jit(solution)/shard_map/ppermute | solution.py:247
  97.3 7.5 %collective-permute-start.7 = (bf16[24,3072]{1,0:T(8,128)(2,1)S(1)}, bf16[24,3072]{1,0:T(8,128)(2,1)S(1)}, u32[]{:S(2)}, u32[]{:S(2)}) collective-permute-start(bf16[24,3072]{1,0:T(8,128)(2,1)S(1)} %add_convert_fusion.6), channel_id=1, source_target_pairs={{0,2},{1,31},{2,4},{3,1},{4,6},{5,3},{6,8},{7,5},{8,10},{9,7},{10,... | collective-permute-start | bytes 442376 | tf_op jit(solution)/shard_map/ppermute | solution.py:242
  102.8 9.7 %collective-permute-start.16 = (f32[24,3072]{1,0:T(8,128)S(1)}, f32[24,3072]{1,0:T(8,128)S(1)}, u32[]{:S(2)}, u32[]{:S(2)}) collective-permute-start(f32[24,3072]{1,0:T(8,128)S(1)} %add_add_fusion.1), channel_id=1, source_target_pairs={{0,30},{1,3},{2,0},{3,5},{4,2},{5,7},{6,4},{7,9},{8,6},{9,11},{10,... | collective-permute-start | bytes 884744 | tf_op jit(solution)/shard_map/ppermute | solution.py:247
  105.7 11.4 %collective-permute-start.8 = (f32[24,3072]{1,0:T(8,128)S(1)}, f32[24,3072]{1,0:T(8,128)S(1)}, u32[]{:S(2)}, u32[]{:S(2)}) collective-permute-start(f32[24,3072]{1,0:T(8,128)S(1)} %add_add_fusion.2), channel_id=1, source_target_pairs={{0,2},{1,31},{2,4},{3,1},{4,6},{5,3},{6,8},{7,5},{8,10},{9,7},{10,... | collective-permute-start | bytes 884744 | tf_op jit(solution)/shard_map/ppermute | solution.py:242
  118.4 7.9 %collective-permute-start.17 = (bf16[24,3200]{1,0:T(8,128)(2,1)S(1)}, bf16[24,3200]{1,0:T(8,128)(2,1)S(1)}, u32[]{:S(2)}, u32[]{:S(2)}) collective-permute-start(bf16[24,3200]{1,0:T(8,128)(2,1)S(1)} %get-tuple-element.50), channel_id=1, source_target_pairs={{0,30},{1,3},{2,0},{3,5},{4,2},{5,7},{6,4},{7,9},{8,6},{9,11},{10,... | collective-permute-start | bytes 460808 | tf_op jit(solution)/shard_map/ppermute | solution.py:266
  120.3 8.8 %collective-permute-start.24 = (bf16[24,3200]{1,0:T(8,128)(2,1)S(1)}, bf16[24,3200]{1,0:T(8,128)(2,1)S(1)}, u32[]{:S(2)}, u32[]{:S(2)}) collective-permute-start(bf16[24,3200]{1,0:T(8,128)(2,1)S(1)} %get-tuple-element.50), channel_id=1, source_target_pairs={{0,2},{1,31},{2,4},{3,1},{4,6},{5,3},{6,8},{7,5},{8,10},{9,7},{10,... | collective-permute-start | bytes 460808 | tf_op jit(solution)/shard_map/ppermute | solution.py:263
  126.3 8.1 %collective-permute-start.18 = (bf16[24,3200]{1,0:T(8,128)(2,1)S(1)}, bf16[24,3200]{1,0:T(8,128)(2,1)S(1)}, u32[]{:S(2)}, u32[]{:S(2)}) collective-permute-start(bf16[24,3200]{1,0:T(8,128)(2,1)S(1)} %collective-permute-done.17), channel_id=1, source_target_pairs={{0,30},{1,3},{2,0},{3,5},{4,2},{5,7},{6,4},{7,9},{8,6},{9,11},{10,... | collective-permute-start | bytes 460808 | tf_op jit(solution)/shard_map/ppermute | solution.py:266
  129.1 8.0 %collective-permute-start.25 = (bf16[24,3200]{1,0:T(8,128)(2,1)S(1)}, bf16[24,3200]{1,0:T(8,128)(2,1)S(1)}, u32[]{:S(2)}, u32[]{:S(2)}) collective-permute-start(bf16[24,3200]{1,0:T(8,128)(2,1)S(1)} %collective-permute-done.24), channel_id=1, source_target_pairs={{0,2},{1,31},{2,4},{3,1},{4,6},{5,3},{6,8},{7,5},{8,10},{9,7},{10,... | collective-permute-start | bytes 460808 | tf_op jit(solution)/shard_map/ppermute | solution.py:263
  134.4 8.3 %collective-permute-start.19 = (bf16[24,3200]{1,0:T(8,128)(2,1)S(1)}, bf16[24,3200]{1,0:T(8,128)(2,1)S(1)}, u32[]{:S(2)}, u32[]{:S(2)}) collective-permute-start(bf16[24,3200]{1,0:T(8,128)(2,1)S(1)} %collective-permute-done.18), channel_id=1, source_target_pairs={{0,30},{1,3},{2,0},{3,5},{4,2},{5,7},{6,4},{7,9},{8,6},{9,11},{10,... | collective-permute-start | bytes 460808 | tf_op jit(solution)/shard_map/ppermute | solution.py:266
  137.1 7.5 %collective-permute-start.26 = (bf16[24,3200]{1,0:T(8,128)(2,1)S(1)}, bf16[24,3200]{1,0:T(8,128)(2,1)S(1)}, u32[]{:S(2)}, u32[]{:S(2)}) collective-permute-start(bf16[24,3200]{1,0:T(8,128)(2,1)S(1)} %collective-permute-done.25), channel_id=1, source_target_pairs={{0,2},{1,31},{2,4},{3,1},{4,6},{5,3},{6,8},{7,5},{8,10},{9,7},{10,... | collective-permute-start | bytes 460808 | tf_op jit(solution)/shard_map/ppermute | solution.py:263
  142.7 7.2 %collective-permute-start.20 = (bf16[24,3200]{1,0:T(8,128)(2,1)S(1)}, bf16[24,3200]{1,0:T(8,128)(2,1)S(1)}, u32[]{:S(2)}, u32[]{:S(2)}) collective-permute-start(bf16[24,3200]{1,0:T(8,128)(2,1)S(1)} %collective-permute-done.19), channel_id=1, source_target_pairs={{0,30},{1,3},{2,0},{3,5},{4,2},{5,7},{6,4},{7,9},{8,6},{9,11},{10,... | collective-permute-start | bytes 460808 | tf_op jit(solution)/shard_map/ppermute | solution.py:266
  144.6 7.1 %collective-permute-start.27 = (bf16[24,3200]{1,0:T(8,128)(2,1)S(1)}, bf16[24,3200]{1,0:T(8,128)(2,1)S(1)}, u32[]{:S(2)}, u32[]{:S(2)}) collective-permute-start(bf16[24,3200]{1,0:T(8,128)(2,1)S(1)} %collective-permute-done.26), channel_id=1, source_target_pairs={{0,2},{1,31},{2,4},{3,1},{4,6},{5,3},{6,8},{7,5},{8,10},{9,7},{10,... | collective-permute-start | bytes 460808 | tf_op jit(solution)/shard_map/ppermute | solution.py:263
  149.8 7.2 %collective-permute-start.21 = (bf16[24,3200]{1,0:T(8,128)(2,1)S(1)}, bf16[24,3200]{1,0:T(8,128)(2,1)S(1)}, u32[]{:S(2)}, u32[]{:S(2)}) collective-permute-start(bf16[24,3200]{1,0:T(8,128)(2,1)S(1)} %collective-permute-done.20), channel_id=1, source_target_pairs={{0,30},{1,3},{2,0},{3,5},{4,2},{5,7},{6,4},{7,9},{8,6},{9,11},{10,... | collective-permute-start | bytes 460808 | tf_op jit(solution)/shard_map/ppermute | solution.py:266
  151.8 7.1 %collective-permute-start.28 = (bf16[24,3200]{1,0:T(8,128)(2,1)S(1)}, bf16[24,3200]{1,0:T(8,128)(2,1)S(1)}, u32[]{:S(2)}, u32[]{:S(2)}) collective-permute-start(bf16[24,3200]{1,0:T(8,128)(2,1)S(1)} %collective-permute-done.27), channel_id=1, source_target_pairs={{0,2},{1,31},{2,4},{3,1},{4,6},{5,3},{6,8},{7,5},{8,10},{9,7},{10,... | collective-permute-start | bytes 460808 | tf_op jit(solution)/shard_map/ppermute | solution.py:263
  157.0 7.2 %collective-permute-start.22 = (bf16[24,3200]{1,0:T(8,128)(2,1)S(1)}, bf16[24,3200]{1,0:T(8,128)(2,1)S(1)}, u32[]{:S(2)}, u32[]{:S(2)}) collective-permute-start(bf16[24,3200]{1,0:T(8,128)(2,1)S(1)} %collective-permute-done.21), channel_id=1, source_target_pairs={{0,30},{1,3},{2,0},{3,5},{4,2},{5,7},{6,4},{7,9},{8,6},{9,11},{10,... | collective-permute-start | bytes 460808 | tf_op jit(solution)/shard_map/ppermute | solution.py:266
  158.9 7.1 %collective-permute-start.29 = (bf16[24,3200]{1,0:T(8,128)(2,1)S(1)}, bf16[24,3200]{1,0:T(8,128)(2,1)S(1)}, u32[]{:S(2)}, u32[]{:S(2)}) collective-permute-start(bf16[24,3200]{1,0:T(8,128)(2,1)S(1)} %collective-permute-done.28), channel_id=1, source_target_pairs={{0,2},{1,31},{2,4},{3,1},{4,6},{5,3},{6,8},{7,5},{8,10},{9,7},{10,... | collective-permute-start | bytes 460808 | tf_op jit(solution)/shard_map/ppermute | solution.py:263
  164.1 14.0 %collective-permute-start.23 = (bf16[24,3200]{1,0:T(8,128)(2,1)S(1)}, bf16[24,3200]{1,0:T(8,128)(2,1)S(1)}, u32[]{:S(2)}, u32[]{:S(2)}) collective-permute-start(bf16[24,3200]{1,0:T(8,128)(2,1)S(1)} %collective-permute-done.22), channel_id=1, source_target_pairs={{0,30},{1,3},{2,0},{3,5},{4,2},{5,7},{6,4},{7,9},{8,6},{9,11},{10,... | collective-permute-start | bytes 460808 | tf_op jit(solution)/shard_map/ppermute | solution.py:266
  166.1 7.1 %collective-permute-start.30 = (bf16[24,3200]{1,0:T(8,128)(2,1)S(1)}, bf16[24,3200]{1,0:T(8,128)(2,1)S(1)}, u32[]{:S(2)}, u32[]{:S(2)}) collective-permute-start(bf16[24,3200]{1,0:T(8,128)(2,1)S(1)} %collective-permute-done.29), channel_id=1, source_target_pairs={{0,2},{1,31},{2,4},{3,1},{4,6},{5,3},{6,8},{7,5},{8,10},{9,7},{10,... | collective-permute-start | bytes 460808 | tf_op jit(solution)/shard_map/ppermute | solution.py:263
  173.2 7.9 %collective-permute-start.31 = (bf16[24,3200]{1,0:T(8,128)(2,1)S(1)}, bf16[24,3200]{1,0:T(8,128)(2,1)S(1)}, u32[]{:S(2)}, u32[]{:S(2)}) collective-permute-start(bf16[24,3200]{1,0:T(8,128)(2,1)S(1)} %collective-permute-done.30), channel_id=1, source_target_pairs={{0,2},{1,31},{2,4},{3,1},{4,6},{5,3},{6,8},{7,5},{8,10},{9,7},{10,... | collective-permute-start | bytes 460808 | tf_op jit(solution)/shard_map/ppermute | solution.py:263
  181.2 20.3 %copy-start = (bf16[384,3200]{1,0:T(8,128)(2,1)}, bf16[384,3200]{1,0:T(8,128)(2,1)S(1)}, u32[]{:S(2)}) copy-start(bf16[384,3200]{1,0:T(8,128)(2,1)S(1)} %constant_dynamic-update-slice_fusion.2.kept) | copy-start | bytes 7372804
  181.2 18.9 %collective-permute-start.32 = (bf16[384,3200]{1,0:T(8,128)(2,1)S(1)}, bf16[384,3200]{1,0:T(8,128)(2,1)S(1)}, u32[]{:S(2)}, u32[]{:S(2)}) collective-permute-start(bf16[384,3200]{1,0:T(8,128)(2,1)S(1)} %constant_dynamic-update-slice_fusion.2.kept), channel_id=1, source_target_pairs={{0,1},{1,0},{2,3},{3,2},{4,5},{5,4},{6,7},{7,6},{8,9},{9,8},{10,11... | collective-permute-start | bytes 7372808 | tf_op jit(solution)/shard_map/ppermute | solution.py:269
  200.1 1.5 copy-start.1
  208.5 24.7 %all-to-all-start.2 = ((f32[32,1,192]{2,1,0:T(1,128)}), f32[32,1,192]{2,1,0:T(1,128)S(1)}, u32[]{:S(2)}, u32[]{:S(2)}) async-start(f32[32,1,192]{2,1,0:T(1,128)} %all_to_all.24), calls=%async_computation.2 | async-start | bytes 65536 | tf_op jit(solution)/shard_map/all_to_all | solution.py:275
  228.6 35.4 %copy-start.7 = (f32[192,128]{1,0:T(8,128)S(1)}, f32[192,128]{1,0:T(8,128)}, u32[]{:S(2)}) copy-start(f32[192,128]{1,0:T(8,128)} %get-tuple-element.31) | copy-start | bytes 294916
  233.2 18.4 %all-to-all-start.1 = ((bf16[16,232,128]{2,1,0:T(8,128)(2,1)}), bf16[16,232,128]{2,1,0:T(8,128)(2,1)S(1)}, u32[]{:S(2)}, u32[]{:S(2)}) async-start(bf16[16,232,128]{2,1,0:T(8,128)(2,1)} %get-tuple-element.29), calls=%async_computation.1 | async-start | bytes 1900544 | tf_op jit(solution)/shard_map/all_to_all | solution.py:282
  251.7 25.3 %copy-start.5 = (f32[192,128]{1,0:T(8,128)}, f32[192,128]{1,0:T(8,128)S(1)}, u32[]{:S(2)}) copy-start(f32[192,128]{1,0:T(8,128)S(1)} %convert_reduce_fusion) | copy-start | bytes 294916
  253.3 22.2 %all-to-all-start.3 = ((f32[32,1,384]{2,1,0:T(1,128)}), f32[32,1,384]{2,1,0:T(1,128)S(1)}, u32[]{:S(2)}, u32[]{:S(2)}) async-start(f32[32,1,384]{2,1,0:T(1,128)} %broadcast_in_dim.18), calls=%async_computation.3 | async-start | bytes 98304 | tf_op jit(solution)/shard_map/all_to_all | solution.py:289

commit v4 on v3

--- a/solution.py
+++ b/solution.py
@@ -66,6 +66,107 @@
 
 def one_hot(a, b):
     return jnp.where(a == b, 1.0, 0.0).astype(BF)
+
+
+def columns(lines):
+    lines = lines.astype(F32)
+    return jnp.concatenate([lines, jnp.zeros((8 - lines.shape[0], lines.shape[1]), F32)], 0).T
+
+
+def routing(routes, le, cap, experts):
+    top, rows = routes.shape
+    routes = columns(routes).astype(jnp.int32)
+    lanes = lax.broadcasted_iota(jnp.int32, (rows, experts), 1)
+    chosen = [routes[:, k : k + 1] for k in range(top)]
+    on = [jnp.where(f == lanes, 1.0, 0.0) for f in chosen]
+    shape = (rows, rows)
+    tri = jnp.where(lax.broadcasted_iota(jnp.int32, shape, 0) > lax.broadcasted_iota(jnp.int32, shape, 1), 1.0, 0.0)
+    before = mm(tri.astype(BF), sum(on).astype(BF))
+    out = []
+    for f, o in zip(chosen, on):
+        dest = quotient(f, le, experts)
+        pos = jnp.sum(o * before, axis=1, keepdims=True).astype(jnp.int32)
+        out.append((dest, (f - le * dest) * cap + pos))
+    return out
+
+
+def dispatch(geo, tokens, cotangent, routes, weights, sent, both):
+    le, cap, experts, bl = geo
+    rows, width = tokens.shape
+    n = sent.shape[0]
+    xg = jnp.concatenate([tokens[...], cotangent[...]], 1)
+    both[...] = xg
+    where = routing(routes[...], le, cap, experts)
+    cols = lax.broadcasted_iota(jnp.int32, (rows, n), 1)
+    lanes = lax.broadcasted_iota(jnp.int32, (rows, 2 * width), 1)
+    w = columns(weights[...])
+    left, right = [jnp.zeros((rows, n), F32)], [xg]
+    for k, (dest, within) in enumerate(where):
+        left[0] = left[0] + jnp.where(dest * bl + within == cols, 1.0, 0.0)
+        left.append(jnp.where(dest * bl + le * cap == cols, w[:, k : k + 1], 0.0))
+        right.append(one_hot(within, lanes))
+    left = jnp.concatenate([a.T.astype(BF) for a in left], 1)
+    sent[...] = mm(left, jnp.concatenate(right, 0)).astype(BF)
+
+
+def collect(geo, home, shared, routes, after, token_grad, gate_grad):
+    le, cap, experts, bl = geo
+    n_ep = home.shape[0]
+    rows, width = shared.shape
+    n = n_ep * bl
+    first = home.shape[1] - bl
+    where = routing(routes[...], le, cap, experts)
+    cols = lax.broadcasted_iota(jnp.int32, (rows, n), 1)
+    lanes = lax.broadcasted_iota(jnp.int32, (rows, width), 1)
+    back = home[:, first:, :].astype(F32).reshape(n, width).astype(BF)
+    pick, picked = jnp.zeros((rows, n), F32), []
+    for dest, within in where:
+        pick = pick + jnp.where(dest * bl + within == cols, 1.0, 0.0)
+        line = mm(one_hot(dest * bl + le * cap, cols), back)
+        picked.append(jnp.sum(jnp.where(within == lanes, line, 0.0), axis=1, keepdims=True))
+    picked.append(jnp.zeros((rows, 8 - len(picked)), F32))
+    gate_grad[...] = jnp.concatenate(picked, 1).T[: gate_grad.shape[0]]
+    token_grad[...] = (mm(pick.astype(BF), back) + shared[...]).astype(BF)
+
+
+def gather_norms(home, quarter, shared, lines):
+    _, cols, width = shared.shape
+    hidden_rows = 3 * cols
+    acc = home[0, :hidden_rows, :].astype(F32)
+    for e in range(1, home.shape[0]):
+        acc = acc + home[e, :hidden_rows, :].astype(F32)
+    turned = acc.T
+    for t in range(3):
+        shared[t] = acc[t * cols : (t + 1) * cols]
+    row = jnp.sum(turned * turned, axis=0, keepdims=True)
+    fill = lines.shape[1] * width - quarter.shape[0] * width - hidden_rows
+    row = jnp.concatenate([row, jnp.zeros((1, fill), F32)], 1)
+    parts = [quarter[...]] + [row[:, a : a + width] for a in range(0, row.shape[1], width)]
+    lines[...] = jnp.broadcast_to(jnp.concatenate(parts, 0).astype(BF)[None], lines.shape)
+
+
+def finish_norms(scale, lines, e_norm, s_norm):
+    n, block, width = lines.shape
+    _, le, hidden = e_norm.shape
+    cols = s_norm.shape[1]
+    q = 3 * le * hidden // (4 * width)
+    rows = []
+    for c in range(2):
+        for b in range(2):
+            acc = lines[2 * b + c].astype(F32)
+            for d in range(4 + 2 * b + c, n, 4):
+                acc = acc + lines[d].astype(F32)
+            rows.append(acc)
+    whole = rows[0] + rows[1] + rows[2] + rows[3]
+    rows = [r[i : i + 1] * scale for r in rows for i in range(q)]
+    per = hidden // width
+    for t in range(3):
+        for e in range(le):
+            at = (t * le + e) * per
+            e_norm[t, e : e + 1, :] = jnp.concatenate(rows[at : at + per], 1)
+    line = jnp.concatenate([whole[i : i + 1] for i in range(q, block)], 1) * scale
+    for t in range(3):
+        s_norm[t : t + 1, :] = line[:, t * cols : (t + 1) * cols]
 
 
 def project(sizes, pos, got, both, eg, eu, ed, sg, su, sd, own_r, own_l, out_r, out_l, xt_ref, gt_ref, xs_ref, gs_ref):
@@ -108,15 +209,20 @@
     return out
 
 
-def expert_grads(kept, other, xt, gt, stack, sq):
+def expert_grads(kept, other, xt, gt, after, stack, sq):
     _, le, width, hidden = stack.shape
     for t, lhs in enumerate((xt, xt, gt)):
         r = over_rows(lhs, (kept, other), slice(t * hidden, (t + 1) * hidden)).reshape(le, width, hidden)
         stack[t] = r.astype(BF)
-        sq[t] = jnp.sum(r * r, axis=1)
-
-
-def row_grads(sizes, pos, kept, other, eg, eu, sg, su, xs, gs, after, out, shared):
+        total = jnp.sum(r * r, axis=1, keepdims=True)
+        per = hidden // width
+        for e in range(le):
+            for q in range(per):
+                at = (t * le + e) * per + q
+                sq[at : at + 1, :] = total[e, :, q * width : (q + 1) * width]
+
+
+def row_grads(sizes, pos, kept, other, eg, eu, sg, su, xs, gs, out, shared):
     le, width, hidden = eg.shape
     ls, bl = sizes[2], sizes[4]
     n_ep, rows = out.shape[0], shared.shape[0]
@@ -192,26 +298,14 @@
     bwd = [(i, (i - 2 + 4 * (i % 2)) % n_tp) for i in range(n_tp)]
     swap = [(i, i ^ 1) for i in range(n_tp)]
 
-    ids = jnp.arange(experts, dtype=jnp.int32)
-    on = [hot(routes[:, k : k + 1], ids[None, :]) for k in range(top)]
-    tri = (jnp.arange(rows)[:, None] > jnp.arange(rows)[None, :]).astype(BF)
-    before = mm(tri, sum(on))
-    dest, within = [], []
-    for k in range(top):
-        pos = jnp.sum(on[k].astype(F32) * before, axis=1).astype(jnp.int32)
-        dest.append(routes[:, k] // le)
-        within.append(routes[:, k] % le * cap + pos)
-    blk = jnp.arange(n_ep * bl, dtype=jnp.int32)
-    spread = sum(hot(blk[:, None], (dest[k] * bl + within[k])[None, :]) for k in range(top))
-    tail = hot(blk[:, None], (jnp.arange(n_ep, dtype=jnp.int32) * bl + ls)[None, :])
+    geo = (le, cap, experts, bl)
+    lanes = jnp.arange(2 * width, dtype=jnp.int32)
     groups = jnp.arange(n_ep, dtype=jnp.int32)
-    lanes = jnp.arange(2 * width, dtype=jnp.int32)
-    w_block = sum(
-        mm(hot(groups[:, None], dest[k][None, :]) * gate_weights[:, k][None, :], hot(within[k][:, None], lanes[None, :]))
-        for k in range(top)
-    ).astype(BF)
-    both = jnp.concatenate([tokens, cotangent], axis=1)
-    sent = mm(jnp.concatenate([spread, tail], 1), jnp.concatenate([both, w_block], 0)).astype(BF)
+    sent, both = call(
+        functools.partial(dispatch, geo),
+        [((n_ep * bl, 2 * width), BF), ((rows, 2 * width), BF)],
+        tokens, cotangent, routes.T, gate_weights.T,
+    )
     got = lax.all_to_all(sent.reshape(n_ep, bl, 2 * width), "ep", 0, 0, tiled=True)
 
     sizes = (nz, piece, ls, cap, bl, slots)
@@ -269,42 +363,36 @@
     grads = (kept, lax.ppermute(kept, "tp", swap))
 
     cols = hidden // n_ep
-    stack, e_sq = call(
-        expert_grads, [((3, le, width, hidden), BF), ((3, le, hidden), F32)], *grads, xt, gt
-    )
-    piece_sq = lax.all_to_all(e_sq.reshape(n_tp, -1), "tp", 0, 0, tiled=True)
-    piece_sq = jnp.sum(piece_sq, axis=0)
     out, shared_part = call(
         functools.partial(row_grads, sizes),
         [((n_ep, 3 * cols + bl, width), BF), ((rows, width), F32)],
-        pos, *grads, e_gate, e_up, s_gate, s_up, xs, gs, e_sq, smem=1, rest=1,
+        pos, *grads, e_gate, e_up, s_gate, s_up, xs, gs, smem=1,
     )
     home = lax.all_to_all(out, "ep", 0, 0, tiled=True)
-    sh_home, home = home[:, : 3 * cols], home[:, 3 * cols :]
-    lane1 = jnp.arange(width, dtype=jnp.int32)
-    shared = jnp.sum(sh_home.astype(F32), axis=0).reshape(3, cols, width)
-    s_sq = jnp.sum(shared * shared, axis=2).reshape(-1)
-    line = jnp.concatenate([piece_sq, s_sq])
-    home, line = lax.optimization_barrier((home, line))
-    lines = lax.all_to_all(jnp.broadcast_to(line[None], (n_tp, line.size)), "tp", 0, 0, tiled=True)
-    rows_home = home.reshape(n_ep * bl, width)
-    token_grad = (mm(spread, rows_home, ((0,), (0,))) + shared_part).astype(BF)
-    wg_home = home[:, ls]
-    gate_grad = []
-    for k in range(top):
-        line = mm(hot(dest[k][:, None], groups[None, :]), wg_home)
-        gate_grad.append(jnp.sum(jnp.where(within[k][:, None] == lane1[None, :], line, 0.0), axis=1))
-    gate_grad = jnp.stack(gate_grad, 1).astype(BF)
-    scale = 1.0 / (width * n_tp)
-    n_e = piece_sq.size
-    return (
-        token_grad,
-        gate_grad,
-        stack,
-        jnp.swapaxes(shared, 1, 2),
-        lines[:, :n_e].reshape(3, le, hidden) * scale,
-        jnp.sum(lines[:, n_e:], axis=0).reshape(3, cols) * scale,
-    )
+    stack, e_sq = call(
+        expert_grads, [((3, le, width, hidden), BF), ((3 * le * hidden // width, width), F32)], *grads, xt, gt, out, rest=1
+    )
+    e_sq = e_sq.reshape(2, -1, width)
+    other_sq = lax.ppermute(jnp.where(c == 0, e_sq[1], e_sq[0]), "tp", swap)
+    e_sq = (jnp.where(c == 0, e_sq[0], e_sq[1]) + other_sq).reshape(2, -1, width)
+    other_sq = lax.ppermute(jnp.where(z % 2 == 0, e_sq[1], e_sq[0]), "tp", [(i, i ^ 2) for i in range(n_tp)])
+    e_sq = jnp.where(z % 2 == 0, e_sq[0], e_sq[1]) + other_sq
+    n_lines = (e_sq.shape[0] + -(-3 * cols // width) + 15) // 16 * 16
+    shared, lines = call(
+        gather_norms, [((3, cols, width), F32), ((n_tp, n_lines, width), BF)], home, e_sq
+    )
+    got_lines = lax.all_to_all(lines, "tp", 0, 0, tiled=True)
+    token_grad, gate_grad = call(
+        functools.partial(collect, geo),
+        [((rows, width), BF), ((top, rows), F32)],
+        home, shared_part, routes.T, lines, rest=1,
+    )
+    e_norm, s_norm = call(
+        functools.partial(finish_norms, 1.0 / (width * n_tp)),
+        [((3, le, hidden), F32), ((3, cols), F32)],
+        got_lines,
+    )
+    return token_grad, gate_grad.astype(BF).T, stack, jnp.swapaxes(shared, 1, 2), e_norm, s_norm
 
 
 def solution(mesh):

time: 279 us -> 262 us (0.939)
  waiting for transfers between devices: 56.7 us -> 41.7 us
  Pallas kernels: 21.8 us -> 31.1 us
  local copies, waits for them, and re-layouts: 9.49 us -> 3.71 us
  starting transfers between devices: 165 us -> 162 us
    all_to_all x1, waiting for transfers between devices: 14.7 us -> 0.18 us  [body(): home = lax.all_to_all(out, 'ep', 0, 0, tiled=True)]
    pallas_call x3 -> x7, Pallas kernels: 21.8 us -> 31.1 us  [call(): pl.pallas_call(kernel, out_shape=[jax.ShapeDtypeStruct(s, d) for s, d in...]
    all_to_all x2 -> x1, starting transfers between devices: 22.4 us -> 13.9 us  [body(): got_lines = lax.all_to_all(lines, 'tp', 0, 0, tiled=True)]
    ppermute x0 -> x2, starting transfers between devices: none -> 4.19 us  [the longest x1 2.27 us: body(): other_sq = lax.ppermute(jnp.where(c == 0, e_sq[1], e_sq[0]), 'tp', swap)]
    all_to_all x2 -> x1, waiting for transfers between devices: 15.6 us -> 11.9 us  [body(): got_lines = lax.all_to_all(lines, 'tp', 0, 0, tiled=True)]
    ppermute x0 -> x2, waiting for transfers between devices: none -> 3.55 us  [the longest x1 2.76 us: body(): lax.ppermute(jnp.where(z % 2 == 0, e_sq[1], e_sq[0]), 'tp', [(i, i ^ 2) f...]
  transfers between devices with their start and end apart: 37 -> 38, of which waited for: 17 -> 18; matrix products, arithmetic and copies ran while one was open for 7% -> 8% of each run, Pallas kernels for 3% -> 3%
where the time goes in v4:
time: 262 us; the launch traced here: 260 us
  starting transfers between devices  162 us (62%)
  waiting for transfers between devices  41.7 us (16%)
  Pallas kernels  31.1 us (12%)
  other arithmetic  19.9 us (8%)
  local copies, waits for them, and re-layouts  3.71 us (1%)
    ppermute x16, starting transfers between devices, body(): right = lax.ppermute(right, 'tp', fwd)  82.7 us
    pallas_call x7, Pallas kernels, call(): pl.pallas_call(kernel, out_shape=[jax.ShapeDtypeStruct(s, d) for s, d in...  31.1 us
    ppermute x14, starting transfers between devices, body(): left = lax.ppermute(left, 'tp', bwd)  26.8 us
    ppermute x1, starting transfers between devices, body(): grads = (kept, lax.ppermute(kept, 'tp', swap))  14.8 us
    all_to_all x1, starting transfers between devices, body(): got_lines = lax.all_to_all(lines, 'tp', 0, 0, tiled=True)  13.9 us
    all_to_all x1, waiting for transfers between devices, body(): got_lines = lax.all_to_all(lines, 'tp', 0, 0, tiled=True)  11.9 us
    ppermute x16, waiting for transfers between devices, body(): right = lax.ppermute(right, 'tp', fwd)  10.9 us
    all_to_all x1, starting transfers between devices, body(): lax.all_to_all(sent.reshape(n_ep, bl, 2 * width), 'ep', 0, 0, tiled=True)  7.57 us
  transfers between devices with their start and end apart: 38, of which 18 were waited for; matrix products, arithmetic and copies ran while one was open for 8% of the time, Pallas kernels for 3%

profile of v4, /device:TPU:1, one launch (start us, length us, event | category | flops | bytes accessed | tf_op | source)
XLA Modules:
  0.0 259.6 jit_solution(11698391008096587098)
XLA Ops:
  0.6 3.0 %shard_map.145 = (bf16[640,256]{1,0:T(8,128)(2,1)}, bf16[192,256]{1,0:T(8,128)(2,1)}) custom-call(bf16[192,128]{1,0:T(8,128)(2,1)} %tokens.1, bf16[192,128]{1,0:T(8,128)(2,1)} %cotangent.1, s32[2,192]{1,0:T(2,128)} %bitcast.14, bf16[2,192]{1,0:T(2,128)(2,1)} %bitcast.16), custom_call_target="tpu_custom_call" | custom-call | tf_op jit(solution)/shard_map/pallas_call | solution.py:30
  3.6 7.6 %all-to-all-start = ((bf16[16,40,256]{2,1,0:T(8,128)(2,1)}), bf16[16,40,256]{2,1,0:T(8,128)(2,1)S(1)}, u32[]{:S(2)}, u32[]{:S(2)}) async-start(bf16[16,40,256]{2,1,0:T(8,128)(2,1)} %bitcast.13), calls=%async_computation | async-start | bytes 655360 | tf_op jit(solution)/shard_map/all_to_all | solution.py:309
  11.8 7.3 %all-to-all-done = bf16[16,40,256]{2,1,0:T(8,128)(2,1)S(1)} async-done(((bf16[16,40,256]{2,1,0:T(8,128)(2,1)}), bf16[16,40,256]{2,1,0:T(8,128)(2,1)S(1)}, u32[]{:S(2)}, u32[]{:S(2)}) %all-to-all-start) | async-done | bytes 327712 | tf_op jit(solution)/shard_map/all_to_all | solution.py:309
  19.8 8.9 %shard_map.146 = (f32[216,3072]{1,0:T(8,128)}, f32[168,3072]{1,0:T(8,128)}, bf16[216,3072]{1,0:T(8,128)(2,1)}, bf16[168,3072]{1,0:T(8,128)(2,1)}, bf16[256,768]{...) custom-call(s32[2]{0:T(128)} %pad_add_fusion.pos, ...), custom_call_target="tpu_custom_call" | custom-call | tf_op jit(solution)/shard_map/pallas_call | solution.py:30
  28.7 6.1 %collective-permute-start = (bf16[216,3072]{1,0:T(8,128)(2,1)}, bf16[216,3072]{1,0:T(8,128)(2,1)}, u32[]{:S(2)}, u32[]{:S(2)}) collective-permute-start(bf16[216,3072]{1,0:T(8,128)(2,1)} %get-tuple-element.29), channel_id=1, source_target_pairs={{0,1},{1,0},{2,3},{3,2},{4,5},{5,4},{6,7},{7,6},{8,9},{9,8},{10,11... | collective-permute-start | bytes 3981320 | tf_op jit(solution)/shard_map/ppermute | solution.py:323
  34.8 1.9 collective-permute-start.9
  38.9 9.6 %collective-permute-start.1 = (bf16[24,3072]{1,0:T(8,128)(2,1)S(1)}, bf16[24,3072]{1,0:T(8,128)(2,1)S(1)}, u32[]{:S(2)}, u32[]{:S(2)}) collective-permute-start(bf16[24,3072]{1,0:T(8,128)(2,1)S(1)} %add_convert_fusion.12), channel_id=1, source_target_pairs={{0,2},{1,31},{2,4},{3,1},{4,6},{5,3},{6,8},{7,5},{8,10},{9,7},{10,... | collective-permute-start | bytes 442376 | tf_op jit(solution)/shard_map/ppermute | solution.py:336
  49.6 1.9 collective-permute-start.10
  52.6 4.6 %collective-permute-start.2 = (bf16[24,3072]{1,0:T(8,128)(2,1)S(1)}, bf16[24,3072]{1,0:T(8,128)(2,1)S(1)}, u32[]{:S(2)}, u32[]{:S(2)}) collective-permute-start(bf16[24,3072]{1,0:T(8,128)(2,1)S(1)} %add_convert_fusion.11), channel_id=1, source_target_pairs={{0,2},{1,31},{2,4},{3,1},{4,6},{5,3},{6,8},{7,5},{8,10},{9,7},{10,... | collective-permute-start | bytes 442376 | tf_op jit(solution)/shard_map/ppermute | solution.py:336
  58.2 1.9 collective-permute-start.11
  61.1 4.6 %collective-permute-start.3 = (bf16[24,3072]{1,0:T(8,128)(2,1)S(1)}, bf16[24,3072]{1,0:T(8,128)(2,1)S(1)}, u32[]{:S(2)}, u32[]{:S(2)}) collective-permute-start(bf16[24,3072]{1,0:T(8,128)(2,1)S(1)} %add_convert_fusion.10), channel_id=1, source_target_pairs={{0,2},{1,31},{2,4},{3,1},{4,6},{5,3},{6,8},{7,5},{8,10},{9,7},{10,... | collective-permute-start | bytes 442376 | tf_op jit(solution)/shard_map/ppermute | solution.py:336
  66.8 1.9 collective-permute-start.12
  69.7 4.6 %collective-permute-start.4 = (bf16[24,3072]{1,0:T(8,128)(2,1)S(1)}, bf16[24,3072]{1,0:T(8,128)(2,1)S(1)}, u32[]{:S(2)}, u32[]{:S(2)}) collective-permute-start(bf16[24,3072]{1,0:T(8,128)(2,1)S(1)} %add_convert_fusion.9), channel_id=1, source_target_pairs={{0,2},{1,31},{2,4},{3,1},{4,6},{5,3},{6,8},{7,5},{8,10},{9,7},{10,... | collective-permute-start | bytes 442376 | tf_op jit(solution)/shard_map/ppermute | solution.py:336
  75.2 1.9 collective-permute-start.13
  78.2 4.6 %collective-permute-start.5 = (bf16[24,3072]{1,0:T(8,128)(2,1)S(1)}, bf16[24,3072]{1,0:T(8,128)(2,1)S(1)}, u32[]{:S(2)}, u32[]{:S(2)}) collective-permute-start(bf16[24,3072]{1,0:T(8,128)(2,1)S(1)} %add_convert_fusion.8), channel_id=1, source_target_pairs={{0,2},{1,31},{2,4},{3,1},{4,6},{5,3},{6,8},{7,5},{8,10},{9,7},{10,... | collective-permute-start | bytes 442376 | tf_op jit(solution)/shard_map/ppermute | solution.py:336
  83.7 1.9 collective-permute-start.14
  86.6 4.6 %collective-permute-start.6 = (bf16[24,3072]{1,0:T(8,128)(2,1)S(1)}, bf16[24,3072]{1,0:T(8,128)(2,1)S(1)}, u32[]{:S(2)}, u32[]{:S(2)}) collective-permute-start(bf16[24,3072]{1,0:T(8,128)(2,1)S(1)} %add_convert_fusion.7), channel_id=1, source_target_pairs={{0,2},{1,31},{2,4},{3,1},{4,6},{5,3},{6,8},{7,5},{8,10},{9,7},{10,... | collective-permute-start | bytes 442376 | tf_op jit(solution)/shard_map/ppermute | solution.py:336
  92.2 1.9 collective-permute-start.15
  95.1 4.6 %collective-permute-start.7 = (bf16[24,3072]{1,0:T(8,128)(2,1)S(1)}, bf16[24,3072]{1,0:T(8,128)(2,1)S(1)}, u32[]{:S(2)}, u32[]{:S(2)}) collective-permute-start(bf16[24,3072]{1,0:T(8,128)(2,1)S(1)} %add_convert_fusion.6), channel_id=1, source_target_pairs={{0,2},{1,31},{2,4},{3,1},{4,6},{5,3},{6,8},{7,5},{8,10},{9,7},{10,... | collective-permute-start | bytes 442376 | tf_op jit(solution)/shard_map/ppermute | solution.py:336
  100.6 1.9 collective-permute-start.16
  103.5 4.8 %collective-permute-start.8 = (f32[24,3072]{1,0:T(8,128)S(1)}, f32[24,3072]{1,0:T(8,128)S(1)}, u32[]{:S(2)}, u32[]{:S(2)}) collective-permute-start(f32[24,3072]{1,0:T(8,128)S(1)} %add_add_fusion.2), channel_id=1, source_target_pairs={{0,2},{1,31},{2,4},{3,1},{4,6},{5,3},{6,8},{7,5},{8,10},{9,7},{10,... | collective-permute-start | bytes 884744 | tf_op jit(solution)/shard_map/ppermute | solution.py:336
  110.4 4.6 %collective-permute-done.8 = f32[24,3072]{1,0:T(8,128)S(1)} collective-permute-done((f32[24,3072]{1,0:T(8,128)S(1)}, f32[24,3072]{1,0:T(8,128)S(1)}, u32[]{:S(2)}, u32[]{:S(2)}) %collective-permute-start.8) | collective-permute-done | bytes 294944 | tf_op jit(solution)/shard_map/ppermute | solution.py:336
  116.2 1.9 collective-permute-start.17
  118.1 5.3 %collective-permute-start.24 = (bf16[24,3200]{1,0:T(8,128)(2,1)S(1)}, bf16[24,3200]{1,0:T(8,128)(2,1)S(1)}, u32[]{:S(2)}, u32[]{:S(2)}) collective-permute-start(bf16[24,3200]{1,0:T(8,128)(2,1)S(1)} %get-tuple-element.50), channel_id=1, source_target_pairs={{0,2},{1,31},{2,4},{3,1},{4,6},{5,3},{6,8},{7,5},{8,10},{9,7},{10,... | collective-permute-start | bytes 460808 | tf_op jit(solution)/shard_map/ppermute | solution.py:357
  124.1 1.9 collective-permute-start.18
  126.8 5.0 %collective-permute-start.25 = (bf16[24,3200]{1,0:T(8,128)(2,1)S(1)}, bf16[24,3200]{1,0:T(8,128)(2,1)S(1)}, u32[]{:S(2)}, u32[]{:S(2)}) collective-permute-start(bf16[24,3200]{1,0:T(8,128)(2,1)S(1)} %collective-permute-done.24), channel_id=1, source_target_pairs={{0,2},{1,31},{2,4},{3,1},{4,6},{5,3},{6,8},{7,5},{8,10},{9,7},{10,... | collective-permute-start | bytes 460808 | tf_op jit(solution)/shard_map/ppermute | solution.py:357
  132.2 1.9 collective-permute-start.19
  134.9 5.3 %collective-permute-start.26 = (bf16[24,3200]{1,0:T(8,128)(2,1)S(1)}, bf16[24,3200]{1,0:T(8,128)(2,1)S(1)}, u32[]{:S(2)}, u32[]{:S(2)}) collective-permute-start(bf16[24,3200]{1,0:T(8,128)(2,1)S(1)} %collective-permute-done.25), channel_id=1, source_target_pairs={{0,2},{1,31},{2,4},{3,1},{4,6},{5,3},{6,8},{7,5},{8,10},{9,7},{10,... | collective-permute-start | bytes 460808 | tf_op jit(solution)/shard_map/ppermute | solution.py:357
  140.5 1.9 collective-permute-start.20
  142.4 5.3 %collective-permute-start.27 = (bf16[24,3200]{1,0:T(8,128)(2,1)S(1)}, bf16[24,3200]{1,0:T(8,128)(2,1)S(1)}, u32[]{:S(2)}, u32[]{:S(2)}) collective-permute-start(bf16[24,3200]{1,0:T(8,128)(2,1)S(1)} %collective-permute-done.26), channel_id=1, source_target_pairs={{0,2},{1,31},{2,4},{3,1},{4,6},{5,3},{6,8},{7,5},{8,10},{9,7},{10,... | collective-permute-start | bytes 460808 | tf_op jit(solution)/shard_map/ppermute | solution.py:357
  149.9 5.0 %collective-permute-start.28 = (bf16[24,3200]{1,0:T(8,128)(2,1)S(1)}, bf16[24,3200]{1,0:T(8,128)(2,1)S(1)}, u32[]{:S(2)}, u32[]{:S(2)}) collective-permute-start(bf16[24,3200]{1,0:T(8,128)(2,1)S(1)} %collective-permute-done.27), channel_id=1, source_target_pairs={{0,2},{1,31},{2,4},{3,1},{4,6},{5,3},{6,8},{7,5},{8,10},{9,7},{10,... | collective-permute-start | bytes 460808 | tf_op jit(solution)/shard_map/ppermute | solution.py:357
  157.0 5.0 %collective-permute-start.29 = (bf16[24,3200]{1,0:T(8,128)(2,1)S(1)}, bf16[24,3200]{1,0:T(8,128)(2,1)S(1)}, u32[]{:S(2)}, u32[]{:S(2)}) collective-permute-start(bf16[24,3200]{1,0:T(8,128)(2,1)S(1)} %collective-permute-done.28), channel_id=1, source_target_pairs={{0,2},{1,31},{2,4},{3,1},{4,6},{5,3},{6,8},{7,5},{8,10},{9,7},{10,... | collective-permute-start | bytes 460808 | tf_op jit(solution)/shard_map/ppermute | solution.py:357
  164.2 5.0 %collective-permute-start.30 = (bf16[24,3200]{1,0:T(8,128)(2,1)S(1)}, bf16[24,3200]{1,0:T(8,128)(2,1)S(1)}, u32[]{:S(2)}, u32[]{:S(2)}) collective-permute-start(bf16[24,3200]{1,0:T(8,128)(2,1)S(1)} %collective-permute-done.29), channel_id=1, source_target_pairs={{0,2},{1,31},{2,4},{3,1},{4,6},{5,3},{6,8},{7,5},{8,10},{9,7},{10,... | collective-permute-start | bytes 460808 | tf_op jit(solution)/shard_map/ppermute | solution.py:357
  169.2 2.1 collective-permute-done.30
  171.3 5.0 %collective-permute-start.31 = (bf16[24,3200]{1,0:T(8,128)(2,1)S(1)}, bf16[24,3200]{1,0:T(8,128)(2,1)S(1)}, u32[]{:S(2)}, u32[]{:S(2)}) collective-permute-start(bf16[24,3200]{1,0:T(8,128)(2,1)S(1)} %collective-permute-done.30), channel_id=1, source_target_pairs={{0,2},{1,31},{2,4},{3,1},{4,6},{5,3},{6,8},{7,5},{8,10},{9,7},{10,... | collective-permute-start | bytes 460808 | tf_op jit(solution)/shard_map/ppermute | solution.py:357
  176.3 2.5 collective-permute-done.31
  179.0 14.8 %collective-permute-start.32 = (bf16[384,3200]{1,0:T(8,128)(2,1)S(1)}, bf16[384,3200]{1,0:T(8,128)(2,1)}, u32[]{:S(2)}, u32[]{:S(2)}) collective-permute-start(bf16[384,3200]{1,0:T(8,128)(2,1)S(1)} %constant_dynamic-update-slice_fusion.kept), channel_id=1, source_target_pairs={{0,1},{1,0},{2,3},{3,2},{4,5},{5,4},{6,7},{7,6},{8,9},{9,8},{10,11... | collective-permute-start | bytes 7372808 | tf_op jit(solution)/shard_map/ppermute | solution.py:363
  193.8 4.2 %collective-permute-done.32.other = bf16[384,3200]{1,0:T(8,128)(2,1)} collective-permute-done((bf16[384,3200]{1,0:T(8,128)(2,1)S(1)}, bf16[384,3200]{1,0:T(8,128)(2,1)}, u32[]{:S(2)}, u32[]{:S(2)}) %collective-permute-start.32) | collective-permute-done | bytes 2457632 | tf_op jit(solution)/shard_map/ppermute | solution.py:363
  198.0 7.4 %shard_map.147 = (bf16[16,232,128]{2,1,0:T(8,128)(2,1)}, f32[192,128]{1,0:T(8,128)}) custom-call(s32[2]{0:T(128)} %pad_add_fusion.pos, bf16[384,3200]{1,0:T(8,128)(2,1)} %copy-done, bf16[384,3200]{1,0:T(8,128)(2,1)} %collective-permute-done.32.other, bf16[2,128,1024]{2,1,0:T(8,128)(2,1)} %eg.3, bf16[2,128,1024]{2,1,0:T(8,128)(2,1)} %eu.3, ...), custom_call_target="tpu_custom_call" | custom-call | tf_op jit(solution)/shard_map/pallas_call | solution.py:30
  205.4 3.6 %all-to-all-start.1 = ((bf16[16,232,128]{2,1,0:T(8,128)(2,1)}), bf16[16,232,128]{2,1,0:T(8,128)(2,1)S(1)}, u32[]{:S(2)}, u32[]{:S(2)}) async-start(bf16[16,232,128]{2,1,0:T(8,128)(2,1)} %get-tuple-element.34.after), calls=%async_computation.1 | async-start | bytes 1900544 | tf_op jit(solution)/shard_map/all_to_all | solution.py:371
  209.0 5.5 %shard_map.148 = (bf16[3,2,128,1024]{3,2,1,0:T(8,128)(2,1)}, f32[48,128]{1,0:T(8,128)}) custom-call(bf16[384,3200]{1,0:T(8,128)(2,1)} %copy-done, bf16[384,3200]{1,0:T(8,128)(2,1)} %collective-permute-done.32.other, bf16[256,768]{1,0:T(8,128)(2,1)} %get-tuple-element.36.xt, bf16[256,768]{1,0:T(8,128)(2,1)} %get-tuple-element.37.gt, ...), custom_call_target="tpu_custom_call" | custom-call | tf_op jit(solution)/shard_map/pallas_call | solution.py:30
  215.3 2.3 collective-permute-start.33
  219.1 1.9 collective-permute-start.34
  221.1 2.8 %collective-permute-done.34 = f32[12,128]{1,0:T(8,128)S(1)} collective-permute-done((f32[12,128]{1,0:T(8,128)S(1)}, f32[12,128]{1,0:T(8,128)S(1)}, u32[]{:S(2)}, u32[]{:S(2)}) %collective-permute-start.34) | collective-permute-done | bytes 6176 | tf_op jit(solution)/shard_map/ppermute | solution.py:378
  225.6 2.0 shard_map.149
  227.6 13.9 %all-to-all-start.2 = ((bf16[32,16,128]{2,1,0:T(8,128)(2,1)}), bf16[32,16,128]{2,1,0:T(8,128)(2,1)S(1)}, u32[]{:S(2)}, u32[]{:S(2)}) async-start(bf16[32,16,128]{2,1,0:T(8,128)(2,1)} %get-tuple-element.39.after), calls=%async_computation.2 | async-start | bytes 262144 | tf_op jit(solution)/shard_map/all_to_all | solution.py:384
  241.5 2.7 %shard_map.150 = (bf16[192,128]{1,0:T(8,128)(2,1)}, f32[2,192]{1,0:T(2,128)}) custom-call(bf16[16,232,128]{2,1,0:T(8,128)(2,1)} %copy-done.1, f32[192,128]{1,0:T(8,128)} %get-tuple-element.35.shared, s32[2,192]{1,0:T(2,128)} %bitcast.15, bf16[32,16,128]{2,1,0:T(8,128)(2,1)} %get-tuple-element.39.after), custom_call_target="tpu_custom_call" | custom-call | tf_op jit(solution)/shard_map/pallas_call | solution.py:30
  245.5 11.9 %all-to-all-done.2.lines = bf16[32,16,128]{2,1,0:T(8,128)(2,1)S(1)} async-done(((bf16[32,16,128]{2,1,0:T(8,128)(2,1)}), bf16[32,16,128]{2,1,0:T(8,128)(2,1)S(1)}, u32[]{:S(2)}, u32[]{:S(2)}) %all-to-all-start.2) | async-done | bytes 131104 | tf_op jit(solution)/shard_map/all_to_all | solution.py:384
  (91 shorter events, 37.5 us)
Async XLA Ops:
  3.6 15.5 %all-to-all-start = ((bf16[16,40,256]{2,1,0:T(8,128)(2,1)}), bf16[16,40,256]{2,1,0:T(8,128)(2,1)S(1)}, u32[]{:S(2)}, u32[]{:S(2)}) async-start(bf16[16,40,256]{2,1,0:T(8,128)(2,1)} %bitcast.13), calls=%async_computation | async-start | bytes 655360 | tf_op jit(solution)/shard_map/all_to_all | solution.py:309
  19.1 0.7 copy-start.4
  28.7 31.4 %copy-start.2 = (f32[216,3072]{1,0:T(8,128)S(1)}, f32[216,3072]{1,0:T(8,128)}, u32[]{:S(2)}) copy-start(f32[216,3072]{1,0:T(8,128)} %get-tuple-element.28) | copy-start | bytes 7962628
  28.7 9.1 %collective-permute-start = (bf16[216,3072]{1,0:T(8,128)(2,1)}, bf16[216,3072]{1,0:T(8,128)(2,1)}, u32[]{:S(2)}, u32[]{:S(2)}) collective-permute-start(bf16[216,3072]{1,0:T(8,128)(2,1)} %get-tuple-element.29), channel_id=1, source_target_pairs={{0,1},{1,0},{2,3},{3,2},{4,5},{5,4},{6,7},{7,6},{8,9},{9,8},{10,11... | collective-permute-start | bytes 3981320 | tf_op jit(solution)/shard_map/ppermute | solution.py:323
  34.8 13.7 %collective-permute-start.9 = (bf16[168,3072]{1,0:T(8,128)(2,1)}, bf16[168,3072]{1,0:T(8,128)(2,1)}, u32[]{:S(2)}, u32[]{:S(2)}) collective-permute-start(bf16[168,3072]{1,0:T(8,128)(2,1)} %get-tuple-element.31), channel_id=1, source_target_pairs={{0,1},{1,0},{2,3},{3,2},{4,5},{5,4},{6,7},{7,6},{8,9},{9,8},{10,11... | collective-permute-start | bytes 3096584 | tf_op jit(solution)/shard_map/ppermute | solution.py:324
  36.8 37.5 %copy-start.3 = (f32[168,3072]{1,0:T(8,128)S(1)}, f32[168,3072]{1,0:T(8,128)}, u32[]{:S(2)}) copy-start(f32[168,3072]{1,0:T(8,128)} %get-tuple-element.30) | copy-start | bytes 6193156
  38.9 12.6 %collective-permute-start.1 = (bf16[24,3072]{1,0:T(8,128)(2,1)S(1)}, bf16[24,3072]{1,0:T(8,128)(2,1)S(1)}, u32[]{:S(2)}, u32[]{:S(2)}) collective-permute-start(bf16[24,3072]{1,0:T(8,128)(2,1)S(1)} %add_convert_fusion.12), channel_id=1, source_target_pairs={{0,2},{1,31},{2,4},{3,1},{4,6},{5,3},{6,8},{7,5},{8,10},{9,7},{10,... | collective-permute-start | bytes 442376 | tf_op jit(solution)/shard_map/ppermute | solution.py:336
  49.6 7.6 %collective-permute-start.10 = (bf16[24,3072]{1,0:T(8,128)(2,1)S(1)}, bf16[24,3072]{1,0:T(8,128)(2,1)S(1)}, u32[]{:S(2)}, u32[]{:S(2)}) collective-permute-start(bf16[24,3072]{1,0:T(8,128)(2,1)S(1)} %add_convert_fusion.5), channel_id=1, source_target_pairs={{0,30},{1,3},{2,0},{3,5},{4,2},{5,7},{6,4},{7,9},{8,6},{9,11},{10,... | collective-permute-start | bytes 442376 | tf_op jit(solution)/shard_map/ppermute | solution.py:341
  52.6 7.6 %collective-permute-start.2 = (bf16[24,3072]{1,0:T(8,128)(2,1)S(1)}, bf16[24,3072]{1,0:T(8,128)(2,1)S(1)}, u32[]{:S(2)}, u32[]{:S(2)}) collective-permute-start(bf16[24,3072]{1,0:T(8,128)(2,1)S(1)} %add_convert_fusion.11), channel_id=1, source_target_pairs={{0,2},{1,31},{2,4},{3,1},{4,6},{5,3},{6,8},{7,5},{8,10},{9,7},{10,... | collective-permute-start | bytes 442376 | tf_op jit(solution)/shard_map/ppermute | solution.py:336
  58.2 7.5 %collective-permute-start.11 = (bf16[24,3072]{1,0:T(8,128)(2,1)S(1)}, bf16[24,3072]{1,0:T(8,128)(2,1)S(1)}, u32[]{:S(2)}, u32[]{:S(2)}) collective-permute-start(bf16[24,3072]{1,0:T(8,128)(2,1)S(1)} %add_convert_fusion.4), channel_id=1, source_target_pairs={{0,30},{1,3},{2,0},{3,5},{4,2},{5,7},{6,4},{7,9},{8,6},{9,11},{10,... | collective-permute-start | bytes 442376 | tf_op jit(solution)/shard_map/ppermute | solution.py:341
  61.1 7.6 %collective-permute-start.3 = (bf16[24,3072]{1,0:T(8,128)(2,1)S(1)}, bf16[24,3072]{1,0:T(8,128)(2,1)S(1)}, u32[]{:S(2)}, u32[]{:S(2)}) collective-permute-start(bf16[24,3072]{1,0:T(8,128)(2,1)S(1)} %add_convert_fusion.10), channel_id=1, source_target_pairs={{0,2},{1,31},{2,4},{3,1},{4,6},{5,3},{6,8},{7,5},{8,10},{9,7},{10,... | collective-permute-start | bytes 442376 | tf_op jit(solution)/shard_map/ppermute | solution.py:336
  66.8 7.5 %collective-permute-start.12 = (bf16[24,3072]{1,0:T(8,128)(2,1)S(1)}, bf16[24,3072]{1,0:T(8,128)(2,1)S(1)}, u32[]{:S(2)}, u32[]{:S(2)}) collective-permute-start(bf16[24,3072]{1,0:T(8,128)(2,1)S(1)} %add_convert_fusion.3), channel_id=1, source_target_pairs={{0,30},{1,3},{2,0},{3,5},{4,2},{5,7},{6,4},{7,9},{8,6},{9,11},{10,... | collective-permute-start | bytes 442376 | tf_op jit(solution)/shard_map/ppermute | solution.py:341
  69.7 7.5 %collective-permute-start.4 = (bf16[24,3072]{1,0:T(8,128)(2,1)S(1)}, bf16[24,3072]{1,0:T(8,128)(2,1)S(1)}, u32[]{:S(2)}, u32[]{:S(2)}) collective-permute-start(bf16[24,3072]{1,0:T(8,128)(2,1)S(1)} %add_convert_fusion.9), channel_id=1, source_target_pairs={{0,2},{1,31},{2,4},{3,1},{4,6},{5,3},{6,8},{7,5},{8,10},{9,7},{10,... | collective-permute-start | bytes 442376 | tf_op jit(solution)/shard_map/ppermute | solution.py:336
  75.2 7.5 %collective-permute-start.13 = (bf16[24,3072]{1,0:T(8,128)(2,1)S(1)}, bf16[24,3072]{1,0:T(8,128)(2,1)S(1)}, u32[]{:S(2)}, u32[]{:S(2)}) collective-permute-start(bf16[24,3072]{1,0:T(8,128)(2,1)S(1)} %add_convert_fusion.2), channel_id=1, source_target_pairs={{0,30},{1,3},{2,0},{3,5},{4,2},{5,7},{6,4},{7,9},{8,6},{9,11},{10,... | collective-permute-start | bytes 442376 | tf_op jit(solution)/shard_map/ppermute | solution.py:341
  78.2 7.5 %collective-permute-start.5 = (bf16[24,3072]{1,0:T(8,128)(2,1)S(1)}, bf16[24,3072]{1,0:T(8,128)(2,1)S(1)}, u32[]{:S(2)}, u32[]{:S(2)}) collective-permute-start(bf16[24,3072]{1,0:T(8,128)(2,1)S(1)} %add_convert_fusion.8), channel_id=1, source_target_pairs={{0,2},{1,31},{2,4},{3,1},{4,6},{5,3},{6,8},{7,5},{8,10},{9,7},{10,... | collective-permute-start | bytes 442376 | tf_op jit(solution)/shard_map/ppermute | solution.py:336
  83.7 7.5 %collective-permute-start.14 = (bf16[24,3072]{1,0:T(8,128)(2,1)S(1)}, bf16[24,3072]{1,0:T(8,128)(2,1)S(1)}, u32[]{:S(2)}, u32[]{:S(2)}) collective-permute-start(bf16[24,3072]{1,0:T(8,128)(2,1)S(1)} %add_convert_fusion.1), channel_id=1, source_target_pairs={{0,30},{1,3},{2,0},{3,5},{4,2},{5,7},{6,4},{7,9},{8,6},{9,11},{10,... | collective-permute-start | bytes 442376 | tf_op jit(solution)/shard_map/ppermute | solution.py:341
  86.6 7.5 %collective-permute-start.6 = (bf16[24,3072]{1,0:T(8,128)(2,1)S(1)}, bf16[24,3072]{1,0:T(8,128)(2,1)S(1)}, u32[]{:S(2)}, u32[]{:S(2)}) collective-permute-start(bf16[24,3072]{1,0:T(8,128)(2,1)S(1)} %add_convert_fusion.7), channel_id=1, source_target_pairs={{0,2},{1,31},{2,4},{3,1},{4,6},{5,3},{6,8},{7,5},{8,10},{9,7},{10,... | collective-permute-start | bytes 442376 | tf_op jit(solution)/shard_map/ppermute | solution.py:336
  92.2 7.5 %collective-permute-start.15 = (bf16[24,3072]{1,0:T(8,128)(2,1)S(1)}, bf16[24,3072]{1,0:T(8,128)(2,1)S(1)}, u32[]{:S(2)}, u32[]{:S(2)}) collective-permute-start(bf16[24,3072]{1,0:T(8,128)(2,1)S(1)} %add_convert_fusion), channel_id=1, source_target_pairs={{0,30},{1,3},{2,0},{3,5},{4,2},{5,7},{6,4},{7,9},{8,6},{9,11},{10,... | collective-permute-start | bytes 442376 | tf_op jit(solution)/shard_map/ppermute | solution.py:341
  95.1 7.5 %collective-permute-start.7 = (bf16[24,3072]{1,0:T(8,128)(2,1)S(1)}, bf16[24,3072]{1,0:T(8,128)(2,1)S(1)}, u32[]{:S(2)}, u32[]{:S(2)}) collective-permute-start(bf16[24,3072]{1,0:T(8,128)(2,1)S(1)} %add_convert_fusion.6), channel_id=1, source_target_pairs={{0,2},{1,31},{2,4},{3,1},{4,6},{5,3},{6,8},{7,5},{8,10},{9,7},{10,... | collective-permute-start | bytes 442376 | tf_op jit(solution)/shard_map/ppermute | solution.py:336
  100.6 9.7 %collective-permute-start.16 = (f32[24,3072]{1,0:T(8,128)S(1)}, f32[24,3072]{1,0:T(8,128)S(1)}, u32[]{:S(2)}, u32[]{:S(2)}) collective-permute-start(f32[24,3072]{1,0:T(8,128)S(1)} %add_add_fusion.1), channel_id=1, source_target_pairs={{0,30},{1,3},{2,0},{3,5},{4,2},{5,7},{6,4},{7,9},{8,6},{9,11},{10,... | collective-permute-start | bytes 884744 | tf_op jit(solution)/shard_map/ppermute | solution.py:341
  103.5 11.4 %collective-permute-start.8 = (f32[24,3072]{1,0:T(8,128)S(1)}, f32[24,3072]{1,0:T(8,128)S(1)}, u32[]{:S(2)}, u32[]{:S(2)}) collective-permute-start(f32[24,3072]{1,0:T(8,128)S(1)} %add_add_fusion.2), channel_id=1, source_target_pairs={{0,2},{1,31},{2,4},{3,1},{4,6},{5,3},{6,8},{7,5},{8,10},{9,7},{10,... | collective-permute-start | bytes 884744 | tf_op jit(solution)/shard_map/ppermute | solution.py:336
  116.2 7.9 %collective-permute-start.17 = (bf16[24,3200]{1,0:T(8,128)(2,1)S(1)}, bf16[24,3200]{1,0:T(8,128)(2,1)S(1)}, u32[]{:S(2)}, u32[]{:S(2)}) collective-permute-start(bf16[24,3200]{1,0:T(8,128)(2,1)S(1)} %get-tuple-element.50), channel_id=1, source_target_pairs={{0,30},{1,3},{2,0},{3,5},{4,2},{5,7},{6,4},{7,9},{8,6},{9,11},{10,... | collective-permute-start | bytes 460808 | tf_op jit(solution)/shard_map/ppermute | solution.py:360
  118.1 8.7 %collective-permute-start.24 = (bf16[24,3200]{1,0:T(8,128)(2,1)S(1)}, bf16[24,3200]{1,0:T(8,128)(2,1)S(1)}, u32[]{:S(2)}, u32[]{:S(2)}) collective-permute-start(bf16[24,3200]{1,0:T(8,128)(2,1)S(1)} %get-tuple-element.50), channel_id=1, source_target_pairs={{0,2},{1,31},{2,4},{3,1},{4,6},{5,3},{6,8},{7,5},{8,10},{9,7},{10,... | collective-permute-start | bytes 460808 | tf_op jit(solution)/shard_map/ppermute | solution.py:357
  124.1 8.0 %collective-permute-start.18 = (bf16[24,3200]{1,0:T(8,128)(2,1)S(1)}, bf16[24,3200]{1,0:T(8,128)(2,1)S(1)}, u32[]{:S(2)}, u32[]{:S(2)}) collective-permute-start(bf16[24,3200]{1,0:T(8,128)(2,1)S(1)} %collective-permute-done.17), channel_id=1, source_target_pairs={{0,30},{1,3},{2,0},{3,5},{4,2},{5,7},{6,4},{7,9},{8,6},{9,11},{10,... | collective-permute-start | bytes 460808 | tf_op jit(solution)/shard_map/ppermute | solution.py:360
  126.8 8.0 %collective-permute-start.25 = (bf16[24,3200]{1,0:T(8,128)(2,1)S(1)}, bf16[24,3200]{1,0:T(8,128)(2,1)S(1)}, u32[]{:S(2)}, u32[]{:S(2)}) collective-permute-start(bf16[24,3200]{1,0:T(8,128)(2,1)S(1)} %collective-permute-done.24), channel_id=1, source_target_pairs={{0,2},{1,31},{2,4},{3,1},{4,6},{5,3},{6,8},{7,5},{8,10},{9,7},{10,... | collective-permute-start | bytes 460808 | tf_op jit(solution)/shard_map/ppermute | solution.py:357
  132.2 8.3 %collective-permute-start.19 = (bf16[24,3200]{1,0:T(8,128)(2,1)S(1)}, bf16[24,3200]{1,0:T(8,128)(2,1)S(1)}, u32[]{:S(2)}, u32[]{:S(2)}) collective-permute-start(bf16[24,3200]{1,0:T(8,128)(2,1)S(1)} %collective-permute-done.18), channel_id=1, source_target_pairs={{0,30},{1,3},{2,0},{3,5},{4,2},{5,7},{6,4},{7,9},{8,6},{9,11},{10,... | collective-permute-start | bytes 460808 | tf_op jit(solution)/shard_map/ppermute | solution.py:360
  134.9 7.5 %collective-permute-start.26 = (bf16[24,3200]{1,0:T(8,128)(2,1)S(1)}, bf16[24,3200]{1,0:T(8,128)(2,1)S(1)}, u32[]{:S(2)}, u32[]{:S(2)}) collective-permute-start(bf16[24,3200]{1,0:T(8,128)(2,1)S(1)} %collective-permute-done.25), channel_id=1, source_target_pairs={{0,2},{1,31},{2,4},{3,1},{4,6},{5,3},{6,8},{7,5},{8,10},{9,7},{10,... | collective-permute-start | bytes 460808 | tf_op jit(solution)/shard_map/ppermute | solution.py:357
  140.5 7.5 %collective-permute-start.20 = (bf16[24,3200]{1,0:T(8,128)(2,1)S(1)}, bf16[24,3200]{1,0:T(8,128)(2,1)S(1)}, u32[]{:S(2)}, u32[]{:S(2)}) collective-permute-start(bf16[24,3200]{1,0:T(8,128)(2,1)S(1)} %collective-permute-done.19), channel_id=1, source_target_pairs={{0,30},{1,3},{2,0},{3,5},{4,2},{5,7},{6,4},{7,9},{8,6},{9,11},{10,... | collective-permute-start | bytes 460808 | tf_op jit(solution)/shard_map/ppermute | solution.py:360
  142.4 7.4 %collective-permute-start.27 = (bf16[24,3200]{1,0:T(8,128)(2,1)S(1)}, bf16[24,3200]{1,0:T(8,128)(2,1)S(1)}, u32[]{:S(2)}, u32[]{:S(2)}) collective-permute-start(bf16[24,3200]{1,0:T(8,128)(2,1)S(1)} %collective-permute-done.26), channel_id=1, source_target_pairs={{0,2},{1,31},{2,4},{3,1},{4,6},{5,3},{6,8},{7,5},{8,10},{9,7},{10,... | collective-permute-start | bytes 460808 | tf_op jit(solution)/shard_map/ppermute | solution.py:357
  147.9 7.2 %collective-permute-start.21 = (bf16[24,3200]{1,0:T(8,128)(2,1)S(1)}, bf16[24,3200]{1,0:T(8,128)(2,1)S(1)}, u32[]{:S(2)}, u32[]{:S(2)}) collective-permute-start(bf16[24,3200]{1,0:T(8,128)(2,1)S(1)} %collective-permute-done.20), channel_id=1, source_target_pairs={{0,30},{1,3},{2,0},{3,5},{4,2},{5,7},{6,4},{7,9},{8,6},{9,11},{10,... | collective-permute-start | bytes 460808 | tf_op jit(solution)/shard_map/ppermute | solution.py:360
  149.9 7.1 %collective-permute-start.28 = (bf16[24,3200]{1,0:T(8,128)(2,1)S(1)}, bf16[24,3200]{1,0:T(8,128)(2,1)S(1)}, u32[]{:S(2)}, u32[]{:S(2)}) collective-permute-start(bf16[24,3200]{1,0:T(8,128)(2,1)S(1)} %collective-permute-done.27), channel_id=1, source_target_pairs={{0,2},{1,31},{2,4},{3,1},{4,6},{5,3},{6,8},{7,5},{8,10},{9,7},{10,... | collective-permute-start | bytes 460808 | tf_op jit(solution)/shard_map/ppermute | solution.py:357
  155.1 7.2 %collective-permute-start.22 = (bf16[24,3200]{1,0:T(8,128)(2,1)S(1)}, bf16[24,3200]{1,0:T(8,128)(2,1)S(1)}, u32[]{:S(2)}, u32[]{:S(2)}) collective-permute-start(bf16[24,3200]{1,0:T(8,128)(2,1)S(1)} %collective-permute-done.21), channel_id=1, source_target_pairs={{0,30},{1,3},{2,0},{3,5},{4,2},{5,7},{6,4},{7,9},{8,6},{9,11},{10,... | collective-permute-start | bytes 460808 | tf_op jit(solution)/shard_map/ppermute | solution.py:360
  157.0 7.1 %collective-permute-start.29 = (bf16[24,3200]{1,0:T(8,128)(2,1)S(1)}, bf16[24,3200]{1,0:T(8,128)(2,1)S(1)}, u32[]{:S(2)}, u32[]{:S(2)}) collective-permute-start(bf16[24,3200]{1,0:T(8,128)(2,1)S(1)} %collective-permute-done.28), channel_id=1, source_target_pairs={{0,2},{1,31},{2,4},{3,1},{4,6},{5,3},{6,8},{7,5},{8,10},{9,7},{10,... | collective-permute-start | bytes 460808 | tf_op jit(solution)/shard_map/ppermute | solution.py:357
  162.2 14.1 %collective-permute-start.23 = (bf16[24,3200]{1,0:T(8,128)(2,1)S(1)}, bf16[24,3200]{1,0:T(8,128)(2,1)S(1)}, u32[]{:S(2)}, u32[]{:S(2)}) collective-permute-start(bf16[24,3200]{1,0:T(8,128)(2,1)S(1)} %collective-permute-done.22), channel_id=1, source_target_pairs={{0,30},{1,3},{2,0},{3,5},{4,2},{5,7},{6,4},{7,9},{8,6},{9,11},{10,... | collective-permute-start | bytes 460808 | tf_op jit(solution)/shard_map/ppermute | solution.py:360
  164.2 7.1 %collective-permute-start.30 = (bf16[24,3200]{1,0:T(8,128)(2,1)S(1)}, bf16[24,3200]{1,0:T(8,128)(2,1)S(1)}, u32[]{:S(2)}, u32[]{:S(2)}) collective-permute-start(bf16[24,3200]{1,0:T(8,128)(2,1)S(1)} %collective-permute-done.29), channel_id=1, source_target_pairs={{0,2},{1,31},{2,4},{3,1},{4,6},{5,3},{6,8},{7,5},{8,10},{9,7},{10,... | collective-permute-start | bytes 460808 | tf_op jit(solution)/shard_map/ppermute | solution.py:357
  171.3 7.6 %collective-permute-start.31 = (bf16[24,3200]{1,0:T(8,128)(2,1)S(1)}, bf16[24,3200]{1,0:T(8,128)(2,1)S(1)}, u32[]{:S(2)}, u32[]{:S(2)}) collective-permute-start(bf16[24,3200]{1,0:T(8,128)(2,1)S(1)} %collective-permute-done.30), channel_id=1, source_target_pairs={{0,2},{1,31},{2,4},{3,1},{4,6},{5,3},{6,8},{7,5},{8,10},{9,7},{10,... | collective-permute-start | bytes 460808 | tf_op jit(solution)/shard_map/ppermute | solution.py:357
  179.0 19.0 %copy-start = (bf16[384,3200]{1,0:T(8,128)(2,1)}, bf16[384,3200]{1,0:T(8,128)(2,1)S(1)}, u32[]{:S(2)}) copy-start(bf16[384,3200]{1,0:T(8,128)(2,1)S(1)} %constant_dynamic-update-slice_fusion.kept) | copy-start | bytes 7372804
  179.0 19.0 %collective-permute-start.32 = (bf16[384,3200]{1,0:T(8,128)(2,1)S(1)}, bf16[384,3200]{1,0:T(8,128)(2,1)}, u32[]{:S(2)}, u32[]{:S(2)}) collective-permute-start(bf16[384,3200]{1,0:T(8,128)(2,1)S(1)} %constant_dynamic-update-slice_fusion.kept), channel_id=1, source_target_pairs={{0,1},{1,0},{2,3},{3,2},{4,5},{5,4},{6,7},{7,6},{8,9},{9,8},{10,11... | collective-permute-start | bytes 7372808 | tf_op jit(solution)/shard_map/ppermute | solution.py:363
  205.4 19.2 %all-to-all-start.1 = ((bf16[16,232,128]{2,1,0:T(8,128)(2,1)}), bf16[16,232,128]{2,1,0:T(8,128)(2,1)S(1)}, u32[]{:S(2)}, u32[]{:S(2)}) async-start(bf16[16,232,128]{2,1,0:T(8,128)(2,1)} %get-tuple-element.34.after), calls=%async_computation.1 | async-start | bytes 1900544 | tf_op jit(solution)/shard_map/all_to_all | solution.py:371
  215.3 3.1 %collective-permute-start.33 = (f32[24,128]{1,0:T(8,128)S(1)}, f32[24,128]{1,0:T(8,128)S(1)}, u32[]{:S(2)}, u32[]{:S(2)}) collective-permute-start(f32[24,128]{1,0:T(8,128)S(1)} %slice_select_fusion), channel_id=1, source_target_pairs={{0,1},{1,0},{2,3},{3,2},{4,5},{5,4},{6,7},{7,6},{8,9},{9,8},{10,11... | collective-permute-start | bytes 36872 | tf_op jit(solution)/shard_map/ppermute | solution.py:376
  219.1 4.7 %collective-permute-start.34 = (f32[12,128]{1,0:T(8,128)S(1)}, f32[12,128]{1,0:T(8,128)S(1)}, u32[]{:S(2)}, u32[]{:S(2)}) collective-permute-start(f32[12,128]{1,0:T(8,128)S(1)} %slice_select_fusion.1), channel_id=1, source_target_pairs={{0,2},{1,3},{2,0},{3,1},{4,6},{5,7},{6,4},{7,5},{8,10},{9,11},{10,... | collective-permute-start | bytes 18440 | tf_op jit(solution)/shard_map/ppermute | solution.py:378
  224.6 1.0 copy-start.1
  227.6 29.8 %all-to-all-start.2 = ((bf16[32,16,128]{2,1,0:T(8,128)(2,1)}), bf16[32,16,128]{2,1,0:T(8,128)(2,1)S(1)}, u32[]{:S(2)}, u32[]{:S(2)}) async-start(bf16[32,16,128]{2,1,0:T(8,128)(2,1)} %get-tuple-element.39.after), calls=%async_computation.2 | async-start | bytes 262144 | tf_op jit(solution)/shard_map/all_to_all | solution.py:384
  257.4 0.6 copy-start.5

commit v5 on v4

--- a/solution.py
+++ b/solution.py
@@ -46,12 +46,17 @@
 
 def ring_rows(r, z, c, sizes):
     nz, piece, ls, cap, bl, slots = sizes
-    half = nz * piece
+    sec = nz // 2 * piece
+    half = 2 * sec
     h = (r >= half).astype(jnp.int32)
     inner = r - half * h
-    j = quotient(inner, piece, half)
-    turn = (1 - 2 * c) * (1 - 2 * h) * j
-    place = piece * (2 * ((z + turn) & (nz - 1)) + jnp.abs(c - h)) + inner - piece * j
+    q = (inner >= sec).astype(jnp.int32)
+    inner = inner - sec * q
+    m = quotient(inner, piece, sec)
+    core = jnp.abs(c - h)
+    zeta = (z + core) & (nz - 1)
+    zeta = zeta + q * (1 - 2 * (zeta & 1)) + 2 * (1 - 2 * core) * m
+    place = piece * (2 * ((zeta - core) & (nz - 1)) + core) + inner - piece * m
     block = quotient(place, ls, 2 * half)
     within = place - ls * block
     routed = place < slots
@@ -294,8 +299,9 @@
     piece = total // n_tp
     tp = lax.axis_index("tp")
     z, c = tp // 2, tp % 2
-    fwd = [(i, (i + 2 - 4 * (i % 2)) % n_tp) for i in range(n_tp)]
-    bwd = [(i, (i - 2 + 4 * (i % 2)) % n_tp) for i in range(n_tp)]
+    fwd = [(i, (i + 4 - 8 * (i % 2)) % n_tp) for i in range(n_tp)]
+    bwd = [(b, a) for a, b in fwd]
+    pair = [(i, (2 * ((i // 2 + i % 2) % nz ^ 1) - i % 2) % n_tp) for i in range(n_tp)]
     swap = [(i, i ^ 1) for i in range(n_tp)]
 
     geo = (le, cap, experts, bl)
@@ -310,39 +316,43 @@
 
     sizes = (nz, piece, ls, cap, bl, slots)
     pos = jnp.stack([z, c]).astype(jnp.int32)
-    hops, back_hops = nz // 2, nz - nz // 2 - 1
-    nr, nl = (hops + 1) * piece, back_hops * piece
+    members = nz // 2
+    hops, back_hops = members // 2, members - members // 2 - 1
+    sec = members * piece
     width3 = 3 * hidden
-    own_r, own_l, out_r, out_l, xt, gt, xs, gs = call(
+    own_k, own_s, out_k, out_s, xt, gt, xs, gs = call(
         functools.partial(project, sizes),
-        [((nr, width3), F32), ((nl, width3), F32), ((nr, width3), BF), ((nl, width3), BF)]
-        + [((le * width, total), BF)] * 2
-        + [((width, total), BF)] * 2,
+        [((sec, width3), F32)] * 2 + [((sec, width3), BF)] * 2 + [((le * width, total), BF)] * 2 + [((width, total), BF)] * 2,
         pos, got.reshape(n_ep * bl, 2 * width), both, e_gate, e_up, e_down, s_gate, s_up, s_down, smem=1,
     )
-    oth_r = lax.ppermute(out_r, "tp", swap)
-    oth_l = lax.ppermute(out_l, "tp", swap)
-
-    def at_r(j):
-        rows_j = slice(j * piece, (j + 1) * piece)
-        return own_r[rows_j] + oth_r[rows_j].astype(F32)
-
-    def at_l(j):
-        rows_j = slice((back_hops - j) * piece, (back_hops - j + 1) * piece)
-        return own_l[rows_j] + oth_l[rows_j].astype(F32)
-
-    right, left = at_r(hops).astype(BF), at_l(back_hops).astype(BF)
+    oth_s = lax.ppermute(out_s, "tp", swap)
+    oth_k = lax.ppermute(out_k, "tp", swap)
+    cut = hops * piece
+    to_hi = (own_s[cut:] + oth_s[cut:].astype(F32)).astype(BF)
+    to_lo = (own_s[:cut] + oth_s[:cut].astype(F32)).astype(BF)
+    par_hi = lax.ppermute(to_hi, "tp", pair)
+    par_lo = lax.ppermute(to_lo, "tp", pair)
+
+    on_left = lax.optimization_barrier((own_k[cut + piece :], oth_k[cut + piece :], par_hi[piece:]))
+
+    def at(m):
+        if m > hops:
+            rows_m = slice((m - hops - 1) * piece, (m - hops) * piece)
+            return sum(a[rows_m].astype(F32) for a in on_left)
+        rows_m = slice(m * piece, (m + 1) * piece)
+        par = par_lo[rows_m] if m < hops else par_hi[m * piece - cut : (m + 1) * piece - cut]
+        return own_k[rows_m] + oth_k[rows_m].astype(F32) + par.astype(F32)
+
+    right, left = at(hops).astype(BF), at(hops + 1).astype(BF)
     for t in range(hops):
         right = lax.ppermute(right, "tp", fwd)
         if t < hops - 1:
-            right = right.astype(F32) + at_r(hops - 1 - t)
-            right = right if t == hops - 2 else right.astype(BF)
+            right = (right.astype(F32) + at(hops - 1 - t)).astype(BF)
         if t < back_hops:
             left = lax.ppermute(left, "tp", bwd)
         if t < back_hops - 1:
-            left = left.astype(F32) + at_l(back_hops - 1 - t)
-            left = left if t == back_hops - 2 else left.astype(BF)
-    summed = right.astype(F32) + left.astype(F32) + at_r(0)
+            left = (left.astype(F32) + at(hops + 2 + t)).astype(BF)
+    summed = right.astype(F32) + left.astype(F32) + at(0)
 
     q = tp * piece + jnp.arange(piece, dtype=jnp.int32)
     w_rows = mm(hot((q // ls)[:, None], groups[None, :]), got[:, ls, :])
@@ -351,15 +361,19 @@
     gg, gu, sa, wg = row_backward(summed, own_w)
     block = jnp.concatenate([gg, gu, sa, jnp.broadcast_to(wg, (piece, 128))], 1)
 
-    ring = [None] * nz
+    ring = [None] * members
     ring[0] = right = left = block
     for t in range(1, hops + 1):
         right = lax.ppermute(right, "tp", fwd)
-        ring[-t % nz] = right
+        ring[-t % members] = right
         if t <= back_hops:
             left = lax.ppermute(left, "tp", bwd)
             ring[t] = left
-    kept = jnp.concatenate(ring, 0)
+    lo = jnp.concatenate(ring[:hops], 0)
+    hi = jnp.concatenate(ring[hops:], 0)
+    lo_o = lax.ppermute(lo, "tp", pair)
+    hi_o = lax.ppermute(hi, "tp", pair)
+    kept = jnp.concatenate([lo, hi, lo_o, hi_o], 0)
     grads = (kept, lax.ppermute(kept, "tp", swap))
 
     cols = hidden // n_ep

time: 262 us -> 236 us (0.901)
  starting transfers between devices: 162 us -> 116 us
  waiting for transfers between devices: 41.7 us -> 72.6 us
  other arithmetic: 19.9 us -> 8.83 us
    ppermute x16 -> x8, starting transfers between devices: 82.7 us -> 39.8 us  [body(): right = lax.ppermute(right, 'tp', fwd)]
    ppermute x2 -> x6, waiting for transfers between devices: 0.04 us -> 15.5 us  [the longest x1 10.5 us: body(): hi_o = lax.ppermute(hi, 'tp', pair)]
    ppermute x2 -> x6, starting transfers between devices: 8 us -> 23.1 us  [the longest x1 9.64 us: body(): par_hi = lax.ppermute(to_hi, 'tp', pair)]
    ppermute x14 -> x6, waiting for transfers between devices: 3.62 us -> 17.3 us  [body(): left = lax.ppermute(left, 'tp', bwd)]
    ppermute x14 -> x6, starting transfers between devices: 26.8 us -> 17.5 us  [body(): left = lax.ppermute(left, 'tp', bwd)]
    convert_element_type x13 -> x8, other arithmetic: 12.9 us -> 4.53 us  [the longest x1 3.15 us: body(): to_lo = (own_s[:cut] + oth_s[:cut].astype(F32)).astype(BF)]
    ppermute x1, starting transfers between devices: 14.8 us -> 8.15 us  [body(): grads = (kept, lax.ppermute(kept, 'tp', swap))]
    add x3 -> x1, other arithmetic: 2.9 us -> 0.09 us  [body(): summed = right.astype(F32) + left.astype(F32) + at(0)]
  transfers between devices with their start and end apart: 38 -> 26, of which waited for: 18 -> 19; matrix products, arithmetic and copies ran while one was open for 8% -> 5% of each run, Pallas kernels for 3% -> 4%
where the time goes in v5:
time: 236 us; the launch traced here: 234 us
  starting transfers between devices  116 us (49%)
  waiting for transfers between devices  72.6 us (31%)
  Pallas kernels  31.2 us (13%)
  other arithmetic  8.83 us (4%)
  local copies, waits for them, and re-layouts  4.63 us (2%)
    ppermute x8, starting transfers between devices, body(): right = lax.ppermute(right, 'tp', fwd)  39.8 us
    pallas_call x7, Pallas kernels, call(): pl.pallas_call(kernel, out_shape=[jax.ShapeDtypeStruct(s, d) for s, d in...  31.2 us
    ppermute x6, starting transfers between devices, body(): left = lax.ppermute(left, 'tp', bwd)  17.5 us
    ppermute x6, waiting for transfers between devices, body(): left = lax.ppermute(left, 'tp', bwd)  17.3 us
    ppermute x8, waiting for transfers between devices, body(): right = lax.ppermute(right, 'tp', fwd)  12.5 us
    all_to_all x1, waiting for transfers between devices, body(): got_lines = lax.all_to_all(lines, 'tp', 0, 0, tiled=True)  11.9 us
    all_to_all x1, starting transfers between devices, body(): got_lines = lax.all_to_all(lines, 'tp', 0, 0, tiled=True)  11.7 us
    ppermute x1, waiting for transfers between devices, body(): hi_o = lax.ppermute(hi, 'tp', pair)  10.5 us
  transfers between devices with their start and end apart: 26, of which 19 were waited for; matrix products, arithmetic and copies ran while one was open for 5% of the time, Pallas kernels for 4%

profile of v5, /device:TPU:1, one launch (start us, length us, event | category | flops | bytes accessed | tf_op | source)
XLA Modules:
  0.0 234.5 jit_solution(12454244020063144586)
XLA Ops:
  0.6 3.0 %shard_map.145 = (bf16[640,256]{1,0:T(8,128)(2,1)}, bf16[192,256]{1,0:T(8,128)(2,1)}) custom-call(bf16[192,128]{1,0:T(8,128)(2,1)} %tokens.1, bf16[192,128]{1,0:T(8,128)(2,1)} %cotangent.1, s32[2,192]{1,0:T(2,128)} %bitcast.14, bf16[2,192]{1,0:T(2,128)(2,1)} %bitcast.16), custom_call_target="tpu_custom_call" | custom-call | tf_op jit(solution)/shard_map/pallas_call | solution.py:30
  3.6 7.6 %all-to-all-start = ((bf16[16,40,256]{2,1,0:T(8,128)(2,1)}), bf16[16,40,256]{2,1,0:T(8,128)(2,1)S(1)}, u32[]{:S(2)}, u32[]{:S(2)}) async-start(bf16[16,40,256]{2,1,0:T(8,128)(2,1)} %bitcast.13), calls=%async_computation | async-start | bytes 655360 | tf_op jit(solution)/shard_map/all_to_all | solution.py:315
  11.8 7.3 %all-to-all-done = bf16[16,40,256]{2,1,0:T(8,128)(2,1)S(1)} async-done(((bf16[16,40,256]{2,1,0:T(8,128)(2,1)}), bf16[16,40,256]{2,1,0:T(8,128)(2,1)S(1)}, u32[]{:S(2)}, u32[]{:S(2)}) %all-to-all-start) | async-done | bytes 327712 | tf_op jit(solution)/shard_map/all_to_all | solution.py:315
  19.8 8.9 %shard_map.146 = (f32[192,3072]{1,0:T(8,128)}, f32[192,3072]{1,0:T(8,128)}, bf16[192,3072]{1,0:T(8,128)(2,1)}, bf16[192,3072]{1,0:T(8,128)(2,1)}, bf16[256,768]{...) custom-call(s32[2]{0:T(128)} %pad_add_fusion.pos, ...), custom_call_target="tpu_custom_call" | custom-call | tf_op jit(solution)/shard_map/pallas_call | solution.py:30
  28.7 5.8 %collective-permute-start.1 = (bf16[192,3072]{1,0:T(8,128)(2,1)}, bf16[192,3072]{1,0:T(8,128)(2,1)S(1)}, u32[]{:S(2)}, u32[]{:S(2)}) collective-permute-start(bf16[192,3072]{1,0:T(8,128)(2,1)} %get-tuple-element.34), channel_id=1, source_target_pairs={{0,1},{1,0},{2,3},{3,2},{4,5},{5,4},{6,7},{7,6},{8,9},{9,8},{10,11... | collective-permute-start | bytes 3538952 | tf_op jit(solution)/shard_map/ppermute | solution.py:328
  34.6 1.9 collective-permute-start
  37.2 3.2 %add_convert_fusion = (bf16[96,3072]{1,0:T(8,128)(2,1)}, bf16[96,3072]{1,0:T(8,128)(2,1)}) fusion(f32[192,3072]{1,0:T(8,128)} %get-tuple-element.33, bf16[192,3072]{1,0:T(8,128)(2,1)S(1)} %collective-permute-done.1), kind=kLoop, calls=%fused_computation | loop fusion | flops 1769472 | bytes 4718592 | tf_op jit(solution)/shard_map/convert_element_type | solution.py:332
  40.4 9.6 %collective-permute-start.2 = (bf16[96,3072]{1,0:T(8,128)(2,1)}, bf16[96,3072]{1,0:T(8,128)(2,1)}, u32[]{:S(2)}, u32[]{:S(2)}) collective-permute-start(bf16[96,3072]{1,0:T(8,128)(2,1)} %get-tuple-element.53), channel_id=1, source_target_pairs={{0,2},{1,31},{2,0},{3,5},{4,6},{5,3},{6,4},{7,9},{8,10},{9,7},{10,... | collective-permute-start | bytes 1769480 | tf_op jit(solution)/shard_map/ppermute | solution.py:333
  51.3 1.9 collective-permute-start.4
  53.3 4.3 %collective-permute-done.2 = bf16[96,3072]{1,0:T(8,128)(2,1)} collective-permute-done((bf16[96,3072]{1,0:T(8,128)(2,1)}, bf16[96,3072]{1,0:T(8,128)(2,1)}, u32[]{:S(2)}, u32[]{:S(2)}) %collective-permute-start.2) | collective-permute-done | bytes 589856 | tf_op jit(solution)/shard_map/ppermute | solution.py:333
  58.6 4.1 %collective-permute-start.3 = (bf16[24,3072]{1,0:T(8,128)(2,1)S(1)}, bf16[24,3072]{1,0:T(8,128)(2,1)S(1)}, u32[]{:S(2)}, u32[]{:S(2)}) collective-permute-start(bf16[24,3072]{1,0:T(8,128)(2,1)S(1)} %add_convert_fusion.8), channel_id=1, source_target_pairs={{0,4},{1,29},{2,6},{3,31},{4,8},{5,1},{6,10},{7,3},{8,12},{9,5},{1... | collective-permute-start | bytes 442376 | tf_op jit(solution)/shard_map/ppermute | solution.py:348
  63.8 2.1 collective-permute-start.8
  66.0 5.7 %collective-permute-start.5 = (bf16[24,3072]{1,0:T(8,128)(2,1)S(1)}, bf16[24,3072]{1,0:T(8,128)(2,1)S(1)}, u32[]{:S(2)}, u32[]{:S(2)}) collective-permute-start(bf16[24,3072]{1,0:T(8,128)(2,1)S(1)} %add_convert_fusion.7), channel_id=1, source_target_pairs={{0,4},{1,29},{2,6},{3,31},{4,8},{5,1},{6,10},{7,3},{8,12},{9,5},{1... | collective-permute-start | bytes 442376 | tf_op jit(solution)/shard_map/ppermute | solution.py:348
  71.7 1.2 collective-permute-done.8
  72.9 1.9 collective-permute-start.9
  75.0 5.5 %collective-permute-start.6 = (bf16[24,3072]{1,0:T(8,128)(2,1)S(1)}, bf16[24,3072]{1,0:T(8,128)(2,1)S(1)}, u32[]{:S(2)}, u32[]{:S(2)}) collective-permute-start(bf16[24,3072]{1,0:T(8,128)(2,1)S(1)} %add_convert_fusion.6), channel_id=1, source_target_pairs={{0,4},{1,29},{2,6},{3,31},{4,8},{5,1},{6,10},{7,3},{8,12},{9,5},{1... | collective-permute-start | bytes 442376 | tf_op jit(solution)/shard_map/ppermute | solution.py:348
  80.4 2.1 collective-permute-done.9
  82.6 1.9 collective-permute-start.10
  84.6 5.8 %collective-permute-start.7 = (bf16[24,3072]{1,0:T(8,128)(2,1)S(1)}, bf16[24,3072]{1,0:T(8,128)(2,1)S(1)}, u32[]{:S(2)}, u32[]{:S(2)}) collective-permute-start(bf16[24,3072]{1,0:T(8,128)(2,1)S(1)} %add_convert_fusion.5), channel_id=1, source_target_pairs={{0,4},{1,29},{2,6},{3,31},{4,8},{5,1},{6,10},{7,3},{8,12},{9,5},{1... | collective-permute-start | bytes 442376 | tf_op jit(solution)/shard_map/ppermute | solution.py:348
  90.4 2.2 collective-permute-done.10
  92.7 4.6 %collective-permute-done.7 = bf16[24,3072]{1,0:T(8,128)(2,1)S(1)} collective-permute-done((bf16[24,3072]{1,0:T(8,128)(2,1)S(1)}, bf16[24,3072]{1,0:T(8,128)(2,1)S(1)}, u32[]{:S(2)}, u32[]{:S(2)}) %collective-permute-start.7) | collective-permute-done | bytes 147488 | tf_op jit(solution)/shard_map/ppermute | solution.py:348
  97.7 3.7 %collective-permute-start.14 = (bf16[24,3200]{1,0:T(8,128)(2,1)S(1)}, bf16[24,3200]{1,0:T(8,128)(2,1)S(1)}, u32[]{:S(2)}, u32[]{:S(2)}) collective-permute-start(bf16[24,3200]{1,0:T(8,128)(2,1)S(1)} %get-tuple-element.58), channel_id=1, source_target_pairs={{0,4},{1,29},{2,6},{3,31},{4,8},{5,1},{6,10},{7,3},{8,12},{9,5},{1... | collective-permute-start | bytes 460808 | tf_op jit(solution)/shard_map/ppermute | solution.py:367
  101.4 3.6 %collective-permute-start.11 = (bf16[24,3200]{1,0:T(8,128)(2,1)S(1)}, bf16[24,3200]{1,0:T(8,128)(2,1)S(1)}, u32[]{:S(2)}, u32[]{:S(2)}) collective-permute-start(bf16[24,3200]{1,0:T(8,128)(2,1)S(1)} %get-tuple-element.58), channel_id=1, source_target_pairs={{4,0},{29,1},{6,2},{31,3},{8,4},{1,5},{10,6},{3,7},{12,8},{5,9},{1... | collective-permute-start | bytes 460808 | tf_op jit(solution)/shard_map/ppermute | solution.py:370
  106.0 4.7 %collective-permute-start.15 = (bf16[24,3200]{1,0:T(8,128)(2,1)S(1)}, bf16[24,3200]{1,0:T(8,128)(2,1)S(1)}, u32[]{:S(2)}, u32[]{:S(2)}) collective-permute-start(bf16[24,3200]{1,0:T(8,128)(2,1)S(1)} %collective-permute-done.14), channel_id=1, source_target_pairs={{0,4},{1,29},{2,6},{3,31},{4,8},{5,1},{6,10},{7,3},{8,12},{9,5},{1... | collective-permute-start | bytes 460808 | tf_op jit(solution)/shard_map/ppermute | solution.py:367
  111.3 5.2 %collective-permute-start.12 = (bf16[24,3200]{1,0:T(8,128)(2,1)S(1)}, bf16[24,3200]{1,0:T(8,128)(2,1)S(1)}, u32[]{:S(2)}, u32[]{:S(2)}) collective-permute-start(bf16[24,3200]{1,0:T(8,128)(2,1)S(1)} %collective-permute-done.11), channel_id=1, source_target_pairs={{4,0},{29,1},{6,2},{31,3},{8,4},{1,5},{10,6},{3,7},{12,8},{5,9},{1... | collective-permute-start | bytes 460808 | tf_op jit(solution)/shard_map/ppermute | solution.py:370
  116.9 3.9 %collective-permute-start.16 = (bf16[24,3200]{1,0:T(8,128)(2,1)S(1)}, bf16[24,3200]{1,0:T(8,128)(2,1)S(1)}, u32[]{:S(2)}, u32[]{:S(2)}) collective-permute-start(bf16[24,3200]{1,0:T(8,128)(2,1)S(1)} %collective-permute-done.15), channel_id=1, source_target_pairs={{0,4},{1,29},{2,6},{3,31},{4,8},{5,1},{6,10},{7,3},{8,12},{9,5},{1... | collective-permute-start | bytes 460808 | tf_op jit(solution)/shard_map/ppermute | solution.py:367
  120.8 4.9 %collective-permute-done.12 = bf16[24,3200]{1,0:T(8,128)(2,1)S(1)} collective-permute-done((bf16[24,3200]{1,0:T(8,128)(2,1)S(1)}, bf16[24,3200]{1,0:T(8,128)(2,1)S(1)}, u32[]{:S(2)}, u32[]{:S(2)}) %collective-permute-start.12) | collective-permute-done | bytes 153632 | tf_op jit(solution)/shard_map/ppermute | solution.py:370
  125.7 2.8 %collective-permute-start.13 = (bf16[24,3200]{1,0:T(8,128)(2,1)S(1)}, bf16[24,3200]{1,0:T(8,128)(2,1)S(1)}, u32[]{:S(2)}, u32[]{:S(2)}) collective-permute-start(bf16[24,3200]{1,0:T(8,128)(2,1)S(1)} %collective-permute-done.12), channel_id=1, source_target_pairs={{4,0},{29,1},{6,2},{31,3},{8,4},{1,5},{10,6},{3,7},{12,8},{5,9},{1... | collective-permute-start | bytes 460808 | tf_op jit(solution)/shard_map/ppermute | solution.py:370
  128.5 6.3 %collective-permute-done.13 = bf16[24,3200]{1,0:T(8,128)(2,1)S(1)} collective-permute-done((bf16[24,3200]{1,0:T(8,128)(2,1)S(1)}, bf16[24,3200]{1,0:T(8,128)(2,1)S(1)}, u32[]{:S(2)}, u32[]{:S(2)}) %collective-permute-start.13) | collective-permute-done | bytes 153632 | tf_op jit(solution)/shard_map/ppermute | solution.py:370
  134.8 1.9 collective-permute-start.18
  136.8 6.4 %collective-permute-start.17 = (bf16[24,3200]{1,0:T(8,128)(2,1)S(1)}, bf16[24,3200]{1,0:T(8,128)(2,1)S(1)}, u32[]{:S(2)}, u32[]{:S(2)}) collective-permute-start(bf16[24,3200]{1,0:T(8,128)(2,1)S(1)} %collective-permute-done.16), channel_id=1, source_target_pairs={{0,4},{1,29},{2,6},{3,31},{4,8},{5,1},{6,10},{7,3},{8,12},{9,5},{1... | collective-permute-start | bytes 460808 | tf_op jit(solution)/shard_map/ppermute | solution.py:367
  143.2 6.4 %collective-permute-done.17 = bf16[24,3200]{1,0:T(8,128)(2,1)S(1)} collective-permute-done((bf16[24,3200]{1,0:T(8,128)(2,1)S(1)}, bf16[24,3200]{1,0:T(8,128)(2,1)S(1)}, u32[]{:S(2)}, u32[]{:S(2)}) %collective-permute-start.17) | collective-permute-done | bytes 153632 | tf_op jit(solution)/shard_map/ppermute | solution.py:367
  149.7 1.9 collective-permute-start.19
  151.8 10.5 %collective-permute-done.19 = bf16[96,3200]{1,0:T(8,128)(2,1)S(1)} collective-permute-done((bf16[96,3200]{1,0:T(8,128)(2,1)S(1)}, bf16[96,3200]{1,0:T(8,128)(2,1)S(1)}, u32[]{:S(2)}, u32[]{:S(2)}) %collective-permute-start.19) | collective-permute-done | bytes 614432 | tf_op jit(solution)/shard_map/ppermute | solution.py:375
  162.3 8.2 %collective-permute-start.20 = (bf16[384,3200]{1,0:T(8,128)(2,1)S(1)}, bf16[384,3200]{1,0:T(8,128)(2,1)}, u32[]{:S(2)}, u32[]{:S(2)}) collective-permute-start(bf16[384,3200]{1,0:T(8,128)(2,1)S(1)} %constant_dynamic-update-slice_fusion.kept), channel_id=1, source_target_pairs={{0,1},{1,0},{2,3},{3,2},{4,5},{5,4},{6,7},{7,6},{8,9},{9,8},{10,11... | collective-permute-start | bytes 7372808 | tf_op jit(solution)/shard_map/ppermute | solution.py:377
  170.5 4.4 %collective-permute-done.20.other = bf16[384,3200]{1,0:T(8,128)(2,1)} collective-permute-done((bf16[384,3200]{1,0:T(8,128)(2,1)S(1)}, bf16[384,3200]{1,0:T(8,128)(2,1)}, u32[]{:S(2)}, u32[]{:S(2)}) %collective-permute-start.20) | collective-permute-done | bytes 2457632 | tf_op jit(solution)/shard_map/ppermute | solution.py:377
  174.9 7.4 %shard_map.147 = (bf16[16,232,128]{2,1,0:T(8,128)(2,1)}, f32[192,128]{1,0:T(8,128)}) custom-call(s32[2]{0:T(128)} %pad_add_fusion.pos, bf16[384,3200]{1,0:T(8,128)(2,1)} %copy-done, bf16[384,3200]{1,0:T(8,128)(2,1)} %collective-permute-done.20.other, bf16[2,128,1024]{2,1,0:T(8,128)(2,1)} %eg.3, bf16[2,128,1024]{2,1,0:T(8,128)(2,1)} %eu.3, ...), custom_call_target="tpu_custom_call" | custom-call | tf_op jit(solution)/shard_map/pallas_call | solution.py:30
  182.3 3.8 %all-to-all-start.1 = ((bf16[16,232,128]{2,1,0:T(8,128)(2,1)}), bf16[16,232,128]{2,1,0:T(8,128)(2,1)S(1)}, u32[]{:S(2)}, u32[]{:S(2)}) async-start(bf16[16,232,128]{2,1,0:T(8,128)(2,1)} %get-tuple-element.40.after), calls=%async_computation.1 | async-start | bytes 1900544 | tf_op jit(solution)/shard_map/all_to_all | solution.py:385
  186.1 5.5 %shard_map.148 = (bf16[3,2,128,1024]{3,2,1,0:T(8,128)(2,1)}, f32[48,128]{1,0:T(8,128)}) custom-call(bf16[384,3200]{1,0:T(8,128)(2,1)} %copy-done, bf16[384,3200]{1,0:T(8,128)(2,1)} %collective-permute-done.20.other, bf16[256,768]{1,0:T(8,128)(2,1)} %get-tuple-element.42.xt, bf16[256,768]{1,0:T(8,128)(2,1)} %get-tuple-element.43.gt, ...), custom_call_target="tpu_custom_call" | custom-call | tf_op jit(solution)/shard_map/pallas_call | solution.py:30
  192.4 2.3 collective-permute-start.21
  196.2 1.9 collective-permute-start.22
  198.1 2.5 %collective-permute-done.22 = f32[12,128]{1,0:T(8,128)S(1)} collective-permute-done((f32[12,128]{1,0:T(8,128)S(1)}, f32[12,128]{1,0:T(8,128)S(1)}, u32[]{:S(2)}, u32[]{:S(2)}) %collective-permute-start.22) | collective-permute-done | bytes 6176 | tf_op jit(solution)/shard_map/ppermute | solution.py:392
  202.7 2.0 shard_map.149
  204.7 11.7 %all-to-all-start.2 = ((bf16[32,16,128]{2,1,0:T(8,128)(2,1)}), bf16[32,16,128]{2,1,0:T(8,128)(2,1)S(1)}, u32[]{:S(2)}, u32[]{:S(2)}) async-start(bf16[32,16,128]{2,1,0:T(8,128)(2,1)} %get-tuple-element.45.after), calls=%async_computation.2 | async-start | bytes 262144 | tf_op jit(solution)/shard_map/all_to_all | solution.py:398
  216.4 2.7 %shard_map.150 = (bf16[192,128]{1,0:T(8,128)(2,1)}, f32[2,192]{1,0:T(2,128)}) custom-call(bf16[16,232,128]{2,1,0:T(8,128)(2,1)} %copy-done.1, f32[192,128]{1,0:T(8,128)} %get-tuple-element.41.shared, s32[2,192]{1,0:T(2,128)} %bitcast.15, bf16[32,16,128]{2,1,0:T(8,128)(2,1)} %get-tuple-element.45.after), custom_call_target="tpu_custom_call" | custom-call | tf_op jit(solution)/shard_map/pallas_call | solution.py:30
  219.1 1.2 convert_bitcast_fusion
  220.4 11.9 %all-to-all-done.2.lines = bf16[32,16,128]{2,1,0:T(8,128)(2,1)S(1)} async-done(((bf16[32,16,128]{2,1,0:T(8,128)(2,1)}), bf16[32,16,128]{2,1,0:T(8,128)(2,1)S(1)}, u32[]{:S(2)}, u32[]{:S(2)}) %all-to-all-start.2) | async-done | bytes 131104 | tf_op jit(solution)/shard_map/all_to_all | solution.py:398
  232.9 1.6 shard_map.151
  (57 shorter events, 13.4 us)
Async XLA Ops:
  3.6 15.5 %all-to-all-start = ((bf16[16,40,256]{2,1,0:T(8,128)(2,1)}), bf16[16,40,256]{2,1,0:T(8,128)(2,1)S(1)}, u32[]{:S(2)}, u32[]{:S(2)}) async-start(bf16[16,40,256]{2,1,0:T(8,128)(2,1)} %bitcast.13), calls=%async_computation | async-start | bytes 655360 | tf_op jit(solution)/shard_map/all_to_all | solution.py:315
  19.1 0.7 copy-start.3
  28.7 8.5 %collective-permute-start.1 = (bf16[192,3072]{1,0:T(8,128)(2,1)}, bf16[192,3072]{1,0:T(8,128)(2,1)S(1)}, u32[]{:S(2)}, u32[]{:S(2)}) collective-permute-start(bf16[192,3072]{1,0:T(8,128)(2,1)} %get-tuple-element.34), channel_id=1, source_target_pairs={{0,1},{1,0},{2,3},{3,2},{4,5},{5,4},{6,7},{7,6},{8,9},{9,8},{10,11... | collective-permute-start | bytes 3538952 | tf_op jit(solution)/shard_map/ppermute | solution.py:328
  34.6 18.6 %collective-permute-start = (bf16[192,3072]{1,0:T(8,128)(2,1)}, bf16[192,3072]{1,0:T(8,128)(2,1)S(1)}, u32[]{:S(2)}, u32[]{:S(2)}) collective-permute-start(bf16[192,3072]{1,0:T(8,128)(2,1)} %get-tuple-element.32), channel_id=1, source_target_pairs={{0,1},{1,0},{2,3},{3,2},{4,5},{5,4},{6,7},{7,6},{8,9},{9,8},{10,11... | collective-permute-start | bytes 3538952 | tf_op jit(solution)/shard_map/ppermute | solution.py:329
  37.2 12.8 %copy-start.2 = (f32[192,3072]{1,0:T(8,128)S(1)}, f32[192,3072]{1,0:T(8,128)}, u32[]{:S(2)}) copy-start(f32[192,3072]{1,0:T(8,128)} %get-tuple-element.31) | copy-start | bytes 7077892
  40.4 17.2 %collective-permute-start.2 = (bf16[96,3072]{1,0:T(8,128)(2,1)}, bf16[96,3072]{1,0:T(8,128)(2,1)}, u32[]{:S(2)}, u32[]{:S(2)}) collective-permute-start(bf16[96,3072]{1,0:T(8,128)(2,1)} %get-tuple-element.53), channel_id=1, source_target_pairs={{0,2},{1,31},{2,0},{3,5},{4,6},{5,3},{6,4},{7,9},{8,10},{9,7},{10,... | collective-permute-start | bytes 1769480 | tf_op jit(solution)/shard_map/ppermute | solution.py:333
  51.3 14.6 %collective-permute-start.4 = (bf16[96,3072]{1,0:T(8,128)(2,1)}, bf16[96,3072]{1,0:T(8,128)(2,1)S(1)}, u32[]{:S(2)}, u32[]{:S(2)}) collective-permute-start(bf16[96,3072]{1,0:T(8,128)(2,1)} %get-tuple-element.52), channel_id=1, source_target_pairs={{0,2},{1,31},{2,0},{3,5},{4,6},{5,3},{6,4},{7,9},{8,10},{9,7},{10,... | collective-permute-start | bytes 1769480 | tf_op jit(solution)/shard_map/ppermute | solution.py:334
  58.6 7.3 %collective-permute-start.3 = (bf16[24,3072]{1,0:T(8,128)(2,1)S(1)}, bf16[24,3072]{1,0:T(8,128)(2,1)S(1)}, u32[]{:S(2)}, u32[]{:S(2)}) collective-permute-start(bf16[24,3072]{1,0:T(8,128)(2,1)S(1)} %add_convert_fusion.8), channel_id=1, source_target_pairs={{0,4},{1,29},{2,6},{3,31},{4,8},{5,1},{6,10},{7,3},{8,12},{9,5},{1... | collective-permute-start | bytes 442376 | tf_op jit(solution)/shard_map/ppermute | solution.py:348
  63.8 9.1 %collective-permute-start.8 = (bf16[24,3072]{1,0:T(8,128)(2,1)S(1)}, bf16[24,3072]{1,0:T(8,128)(2,1)S(1)}, u32[]{:S(2)}, u32[]{:S(2)}) collective-permute-start(bf16[24,3072]{1,0:T(8,128)(2,1)S(1)} %add_convert_fusion.4), channel_id=1, source_target_pairs={{4,0},{29,1},{6,2},{31,3},{8,4},{1,5},{10,6},{3,7},{12,8},{5,9},{1... | collective-permute-start | bytes 442376 | tf_op jit(solution)/shard_map/ppermute | solution.py:352
  66.0 8.9 %collective-permute-start.5 = (bf16[24,3072]{1,0:T(8,128)(2,1)S(1)}, bf16[24,3072]{1,0:T(8,128)(2,1)S(1)}, u32[]{:S(2)}, u32[]{:S(2)}) collective-permute-start(bf16[24,3072]{1,0:T(8,128)(2,1)S(1)} %add_convert_fusion.7), channel_id=1, source_target_pairs={{0,4},{1,29},{2,6},{3,31},{4,8},{5,1},{6,10},{7,3},{8,12},{9,5},{1... | collective-permute-start | bytes 442376 | tf_op jit(solution)/shard_map/ppermute | solution.py:348
  72.9 9.6 %collective-permute-start.9 = (bf16[24,3072]{1,0:T(8,128)(2,1)S(1)}, bf16[24,3072]{1,0:T(8,128)(2,1)S(1)}, u32[]{:S(2)}, u32[]{:S(2)}) collective-permute-start(bf16[24,3072]{1,0:T(8,128)(2,1)S(1)} %add_convert_fusion.3), channel_id=1, source_target_pairs={{4,0},{29,1},{6,2},{31,3},{8,4},{1,5},{10,6},{3,7},{12,8},{5,9},{1... | collective-permute-start | bytes 442376 | tf_op jit(solution)/shard_map/ppermute | solution.py:352
  75.0 9.6 %collective-permute-start.6 = (bf16[24,3072]{1,0:T(8,128)(2,1)S(1)}, bf16[24,3072]{1,0:T(8,128)(2,1)S(1)}, u32[]{:S(2)}, u32[]{:S(2)}) collective-permute-start(bf16[24,3072]{1,0:T(8,128)(2,1)S(1)} %add_convert_fusion.6), channel_id=1, source_target_pairs={{0,4},{1,29},{2,6},{3,31},{4,8},{5,1},{6,10},{7,3},{8,12},{9,5},{1... | collective-permute-start | bytes 442376 | tf_op jit(solution)/shard_map/ppermute | solution.py:348
  82.6 10.1 %collective-permute-start.10 = (bf16[24,3072]{1,0:T(8,128)(2,1)S(1)}, bf16[24,3072]{1,0:T(8,128)(2,1)S(1)}, u32[]{:S(2)}, u32[]{:S(2)}) collective-permute-start(bf16[24,3072]{1,0:T(8,128)(2,1)S(1)} %add_convert_fusion.2), channel_id=1, source_target_pairs={{4,0},{29,1},{6,2},{31,3},{8,4},{1,5},{10,6},{3,7},{12,8},{5,9},{1... | collective-permute-start | bytes 442376 | tf_op jit(solution)/shard_map/ppermute | solution.py:352
  84.6 12.7 %collective-permute-start.7 = (bf16[24,3072]{1,0:T(8,128)(2,1)S(1)}, bf16[24,3072]{1,0:T(8,128)(2,1)S(1)}, u32[]{:S(2)}, u32[]{:S(2)}) collective-permute-start(bf16[24,3072]{1,0:T(8,128)(2,1)S(1)} %add_convert_fusion.5), channel_id=1, source_target_pairs={{0,4},{1,29},{2,6},{3,31},{4,8},{5,1},{6,10},{7,3},{8,12},{9,5},{1... | collective-permute-start | bytes 442376 | tf_op jit(solution)/shard_map/ppermute | solution.py:348
  97.7 8.3 %collective-permute-start.14 = (bf16[24,3200]{1,0:T(8,128)(2,1)S(1)}, bf16[24,3200]{1,0:T(8,128)(2,1)S(1)}, u32[]{:S(2)}, u32[]{:S(2)}) collective-permute-start(bf16[24,3200]{1,0:T(8,128)(2,1)S(1)} %get-tuple-element.58), channel_id=1, source_target_pairs={{0,4},{1,29},{2,6},{3,31},{4,8},{5,1},{6,10},{7,3},{8,12},{9,5},{1... | collective-permute-start | bytes 460808 | tf_op jit(solution)/shard_map/ppermute | solution.py:367
  101.4 9.9 %collective-permute-start.11 = (bf16[24,3200]{1,0:T(8,128)(2,1)S(1)}, bf16[24,3200]{1,0:T(8,128)(2,1)S(1)}, u32[]{:S(2)}, u32[]{:S(2)}) collective-permute-start(bf16[24,3200]{1,0:T(8,128)(2,1)S(1)} %get-tuple-element.58), channel_id=1, source_target_pairs={{4,0},{29,1},{6,2},{31,3},{8,4},{1,5},{10,6},{3,7},{12,8},{5,9},{1... | collective-permute-start | bytes 460808 | tf_op jit(solution)/shard_map/ppermute | solution.py:370
  106.0 10.9 %collective-permute-start.15 = (bf16[24,3200]{1,0:T(8,128)(2,1)S(1)}, bf16[24,3200]{1,0:T(8,128)(2,1)S(1)}, u32[]{:S(2)}, u32[]{:S(2)}) collective-permute-start(bf16[24,3200]{1,0:T(8,128)(2,1)S(1)} %collective-permute-done.14), channel_id=1, source_target_pairs={{0,4},{1,29},{2,6},{3,31},{4,8},{5,1},{6,10},{7,3},{8,12},{9,5},{1... | collective-permute-start | bytes 460808 | tf_op jit(solution)/shard_map/ppermute | solution.py:367
  111.3 14.4 %collective-permute-start.12 = (bf16[24,3200]{1,0:T(8,128)(2,1)S(1)}, bf16[24,3200]{1,0:T(8,128)(2,1)S(1)}, u32[]{:S(2)}, u32[]{:S(2)}) collective-permute-start(bf16[24,3200]{1,0:T(8,128)(2,1)S(1)} %collective-permute-done.11), channel_id=1, source_target_pairs={{4,0},{29,1},{6,2},{31,3},{8,4},{1,5},{10,6},{3,7},{12,8},{5,9},{1... | collective-permute-start | bytes 460808 | tf_op jit(solution)/shard_map/ppermute | solution.py:370
  116.9 19.9 %collective-permute-start.16 = (bf16[24,3200]{1,0:T(8,128)(2,1)S(1)}, bf16[24,3200]{1,0:T(8,128)(2,1)S(1)}, u32[]{:S(2)}, u32[]{:S(2)}) collective-permute-start(bf16[24,3200]{1,0:T(8,128)(2,1)S(1)} %collective-permute-done.15), channel_id=1, source_target_pairs={{0,4},{1,29},{2,6},{3,31},{4,8},{5,1},{6,10},{7,3},{8,12},{9,5},{1... | collective-permute-start | bytes 460808 | tf_op jit(solution)/shard_map/ppermute | solution.py:367
  125.7 9.1 %collective-permute-start.13 = (bf16[24,3200]{1,0:T(8,128)(2,1)S(1)}, bf16[24,3200]{1,0:T(8,128)(2,1)S(1)}, u32[]{:S(2)}, u32[]{:S(2)}) collective-permute-start(bf16[24,3200]{1,0:T(8,128)(2,1)S(1)} %collective-permute-done.12), channel_id=1, source_target_pairs={{4,0},{29,1},{6,2},{31,3},{8,4},{1,5},{10,6},{3,7},{12,8},{5,9},{1... | collective-permute-start | bytes 460808 | tf_op jit(solution)/shard_map/ppermute | solution.py:370
  134.8 16.9 %collective-permute-start.18 = (bf16[96,3200]{1,0:T(8,128)(2,1)S(1)}, bf16[96,3200]{1,0:T(8,128)(2,1)S(1)}, u32[]{:S(2)}, u32[]{:S(2)}) collective-permute-start(bf16[96,3200]{1,0:T(8,128)(2,1)S(1)} %pad_maximum_fusion), channel_id=1, source_target_pairs={{0,2},{1,31},{2,0},{3,5},{4,6},{5,3},{6,4},{7,9},{8,10},{9,7},{10,... | collective-permute-start | bytes 1843208 | tf_op jit(solution)/shard_map/ppermute | solution.py:374
  136.8 12.9 %collective-permute-start.17 = (bf16[24,3200]{1,0:T(8,128)(2,1)S(1)}, bf16[24,3200]{1,0:T(8,128)(2,1)S(1)}, u32[]{:S(2)}, u32[]{:S(2)}) collective-permute-start(bf16[24,3200]{1,0:T(8,128)(2,1)S(1)} %collective-permute-done.16), channel_id=1, source_target_pairs={{0,4},{1,29},{2,6},{3,31},{4,8},{5,1},{6,10},{7,3},{8,12},{9,5},{1... | collective-permute-start | bytes 460808 | tf_op jit(solution)/shard_map/ppermute | solution.py:367
  149.7 12.6 %collective-permute-start.19 = (bf16[96,3200]{1,0:T(8,128)(2,1)S(1)}, bf16[96,3200]{1,0:T(8,128)(2,1)S(1)}, u32[]{:S(2)}, u32[]{:S(2)}) collective-permute-start(bf16[96,3200]{1,0:T(8,128)(2,1)S(1)} %pad_maximum_fusion.1), channel_id=1, source_target_pairs={{0,2},{1,31},{2,0},{3,5},{4,6},{5,3},{6,4},{7,9},{8,10},{9,7},{10,... | collective-permute-start | bytes 1843208 | tf_op jit(solution)/shard_map/ppermute | solution.py:375
  162.3 12.6 %copy-start = (bf16[384,3200]{1,0:T(8,128)(2,1)}, bf16[384,3200]{1,0:T(8,128)(2,1)S(1)}, u32[]{:S(2)}) copy-start(bf16[384,3200]{1,0:T(8,128)(2,1)S(1)} %constant_dynamic-update-slice_fusion.kept) | copy-start | bytes 7372804
  162.3 12.6 %collective-permute-start.20 = (bf16[384,3200]{1,0:T(8,128)(2,1)S(1)}, bf16[384,3200]{1,0:T(8,128)(2,1)}, u32[]{:S(2)}, u32[]{:S(2)}) collective-permute-start(bf16[384,3200]{1,0:T(8,128)(2,1)S(1)} %constant_dynamic-update-slice_fusion.kept), channel_id=1, source_target_pairs={{0,1},{1,0},{2,3},{3,2},{4,5},{5,4},{6,7},{7,6},{8,9},{9,8},{10,11... | collective-permute-start | bytes 7372808 | tf_op jit(solution)/shard_map/ppermute | solution.py:377
  182.3 19.4 %all-to-all-start.1 = ((bf16[16,232,128]{2,1,0:T(8,128)(2,1)}), bf16[16,232,128]{2,1,0:T(8,128)(2,1)S(1)}, u32[]{:S(2)}, u32[]{:S(2)}) async-start(bf16[16,232,128]{2,1,0:T(8,128)(2,1)} %get-tuple-element.40.after), calls=%async_computation.1 | async-start | bytes 1900544 | tf_op jit(solution)/shard_map/all_to_all | solution.py:385
  192.4 3.1 %collective-permute-start.21 = (f32[24,128]{1,0:T(8,128)S(1)}, f32[24,128]{1,0:T(8,128)S(1)}, u32[]{:S(2)}, u32[]{:S(2)}) collective-permute-start(f32[24,128]{1,0:T(8,128)S(1)} %slice_select_fusion), channel_id=1, source_target_pairs={{0,1},{1,0},{2,3},{3,2},{4,5},{5,4},{6,7},{7,6},{8,9},{9,8},{10,11... | collective-permute-start | bytes 36872 | tf_op jit(solution)/shard_map/ppermute | solution.py:390
  196.2 4.4 %collective-permute-start.22 = (f32[12,128]{1,0:T(8,128)S(1)}, f32[12,128]{1,0:T(8,128)S(1)}, u32[]{:S(2)}, u32[]{:S(2)}) collective-permute-start(f32[12,128]{1,0:T(8,128)S(1)} %slice_select_fusion.1), channel_id=1, source_target_pairs={{0,2},{1,3},{2,0},{3,1},{4,6},{5,7},{6,4},{7,5},{8,10},{9,11},{10,... | collective-permute-start | bytes 18440 | tf_op jit(solution)/shard_map/ppermute | solution.py:392
  201.7 0.9 copy-start.1
  204.7 27.5 %all-to-all-start.2 = ((bf16[32,16,128]{2,1,0:T(8,128)(2,1)}), bf16[32,16,128]{2,1,0:T(8,128)(2,1)S(1)}, u32[]{:S(2)}, u32[]{:S(2)}) async-start(bf16[32,16,128]{2,1,0:T(8,128)(2,1)} %get-tuple-element.45.after), calls=%async_computation.2 | async-start | bytes 262144 | tf_op jit(solution)/shard_map/all_to_all | solution.py:398
  232.2 0.6 copy-start.4

commit v6 on v5

--- a/solution.py
+++ b/solution.py
@@ -24,7 +24,7 @@
     return (a == b).astype(BF)
 
 
-def call(kernel, outs, *args, smem=0, rest=0):
+def call(kernel, outs, *args, smem=0, rest=0, limit=None):
     first = [pl.BlockSpec(memory_space=pltpu.SMEM)] * smem
     last = [pl.BlockSpec(memory_space=pl.ANY)] * rest
     return pl.pallas_call(
@@ -32,6 +32,7 @@
         out_shape=[jax.ShapeDtypeStruct(s, d) for s, d in outs],
         in_specs=first + [VM] * (len(args) - smem - rest) + last,
         out_specs=[VM] * len(outs),
+        compiler_params=pltpu.CompilerParams(vmem_limit_bytes=limit),
     )(*args)
 
 
@@ -55,7 +56,7 @@
     m = quotient(inner, piece, sec)
     core = jnp.abs(c - h)
     zeta = (z + core) & (nz - 1)
-    zeta = zeta + q * (1 - 2 * (zeta & 1)) + 2 * (1 - 2 * core) * m
+    zeta = zeta + q * (1 - 2 * (zeta & 1)) + 2 * (1 - 2 * core) * (m + nz // 4)
     place = piece * (2 * ((zeta - core) & (nz - 1)) + core) + inner - piece * m
     block = quotient(place, ls, 2 * half)
     within = place - ls * block
@@ -174,11 +175,18 @@
         s_norm[t : t + 1, :] = line[:, t * cols : (t + 1) * cols]
 
 
-def project(sizes, pos, got, both, eg, eu, ed, sg, su, sd, own_r, own_l, out_r, out_l, xt_ref, gt_ref, xs_ref, gs_ref):
-    le, width, hidden = eg.shape
+def project(sizes, pos, got, both, *refs):
+    weights, results = refs[:6], refs[6:10]
+    xt_ref, gt_ref, xs_ref, gs_ref = refs[10:14]
+    held, made = refs[14:20], refs[20:24]
+    sem_in, sem_out = refs[24], refs[25]
+    le, width, hidden = held[0].shape
+    loads = [pltpu.make_async_copy(weights[k], held[k], sem_in.at[k]) for k in range(6)]
+    for load in loads:
+        load.start()
     nb, rows = got.shape[0], both.shape[0]
-    nr, nl = own_r.shape[0], own_l.shape[0]
-    half = nr + nl
+    sec = made[0].shape[0]
+    half = 2 * sec
     z, c = pos[0], pos[1]
     src, kd, _, _ = ring_rows(along(2 * half, 0), z, c, sizes)
     cols = lax.broadcasted_iota(jnp.int32, (2 * half, nb), 1)
@@ -187,14 +195,18 @@
     part = [jnp.where(kd == e, mine, 0.0).astype(BF) for e in range(le + 1)]
     x = jnp.concatenate([p[:, :width] for p in part[:le]], 1)
     g = jnp.concatenate([p[:, width:] for p in part[:le]], 1)
-    todo = ((x, part[le][:, :width], eg, sg), (x, part[le][:, :width], eu, su), (g, part[le][:, width:], ed, sd))
-    for t, (xe, xs, we, ws) in enumerate(todo):
+    stores = []
+    for t, (xe, xs) in enumerate(((x, part[le][:, :width]), (x, part[le][:, :width]), (g, part[le][:, width:]))):
         cut = slice(t * hidden, (t + 1) * hidden)
-        p = mm(xe, we[...].reshape(le * width, hidden)) + mm(xs, ws[...])
-        own_r[:, cut] = p[:nr]
-        own_l[:, cut] = p[nr:half]
-        out_r[:, cut] = p[half : half + nr].astype(BF)
-        out_l[:, cut] = p[half + nr :].astype(BF)
+        loads[t].wait()
+        loads[3 + t].wait()
+        p = mm(xe, held[t][...].reshape(le * width, hidden)) + mm(xs, held[3 + t][...])
+        for k in (3, 1, 2, 0):
+            at = (0, sec, half, half + sec)[k]
+            made[k][:, cut] = p[at : at + sec].astype(made[k].dtype)
+            store = pltpu.make_async_copy(made[k].at[:, cut], results[k].at[:, cut], sem_out.at[t, k])
+            store.start()
+            stores.append(store)
     _, kr, _, _ = ring_rows(along(2 * half, 1), z, c, sizes)
     mine_t = mine.T
     for e in range(le + 1):
@@ -202,6 +214,8 @@
         to_x, to_g, at = (xt_ref, gt_ref, e * width) if e < le else (xs_ref, gs_ref, 0)
         to_x[at : at + width, :] = both_t[:width]
         to_g[at : at + width, :] = both_t[width:]
+    for store in stores:
+        store.wait()
 
 
 def over_rows(lhs, parts, cut):
@@ -214,10 +228,17 @@
     return out
 
 
-def expert_grads(kept, other, xt, gt, after, stack, sq):
+def stack_rows(*refs):
+    at, out = 0, refs[-1]
+    for ref in refs[:-1]:
+        out[at : at + ref.shape[0], :] = ref[...]
+        at += ref.shape[0]
+
+
+def expert_grads(g0, g1, g2, g3, xt, gt, after, stack, sq):
     _, le, width, hidden = stack.shape
     for t, lhs in enumerate((xt, xt, gt)):
-        r = over_rows(lhs, (kept, other), slice(t * hidden, (t + 1) * hidden)).reshape(le, width, hidden)
+        r = over_rows(lhs, (g0, g1, g2, g3), slice(t * hidden, (t + 1) * hidden)).reshape(le, width, hidden)
         stack[t] = r.astype(BF)
         total = jnp.sum(r * r, axis=1, keepdims=True)
         per = hidden // width
@@ -227,20 +248,20 @@
                 sq[at : at + 1, :] = total[e, :, q * width : (q + 1) * width]
 
 
-def row_grads(sizes, pos, kept, other, eg, eu, sg, su, xs, gs, out, shared):
+def row_grads(sizes, pos, g0, g1, g2, g3, eg, eu, sg, su, xs, gs, out, shared):
     le, width, hidden = eg.shape
     ls, bl = sizes[2], sizes[4]
     n_ep, rows = out.shape[0], shared.shape[0]
     nb = n_ep * bl
     cols = hidden // n_ep
     for t, lhs in enumerate((xs, xs, gs)):
-        r = over_rows(lhs, (kept, other), slice(t * hidden, (t + 1) * hidden))
+        r = over_rows(lhs, (g0, g1, g2, g3), slice(t * hidden, (t + 1) * hidden))
         out[:, t * cols : (t + 1) * cols, :] = r.T.astype(BF).reshape(n_ep, cols, width)
     total = 2 * sizes[0] * sizes[1]
     z, c = pos[0], pos[1]
     _, kd, _, within = ring_rows(along(total, 0), z, c, sizes)
     slots, wg, at = [], [], 0
-    for src in (kept, other):
+    for src in (g0, g1, g2, g3):
         n = src.shape[0]
         gg, gu = src[:, :hidden], src[:, hidden : 2 * hidden]
         se = mm(gg, eg[...].reshape(le * width, hidden), NT) + mm(gu, eu[...].reshape(le * width, hidden), NT)
@@ -320,28 +341,38 @@
     hops, back_hops = members // 2, members - members // 2 - 1
     sec = members * piece
     width3 = 3 * hidden
-    own_k, own_s, out_k, out_s, xt, gt, xs, gs = call(
+    big = [((sec, width3), F32)] * 2 + [((sec, width3), BF)] * 2
+    turned = [((le * width, total), BF)] * 2 + [((width, total), BF)] * 2
+    weights = (e_gate, e_up, e_down, s_gate, s_up, s_down)
+    anywhere = pl.BlockSpec(memory_space=pl.ANY)
+    own_k, own_s, out_k, out_s, xt, gt, xs, gs = pl.pallas_call(
         functools.partial(project, sizes),
-        [((sec, width3), F32)] * 2 + [((sec, width3), BF)] * 2 + [((le * width, total), BF)] * 2 + [((width, total), BF)] * 2,
-        pos, got.reshape(n_ep * bl, 2 * width), both, e_gate, e_up, e_down, s_gate, s_up, s_down, smem=1,
-    )
+        out_shape=[jax.ShapeDtypeStruct(a, d) for a, d in big + turned],
+        in_specs=[pl.BlockSpec(memory_space=pltpu.SMEM), VM, VM] + [anywhere] * 6,
+        out_specs=[anywhere] * 4 + [VM] * 4,
+        scratch_shapes=[pltpu.VMEM(w.shape, BF) for w in weights]
+        + [pltpu.VMEM(a, d) for a, d in big]
+        + [pltpu.SemaphoreType.DMA((6,)), pltpu.SemaphoreType.DMA((3, 4))],
+    )(pos, got.reshape(n_ep * bl, 2 * width), both, *weights)
     oth_s = lax.ppermute(out_s, "tp", swap)
     oth_k = lax.ppermute(out_k, "tp", swap)
-    cut = hops * piece
-    to_hi = (own_s[cut:] + oth_s[cut:].astype(F32)).astype(BF)
-    to_lo = (own_s[:cut] + oth_s[:cut].astype(F32)).astype(BF)
-    par_hi = lax.ppermute(to_hi, "tp", pair)
-    par_lo = lax.ppermute(to_lo, "tp", pair)
-
-    on_left = lax.optimization_barrier((own_k[cut + piece :], oth_k[cut + piece :], par_hi[piece:]))
+    cut = 2 * piece
+    to_a = (own_s[:cut] + oth_s[:cut].astype(F32)).astype(BF)
+    to_b = (own_s[cut:] + oth_s[cut:].astype(F32)).astype(BF)
+    par_a = lax.ppermute(to_a, "tp", pair)
+    par_b = lax.ppermute(to_b, "tp", pair)
+    left_rows = slice(cut, hops * piece)
+    on_left = lax.optimization_barrier((own_k[left_rows], oth_k[left_rows], par_b[: hops * piece - cut]))
 
     def at(m):
-        if m > hops:
-            rows_m = slice((m - hops - 1) * piece, (m - hops) * piece)
-            return sum(a[rows_m].astype(F32) for a in on_left)
-        rows_m = slice(m * piece, (m + 1) * piece)
-        par = par_lo[rows_m] if m < hops else par_hi[m * piece - cut : (m + 1) * piece - cut]
-        return own_k[rows_m] + oth_k[rows_m].astype(F32) + par.astype(F32)
+        p = (m - hops) % members
+        rows_p = slice(p * piece, (p + 1) * piece)
+        par = par_a[rows_p] if p < 2 else par_b[p * piece - cut : (p + 1) * piece - cut]
+        own, oth = own_k, oth_k
+        if 1 < p < hops:
+            (own, oth, par), rows_p = on_left, slice((p - 2) * piece, (p - 1) * piece)
+            par = par[rows_p]
+        return own[rows_p] + oth[rows_p].astype(F32) + par.astype(F32)
 
     right, left = at(hops).astype(BF), at(hops + 1).astype(BF)
     for t in range(hops):
@@ -369,12 +400,15 @@
         if t <= back_hops:
             left = lax.ppermute(left, "tp", bwd)
             ring[t] = left
-    lo = jnp.concatenate(ring[:hops], 0)
-    hi = jnp.concatenate(ring[hops:], 0)
-    lo_o = lax.ppermute(lo, "tp", pair)
-    hi_o = lax.ppermute(hi, "tp", pair)
-    kept = jnp.concatenate([lo, hi, lo_o, hi_o], 0)
-    grads = (kept, lax.ppermute(kept, "tp", swap))
+    parts = ring[hops + 1 :] + ring[:hops]
+    (most,) = call(stack_rows, [((len(parts) * piece, block.shape[1]), BF)], *parts, limit=8 * 2**20)
+    most_o = lax.ppermute(most, "tp", pair)
+    last_o = lax.ppermute(ring[hops], "tp", pair)
+    kept = jnp.concatenate([ring[hops], most], 0)
+    kept_x = lax.ppermute(kept, "tp", swap)
+    paired = jnp.concatenate([last_o, most_o], 0)
+    paired_x = lax.ppermute(paired, "tp", swap)
+    grads = (kept, paired, kept_x, paired_x)
 
     cols = hidden // n_ep
     out, shared_part = call(

time: 236 us -> 227 us (0.962)
  waiting for transfers between devices: 72.6 us -> 54.1 us
  starting transfers between devices: 116 us -> 126 us
    ppermute x6, waiting for transfers between devices: 17.3 us -> 1.51 us  [body(): left = lax.ppermute(left, 'tp', bwd)]
    pallas_call x0 -> x1, Pallas kernels: none -> 10 us  [body(): pl.pallas_call(functools.partial(project, sizes), out_shape=[jax.ShapeDty...]
    ppermute x5 -> x6, waiting for transfers between devices: 19.2 us -> 9.33 us  [the longest x1 6.36 us: body(): last_o = lax.ppermute(ring[hops], 'tp', pair)]
    ppermute x8, starting transfers between devices: 39.8 us -> 48.9 us  [body(): right = lax.ppermute(right, 'tp', fwd)]
    pallas_call x7, Pallas kernels: 31.2 us -> 22.7 us  [call(): pl.pallas_call(kernel, out_shape=[jax.ShapeDtypeStruct(s, d) for s, d in...]
    ppermute x8, waiting for transfers between devices: 12.5 us -> 19.8 us  [body(): right = lax.ppermute(right, 'tp', fwd)]
    ppermute x6, starting transfers between devices: 17.5 us -> 11.7 us  [body(): left = lax.ppermute(left, 'tp', bwd)]
    ppermute x5 -> x6, starting transfers between devices: 23.5 us -> 28.8 us  [the longest x1 9.78 us: body(): par_a = lax.ppermute(to_a, 'tp', pair)]
  transfers between devices with their start and end apart: 26 -> 27, of which waited for: 19 -> 18; matrix products, arithmetic and copies ran while one was open for 5% -> 4% of each run, Pallas kernels for 4% -> 4%
where the time goes in v6:
time: 227 us; the launch traced here: 225 us
  starting transfers between devices  126 us (56%)
  waiting for transfers between devices  54.1 us (24%)
  Pallas kernels  32.7 us (14%)
  other arithmetic  7.51 us (3%)
  local copies, waits for them, and re-layouts  3.53 us (2%)
    ppermute x8, starting transfers between devices, body(): right = lax.ppermute(right, 'tp', fwd)  48.9 us
    pallas_call x7, Pallas kernels, call(): pl.pallas_call(kernel, out_shape=[jax.ShapeDtypeStruct(s, d) for s, d in...  22.7 us
    ppermute x8, waiting for transfers between devices, body(): right = lax.ppermute(right, 'tp', fwd)  19.8 us
    all_to_all x1, starting transfers between devices, body(): got_lines = lax.all_to_all(lines, 'tp', 0, 0, tiled=True)  13.3 us
    all_to_all x1, waiting for transfers between devices, body(): got_lines = lax.all_to_all(lines, 'tp', 0, 0, tiled=True)  11.9 us
    ppermute x6, starting transfers between devices, body(): left = lax.ppermute(left, 'tp', bwd)  11.7 us
    pallas_call x1, Pallas kernels, body(): pl.pallas_call(functools.partial(project, sizes), out_shape=[jax.ShapeDty...  10 us
    ppermute x1, starting transfers between devices, body(): par_a = lax.ppermute(to_a, 'tp', pair)  9.78 us
  transfers between devices with their start and end apart: 27, of which 18 were waited for; matrix products, arithmetic and copies ran while one was open for 4% of the time, Pallas kernels for 4%

profile of v6, /device:TPU:1, one launch (start us, length us, event | category | flops | bytes accessed | tf_op | source)
XLA Modules:
  0.0 225.2 jit_solution(3137294045947339116)
XLA Ops:
  0.6 3.0 %shard_map.145 = (bf16[640,256]{1,0:T(8,128)(2,1)}, bf16[192,256]{1,0:T(8,128)(2,1)}) custom-call(bf16[192,128]{1,0:T(8,128)(2,1)} %tokens.1, bf16[192,128]{1,0:T(8,128)(2,1)} %cotangent.1, s32[2,192]{1,0:T(2,128)} %bitcast.14, bf16[2,192]{1,0:T(2,128)(2,1)} %bitcast.16), custom_call_target="tpu_custom_call" | custom-call | tf_op jit(solution)/shard_map/pallas_call | solution.py:30
  3.6 7.6 %all-to-all-start = ((bf16[16,40,256]{2,1,0:T(8,128)(2,1)}), bf16[16,40,256]{2,1,0:T(8,128)(2,1)S(1)}, u32[]{:S(2)}, u32[]{:S(2)}) async-start(bf16[16,40,256]{2,1,0:T(8,128)(2,1)} %bitcast.13), calls=%async_computation | async-start | bytes 655360 | tf_op jit(solution)/shard_map/all_to_all | solution.py:336
  11.8 7.3 %all-to-all-done = bf16[16,40,256]{2,1,0:T(8,128)(2,1)S(1)} async-done(((bf16[16,40,256]{2,1,0:T(8,128)(2,1)}), bf16[16,40,256]{2,1,0:T(8,128)(2,1)S(1)}, u32[]{:S(2)}, u32[]{:S(2)}) %all-to-all-start) | async-done | bytes 327712 | tf_op jit(solution)/shard_map/all_to_all | solution.py:336
  19.8 10.0 %shard_map.146 = (f32[192,3072]{1,0:T(8,128)}, f32[192,3072]{1,0:T(8,128)}, bf16[192,3072]{1,0:T(8,128)(2,1)}, bf16[192,3072]{1,0:T(8,128)(2,1)}, bf16[256,768]{...) custom-call(s32[2]{0:T(128)} %pad_add_fusion.pos, ...), custom_call_target="tpu_custom_call" | custom-call | tf_op jit(solution)/shard_map/pallas_call | solution.py:348
  29.9 5.8 %collective-permute-start.1 = (bf16[192,3072]{1,0:T(8,128)(2,1)}, bf16[192,3072]{1,0:T(8,128)(2,1)S(1)}, u32[]{:S(2)}, u32[]{:S(2)}) collective-permute-start(bf16[192,3072]{1,0:T(8,128)(2,1)} %get-tuple-element.34), channel_id=1, source_target_pairs={{0,1},{1,0},{2,3},{3,2},{4,5},{5,4},{6,7},{7,6},{8,9},{9,8},{10,11... | collective-permute-start | bytes 3538952 | tf_op jit(solution)/shard_map/ppermute | solution.py:357
  35.7 1.9 collective-permute-start
  38.4 1.1 add_convert_fusion.1
  39.5 9.8 %collective-permute-start.2 = (bf16[48,3072]{1,0:T(8,128)(2,1)S(1)}, bf16[48,3072]{1,0:T(8,128)(2,1)S(1)}, u32[]{:S(2)}, u32[]{:S(2)}) collective-permute-start(bf16[48,3072]{1,0:T(8,128)(2,1)S(1)} %add_convert_fusion.1), channel_id=1, source_target_pairs={{0,2},{1,31},{2,0},{3,5},{4,6},{5,3},{6,4},{7,9},{8,10},{9,7},{10,... | collective-permute-start | bytes 884744 | tf_op jit(solution)/shard_map/ppermute | solution.py:362
  49.3 1.6 add_convert_fusion
  50.9 1.9 collective-permute-start.4
  53.5 4.1 %collective-permute-start.3 = (bf16[24,3072]{1,0:T(8,128)(2,1)S(1)}, bf16[24,3072]{1,0:T(8,128)(2,1)S(1)}, u32[]{:S(2)}, u32[]{:S(2)}) collective-permute-start(bf16[24,3072]{1,0:T(8,128)(2,1)S(1)} %get-tuple-element.52), channel_id=1, source_target_pairs={{0,4},{1,29},{2,6},{3,31},{4,8},{5,1},{6,10},{7,3},{8,12},{9,5},{1... | collective-permute-start | bytes 442376 | tf_op jit(solution)/shard_map/ppermute | solution.py:379
  58.9 2.1 collective-permute-start.8
  60.9 8.2 %collective-permute-done.3 = bf16[24,3072]{1,0:T(8,128)(2,1)S(1)} collective-permute-done((bf16[24,3072]{1,0:T(8,128)(2,1)S(1)}, bf16[24,3072]{1,0:T(8,128)(2,1)S(1)}, u32[]{:S(2)}, u32[]{:S(2)}) %collective-permute-start.3) | collective-permute-done | bytes 147488 | tf_op jit(solution)/shard_map/ppermute | solution.py:379
  69.2 6.0 %collective-permute-start.5 = (bf16[24,3072]{1,0:T(8,128)(2,1)S(1)}, bf16[24,3072]{1,0:T(8,128)(2,1)S(1)}, u32[]{:S(2)}, u32[]{:S(2)}) collective-permute-start(bf16[24,3072]{1,0:T(8,128)(2,1)S(1)} %add_convert_fusion.7), channel_id=1, source_target_pairs={{0,4},{1,29},{2,6},{3,31},{4,8},{5,1},{6,10},{7,3},{8,12},{9,5},{1... | collective-permute-start | bytes 442376 | tf_op jit(solution)/shard_map/ppermute | solution.py:379
  75.4 1.9 collective-permute-start.9
  78.2 7.5 %collective-permute-start.6 = (bf16[24,3072]{1,0:T(8,128)(2,1)S(1)}, bf16[24,3072]{1,0:T(8,128)(2,1)S(1)}, u32[]{:S(2)}, u32[]{:S(2)}) collective-permute-start(bf16[24,3072]{1,0:T(8,128)(2,1)S(1)} %add_convert_fusion.6), channel_id=1, source_target_pairs={{0,4},{1,29},{2,6},{3,31},{4,8},{5,1},{6,10},{7,3},{8,12},{9,5},{1... | collective-permute-start | bytes 442376 | tf_op jit(solution)/shard_map/ppermute | solution.py:379
  85.8 1.9 collective-permute-start.10
  88.3 6.0 %collective-permute-start.7 = (bf16[24,3072]{1,0:T(8,128)(2,1)S(1)}, bf16[24,3072]{1,0:T(8,128)(2,1)S(1)}, u32[]{:S(2)}, u32[]{:S(2)}) collective-permute-start(bf16[24,3072]{1,0:T(8,128)(2,1)S(1)} %add_convert_fusion.5), channel_id=1, source_target_pairs={{0,4},{1,29},{2,6},{3,31},{4,8},{5,1},{6,10},{7,3},{8,12},{9,5},{1... | collective-permute-start | bytes 442376 | tf_op jit(solution)/shard_map/ppermute | solution.py:379
  94.4 3.5 %collective-permute-done.7 = bf16[24,3072]{1,0:T(8,128)(2,1)S(1)} collective-permute-done((bf16[24,3072]{1,0:T(8,128)(2,1)S(1)}, bf16[24,3072]{1,0:T(8,128)(2,1)S(1)}, u32[]{:S(2)}, u32[]{:S(2)}) %collective-permute-start.7) | collective-permute-done | bytes 147488 | tf_op jit(solution)/shard_map/ppermute | solution.py:379
  98.3 5.9 %collective-permute-start.11 = (bf16[24,3200]{1,0:T(8,128)(2,1)S(1)}, bf16[24,3200]{1,0:T(8,128)(2,1)S(1)}, u32[]{:S(2)}, u32[]{:S(2)}) collective-permute-start(bf16[24,3200]{1,0:T(8,128)(2,1)S(1)} %pad_maximum_fusion.1.refs_3_), channel_id=1, source_target_pairs={{0,4},{1,29},{2,6},{3,31},{4,8},{5,1},{6,10},{7,3},{8,12},{9,5},{1... | collective-permute-start | bytes 460808 | tf_op jit(solution)/shard_map/ppermute | solution.py:398
  104.2 1.9 collective-permute-start.15
  106.1 3.4 %collective-permute-done.11.refs_2_ = bf16[24,3200]{1,0:T(8,128)(2,1)S(1)} collective-permute-done((bf16[24,3200]{1,0:T(8,128)(2,1)S(1)}, bf16[24,3200]{1,0:T(8,128)(2,1)S(1)}, u32[]{:S(2)}, u32[]{:S(2)}) %collective-permute-start.11) | collective-permute-done | bytes 153632 | tf_op jit(solution)/shard_map/ppermute | solution.py:398
  109.6 5.9 %collective-permute-start.12 = (bf16[24,3200]{1,0:T(8,128)(2,1)S(1)}, bf16[24,3200]{1,0:T(8,128)(2,1)S(1)}, u32[]{:S(2)}, u32[]{:S(2)}) collective-permute-start(bf16[24,3200]{1,0:T(8,128)(2,1)S(1)} %collective-permute-done.11.refs_2_), channel_id=1, source_target_pairs={{0,4},{1,29},{2,6},{3,31},{4,8},{5,1},{6,10},{7,3},{8,12},{9,5},{1... | collective-permute-start | bytes 460808 | tf_op jit(solution)/shard_map/ppermute | solution.py:398
  115.5 1.9 collective-permute-start.16
  118.2 7.5 %collective-permute-start.13 = (bf16[24,3200]{1,0:T(8,128)(2,1)S(1)}, bf16[24,3200]{1,0:T(8,128)(2,1)S(1)}, u32[]{:S(2)}, u32[]{:S(2)}) collective-permute-start(bf16[24,3200]{1,0:T(8,128)(2,1)S(1)} %collective-permute-done.12.refs_1_), channel_id=1, source_target_pairs={{0,4},{1,29},{2,6},{3,31},{4,8},{5,1},{6,10},{7,3},{8,12},{9,5},{1... | collective-permute-start | bytes 460808 | tf_op jit(solution)/shard_map/ppermute | solution.py:398
  125.7 1.9 collective-permute-start.17
  128.0 5.9 %collective-permute-start.14 = (bf16[24,3200]{1,0:T(8,128)(2,1)S(1)}, bf16[24,3200]{1,0:T(8,128)(2,1)S(1)}, u32[]{:S(2)}, u32[]{:S(2)}) collective-permute-start(bf16[24,3200]{1,0:T(8,128)(2,1)S(1)} %collective-permute-done.13.refs_0_), channel_id=1, source_target_pairs={{0,4},{1,29},{2,6},{3,31},{4,8},{5,1},{6,10},{7,3},{8,12},{9,5},{1... | collective-permute-start | bytes 460808 | tf_op jit(solution)/shard_map/ppermute | solution.py:398
  133.9 1.5 collective-permute-done.17.refs_6_
  135.5 1.9 collective-permute-start.19
  137.4 2.2 collective-permute-done.14
  139.6 5.3 %collective-permute-start.18 = (bf16[24,3200]{1,0:T(8,128)(2,1)S(1)}, bf16[24,3200]{1,0:T(8,128)(2,1)S(1)}, u32[]{:S(2)}, u32[]{:S(2)}) collective-permute-start(bf16[24,3200]{1,0:T(8,128)(2,1)S(1)} %collective-permute-done.14), channel_id=1, source_target_pairs={{0,2},{1,31},{2,0},{3,5},{4,6},{5,3},{6,4},{7,9},{8,10},{9,7},{10,... | collective-permute-start | bytes 460808 | tf_op jit(solution)/shard_map/ppermute | solution.py:406
  145.0 4.4 %collective-permute-start.20 = (bf16[192,3200]{1,0:T(8,128)(2,1)S(1)}, bf16[192,3200]{1,0:T(8,128)(2,1)}, u32[]{:S(2)}, u32[]{:S(2)}) collective-permute-start(bf16[192,3200]{1,0:T(8,128)(2,1)S(1)} %pad_maximum_fusion.g0), channel_id=1, source_target_pairs={{0,1},{1,0},{2,3},{3,2},{4,5},{5,4},{6,7},{7,6},{8,9},{9,8},{10,11... | collective-permute-start | bytes 3686408 | tf_op jit(solution)/shard_map/ppermute | solution.py:408
  149.5 6.4 %collective-permute-done.18 = bf16[24,3200]{1,0:T(8,128)(2,1)S(1)} collective-permute-done((bf16[24,3200]{1,0:T(8,128)(2,1)S(1)}, bf16[24,3200]{1,0:T(8,128)(2,1)S(1)}, u32[]{:S(2)}, u32[]{:S(2)}) %collective-permute-start.18) | collective-permute-done | bytes 153632 | tf_op jit(solution)/shard_map/ppermute | solution.py:406
  156.0 5.4 %collective-permute-start.21 = (bf16[192,3200]{1,0:T(8,128)(2,1)S(1)}, bf16[192,3200]{1,0:T(8,128)(2,1)}, u32[]{:S(2)}, u32[]{:S(2)}) collective-permute-start(bf16[192,3200]{1,0:T(8,128)(2,1)S(1)} %constant_dynamic-update-slice_fusion.g1), channel_id=1, source_target_pairs={{0,1},{1,0},{2,3},{3,2},{4,5},{5,4},{6,7},{7,6},{8,9},{9,8},{10,11... | collective-permute-start | bytes 3686408 | tf_op jit(solution)/shard_map/ppermute | solution.py:410
  161.5 2.5 %collective-permute-done.21.g3 = bf16[192,3200]{1,0:T(8,128)(2,1)} collective-permute-done((bf16[192,3200]{1,0:T(8,128)(2,1)S(1)}, bf16[192,3200]{1,0:T(8,128)(2,1)}, u32[]{:S(2)}, u32[]{:S(2)}) %collective-permute-start.21) | collective-permute-done | bytes 1228832 | tf_op jit(solution)/shard_map/ppermute | solution.py:410
  163.9 7.7 %shard_map.148 = (bf16[16,232,128]{2,1,0:T(8,128)(2,1)}, f32[192,128]{1,0:T(8,128)}) custom-call(s32[2]{0:T(128)} %pad_add_fusion.pos, bf16[192,3200]{1,0:T(8,128)(2,1)} %copy-done, bf16[192,3200]{1,0:T(8,128)(2,1)} %copy-done.2, bf16[192,3200]{1,0:T(8,128)(2,1)} %collective-permute-done.20.g2, bf16[192,3200]{1,0:T(8,128)(2,1)} %collective-permute-done.21.g3, ...), custom_call_target="tpu_custom_call" | custom-call | tf_op jit(solution)/shard_map/pallas_call | solution.py:30
  171.7 3.6 %all-to-all-start.1 = ((bf16[16,232,128]{2,1,0:T(8,128)(2,1)}), bf16[16,232,128]{2,1,0:T(8,128)(2,1)S(1)}, u32[]{:S(2)}, u32[]{:S(2)}) async-start(bf16[16,232,128]{2,1,0:T(8,128)(2,1)} %get-tuple-element.40.after), calls=%async_computation.1 | async-start | bytes 1900544 | tf_op jit(solution)/shard_map/all_to_all | solution.py:419
  175.3 5.6 %shard_map.149 = (bf16[3,2,128,1024]{3,2,1,0:T(8,128)(2,1)}, f32[48,128]{1,0:T(8,128)}) custom-call(bf16[192,3200]{1,0:T(8,128)(2,1)} %copy-done, bf16[192,3200]{1,0:T(8,128)(2,1)} %copy-done.2, bf16[192,3200]{1,0:T(8,128)(2,1)} %collective-permute-done.20.g2, bf16[192,3200]{1,0:T(8,128)(2,1)} %collective-permute-done.21.g3, ...), custom_call_target="tpu_custom_call" | custom-call | tf_op jit(solution)/shard_map/pallas_call | solution.py:30
  181.6 2.3 %collective-permute-start.22 = (f32[24,128]{1,0:T(8,128)S(1)}, f32[24,128]{1,0:T(8,128)S(1)}, u32[]{:S(2)}, u32[]{:S(2)}) collective-permute-start(f32[24,128]{1,0:T(8,128)S(1)} %slice_select_fusion), channel_id=1, source_target_pairs={{0,1},{1,0},{2,3},{3,2},{4,5},{5,4},{6,7},{7,6},{8,9},{9,8},{10,11... | collective-permute-start | bytes 36872 | tf_op jit(solution)/shard_map/ppermute | solution.py:424
  185.4 1.9 collective-permute-start.23
  187.4 2.8 %collective-permute-done.23 = f32[12,128]{1,0:T(8,128)S(1)} collective-permute-done((f32[12,128]{1,0:T(8,128)S(1)}, f32[12,128]{1,0:T(8,128)S(1)}, u32[]{:S(2)}, u32[]{:S(2)}) %collective-permute-start.23) | collective-permute-done | bytes 6176 | tf_op jit(solution)/shard_map/ppermute | solution.py:426
  190.8 1.0 copy-done.1
  191.8 2.0 shard_map.150
  193.8 13.3 %all-to-all-start.2 = ((bf16[32,16,128]{2,1,0:T(8,128)(2,1)}), bf16[32,16,128]{2,1,0:T(8,128)(2,1)S(1)}, u32[]{:S(2)}, u32[]{:S(2)}) async-start(bf16[32,16,128]{2,1,0:T(8,128)(2,1)} %get-tuple-element.45.after), calls=%async_computation.2 | async-start | bytes 262144 | tf_op jit(solution)/shard_map/all_to_all | solution.py:432
  207.1 2.7 %shard_map.151 = (bf16[192,128]{1,0:T(8,128)(2,1)}, f32[2,192]{1,0:T(2,128)}) custom-call(bf16[16,232,128]{2,1,0:T(8,128)(2,1)} %copy-done.1, f32[192,128]{1,0:T(8,128)} %get-tuple-element.41.shared, s32[2,192]{1,0:T(2,128)} %bitcast.15, bf16[32,16,128]{2,1,0:T(8,128)(2,1)} %get-tuple-element.45.after), custom_call_target="tpu_custom_call" | custom-call | tf_op jit(solution)/shard_map/pallas_call | solution.py:30
  209.8 1.2 convert_bitcast_fusion
  211.1 11.9 %all-to-all-done.2.lines = bf16[32,16,128]{2,1,0:T(8,128)(2,1)S(1)} async-done(((bf16[32,16,128]{2,1,0:T(8,128)(2,1)}), bf16[32,16,128]{2,1,0:T(8,128)(2,1)S(1)}, u32[]{:S(2)}, u32[]{:S(2)}) %all-to-all-start.2) | async-done | bytes 131104 | tf_op jit(solution)/shard_map/all_to_all | solution.py:432
  223.6 1.6 shard_map.152
  (54 shorter events, 11.0 us)
Async XLA Ops:
  3.6 15.5 %all-to-all-start = ((bf16[16,40,256]{2,1,0:T(8,128)(2,1)}), bf16[16,40,256]{2,1,0:T(8,128)(2,1)S(1)}, u32[]{:S(2)}, u32[]{:S(2)}) async-start(bf16[16,40,256]{2,1,0:T(8,128)(2,1)} %bitcast.13), calls=%async_computation | async-start | bytes 655360 | tf_op jit(solution)/shard_map/all_to_all | solution.py:336
  19.1 0.7 copy-start.4
  29.9 8.5 %collective-permute-start.1 = (bf16[192,3072]{1,0:T(8,128)(2,1)}, bf16[192,3072]{1,0:T(8,128)(2,1)S(1)}, u32[]{:S(2)}, u32[]{:S(2)}) collective-permute-start(bf16[192,3072]{1,0:T(8,128)(2,1)} %get-tuple-element.34), channel_id=1, source_target_pairs={{0,1},{1,0},{2,3},{3,2},{4,5},{5,4},{6,7},{7,6},{8,9},{9,8},{10,11... | collective-permute-start | bytes 3538952 | tf_op jit(solution)/shard_map/ppermute | solution.py:357
  35.7 17.2 %collective-permute-start = (bf16[192,3072]{1,0:T(8,128)(2,1)}, bf16[192,3072]{1,0:T(8,128)(2,1)S(1)}, u32[]{:S(2)}, u32[]{:S(2)}) collective-permute-start(bf16[192,3072]{1,0:T(8,128)(2,1)} %get-tuple-element.32), channel_id=1, source_target_pairs={{0,1},{1,0},{2,3},{3,2},{4,5},{5,4},{6,7},{7,6},{8,9},{9,8},{10,11... | collective-permute-start | bytes 3538952 | tf_op jit(solution)/shard_map/ppermute | solution.py:358
  39.5 13.9 %copy-start.3 = (f32[192,3072]{1,0:T(8,128)S(1)}, f32[192,3072]{1,0:T(8,128)}, u32[]{:S(2)}) copy-start(f32[192,3072]{1,0:T(8,128)} %get-tuple-element.31) | copy-start | bytes 7077892
  39.5 13.9 %collective-permute-start.2 = (bf16[48,3072]{1,0:T(8,128)(2,1)S(1)}, bf16[48,3072]{1,0:T(8,128)(2,1)S(1)}, u32[]{:S(2)}, u32[]{:S(2)}) collective-permute-start(bf16[48,3072]{1,0:T(8,128)(2,1)S(1)} %add_convert_fusion.1), channel_id=1, source_target_pairs={{0,2},{1,31},{2,0},{3,5},{4,6},{5,3},{6,4},{7,9},{8,10},{9,7},{10,... | collective-permute-start | bytes 884744 | tf_op jit(solution)/shard_map/ppermute | solution.py:362
  50.9 18.2 %collective-permute-start.4 = (bf16[144,3072]{1,0:T(8,128)(2,1)S(1)}, bf16[144,3072]{1,0:T(8,128)(2,1)S(1)}, u32[]{:S(2)}, u32[]{:S(2)}) collective-permute-start(bf16[144,3072]{1,0:T(8,128)(2,1)S(1)} %add_convert_fusion), channel_id=1, source_target_pairs={{0,2},{1,31},{2,0},{3,5},{4,6},{5,3},{6,4},{7,9},{8,10},{9,7},{10,... | collective-permute-start | bytes 2654216 | tf_op jit(solution)/shard_map/ppermute | solution.py:363
  53.5 15.7 %collective-permute-start.3 = (bf16[24,3072]{1,0:T(8,128)(2,1)S(1)}, bf16[24,3072]{1,0:T(8,128)(2,1)S(1)}, u32[]{:S(2)}, u32[]{:S(2)}) collective-permute-start(bf16[24,3072]{1,0:T(8,128)(2,1)S(1)} %get-tuple-element.52), channel_id=1, source_target_pairs={{0,4},{1,29},{2,6},{3,31},{4,8},{5,1},{6,10},{7,3},{8,12},{9,5},{1... | collective-permute-start | bytes 442376 | tf_op jit(solution)/shard_map/ppermute | solution.py:379
  58.9 16.5 %collective-permute-start.8 = (bf16[24,3072]{1,0:T(8,128)(2,1)S(1)}, bf16[24,3072]{1,0:T(8,128)(2,1)S(1)}, u32[]{:S(2)}, u32[]{:S(2)}) collective-permute-start(bf16[24,3072]{1,0:T(8,128)(2,1)S(1)} %get-tuple-element.53), channel_id=1, source_target_pairs={{4,0},{29,1},{6,2},{31,3},{8,4},{1,5},{10,6},{3,7},{12,8},{5,9},{1... | collective-permute-start | bytes 442376 | tf_op jit(solution)/shard_map/ppermute | solution.py:383
  69.2 8.8 %collective-permute-start.5 = (bf16[24,3072]{1,0:T(8,128)(2,1)S(1)}, bf16[24,3072]{1,0:T(8,128)(2,1)S(1)}, u32[]{:S(2)}, u32[]{:S(2)}) collective-permute-start(bf16[24,3072]{1,0:T(8,128)(2,1)S(1)} %add_convert_fusion.7), channel_id=1, source_target_pairs={{0,4},{1,29},{2,6},{3,31},{4,8},{5,1},{6,10},{7,3},{8,12},{9,5},{1... | collective-permute-start | bytes 442376 | tf_op jit(solution)/shard_map/ppermute | solution.py:379
  75.4 10.3 %collective-permute-start.9 = (bf16[24,3072]{1,0:T(8,128)(2,1)S(1)}, bf16[24,3072]{1,0:T(8,128)(2,1)S(1)}, u32[]{:S(2)}, u32[]{:S(2)}) collective-permute-start(bf16[24,3072]{1,0:T(8,128)(2,1)S(1)} %add_convert_fusion.3), channel_id=1, source_target_pairs={{4,0},{29,1},{6,2},{31,3},{8,4},{1,5},{10,6},{3,7},{12,8},{5,9},{1... | collective-permute-start | bytes 442376 | tf_op jit(solution)/shard_map/ppermute | solution.py:383
  78.2 10.1 %collective-permute-start.6 = (bf16[24,3072]{1,0:T(8,128)(2,1)S(1)}, bf16[24,3072]{1,0:T(8,128)(2,1)S(1)}, u32[]{:S(2)}, u32[]{:S(2)}) collective-permute-start(bf16[24,3072]{1,0:T(8,128)(2,1)S(1)} %add_convert_fusion.6), channel_id=1, source_target_pairs={{0,4},{1,29},{2,6},{3,31},{4,8},{5,1},{6,10},{7,3},{8,12},{9,5},{1... | collective-permute-start | bytes 442376 | tf_op jit(solution)/shard_map/ppermute | solution.py:379
  85.8 8.6 %collective-permute-start.10 = (bf16[24,3072]{1,0:T(8,128)(2,1)S(1)}, bf16[24,3072]{1,0:T(8,128)(2,1)S(1)}, u32[]{:S(2)}, u32[]{:S(2)}) collective-permute-start(bf16[24,3072]{1,0:T(8,128)(2,1)S(1)} %add_convert_fusion.2), channel_id=1, source_target_pairs={{4,0},{29,1},{6,2},{31,3},{8,4},{1,5},{10,6},{3,7},{12,8},{5,9},{1... | collective-permute-start | bytes 442376 | tf_op jit(solution)/shard_map/ppermute | solution.py:383
  88.3 9.6 %collective-permute-start.7 = (bf16[24,3072]{1,0:T(8,128)(2,1)S(1)}, bf16[24,3072]{1,0:T(8,128)(2,1)S(1)}, u32[]{:S(2)}, u32[]{:S(2)}) collective-permute-start(bf16[24,3072]{1,0:T(8,128)(2,1)S(1)} %add_convert_fusion.5), channel_id=1, source_target_pairs={{0,4},{1,29},{2,6},{3,31},{4,8},{5,1},{6,10},{7,3},{8,12},{9,5},{1... | collective-permute-start | bytes 442376 | tf_op jit(solution)/shard_map/ppermute | solution.py:379
  98.3 11.3 %collective-permute-start.11 = (bf16[24,3200]{1,0:T(8,128)(2,1)S(1)}, bf16[24,3200]{1,0:T(8,128)(2,1)S(1)}, u32[]{:S(2)}, u32[]{:S(2)}) collective-permute-start(bf16[24,3200]{1,0:T(8,128)(2,1)S(1)} %pad_maximum_fusion.1.refs_3_), channel_id=1, source_target_pairs={{0,4},{1,29},{2,6},{3,31},{4,8},{5,1},{6,10},{7,3},{8,12},{9,5},{1... | collective-permute-start | bytes 460808 | tf_op jit(solution)/shard_map/ppermute | solution.py:398
  104.2 11.3 %collective-permute-start.15 = (bf16[24,3200]{1,0:T(8,128)(2,1)S(1)}, bf16[24,3200]{1,0:T(8,128)(2,1)S(1)}, u32[]{:S(2)}, u32[]{:S(2)}) collective-permute-start(bf16[24,3200]{1,0:T(8,128)(2,1)S(1)} %pad_maximum_fusion.1.refs_3_), channel_id=1, source_target_pairs={{4,0},{29,1},{6,2},{31,3},{8,4},{1,5},{10,6},{3,7},{12,8},{5,9},{1... | collective-permute-start | bytes 460808 | tf_op jit(solution)/shard_map/ppermute | solution.py:401
  109.6 8.6 %collective-permute-start.12 = (bf16[24,3200]{1,0:T(8,128)(2,1)S(1)}, bf16[24,3200]{1,0:T(8,128)(2,1)S(1)}, u32[]{:S(2)}, u32[]{:S(2)}) collective-permute-start(bf16[24,3200]{1,0:T(8,128)(2,1)S(1)} %collective-permute-done.11.refs_2_), channel_id=1, source_target_pairs={{0,4},{1,29},{2,6},{3,31},{4,8},{5,1},{6,10},{7,3},{8,12},{9,5},{1... | collective-permute-start | bytes 460808 | tf_op jit(solution)/shard_map/ppermute | solution.py:398
  115.5 10.2 %collective-permute-start.16 = (bf16[24,3200]{1,0:T(8,128)(2,1)S(1)}, bf16[24,3200]{1,0:T(8,128)(2,1)S(1)}, u32[]{:S(2)}, u32[]{:S(2)}) collective-permute-start(bf16[24,3200]{1,0:T(8,128)(2,1)S(1)} %collective-permute-done.15.refs_4_), channel_id=1, source_target_pairs={{4,0},{29,1},{6,2},{31,3},{8,4},{1,5},{10,6},{3,7},{12,8},{5,9},{1... | collective-permute-start | bytes 460808 | tf_op jit(solution)/shard_map/ppermute | solution.py:401
  118.2 9.8 %collective-permute-start.13 = (bf16[24,3200]{1,0:T(8,128)(2,1)S(1)}, bf16[24,3200]{1,0:T(8,128)(2,1)S(1)}, u32[]{:S(2)}, u32[]{:S(2)}) collective-permute-start(bf16[24,3200]{1,0:T(8,128)(2,1)S(1)} %collective-permute-done.12.refs_1_), channel_id=1, source_target_pairs={{0,4},{1,29},{2,6},{3,31},{4,8},{5,1},{6,10},{7,3},{8,12},{9,5},{1... | collective-permute-start | bytes 460808 | tf_op jit(solution)/shard_map/ppermute | solution.py:398
  125.7 9.7 %collective-permute-start.17 = (bf16[24,3200]{1,0:T(8,128)(2,1)S(1)}, bf16[24,3200]{1,0:T(8,128)(2,1)S(1)}, u32[]{:S(2)}, u32[]{:S(2)}) collective-permute-start(bf16[24,3200]{1,0:T(8,128)(2,1)S(1)} %collective-permute-done.16.refs_5_), channel_id=1, source_target_pairs={{4,0},{29,1},{6,2},{31,3},{8,4},{1,5},{10,6},{3,7},{12,8},{5,9},{1... | collective-permute-start | bytes 460808 | tf_op jit(solution)/shard_map/ppermute | solution.py:401
  128.0 11.6 %collective-permute-start.14 = (bf16[24,3200]{1,0:T(8,128)(2,1)S(1)}, bf16[24,3200]{1,0:T(8,128)(2,1)S(1)}, u32[]{:S(2)}, u32[]{:S(2)}) collective-permute-start(bf16[24,3200]{1,0:T(8,128)(2,1)S(1)} %collective-permute-done.13.refs_0_), channel_id=1, source_target_pairs={{0,4},{1,29},{2,6},{3,31},{4,8},{5,1},{6,10},{7,3},{8,12},{9,5},{1... | collective-permute-start | bytes 460808 | tf_op jit(solution)/shard_map/ppermute | solution.py:398
  135.5 20.3 %collective-permute-start.19 = (bf16[168,3200]{1,0:T(8,128)(2,1)S(1)}, bf16[168,3200]{1,0:T(8,128)(2,1)S(1)}, u32[]{:S(2)}, u32[]{:S(2)}) collective-permute-start(bf16[168,3200]{1,0:T(8,128)(2,1)S(1)} %shard_map.147), channel_id=1, source_target_pairs={{0,2},{1,31},{2,0},{3,5},{4,6},{5,3},{6,4},{7,9},{8,10},{9,7},{10,... | collective-permute-start | bytes 3225608 | tf_op jit(solution)/shard_map/ppermute | solution.py:405
  139.6 16.2 %collective-permute-start.18 = (bf16[24,3200]{1,0:T(8,128)(2,1)S(1)}, bf16[24,3200]{1,0:T(8,128)(2,1)S(1)}, u32[]{:S(2)}, u32[]{:S(2)}) collective-permute-start(bf16[24,3200]{1,0:T(8,128)(2,1)S(1)} %collective-permute-done.14), channel_id=1, source_target_pairs={{0,2},{1,31},{2,0},{3,5},{4,6},{5,3},{6,4},{7,9},{8,10},{9,7},{10,... | collective-permute-start | bytes 460808 | tf_op jit(solution)/shard_map/ppermute | solution.py:406
  145.0 11.0 %copy-start = (bf16[192,3200]{1,0:T(8,128)(2,1)}, bf16[192,3200]{1,0:T(8,128)(2,1)S(1)}, u32[]{:S(2)}) copy-start(bf16[192,3200]{1,0:T(8,128)(2,1)S(1)} %pad_maximum_fusion.g0) | copy-start | bytes 3686404
  145.0 16.4 %collective-permute-start.20 = (bf16[192,3200]{1,0:T(8,128)(2,1)S(1)}, bf16[192,3200]{1,0:T(8,128)(2,1)}, u32[]{:S(2)}, u32[]{:S(2)}) collective-permute-start(bf16[192,3200]{1,0:T(8,128)(2,1)S(1)} %pad_maximum_fusion.g0), channel_id=1, source_target_pairs={{0,1},{1,0},{2,3},{3,2},{4,5},{5,4},{6,7},{7,6},{8,9},{9,8},{10,11... | collective-permute-start | bytes 3686408 | tf_op jit(solution)/shard_map/ppermute | solution.py:408
  156.0 7.9 %copy-start.2 = (bf16[192,3200]{1,0:T(8,128)(2,1)}, bf16[192,3200]{1,0:T(8,128)(2,1)S(1)}, u32[]{:S(2)}) copy-start(bf16[192,3200]{1,0:T(8,128)(2,1)S(1)} %constant_dynamic-update-slice_fusion.g1) | copy-start | bytes 3686404
  156.0 7.9 %collective-permute-start.21 = (bf16[192,3200]{1,0:T(8,128)(2,1)S(1)}, bf16[192,3200]{1,0:T(8,128)(2,1)}, u32[]{:S(2)}, u32[]{:S(2)}) collective-permute-start(bf16[192,3200]{1,0:T(8,128)(2,1)S(1)} %constant_dynamic-update-slice_fusion.g1), channel_id=1, source_target_pairs={{0,1},{1,0},{2,3},{3,2},{4,5},{5,4},{6,7},{7,6},{8,9},{9,8},{10,11... | collective-permute-start | bytes 3686408 | tf_op jit(solution)/shard_map/ppermute | solution.py:410
  171.7 19.1 %all-to-all-start.1 = ((bf16[16,232,128]{2,1,0:T(8,128)(2,1)}), bf16[16,232,128]{2,1,0:T(8,128)(2,1)S(1)}, u32[]{:S(2)}, u32[]{:S(2)}) async-start(bf16[16,232,128]{2,1,0:T(8,128)(2,1)} %get-tuple-element.40.after), calls=%async_computation.1 | async-start | bytes 1900544 | tf_op jit(solution)/shard_map/all_to_all | solution.py:419
  181.6 3.1 %collective-permute-start.22 = (f32[24,128]{1,0:T(8,128)S(1)}, f32[24,128]{1,0:T(8,128)S(1)}, u32[]{:S(2)}, u32[]{:S(2)}) collective-permute-start(f32[24,128]{1,0:T(8,128)S(1)} %slice_select_fusion), channel_id=1, source_target_pairs={{0,1},{1,0},{2,3},{3,2},{4,5},{5,4},{6,7},{7,6},{8,9},{9,8},{10,11... | collective-permute-start | bytes 36872 | tf_op jit(solution)/shard_map/ppermute | solution.py:424
  185.4 4.7 %collective-permute-start.23 = (f32[12,128]{1,0:T(8,128)S(1)}, f32[12,128]{1,0:T(8,128)S(1)}, u32[]{:S(2)}, u32[]{:S(2)}) collective-permute-start(f32[12,128]{1,0:T(8,128)S(1)} %slice_select_fusion.1), channel_id=1, source_target_pairs={{0,2},{1,3},{2,0},{3,1},{4,6},{5,7},{6,4},{7,5},{8,10},{9,11},{10,... | collective-permute-start | bytes 18440 | tf_op jit(solution)/shard_map/ppermute | solution.py:426
  190.8 1.0 copy-start.1
  193.8 29.2 %all-to-all-start.2 = ((bf16[32,16,128]{2,1,0:T(8,128)(2,1)}), bf16[32,16,128]{2,1,0:T(8,128)(2,1)S(1)}, u32[]{:S(2)}, u32[]{:S(2)}) async-start(bf16[32,16,128]{2,1,0:T(8,128)(2,1)} %get-tuple-element.45.after), calls=%async_computation.2 | async-start | bytes 262144 | tf_op jit(solution)/shard_map/all_to_all | solution.py:432
  223.0 0.7 copy-start.5

commit v7 on v6

--- a/solution.py
+++ b/solution.py
@@ -151,18 +151,20 @@
     lines[...] = jnp.broadcast_to(jnp.concatenate(parts, 0).astype(BF)[None], lines.shape)
 
 
-def finish_norms(scale, lines, e_norm, s_norm):
+def finish_norms(scale, pos, lines, other, e_norm, s_norm):
     n, block, width = lines.shape
     _, le, hidden = e_norm.shape
     cols = s_norm.shape[1]
     q = 3 * le * hidden // (4 * width)
-    rows = []
-    for c in range(2):
+    c = pos[1]
+    sums = []
+    for ref in (lines, other):
         for b in range(2):
-            acc = lines[2 * b + c].astype(F32)
-            for d in range(4 + 2 * b + c, n, 4):
-                acc = acc + lines[d].astype(F32)
-            rows.append(acc)
+            acc = ref[b].astype(F32)
+            for d in range(2 + b, n, 2):
+                acc = acc + ref[d].astype(F32)
+            sums.append(acc)
+    rows = [jnp.where(c == 0, sums[k], sums[(k + 2) % 4]) for k in range(4)]
     whole = rows[0] + rows[1] + rows[2] + rows[3]
     rows = [r[i : i + 1] * scale for r in rows for i in range(q)]
     per = hidden // width
@@ -178,12 +180,16 @@
 def project(sizes, pos, got, both, *refs):
     weights, results = refs[:6], refs[6:10]
     xt_ref, gt_ref, xs_ref, gs_ref = refs[10:14]
-    held, made = refs[14:20], refs[20:24]
-    sem_in, sem_out = refs[24], refs[25]
-    le, width, hidden = held[0].shape
-    loads = [pltpu.make_async_copy(weights[k], held[k], sem_in.at[k]) for k in range(6)]
-    for load in loads:
-        load.start()
+    held, made = refs[14:17], refs[17:21]
+    sem_in, sem_out = refs[21], refs[22]
+    le, width, hidden = weights[0].shape
+    loads = []
+    for t in range(3):
+        for e in range(le + 1):
+            src = weights[t].at[e] if e < le else weights[3 + t]
+            to = held[t].at[e * width : (e + 1) * width, :]
+            loads.append(pltpu.make_async_copy(src, to, sem_in.at[t, e]))
+            loads[-1].start()
     nb, rows = got.shape[0], both.shape[0]
     sec = made[0].shape[0]
     half = 2 * sec
@@ -193,14 +199,14 @@
     mine = mm(one_hot(src, cols), got[...])
     mine = mine + mm(one_hot(src - nb, lax.broadcasted_iota(jnp.int32, (2 * half, rows), 1)), both[...])
     part = [jnp.where(kd == e, mine, 0.0).astype(BF) for e in range(le + 1)]
-    x = jnp.concatenate([p[:, :width] for p in part[:le]], 1)
-    g = jnp.concatenate([p[:, width:] for p in part[:le]], 1)
+    x = jnp.concatenate([p[:, :width] for p in part], 1)
+    g = jnp.concatenate([p[:, width:] for p in part], 1)
     stores = []
-    for t, (xe, xs) in enumerate(((x, part[le][:, :width]), (x, part[le][:, :width]), (g, part[le][:, width:]))):
+    for t, lhs in enumerate((x, x, g)):
         cut = slice(t * hidden, (t + 1) * hidden)
-        loads[t].wait()
-        loads[3 + t].wait()
-        p = mm(xe, held[t][...].reshape(le * width, hidden)) + mm(xs, held[3 + t][...])
+        for load in loads[t * (le + 1) : (t + 1) * (le + 1)]:
+            load.wait()
+        p = mm(lhs, held[t][...])
         for k in (3, 1, 2, 0):
             at = (0, sec, half, half + sec)[k]
             made[k][:, cut] = p[at : at + sec].astype(made[k].dtype)
@@ -350,24 +356,24 @@
         out_shape=[jax.ShapeDtypeStruct(a, d) for a, d in big + turned],
         in_specs=[pl.BlockSpec(memory_space=pltpu.SMEM), VM, VM] + [anywhere] * 6,
         out_specs=[anywhere] * 4 + [VM] * 4,
-        scratch_shapes=[pltpu.VMEM(w.shape, BF) for w in weights]
+        scratch_shapes=[pltpu.VMEM(((le + 1) * width, hidden), BF)] * 3
         + [pltpu.VMEM(a, d) for a, d in big]
-        + [pltpu.SemaphoreType.DMA((6,)), pltpu.SemaphoreType.DMA((3, 4))],
+        + [pltpu.SemaphoreType.DMA((3, le + 1)), pltpu.SemaphoreType.DMA((3, 4))],
     )(pos, got.reshape(n_ep * bl, 2 * width), both, *weights)
     oth_s = lax.ppermute(out_s, "tp", swap)
     oth_k = lax.ppermute(out_k, "tp", swap)
-    cut = 2 * piece
+    cut = (hops + 1) * piece
     to_a = (own_s[:cut] + oth_s[:cut].astype(F32)).astype(BF)
     to_b = (own_s[cut:] + oth_s[cut:].astype(F32)).astype(BF)
     par_a = lax.ppermute(to_a, "tp", pair)
     par_b = lax.ppermute(to_b, "tp", pair)
-    left_rows = slice(cut, hops * piece)
-    on_left = lax.optimization_barrier((own_k[left_rows], oth_k[left_rows], par_b[: hops * piece - cut]))
+    left_rows = slice(2 * piece, hops * piece)
+    on_left = lax.optimization_barrier((own_k[left_rows], oth_k[left_rows], par_a[left_rows]))
 
     def at(m):
         p = (m - hops) % members
         rows_p = slice(p * piece, (p + 1) * piece)
-        par = par_a[rows_p] if p < 2 else par_b[p * piece - cut : (p + 1) * piece - cut]
+        par = par_a[rows_p] if p <= hops else par_b[p * piece - cut : (p + 1) * piece - cut]
         own, oth = own_k, oth_k
         if 1 < p < hops:
             (own, oth, par), rows_p = on_left, slice((p - 2) * piece, (p - 1) * piece)
@@ -427,18 +433,20 @@
     e_sq = jnp.where(z % 2 == 0, e_sq[0], e_sq[1]) + other_sq
     n_lines = (e_sq.shape[0] + -(-3 * cols // width) + 15) // 16 * 16
     shared, lines = call(
-        gather_norms, [((3, cols, width), F32), ((n_tp, n_lines, width), BF)], home, e_sq
-    )
-    got_lines = lax.all_to_all(lines, "tp", 0, 0, tiled=True)
+        gather_norms, [((3, cols, width), F32), ((nz, n_lines, width), BF)], home, e_sq
+    )
+    same_core = [[2 * i + k for i in range(nz)] for k in range(2)]
+    got_lines = lax.all_to_all(lines, "tp", 0, 0, axis_index_groups=same_core, tiled=True)
     token_grad, gate_grad = call(
         functools.partial(collect, geo),
         [((rows, width), BF), ((top, rows), F32)],
         home, shared_part, routes.T, lines, rest=1,
     )
+    other_lines = lax.ppermute(got_lines, "tp", swap)
     e_norm, s_norm = call(
         functools.partial(finish_norms, 1.0 / (width * n_tp)),
         [((3, le, hidden), F32), ((3, cols), F32)],
-        got_lines,
+        pos, got_lines, other_lines, smem=1,
     )
     return token_grad, gate_grad.astype(BF).T, stack, jnp.swapaxes(shared, 1, 2), e_norm, s_norm
 

time: 227 us -> 230 us (1.013)
  other arithmetic: 7.51 us -> 10.9 us
    ppermute x6, waiting for transfers between devices: 1.51 us -> 14.6 us  [body(): left = lax.ppermute(left, 'tp', bwd)]
    ppermute x8, waiting for transfers between devices: 19.8 us -> 6.95 us  [body(): right = lax.ppermute(right, 'tp', fwd)]
    ppermute x8, starting transfers between devices: 48.9 us -> 37.9 us  [body(): right = lax.ppermute(right, 'tp', fwd)]
    ppermute x1, waiting for transfers between devices: 0.5 us -> 5.85 us  [body(): par_a = lax.ppermute(to_a, 'tp', pair)]
    ppermute x0 -> x1, starting transfers between devices: none -> 5.13 us  [body(): other_lines = lax.ppermute(got_lines, 'tp', swap)]
    ppermute x1, starting transfers between devices: 4.44 us -> 8.59 us  [body(): kept_x = lax.ppermute(kept, 'tp', swap)]
    all_to_all x1, starting transfers between devices: 13.3 us -> 9.51 us  [body(): lax.all_to_all(lines, 'tp', 0, 0, axis_index_groups=same_core, tiled=True)]
    ppermute x6, starting transfers between devices: 11.7 us -> 15 us  [body(): left = lax.ppermute(left, 'tp', bwd)]
  transfers between devices with their start and end apart: 27 -> 28, of which waited for: 18 -> 19; matrix products, arithmetic and copies ran while one was open for 4% -> 5% of each run, Pallas kernels for 4% -> 4%
where the time goes in v7:
time: 230 us; the launch traced here: 228 us
  starting transfers between devices  128 us (56%)
  waiting for transfers between devices  52.4 us (23%)
  Pallas kernels  30.8 us (13%)
  other arithmetic  10.9 us (5%)
  local copies, waits for them, and re-layouts  4.46 us (2%)
    ppermute x8, starting transfers between devices, body(): right = lax.ppermute(right, 'tp', fwd)  37.9 us
    pallas_call x7, Pallas kernels, call(): pl.pallas_call(kernel, out_shape=[jax.ShapeDtypeStruct(s, d) for s, d in...  22.7 us
    ppermute x6, starting transfers between devices, body(): left = lax.ppermute(left, 'tp', bwd)  15 us
    ppermute x6, waiting for transfers between devices, body(): left = lax.ppermute(left, 'tp', bwd)  14.6 us
    ppermute x1, starting transfers between devices, body(): par_a = lax.ppermute(to_a, 'tp', pair)  9.64 us
    all_to_all x1, starting transfers between devices, body(): lax.all_to_all(lines, 'tp', 0, 0, axis_index_groups=same_core, tiled=True)  9.51 us
    all_to_all x1, waiting for transfers between devices, body(): lax.all_to_all(lines, 'tp', 0, 0, axis_index_groups=same_core, tiled=True)  8.85 us
    ppermute x1, starting transfers between devices, body(): kept_x = lax.ppermute(kept, 'tp', swap)  8.59 us
  transfers between devices with their start and end apart: 28, of which 19 were waited for; matrix products, arithmetic and copies ran while one was open for 5% of the time, Pallas kernels for 4%

profile of v7, /device:TPU:1, one launch (start us, length us, event | category | flops | bytes accessed | tf_op | source)
XLA Modules:
  0.0 228.2 jit_solution(5079974994347694920)
XLA Ops:
  0.6 3.0 %shard_map.145 = (bf16[640,256]{1,0:T(8,128)(2,1)}, bf16[192,256]{1,0:T(8,128)(2,1)}) custom-call(bf16[192,128]{1,0:T(8,128)(2,1)} %tokens.1, bf16[192,128]{1,0:T(8,128)(2,1)} %cotangent.1, s32[2,192]{1,0:T(2,128)} %bitcast.14, bf16[2,192]{1,0:T(2,128)(2,1)} %bitcast.16), custom_call_target="tpu_custom_call" | custom-call | tf_op jit(solution)/shard_map/pallas_call | solution.py:30
  3.6 7.6 %all-to-all-start = ((bf16[16,40,256]{2,1,0:T(8,128)(2,1)}), bf16[16,40,256]{2,1,0:T(8,128)(2,1)S(1)}, u32[]{:S(2)}, u32[]{:S(2)}) async-start(bf16[16,40,256]{2,1,0:T(8,128)(2,1)} %bitcast.13), calls=%async_computation | async-start | bytes 655360 | tf_op jit(solution)/shard_map/all_to_all | solution.py:342
  11.8 7.3 %all-to-all-done = bf16[16,40,256]{2,1,0:T(8,128)(2,1)S(1)} async-done(((bf16[16,40,256]{2,1,0:T(8,128)(2,1)}), bf16[16,40,256]{2,1,0:T(8,128)(2,1)S(1)}, u32[]{:S(2)}, u32[]{:S(2)}) %all-to-all-start) | async-done | bytes 327712 | tf_op jit(solution)/shard_map/all_to_all | solution.py:342
  19.9 8.1 %shard_map.146 = (f32[192,3072]{1,0:T(8,128)}, f32[192,3072]{1,0:T(8,128)}, bf16[192,3072]{1,0:T(8,128)(2,1)}, bf16[192,3072]{1,0:T(8,128)(2,1)}, bf16[256,768]{...) custom-call(s32[2]{0:T(128)} %pad_add_fusion.pos, ...), custom_call_target="tpu_custom_call" | custom-call | tf_op jit(solution)/shard_map/pallas_call | solution.py:354
  28.0 5.8 %collective-permute-start.1 = (bf16[192,3072]{1,0:T(8,128)(2,1)}, bf16[192,3072]{1,0:T(8,128)(2,1)S(1)}, u32[]{:S(2)}, u32[]{:S(2)}) collective-permute-start(bf16[192,3072]{1,0:T(8,128)(2,1)} %get-tuple-element.34), channel_id=1, source_target_pairs={{0,1},{1,0},{2,3},{3,2},{4,5},{5,4},{6,7},{7,6},{8,9},{9,8},{10,11... | collective-permute-start | bytes 3538952 | tf_op jit(solution)/shard_map/ppermute | solution.py:363
  33.9 1.9 collective-permute-start
  36.5 2.9 %add_convert_fusion = bf16[120,3072]{1,0:T(8,128)(2,1)} fusion(f32[192,3072]{1,0:T(8,128)} %get-tuple-element.33, bf16[192,3072]{1,0:T(8,128)(2,1)S(1)} %collective-permute-done.1), kind=kLoop, calls=%fused_computation | loop fusion | flops 1105920 | bytes 2949120 | tf_op jit(solution)/shard_map/convert_element_type | solution.py:366
  39.4 9.6 %collective-permute-start.2 = (bf16[120,3072]{1,0:T(8,128)(2,1)}, bf16[120,3072]{1,0:T(8,128)(2,1)}, u32[]{:S(2)}, u32[]{:S(2)}) collective-permute-start(bf16[120,3072]{1,0:T(8,128)(2,1)} %add_convert_fusion), channel_id=1, source_target_pairs={{0,2},{1,31},{2,0},{3,5},{4,6},{5,3},{6,4},{7,9},{8,10},{9,7},{10,... | collective-permute-start | bytes 2211848 | tf_op jit(solution)/shard_map/ppermute | solution.py:368
  49.1 1.4 add_convert_fusion.1
  50.4 1.9 collective-permute-start.4
  52.4 5.8 %collective-permute-done.2 = bf16[120,3072]{1,0:T(8,128)(2,1)} collective-permute-done((bf16[120,3072]{1,0:T(8,128)(2,1)}, bf16[120,3072]{1,0:T(8,128)(2,1)}, u32[]{:S(2)}, u32[]{:S(2)}) %collective-permute-start.2) | collective-permute-done | bytes 737312 | tf_op jit(solution)/shard_map/ppermute | solution.py:368
  59.3 4.1 %collective-permute-start.3 = (bf16[24,3072]{1,0:T(8,128)(2,1)S(1)}, bf16[24,3072]{1,0:T(8,128)(2,1)S(1)}, u32[]{:S(2)}, u32[]{:S(2)}) collective-permute-start(bf16[24,3072]{1,0:T(8,128)(2,1)S(1)} %get-tuple-element.52), channel_id=1, source_target_pairs={{0,4},{1,29},{2,6},{3,31},{4,8},{5,1},{6,10},{7,3},{8,12},{9,5},{1... | collective-permute-start | bytes 442376 | tf_op jit(solution)/shard_map/ppermute | solution.py:385
  64.7 2.1 collective-permute-start.8
  67.8 5.3 %collective-permute-start.5 = (bf16[24,3072]{1,0:T(8,128)(2,1)S(1)}, bf16[24,3072]{1,0:T(8,128)(2,1)S(1)}, u32[]{:S(2)}, u32[]{:S(2)}) collective-permute-start(bf16[24,3072]{1,0:T(8,128)(2,1)S(1)} %add_convert_fusion.7), channel_id=1, source_target_pairs={{0,4},{1,29},{2,6},{3,31},{4,8},{5,1},{6,10},{7,3},{8,12},{9,5},{1... | collective-permute-start | bytes 442376 | tf_op jit(solution)/shard_map/ppermute | solution.py:385
  73.8 1.9 collective-permute-start.9
  75.9 5.4 %collective-permute-start.6 = (bf16[24,3072]{1,0:T(8,128)(2,1)S(1)}, bf16[24,3072]{1,0:T(8,128)(2,1)S(1)}, u32[]{:S(2)}, u32[]{:S(2)}) collective-permute-start(bf16[24,3072]{1,0:T(8,128)(2,1)S(1)} %add_convert_fusion.6), channel_id=1, source_target_pairs={{0,4},{1,29},{2,6},{3,31},{4,8},{5,1},{6,10},{7,3},{8,12},{9,5},{1... | collective-permute-start | bytes 442376 | tf_op jit(solution)/shard_map/ppermute | solution.py:385
  81.3 1.7 collective-permute-done.9
  83.1 1.9 collective-permute-start.10
  85.4 5.9 %collective-permute-start.7 = (bf16[24,3072]{1,0:T(8,128)(2,1)S(1)}, bf16[24,3072]{1,0:T(8,128)(2,1)S(1)}, u32[]{:S(2)}, u32[]{:S(2)}) collective-permute-start(bf16[24,3072]{1,0:T(8,128)(2,1)S(1)} %add_convert_fusion.5), channel_id=1, source_target_pairs={{0,4},{1,29},{2,6},{3,31},{4,8},{5,1},{6,10},{7,3},{8,12},{9,5},{1... | collective-permute-start | bytes 442376 | tf_op jit(solution)/shard_map/ppermute | solution.py:385
  91.3 2.2 collective-permute-done.10
  93.5 4.9 %collective-permute-done.7 = bf16[24,3072]{1,0:T(8,128)(2,1)S(1)} collective-permute-done((bf16[24,3072]{1,0:T(8,128)(2,1)S(1)}, bf16[24,3072]{1,0:T(8,128)(2,1)S(1)}, u32[]{:S(2)}, u32[]{:S(2)}) %collective-permute-start.7) | collective-permute-done | bytes 147488 | tf_op jit(solution)/shard_map/ppermute | solution.py:385
  99.6 3.6 %collective-permute-start.11 = (bf16[24,3200]{1,0:T(8,128)(2,1)S(1)}, bf16[24,3200]{1,0:T(8,128)(2,1)S(1)}, u32[]{:S(2)}, u32[]{:S(2)}) collective-permute-start(bf16[24,3200]{1,0:T(8,128)(2,1)S(1)} %pad_maximum_fusion.1.refs_3_), channel_id=1, source_target_pairs={{0,4},{1,29},{2,6},{3,31},{4,8},{5,1},{6,10},{7,3},{8,12},{9,5},{1... | collective-permute-start | bytes 460808 | tf_op jit(solution)/shard_map/ppermute | solution.py:404
  103.2 3.1 %collective-permute-start.15 = (bf16[24,3200]{1,0:T(8,128)(2,1)S(1)}, bf16[24,3200]{1,0:T(8,128)(2,1)S(1)}, u32[]{:S(2)}, u32[]{:S(2)}) collective-permute-start(bf16[24,3200]{1,0:T(8,128)(2,1)S(1)} %pad_maximum_fusion.1.refs_3_), channel_id=1, source_target_pairs={{4,0},{29,1},{6,2},{31,3},{8,4},{1,5},{10,6},{3,7},{12,8},{5,9},{1... | collective-permute-start | bytes 460808 | tf_op jit(solution)/shard_map/ppermute | solution.py:407
  107.0 4.4 %collective-permute-start.12 = (bf16[24,3200]{1,0:T(8,128)(2,1)S(1)}, bf16[24,3200]{1,0:T(8,128)(2,1)S(1)}, u32[]{:S(2)}, u32[]{:S(2)}) collective-permute-start(bf16[24,3200]{1,0:T(8,128)(2,1)S(1)} %collective-permute-done.11.refs_2_), channel_id=1, source_target_pairs={{0,4},{1,29},{2,6},{3,31},{4,8},{5,1},{6,10},{7,3},{8,12},{9,5},{1... | collective-permute-start | bytes 460808 | tf_op jit(solution)/shard_map/ppermute | solution.py:404
  111.4 1.9 collective-permute-done.15.refs_4_
  113.3 4.1 %collective-permute-start.16 = (bf16[24,3200]{1,0:T(8,128)(2,1)S(1)}, bf16[24,3200]{1,0:T(8,128)(2,1)S(1)}, u32[]{:S(2)}, u32[]{:S(2)}) collective-permute-start(bf16[24,3200]{1,0:T(8,128)(2,1)S(1)} %collective-permute-done.15.refs_4_), channel_id=1, source_target_pairs={{4,0},{29,1},{6,2},{31,3},{8,4},{1,5},{10,6},{3,7},{12,8},{5,9},{1... | collective-permute-start | bytes 460808 | tf_op jit(solution)/shard_map/ppermute | solution.py:407
  118.4 3.8 %collective-permute-start.13 = (bf16[24,3200]{1,0:T(8,128)(2,1)S(1)}, bf16[24,3200]{1,0:T(8,128)(2,1)S(1)}, u32[]{:S(2)}, u32[]{:S(2)}) collective-permute-start(bf16[24,3200]{1,0:T(8,128)(2,1)S(1)} %collective-permute-done.12.refs_1_), channel_id=1, source_target_pairs={{0,4},{1,29},{2,6},{3,31},{4,8},{5,1},{6,10},{7,3},{8,12},{9,5},{1... | collective-permute-start | bytes 460808 | tf_op jit(solution)/shard_map/ppermute | solution.py:404
  122.2 4.7 %collective-permute-done.16.refs_5_ = bf16[24,3200]{1,0:T(8,128)(2,1)S(1)} collective-permute-done((bf16[24,3200]{1,0:T(8,128)(2,1)S(1)}, bf16[24,3200]{1,0:T(8,128)(2,1)S(1)}, u32[]{:S(2)}, u32[]{:S(2)}) %collective-permute-start.16) | collective-permute-done | bytes 153632 | tf_op jit(solution)/shard_map/ppermute | solution.py:407
  127.0 1.9 collective-permute-start.17
  128.9 5.5 %collective-permute-start.14 = (bf16[24,3200]{1,0:T(8,128)(2,1)S(1)}, bf16[24,3200]{1,0:T(8,128)(2,1)S(1)}, u32[]{:S(2)}, u32[]{:S(2)}) collective-permute-start(bf16[24,3200]{1,0:T(8,128)(2,1)S(1)} %collective-permute-done.13.refs_0_), channel_id=1, source_target_pairs={{0,4},{1,29},{2,6},{3,31},{4,8},{5,1},{6,10},{7,3},{8,12},{9,5},{1... | collective-permute-start | bytes 460808 | tf_op jit(solution)/shard_map/ppermute | solution.py:404
  134.4 3.5 %collective-permute-done.17.refs_6_ = bf16[24,3200]{1,0:T(8,128)(2,1)S(1)} collective-permute-done((bf16[24,3200]{1,0:T(8,128)(2,1)S(1)}, bf16[24,3200]{1,0:T(8,128)(2,1)S(1)}, u32[]{:S(2)}, u32[]{:S(2)}) %collective-permute-start.17) | collective-permute-done | bytes 153632 | tf_op jit(solution)/shard_map/ppermute | solution.py:407
  137.9 1.9 collective-permute-start.19
  139.9 7.8 %collective-permute-start.18 = (bf16[24,3200]{1,0:T(8,128)(2,1)S(1)}, bf16[24,3200]{1,0:T(8,128)(2,1)S(1)}, u32[]{:S(2)}, u32[]{:S(2)}) collective-permute-start(bf16[24,3200]{1,0:T(8,128)(2,1)S(1)} %collective-permute-done.14), channel_id=1, source_target_pairs={{0,2},{1,31},{2,0},{3,5},{4,6},{5,3},{6,4},{7,9},{8,10},{9,7},{10,... | collective-permute-start | bytes 460808 | tf_op jit(solution)/shard_map/ppermute | solution.py:412
  147.8 8.6 %collective-permute-start.20 = (bf16[192,3200]{1,0:T(8,128)(2,1)S(1)}, bf16[192,3200]{1,0:T(8,128)(2,1)}, u32[]{:S(2)}, u32[]{:S(2)}) collective-permute-start(bf16[192,3200]{1,0:T(8,128)(2,1)S(1)} %pad_maximum_fusion.g0), channel_id=1, source_target_pairs={{0,1},{1,0},{2,3},{3,2},{4,5},{5,4},{6,7},{7,6},{8,9},{9,8},{10,11... | collective-permute-start | bytes 3686408 | tf_op jit(solution)/shard_map/ppermute | solution.py:414
  156.4 3.5 %collective-permute-done.18 = bf16[24,3200]{1,0:T(8,128)(2,1)S(1)} collective-permute-done((bf16[24,3200]{1,0:T(8,128)(2,1)S(1)}, bf16[24,3200]{1,0:T(8,128)(2,1)S(1)}, u32[]{:S(2)}, u32[]{:S(2)}) %collective-permute-start.18) | collective-permute-done | bytes 153632 | tf_op jit(solution)/shard_map/ppermute | solution.py:412
  160.1 5.9 %collective-permute-start.21 = (bf16[192,3200]{1,0:T(8,128)(2,1)S(1)}, bf16[192,3200]{1,0:T(8,128)(2,1)}, u32[]{:S(2)}, u32[]{:S(2)}) collective-permute-start(bf16[192,3200]{1,0:T(8,128)(2,1)S(1)} %constant_dynamic-update-slice_fusion.g1), channel_id=1, source_target_pairs={{0,1},{1,0},{2,3},{3,2},{4,5},{5,4},{6,7},{7,6},{8,9},{9,8},{10,11... | collective-permute-start | bytes 3686408 | tf_op jit(solution)/shard_map/ppermute | solution.py:416
  166.0 2.5 %collective-permute-done.21.g3 = bf16[192,3200]{1,0:T(8,128)(2,1)} collective-permute-done((bf16[192,3200]{1,0:T(8,128)(2,1)S(1)}, bf16[192,3200]{1,0:T(8,128)(2,1)}, u32[]{:S(2)}, u32[]{:S(2)}) %collective-permute-start.21) | collective-permute-done | bytes 1228832 | tf_op jit(solution)/shard_map/ppermute | solution.py:416
  168.5 7.7 %shard_map.148 = (bf16[16,232,128]{2,1,0:T(8,128)(2,1)}, f32[192,128]{1,0:T(8,128)}) custom-call(s32[2]{0:T(128)} %pad_add_fusion.pos, bf16[192,3200]{1,0:T(8,128)(2,1)} %copy-done, bf16[192,3200]{1,0:T(8,128)(2,1)} %copy-done.2, bf16[192,3200]{1,0:T(8,128)(2,1)} %collective-permute-done.20.g2, bf16[192,3200]{1,0:T(8,128)(2,1)} %collective-permute-done.21.g3, ...), custom_call_target="tpu_custom_call" | custom-call | tf_op jit(solution)/shard_map/pallas_call | solution.py:30
  176.2 3.6 %all-to-all-start.1 = ((bf16[16,232,128]{2,1,0:T(8,128)(2,1)}), bf16[16,232,128]{2,1,0:T(8,128)(2,1)S(1)}, u32[]{:S(2)}, u32[]{:S(2)}) async-start(bf16[16,232,128]{2,1,0:T(8,128)(2,1)} %get-tuple-element.40.after), calls=%async_computation.1 | async-start | bytes 1900544 | tf_op jit(solution)/shard_map/all_to_all | solution.py:425
  179.9 5.6 %shard_map.149 = (bf16[3,2,128,1024]{3,2,1,0:T(8,128)(2,1)}, f32[48,128]{1,0:T(8,128)}) custom-call(bf16[192,3200]{1,0:T(8,128)(2,1)} %copy-done, bf16[192,3200]{1,0:T(8,128)(2,1)} %copy-done.2, bf16[192,3200]{1,0:T(8,128)(2,1)} %collective-permute-done.20.g2, bf16[192,3200]{1,0:T(8,128)(2,1)} %collective-permute-done.21.g3, ...), custom_call_target="tpu_custom_call" | custom-call | tf_op jit(solution)/shard_map/pallas_call | solution.py:30
  186.2 2.3 collective-permute-start.22
  190.0 3.6 %collective-permute-start.23 = (f32[12,128]{1,0:T(8,128)S(1)}, f32[12,128]{1,0:T(8,128)S(1)}, u32[]{:S(2)}, u32[]{:S(2)}) collective-permute-start(f32[12,128]{1,0:T(8,128)S(1)} %slice_select_fusion.1), channel_id=1, source_target_pairs={{0,2},{1,3},{2,0},{3,1},{4,6},{5,7},{6,4},{7,5},{8,10},{9,11},{10,... | collective-permute-start | bytes 18440 | tf_op jit(solution)/shard_map/ppermute | solution.py:432
  196.5 2.0 shard_map.150
  198.5 9.5 %all-to-all-start.2 = ((bf16[16,16,128]{2,1,0:T(8,128)(2,1)}), bf16[16,16,128]{2,1,0:T(8,128)(2,1)S(1)}, u32[]{:S(2)}, u32[]{:S(2)}) async-start(bf16[16,16,128]{2,1,0:T(8,128)(2,1)} %get-tuple-element.45.after), calls=%async_computation.2 | async-start | bytes 131072 | tf_op jit(solution)/shard_map/all_to_all | solution.py:439
  208.0 2.7 %shard_map.151 = (bf16[192,128]{1,0:T(8,128)(2,1)}, f32[2,192]{1,0:T(2,128)}) custom-call(bf16[16,232,128]{2,1,0:T(8,128)(2,1)} %copy-done.1, f32[192,128]{1,0:T(8,128)} %get-tuple-element.41.shared, s32[2,192]{1,0:T(2,128)} %bitcast.15, bf16[16,16,128]{2,1,0:T(8,128)(2,1)} %get-tuple-element.45.after), custom_call_target="tpu_custom_call" | custom-call | tf_op jit(solution)/shard_map/pallas_call | solution.py:30
  210.7 8.9 %all-to-all-done.2.lines = bf16[16,16,128]{2,1,0:T(8,128)(2,1)S(1)} async-done(((bf16[16,16,128]{2,1,0:T(8,128)(2,1)}), bf16[16,16,128]{2,1,0:T(8,128)(2,1)S(1)}, u32[]{:S(2)}, u32[]{:S(2)}) %all-to-all-start.2) | async-done | bytes 65568 | tf_op jit(solution)/shard_map/all_to_all | solution.py:439
  219.6 5.1 %collective-permute-start.24 = (bf16[16,16,128]{2,1,0:T(8,128)(2,1)S(1)}, bf16[16,16,128]{2,1,0:T(8,128)(2,1)S(1)}, u32[]{:S(2)}, u32[]{:S(2)}) collective-permute-start(bf16[16,16,128]{2,1,0:T(8,128)(2,1)S(1)} %all-to-all-done.2.lines), channel_id=1, source_target_pairs={{0,1},{1,0},{2,3},{3,2},{4,5},{5,4},{6,7},{7,6},{8,9},{9,8},{10,11... | collective-permute-start | bytes 196616 | tf_op jit(solution)/shard_map/ppermute | solution.py:445
  226.6 1.6 shard_map.152
  (60 shorter events, 17.0 us)
Async XLA Ops:
  3.6 15.5 %all-to-all-start = ((bf16[16,40,256]{2,1,0:T(8,128)(2,1)}), bf16[16,40,256]{2,1,0:T(8,128)(2,1)S(1)}, u32[]{:S(2)}, u32[]{:S(2)}) async-start(bf16[16,40,256]{2,1,0:T(8,128)(2,1)} %bitcast.13), calls=%async_computation | async-start | bytes 655360 | tf_op jit(solution)/shard_map/all_to_all | solution.py:342
  19.1 0.8 copy-start.4
  28.0 8.5 %collective-permute-start.1 = (bf16[192,3072]{1,0:T(8,128)(2,1)}, bf16[192,3072]{1,0:T(8,128)(2,1)S(1)}, u32[]{:S(2)}, u32[]{:S(2)}) collective-permute-start(bf16[192,3072]{1,0:T(8,128)(2,1)} %get-tuple-element.34), channel_id=1, source_target_pairs={{0,1},{1,0},{2,3},{3,2},{4,5},{5,4},{6,7},{7,6},{8,9},{9,8},{10,11... | collective-permute-start | bytes 3538952 | tf_op jit(solution)/shard_map/ppermute | solution.py:363
  33.9 18.5 %collective-permute-start = (bf16[192,3072]{1,0:T(8,128)(2,1)}, bf16[192,3072]{1,0:T(8,128)(2,1)S(1)}, u32[]{:S(2)}, u32[]{:S(2)}) collective-permute-start(bf16[192,3072]{1,0:T(8,128)(2,1)} %get-tuple-element.32), channel_id=1, source_target_pairs={{0,1},{1,0},{2,3},{3,2},{4,5},{5,4},{6,7},{7,6},{8,9},{9,8},{10,11... | collective-permute-start | bytes 3538952 | tf_op jit(solution)/shard_map/ppermute | solution.py:364
  36.5 2.9 %copy-start.5 = (bf16[192,3072]{1,0:T(8,128)(2,1)}, bf16[192,3072]{1,0:T(8,128)(2,1)S(1)}, u32[]{:S(2)}) copy-start(bf16[192,3072]{1,0:T(8,128)(2,1)S(1)} %collective-permute-done.1) | copy-start | bytes 3538948
  36.5 21.7 %copy-start.3 = (f32[192,3072]{1,0:T(8,128)S(1)}, f32[192,3072]{1,0:T(8,128)}, u32[]{:S(2)}) copy-start(f32[192,3072]{1,0:T(8,128)} %get-tuple-element.31) | copy-start | bytes 7077892
  39.4 18.8 %collective-permute-start.2 = (bf16[120,3072]{1,0:T(8,128)(2,1)}, bf16[120,3072]{1,0:T(8,128)(2,1)}, u32[]{:S(2)}, u32[]{:S(2)}) collective-permute-start(bf16[120,3072]{1,0:T(8,128)(2,1)} %add_convert_fusion), channel_id=1, source_target_pairs={{0,2},{1,31},{2,0},{3,5},{4,6},{5,3},{6,4},{7,9},{8,10},{9,7},{10,... | collective-permute-start | bytes 2211848 | tf_op jit(solution)/shard_map/ppermute | solution.py:368
  50.4 17.3 %collective-permute-start.4 = (bf16[72,3072]{1,0:T(8,128)(2,1)S(1)}, bf16[72,3072]{1,0:T(8,128)(2,1)S(1)}, u32[]{:S(2)}, u32[]{:S(2)}) collective-permute-start(bf16[72,3072]{1,0:T(8,128)(2,1)S(1)} %add_convert_fusion.1), channel_id=1, source_target_pairs={{0,2},{1,31},{2,0},{3,5},{4,6},{5,3},{6,4},{7,9},{8,10},{9,7},{10,... | collective-permute-start | bytes 1327112 | tf_op jit(solution)/shard_map/ppermute | solution.py:369
  59.3 8.5 %collective-permute-start.3 = (bf16[24,3072]{1,0:T(8,128)(2,1)S(1)}, bf16[24,3072]{1,0:T(8,128)(2,1)S(1)}, u32[]{:S(2)}, u32[]{:S(2)}) collective-permute-start(bf16[24,3072]{1,0:T(8,128)(2,1)S(1)} %get-tuple-element.52), channel_id=1, source_target_pairs={{0,4},{1,29},{2,6},{3,31},{4,8},{5,1},{6,10},{7,3},{8,12},{9,5},{1... | collective-permute-start | bytes 442376 | tf_op jit(solution)/shard_map/ppermute | solution.py:385
  64.7 9.1 %collective-permute-start.8 = (bf16[24,3072]{1,0:T(8,128)(2,1)S(1)}, bf16[24,3072]{1,0:T(8,128)(2,1)S(1)}, u32[]{:S(2)}, u32[]{:S(2)}) collective-permute-start(bf16[24,3072]{1,0:T(8,128)(2,1)S(1)} %get-tuple-element.53), channel_id=1, source_target_pairs={{4,0},{29,1},{6,2},{31,3},{8,4},{1,5},{10,6},{3,7},{12,8},{5,9},{1... | collective-permute-start | bytes 442376 | tf_op jit(solution)/shard_map/ppermute | solution.py:389
  67.8 8.0 %collective-permute-start.5 = (bf16[24,3072]{1,0:T(8,128)(2,1)S(1)}, bf16[24,3072]{1,0:T(8,128)(2,1)S(1)}, u32[]{:S(2)}, u32[]{:S(2)}) collective-permute-start(bf16[24,3072]{1,0:T(8,128)(2,1)S(1)} %add_convert_fusion.7), channel_id=1, source_target_pairs={{0,4},{1,29},{2,6},{3,31},{4,8},{5,1},{6,10},{7,3},{8,12},{9,5},{1... | collective-permute-start | bytes 442376 | tf_op jit(solution)/shard_map/ppermute | solution.py:385
  73.8 9.2 %collective-permute-start.9 = (bf16[24,3072]{1,0:T(8,128)(2,1)S(1)}, bf16[24,3072]{1,0:T(8,128)(2,1)S(1)}, u32[]{:S(2)}, u32[]{:S(2)}) collective-permute-start(bf16[24,3072]{1,0:T(8,128)(2,1)S(1)} %add_convert_fusion.3), channel_id=1, source_target_pairs={{4,0},{29,1},{6,2},{31,3},{8,4},{1,5},{10,6},{3,7},{12,8},{5,9},{1... | collective-permute-start | bytes 442376 | tf_op jit(solution)/shard_map/ppermute | solution.py:389
  75.9 9.4 %collective-permute-start.6 = (bf16[24,3072]{1,0:T(8,128)(2,1)S(1)}, bf16[24,3072]{1,0:T(8,128)(2,1)S(1)}, u32[]{:S(2)}, u32[]{:S(2)}) collective-permute-start(bf16[24,3072]{1,0:T(8,128)(2,1)S(1)} %add_convert_fusion.6), channel_id=1, source_target_pairs={{0,4},{1,29},{2,6},{3,31},{4,8},{5,1},{6,10},{7,3},{8,12},{9,5},{1... | collective-permute-start | bytes 442376 | tf_op jit(solution)/shard_map/ppermute | solution.py:385
  83.1 10.5 %collective-permute-start.10 = (bf16[24,3072]{1,0:T(8,128)(2,1)S(1)}, bf16[24,3072]{1,0:T(8,128)(2,1)S(1)}, u32[]{:S(2)}, u32[]{:S(2)}) collective-permute-start(bf16[24,3072]{1,0:T(8,128)(2,1)S(1)} %add_convert_fusion.2), channel_id=1, source_target_pairs={{4,0},{29,1},{6,2},{31,3},{8,4},{1,5},{10,6},{3,7},{12,8},{5,9},{1... | collective-permute-start | bytes 442376 | tf_op jit(solution)/shard_map/ppermute | solution.py:389
  85.4 13.0 %collective-permute-start.7 = (bf16[24,3072]{1,0:T(8,128)(2,1)S(1)}, bf16[24,3072]{1,0:T(8,128)(2,1)S(1)}, u32[]{:S(2)}, u32[]{:S(2)}) collective-permute-start(bf16[24,3072]{1,0:T(8,128)(2,1)S(1)} %add_convert_fusion.5), channel_id=1, source_target_pairs={{0,4},{1,29},{2,6},{3,31},{4,8},{5,1},{6,10},{7,3},{8,12},{9,5},{1... | collective-permute-start | bytes 442376 | tf_op jit(solution)/shard_map/ppermute | solution.py:385
  99.6 7.4 %collective-permute-start.11 = (bf16[24,3200]{1,0:T(8,128)(2,1)S(1)}, bf16[24,3200]{1,0:T(8,128)(2,1)S(1)}, u32[]{:S(2)}, u32[]{:S(2)}) collective-permute-start(bf16[24,3200]{1,0:T(8,128)(2,1)S(1)} %pad_maximum_fusion.1.refs_3_), channel_id=1, source_target_pairs={{0,4},{1,29},{2,6},{3,31},{4,8},{5,1},{6,10},{7,3},{8,12},{9,5},{1... | collective-permute-start | bytes 460808 | tf_op jit(solution)/shard_map/ppermute | solution.py:404
  103.2 10.1 %collective-permute-start.15 = (bf16[24,3200]{1,0:T(8,128)(2,1)S(1)}, bf16[24,3200]{1,0:T(8,128)(2,1)S(1)}, u32[]{:S(2)}, u32[]{:S(2)}) collective-permute-start(bf16[24,3200]{1,0:T(8,128)(2,1)S(1)} %pad_maximum_fusion.1.refs_3_), channel_id=1, source_target_pairs={{4,0},{29,1},{6,2},{31,3},{8,4},{1,5},{10,6},{3,7},{12,8},{5,9},{1... | collective-permute-start | bytes 460808 | tf_op jit(solution)/shard_map/ppermute | solution.py:407
  107.0 11.4 %collective-permute-start.12 = (bf16[24,3200]{1,0:T(8,128)(2,1)S(1)}, bf16[24,3200]{1,0:T(8,128)(2,1)S(1)}, u32[]{:S(2)}, u32[]{:S(2)}) collective-permute-start(bf16[24,3200]{1,0:T(8,128)(2,1)S(1)} %collective-permute-done.11.refs_2_), channel_id=1, source_target_pairs={{0,4},{1,29},{2,6},{3,31},{4,8},{5,1},{6,10},{7,3},{8,12},{9,5},{1... | collective-permute-start | bytes 460808 | tf_op jit(solution)/shard_map/ppermute | solution.py:404
  113.3 13.7 %collective-permute-start.16 = (bf16[24,3200]{1,0:T(8,128)(2,1)S(1)}, bf16[24,3200]{1,0:T(8,128)(2,1)S(1)}, u32[]{:S(2)}, u32[]{:S(2)}) collective-permute-start(bf16[24,3200]{1,0:T(8,128)(2,1)S(1)} %collective-permute-done.15.refs_4_), channel_id=1, source_target_pairs={{4,0},{29,1},{6,2},{31,3},{8,4},{1,5},{10,6},{3,7},{12,8},{5,9},{1... | collective-permute-start | bytes 460808 | tf_op jit(solution)/shard_map/ppermute | solution.py:407
  118.4 10.5 %collective-permute-start.13 = (bf16[24,3200]{1,0:T(8,128)(2,1)S(1)}, bf16[24,3200]{1,0:T(8,128)(2,1)S(1)}, u32[]{:S(2)}, u32[]{:S(2)}) collective-permute-start(bf16[24,3200]{1,0:T(8,128)(2,1)S(1)} %collective-permute-done.12.refs_1_), channel_id=1, source_target_pairs={{0,4},{1,29},{2,6},{3,31},{4,8},{5,1},{6,10},{7,3},{8,12},{9,5},{1... | collective-permute-start | bytes 460808 | tf_op jit(solution)/shard_map/ppermute | solution.py:404
  127.0 10.9 %collective-permute-start.17 = (bf16[24,3200]{1,0:T(8,128)(2,1)S(1)}, bf16[24,3200]{1,0:T(8,128)(2,1)S(1)}, u32[]{:S(2)}, u32[]{:S(2)}) collective-permute-start(bf16[24,3200]{1,0:T(8,128)(2,1)S(1)} %collective-permute-done.16.refs_5_), channel_id=1, source_target_pairs={{4,0},{29,1},{6,2},{31,3},{8,4},{1,5},{10,6},{3,7},{12,8},{5,9},{1... | collective-permute-start | bytes 460808 | tf_op jit(solution)/shard_map/ppermute | solution.py:407
  128.9 11.0 %collective-permute-start.14 = (bf16[24,3200]{1,0:T(8,128)(2,1)S(1)}, bf16[24,3200]{1,0:T(8,128)(2,1)S(1)}, u32[]{:S(2)}, u32[]{:S(2)}) collective-permute-start(bf16[24,3200]{1,0:T(8,128)(2,1)S(1)} %collective-permute-done.13.refs_0_), channel_id=1, source_target_pairs={{0,4},{1,29},{2,6},{3,31},{4,8},{5,1},{6,10},{7,3},{8,12},{9,5},{1... | collective-permute-start | bytes 460808 | tf_op jit(solution)/shard_map/ppermute | solution.py:404
  137.9 22.0 %collective-permute-start.19 = (bf16[168,3200]{1,0:T(8,128)(2,1)S(1)}, bf16[168,3200]{1,0:T(8,128)(2,1)S(1)}, u32[]{:S(2)}, u32[]{:S(2)}) collective-permute-start(bf16[168,3200]{1,0:T(8,128)(2,1)S(1)} %shard_map.147), channel_id=1, source_target_pairs={{0,2},{1,31},{2,0},{3,5},{4,6},{5,3},{6,4},{7,9},{8,10},{9,7},{10,... | collective-permute-start | bytes 3225608 | tf_op jit(solution)/shard_map/ppermute | solution.py:411
  139.9 20.0 %collective-permute-start.18 = (bf16[24,3200]{1,0:T(8,128)(2,1)S(1)}, bf16[24,3200]{1,0:T(8,128)(2,1)S(1)}, u32[]{:S(2)}, u32[]{:S(2)}) collective-permute-start(bf16[24,3200]{1,0:T(8,128)(2,1)S(1)} %collective-permute-done.14), channel_id=1, source_target_pairs={{0,2},{1,31},{2,0},{3,5},{4,6},{5,3},{6,4},{7,9},{8,10},{9,7},{10,... | collective-permute-start | bytes 460808 | tf_op jit(solution)/shard_map/ppermute | solution.py:412
  147.8 12.3 %copy-start = (bf16[192,3200]{1,0:T(8,128)(2,1)}, bf16[192,3200]{1,0:T(8,128)(2,1)S(1)}, u32[]{:S(2)}) copy-start(bf16[192,3200]{1,0:T(8,128)(2,1)S(1)} %pad_maximum_fusion.g0) | copy-start | bytes 3686404
  147.8 18.2 %collective-permute-start.20 = (bf16[192,3200]{1,0:T(8,128)(2,1)S(1)}, bf16[192,3200]{1,0:T(8,128)(2,1)}, u32[]{:S(2)}, u32[]{:S(2)}) collective-permute-start(bf16[192,3200]{1,0:T(8,128)(2,1)S(1)} %pad_maximum_fusion.g0), channel_id=1, source_target_pairs={{0,1},{1,0},{2,3},{3,2},{4,5},{5,4},{6,7},{7,6},{8,9},{9,8},{10,11... | collective-permute-start | bytes 3686408 | tf_op jit(solution)/shard_map/ppermute | solution.py:414
  160.1 8.4 %copy-start.2 = (bf16[192,3200]{1,0:T(8,128)(2,1)}, bf16[192,3200]{1,0:T(8,128)(2,1)S(1)}, u32[]{:S(2)}) copy-start(bf16[192,3200]{1,0:T(8,128)(2,1)S(1)} %constant_dynamic-update-slice_fusion.g1) | copy-start | bytes 3686404
  160.1 8.4 %collective-permute-start.21 = (bf16[192,3200]{1,0:T(8,128)(2,1)S(1)}, bf16[192,3200]{1,0:T(8,128)(2,1)}, u32[]{:S(2)}, u32[]{:S(2)}) collective-permute-start(bf16[192,3200]{1,0:T(8,128)(2,1)S(1)} %constant_dynamic-update-slice_fusion.g1), channel_id=1, source_target_pairs={{0,1},{1,0},{2,3},{3,2},{4,5},{5,4},{6,7},{7,6},{8,9},{9,8},{10,11... | collective-permute-start | bytes 3686408 | tf_op jit(solution)/shard_map/ppermute | solution.py:416
  176.2 19.3 %all-to-all-start.1 = ((bf16[16,232,128]{2,1,0:T(8,128)(2,1)}), bf16[16,232,128]{2,1,0:T(8,128)(2,1)S(1)}, u32[]{:S(2)}, u32[]{:S(2)}) async-start(bf16[16,232,128]{2,1,0:T(8,128)(2,1)} %get-tuple-element.40.after), calls=%async_computation.1 | async-start | bytes 1900544 | tf_op jit(solution)/shard_map/all_to_all | solution.py:425
  186.2 3.1 %collective-permute-start.22 = (f32[24,128]{1,0:T(8,128)S(1)}, f32[24,128]{1,0:T(8,128)S(1)}, u32[]{:S(2)}, u32[]{:S(2)}) collective-permute-start(f32[24,128]{1,0:T(8,128)S(1)} %slice_select_fusion), channel_id=1, source_target_pairs={{0,1},{1,0},{2,3},{3,2},{4,5},{5,4},{6,7},{7,6},{8,9},{9,8},{10,11... | collective-permute-start | bytes 36872 | tf_op jit(solution)/shard_map/ppermute | solution.py:430
  190.0 5.0 %collective-permute-start.23 = (f32[12,128]{1,0:T(8,128)S(1)}, f32[12,128]{1,0:T(8,128)S(1)}, u32[]{:S(2)}, u32[]{:S(2)}) collective-permute-start(f32[12,128]{1,0:T(8,128)S(1)} %slice_select_fusion.1), channel_id=1, source_target_pairs={{0,2},{1,3},{2,0},{3,1},{4,6},{5,7},{6,4},{7,5},{8,10},{9,11},{10,... | collective-permute-start | bytes 18440 | tf_op jit(solution)/shard_map/ppermute | solution.py:432
  195.6 0.9 copy-start.1
  198.5 21.1 %all-to-all-start.2 = ((bf16[16,16,128]{2,1,0:T(8,128)(2,1)}), bf16[16,16,128]{2,1,0:T(8,128)(2,1)S(1)}, u32[]{:S(2)}, u32[]{:S(2)}) async-start(bf16[16,16,128]{2,1,0:T(8,128)(2,1)} %get-tuple-element.45.after), calls=%async_computation.2 | async-start | bytes 131072 | tf_op jit(solution)/shard_map/all_to_all | solution.py:439
  219.6 6.4 %copy-start.6 = (bf16[16,16,128]{2,1,0:T(8,128)(2,1)}, bf16[16,16,128]{2,1,0:T(8,128)(2,1)S(1)}, u32[]{:S(2)}) copy-start(bf16[16,16,128]{2,1,0:T(8,128)(2,1)S(1)} %all-to-all-done.2.lines) | copy-start | bytes 196612
  219.6 6.4 %collective-permute-start.24 = (bf16[16,16,128]{2,1,0:T(8,128)(2,1)S(1)}, bf16[16,16,128]{2,1,0:T(8,128)(2,1)S(1)}, u32[]{:S(2)}, u32[]{:S(2)}) collective-permute-start(bf16[16,16,128]{2,1,0:T(8,128)(2,1)S(1)} %all-to-all-done.2.lines), channel_id=1, source_target_pairs={{0,1},{1,0},{2,3},{3,2},{4,5},{5,4},{6,7},{7,6},{8,9},{9,8},{10,11... | collective-permute-start | bytes 196616 | tf_op jit(solution)/shard_map/ppermute | solution.py:445
  226.0 0.6 copy-start.7

commit v8 on v7

--- a/solution.py
+++ b/solution.py
@@ -362,18 +362,18 @@
     )(pos, got.reshape(n_ep * bl, 2 * width), both, *weights)
     oth_s = lax.ppermute(out_s, "tp", swap)
     oth_k = lax.ppermute(out_k, "tp", swap)
-    cut = (hops + 1) * piece
+    cut = 2 * piece
     to_a = (own_s[:cut] + oth_s[:cut].astype(F32)).astype(BF)
     to_b = (own_s[cut:] + oth_s[cut:].astype(F32)).astype(BF)
     par_a = lax.ppermute(to_a, "tp", pair)
     par_b = lax.ppermute(to_b, "tp", pair)
-    left_rows = slice(2 * piece, hops * piece)
-    on_left = lax.optimization_barrier((own_k[left_rows], oth_k[left_rows], par_a[left_rows]))
+    left_rows = slice(cut, hops * piece)
+    on_left = lax.optimization_barrier((own_k[left_rows], oth_k[left_rows], par_b[: hops * piece - cut]))
 
     def at(m):
         p = (m - hops) % members
         rows_p = slice(p * piece, (p + 1) * piece)
-        par = par_a[rows_p] if p <= hops else par_b[p * piece - cut : (p + 1) * piece - cut]
+        par = par_a[rows_p] if p < 2 else par_b[p * piece - cut : (p + 1) * piece - cut]
         own, oth = own_k, oth_k
         if 1 < p < hops:
             (own, oth, par), rows_p = on_left, slice((p - 2) * piece, (p - 1) * piece)

time: 230 us -> 225 us (0.978)
  other arithmetic: 10.9 us -> 7.54 us
    ppermute x6, waiting for transfers between devices: 14.6 us -> 1.51 us  [body(): left = lax.ppermute(left, 'tp', bwd)]
    ppermute x8, waiting for transfers between devices: 6.95 us -> 19.8 us  [body(): right = lax.ppermute(right, 'tp', fwd)]
    ppermute x8, starting transfers between devices: 37.9 us -> 48.9 us  [body(): right = lax.ppermute(right, 'tp', fwd)]
    ppermute x1, waiting for transfers between devices: 5.85 us -> 0.5 us  [body(): par_a = lax.ppermute(to_a, 'tp', pair)]
    ppermute x1, starting transfers between devices: 8.59 us -> 4.44 us  [body(): kept_x = lax.ppermute(kept, 'tp', swap)]
    ppermute x6, starting transfers between devices: 15 us -> 11.7 us  [body(): left = lax.ppermute(left, 'tp', bwd)]
    ppermute x1, waiting for transfers between devices: 3.53 us -> 6.36 us  [body(): last_o = lax.ppermute(ring[hops], 'tp', pair)]
    ppermute x1, starting transfers between devices: 7.8 us -> 5.3 us  [body(): last_o = lax.ppermute(ring[hops], 'tp', pair)]
  transfers between devices with their start and end apart: 28 -> 28, of which waited for: 19 -> 18; matrix products, arithmetic and copies ran while one was open for 5% -> 4% of each run, Pallas kernels for 4% -> 4%
where the time goes in v8:
time: 225 us; the launch traced here: 223 us
  starting transfers between devices  129 us (57%)
  waiting for transfers between devices  51.1 us (23%)
  Pallas kernels  30.8 us (14%)
  other arithmetic  7.54 us (3%)
  local copies, waits for them, and re-layouts  3.46 us (2%)
    ppermute x8, starting transfers between devices, body(): right = lax.ppermute(right, 'tp', fwd)  48.9 us
    pallas_call x7, Pallas kernels, call(): pl.pallas_call(kernel, out_shape=[jax.ShapeDtypeStruct(s, d) for s, d in...  22.6 us
    ppermute x8, waiting for transfers between devices, body(): right = lax.ppermute(right, 'tp', fwd)  19.8 us
    ppermute x6, starting transfers between devices, body(): left = lax.ppermute(left, 'tp', bwd)  11.7 us
    all_to_all x1, starting transfers between devices, body(): lax.all_to_all(lines, 'tp', 0, 0, axis_index_groups=same_core, tiled=True)  11.2 us
    ppermute x1, starting transfers between devices, body(): par_a = lax.ppermute(to_a, 'tp', pair)  9.78 us
    all_to_all x1, waiting for transfers between devices, body(): lax.all_to_all(lines, 'tp', 0, 0, axis_index_groups=same_core, tiled=True)  8.85 us
    pallas_call x1, Pallas kernels, body(): pl.pallas_call(functools.partial(project, sizes), out_shape=[jax.ShapeDty...  8.2 us
  transfers between devices with their start and end apart: 28, of which 18 were waited for; matrix products, arithmetic and copies ran while one was open for 4% of the time, Pallas kernels for 4%

profile of v8, /device:TPU:1, one launch (start us, length us, event | category | flops | bytes accessed | tf_op | source)
XLA Modules:
  0.0 223.3 jit_solution(1355370611107122405)
XLA Ops:
  0.6 3.0 %shard_map.145 = (bf16[640,256]{1,0:T(8,128)(2,1)}, bf16[192,256]{1,0:T(8,128)(2,1)}) custom-call(bf16[192,128]{1,0:T(8,128)(2,1)} %tokens.1, bf16[192,128]{1,0:T(8,128)(2,1)} %cotangent.1, s32[2,192]{1,0:T(2,128)} %bitcast.14, bf16[2,192]{1,0:T(2,128)(2,1)} %bitcast.16), custom_call_target="tpu_custom_call" | custom-call | tf_op jit(solution)/shard_map/pallas_call | solution.py:30
  3.6 7.6 %all-to-all-start = ((bf16[16,40,256]{2,1,0:T(8,128)(2,1)}), bf16[16,40,256]{2,1,0:T(8,128)(2,1)S(1)}, u32[]{:S(2)}, u32[]{:S(2)}) async-start(bf16[16,40,256]{2,1,0:T(8,128)(2,1)} %bitcast.13), calls=%async_computation | async-start | bytes 655360 | tf_op jit(solution)/shard_map/all_to_all | solution.py:342
  11.8 7.3 %all-to-all-done = bf16[16,40,256]{2,1,0:T(8,128)(2,1)S(1)} async-done(((bf16[16,40,256]{2,1,0:T(8,128)(2,1)}), bf16[16,40,256]{2,1,0:T(8,128)(2,1)S(1)}, u32[]{:S(2)}, u32[]{:S(2)}) %all-to-all-start) | async-done | bytes 327712 | tf_op jit(solution)/shard_map/all_to_all | solution.py:342
  19.8 8.2 %shard_map.146 = (f32[192,3072]{1,0:T(8,128)}, f32[192,3072]{1,0:T(8,128)}, bf16[192,3072]{1,0:T(8,128)(2,1)}, bf16[192,3072]{1,0:T(8,128)(2,1)}, bf16[256,768]{...) custom-call(s32[2]{0:T(128)} %pad_add_fusion.pos, ...), custom_call_target="tpu_custom_call" | custom-call | tf_op jit(solution)/shard_map/pallas_call | solution.py:354
  28.0 5.8 %collective-permute-start.1 = (bf16[192,3072]{1,0:T(8,128)(2,1)}, bf16[192,3072]{1,0:T(8,128)(2,1)S(1)}, u32[]{:S(2)}, u32[]{:S(2)}) collective-permute-start(bf16[192,3072]{1,0:T(8,128)(2,1)} %get-tuple-element.34), channel_id=1, source_target_pairs={{0,1},{1,0},{2,3},{3,2},{4,5},{5,4},{6,7},{7,6},{8,9},{9,8},{10,11... | collective-permute-start | bytes 3538952 | tf_op jit(solution)/shard_map/ppermute | solution.py:363
  33.9 1.9 collective-permute-start
  36.5 1.1 add_convert_fusion.1
  37.7 9.8 %collective-permute-start.2 = (bf16[48,3072]{1,0:T(8,128)(2,1)S(1)}, bf16[48,3072]{1,0:T(8,128)(2,1)S(1)}, u32[]{:S(2)}, u32[]{:S(2)}) collective-permute-start(bf16[48,3072]{1,0:T(8,128)(2,1)S(1)} %add_convert_fusion.1), channel_id=1, source_target_pairs={{0,2},{1,31},{2,0},{3,5},{4,6},{5,3},{6,4},{7,9},{8,10},{9,7},{10,... | collective-permute-start | bytes 884744 | tf_op jit(solution)/shard_map/ppermute | solution.py:368
  47.5 1.6 add_convert_fusion
  49.1 1.9 collective-permute-start.4
  51.7 4.1 %collective-permute-start.3 = (bf16[24,3072]{1,0:T(8,128)(2,1)S(1)}, bf16[24,3072]{1,0:T(8,128)(2,1)S(1)}, u32[]{:S(2)}, u32[]{:S(2)}) collective-permute-start(bf16[24,3072]{1,0:T(8,128)(2,1)S(1)} %get-tuple-element.52), channel_id=1, source_target_pairs={{0,4},{1,29},{2,6},{3,31},{4,8},{5,1},{6,10},{7,3},{8,12},{9,5},{1... | collective-permute-start | bytes 442376 | tf_op jit(solution)/shard_map/ppermute | solution.py:385
  57.0 2.1 collective-permute-start.8
  59.1 8.2 %collective-permute-done.3 = bf16[24,3072]{1,0:T(8,128)(2,1)S(1)} collective-permute-done((bf16[24,3072]{1,0:T(8,128)(2,1)S(1)}, bf16[24,3072]{1,0:T(8,128)(2,1)S(1)}, u32[]{:S(2)}, u32[]{:S(2)}) %collective-permute-start.3) | collective-permute-done | bytes 147488 | tf_op jit(solution)/shard_map/ppermute | solution.py:385
  67.4 6.0 %collective-permute-start.5 = (bf16[24,3072]{1,0:T(8,128)(2,1)S(1)}, bf16[24,3072]{1,0:T(8,128)(2,1)S(1)}, u32[]{:S(2)}, u32[]{:S(2)}) collective-permute-start(bf16[24,3072]{1,0:T(8,128)(2,1)S(1)} %add_convert_fusion.7), channel_id=1, source_target_pairs={{0,4},{1,29},{2,6},{3,31},{4,8},{5,1},{6,10},{7,3},{8,12},{9,5},{1... | collective-permute-start | bytes 442376 | tf_op jit(solution)/shard_map/ppermute | solution.py:385
  73.6 1.9 collective-permute-start.9
  76.3 7.5 %collective-permute-start.6 = (bf16[24,3072]{1,0:T(8,128)(2,1)S(1)}, bf16[24,3072]{1,0:T(8,128)(2,1)S(1)}, u32[]{:S(2)}, u32[]{:S(2)}) collective-permute-start(bf16[24,3072]{1,0:T(8,128)(2,1)S(1)} %add_convert_fusion.6), channel_id=1, source_target_pairs={{0,4},{1,29},{2,6},{3,31},{4,8},{5,1},{6,10},{7,3},{8,12},{9,5},{1... | collective-permute-start | bytes 442376 | tf_op jit(solution)/shard_map/ppermute | solution.py:385
  83.9 1.9 collective-permute-start.10
  86.5 6.0 %collective-permute-start.7 = (bf16[24,3072]{1,0:T(8,128)(2,1)S(1)}, bf16[24,3072]{1,0:T(8,128)(2,1)S(1)}, u32[]{:S(2)}, u32[]{:S(2)}) collective-permute-start(bf16[24,3072]{1,0:T(8,128)(2,1)S(1)} %add_convert_fusion.5), channel_id=1, source_target_pairs={{0,4},{1,29},{2,6},{3,31},{4,8},{5,1},{6,10},{7,3},{8,12},{9,5},{1... | collective-permute-start | bytes 442376 | tf_op jit(solution)/shard_map/ppermute | solution.py:385
  92.5 3.5 %collective-permute-done.7 = bf16[24,3072]{1,0:T(8,128)(2,1)S(1)} collective-permute-done((bf16[24,3072]{1,0:T(8,128)(2,1)S(1)}, bf16[24,3072]{1,0:T(8,128)(2,1)S(1)}, u32[]{:S(2)}, u32[]{:S(2)}) %collective-permute-start.7) | collective-permute-done | bytes 147488 | tf_op jit(solution)/shard_map/ppermute | solution.py:385
  96.4 5.9 %collective-permute-start.11 = (bf16[24,3200]{1,0:T(8,128)(2,1)S(1)}, bf16[24,3200]{1,0:T(8,128)(2,1)S(1)}, u32[]{:S(2)}, u32[]{:S(2)}) collective-permute-start(bf16[24,3200]{1,0:T(8,128)(2,1)S(1)} %pad_maximum_fusion.1.refs_3_), channel_id=1, source_target_pairs={{0,4},{1,29},{2,6},{3,31},{4,8},{5,1},{6,10},{7,3},{8,12},{9,5},{1... | collective-permute-start | bytes 460808 | tf_op jit(solution)/shard_map/ppermute | solution.py:404
  102.4 1.9 collective-permute-start.15
  104.3 3.4 %collective-permute-done.11.refs_2_ = bf16[24,3200]{1,0:T(8,128)(2,1)S(1)} collective-permute-done((bf16[24,3200]{1,0:T(8,128)(2,1)S(1)}, bf16[24,3200]{1,0:T(8,128)(2,1)S(1)}, u32[]{:S(2)}, u32[]{:S(2)}) %collective-permute-start.11) | collective-permute-done | bytes 153632 | tf_op jit(solution)/shard_map/ppermute | solution.py:404
  107.7 5.9 %collective-permute-start.12 = (bf16[24,3200]{1,0:T(8,128)(2,1)S(1)}, bf16[24,3200]{1,0:T(8,128)(2,1)S(1)}, u32[]{:S(2)}, u32[]{:S(2)}) collective-permute-start(bf16[24,3200]{1,0:T(8,128)(2,1)S(1)} %collective-permute-done.11.refs_2_), channel_id=1, source_target_pairs={{0,4},{1,29},{2,6},{3,31},{4,8},{5,1},{6,10},{7,3},{8,12},{9,5},{1... | collective-permute-start | bytes 460808 | tf_op jit(solution)/shard_map/ppermute | solution.py:404
  113.6 1.9 collective-permute-start.16
  116.3 7.5 %collective-permute-start.13 = (bf16[24,3200]{1,0:T(8,128)(2,1)S(1)}, bf16[24,3200]{1,0:T(8,128)(2,1)S(1)}, u32[]{:S(2)}, u32[]{:S(2)}) collective-permute-start(bf16[24,3200]{1,0:T(8,128)(2,1)S(1)} %collective-permute-done.12.refs_1_), channel_id=1, source_target_pairs={{0,4},{1,29},{2,6},{3,31},{4,8},{5,1},{6,10},{7,3},{8,12},{9,5},{1... | collective-permute-start | bytes 460808 | tf_op jit(solution)/shard_map/ppermute | solution.py:404
  123.9 1.9 collective-permute-start.17
  126.2 5.9 %collective-permute-start.14 = (bf16[24,3200]{1,0:T(8,128)(2,1)S(1)}, bf16[24,3200]{1,0:T(8,128)(2,1)S(1)}, u32[]{:S(2)}, u32[]{:S(2)}) collective-permute-start(bf16[24,3200]{1,0:T(8,128)(2,1)S(1)} %collective-permute-done.13.refs_0_), channel_id=1, source_target_pairs={{0,4},{1,29},{2,6},{3,31},{4,8},{5,1},{6,10},{7,3},{8,12},{9,5},{1... | collective-permute-start | bytes 460808 | tf_op jit(solution)/shard_map/ppermute | solution.py:404
  132.1 1.5 collective-permute-done.17.refs_6_
  133.7 1.9 collective-permute-start.19
  135.6 2.2 collective-permute-done.14
  137.8 5.3 %collective-permute-start.18 = (bf16[24,3200]{1,0:T(8,128)(2,1)S(1)}, bf16[24,3200]{1,0:T(8,128)(2,1)S(1)}, u32[]{:S(2)}, u32[]{:S(2)}) collective-permute-start(bf16[24,3200]{1,0:T(8,128)(2,1)S(1)} %collective-permute-done.14), channel_id=1, source_target_pairs={{0,2},{1,31},{2,0},{3,5},{4,6},{5,3},{6,4},{7,9},{8,10},{9,7},{10,... | collective-permute-start | bytes 460808 | tf_op jit(solution)/shard_map/ppermute | solution.py:412
  143.2 4.4 %collective-permute-start.20 = (bf16[192,3200]{1,0:T(8,128)(2,1)S(1)}, bf16[192,3200]{1,0:T(8,128)(2,1)}, u32[]{:S(2)}, u32[]{:S(2)}) collective-permute-start(bf16[192,3200]{1,0:T(8,128)(2,1)S(1)} %pad_maximum_fusion.g0), channel_id=1, source_target_pairs={{0,1},{1,0},{2,3},{3,2},{4,5},{5,4},{6,7},{7,6},{8,9},{9,8},{10,11... | collective-permute-start | bytes 3686408 | tf_op jit(solution)/shard_map/ppermute | solution.py:414
  147.6 6.4 %collective-permute-done.18 = bf16[24,3200]{1,0:T(8,128)(2,1)S(1)} collective-permute-done((bf16[24,3200]{1,0:T(8,128)(2,1)S(1)}, bf16[24,3200]{1,0:T(8,128)(2,1)S(1)}, u32[]{:S(2)}, u32[]{:S(2)}) %collective-permute-start.18) | collective-permute-done | bytes 153632 | tf_op jit(solution)/shard_map/ppermute | solution.py:412
  154.2 5.4 %collective-permute-start.21 = (bf16[192,3200]{1,0:T(8,128)(2,1)S(1)}, bf16[192,3200]{1,0:T(8,128)(2,1)}, u32[]{:S(2)}, u32[]{:S(2)}) collective-permute-start(bf16[192,3200]{1,0:T(8,128)(2,1)S(1)} %constant_dynamic-update-slice_fusion.g1), channel_id=1, source_target_pairs={{0,1},{1,0},{2,3},{3,2},{4,5},{5,4},{6,7},{7,6},{8,9},{9,8},{10,11... | collective-permute-start | bytes 3686408 | tf_op jit(solution)/shard_map/ppermute | solution.py:416
  159.6 2.5 %collective-permute-done.21.g3 = bf16[192,3200]{1,0:T(8,128)(2,1)} collective-permute-done((bf16[192,3200]{1,0:T(8,128)(2,1)S(1)}, bf16[192,3200]{1,0:T(8,128)(2,1)}, u32[]{:S(2)}, u32[]{:S(2)}) %collective-permute-start.21) | collective-permute-done | bytes 1228832 | tf_op jit(solution)/shard_map/ppermute | solution.py:416
  162.1 7.7 %shard_map.148 = (bf16[16,232,128]{2,1,0:T(8,128)(2,1)}, f32[192,128]{1,0:T(8,128)}) custom-call(s32[2]{0:T(128)} %pad_add_fusion.pos, bf16[192,3200]{1,0:T(8,128)(2,1)} %copy-done, bf16[192,3200]{1,0:T(8,128)(2,1)} %copy-done.2, bf16[192,3200]{1,0:T(8,128)(2,1)} %collective-permute-done.20.g2, bf16[192,3200]{1,0:T(8,128)(2,1)} %collective-permute-done.21.g3, ...), custom_call_target="tpu_custom_call" | custom-call | tf_op jit(solution)/shard_map/pallas_call | solution.py:30
  169.8 3.6 %all-to-all-start.1 = ((bf16[16,232,128]{2,1,0:T(8,128)(2,1)}), bf16[16,232,128]{2,1,0:T(8,128)(2,1)S(1)}, u32[]{:S(2)}, u32[]{:S(2)}) async-start(bf16[16,232,128]{2,1,0:T(8,128)(2,1)} %get-tuple-element.40.after), calls=%async_computation.1 | async-start | bytes 1900544 | tf_op jit(solution)/shard_map/all_to_all | solution.py:425
  173.5 5.6 %shard_map.149 = (bf16[3,2,128,1024]{3,2,1,0:T(8,128)(2,1)}, f32[48,128]{1,0:T(8,128)}) custom-call(bf16[192,3200]{1,0:T(8,128)(2,1)} %copy-done, bf16[192,3200]{1,0:T(8,128)(2,1)} %copy-done.2, bf16[192,3200]{1,0:T(8,128)(2,1)} %collective-permute-done.20.g2, bf16[192,3200]{1,0:T(8,128)(2,1)} %collective-permute-done.21.g3, ...), custom_call_target="tpu_custom_call" | custom-call | tf_op jit(solution)/shard_map/pallas_call | solution.py:30
  179.8 2.3 %collective-permute-start.22 = (f32[24,128]{1,0:T(8,128)S(1)}, f32[24,128]{1,0:T(8,128)S(1)}, u32[]{:S(2)}, u32[]{:S(2)}) collective-permute-start(f32[24,128]{1,0:T(8,128)S(1)} %slice_select_fusion), channel_id=1, source_target_pairs={{0,1},{1,0},{2,3},{3,2},{4,5},{5,4},{6,7},{7,6},{8,9},{9,8},{10,11... | collective-permute-start | bytes 36872 | tf_op jit(solution)/shard_map/ppermute | solution.py:430
  183.6 1.9 collective-permute-start.23
  185.5 2.8 %collective-permute-done.23 = f32[12,128]{1,0:T(8,128)S(1)} collective-permute-done((f32[12,128]{1,0:T(8,128)S(1)}, f32[12,128]{1,0:T(8,128)S(1)}, u32[]{:S(2)}, u32[]{:S(2)}) %collective-permute-start.23) | collective-permute-done | bytes 6176 | tf_op jit(solution)/shard_map/ppermute | solution.py:432
  189.9 2.0 shard_map.150
  191.9 11.2 %all-to-all-start.2 = ((bf16[16,16,128]{2,1,0:T(8,128)(2,1)}), bf16[16,16,128]{2,1,0:T(8,128)(2,1)S(1)}, u32[]{:S(2)}, u32[]{:S(2)}) async-start(bf16[16,16,128]{2,1,0:T(8,128)(2,1)} %get-tuple-element.45.after), calls=%async_computation.2 | async-start | bytes 131072 | tf_op jit(solution)/shard_map/all_to_all | solution.py:439
  203.2 2.7 %shard_map.151 = (bf16[192,128]{1,0:T(8,128)(2,1)}, f32[2,192]{1,0:T(2,128)}) custom-call(bf16[16,232,128]{2,1,0:T(8,128)(2,1)} %copy-done.1, f32[192,128]{1,0:T(8,128)} %get-tuple-element.41.shared, s32[2,192]{1,0:T(2,128)} %bitcast.15, bf16[16,16,128]{2,1,0:T(8,128)(2,1)} %get-tuple-element.45.after), custom_call_target="tpu_custom_call" | custom-call | tf_op jit(solution)/shard_map/pallas_call | solution.py:30
  205.9 8.9 %all-to-all-done.2.lines = bf16[16,16,128]{2,1,0:T(8,128)(2,1)S(1)} async-done(((bf16[16,16,128]{2,1,0:T(8,128)(2,1)}), bf16[16,16,128]{2,1,0:T(8,128)(2,1)S(1)}, u32[]{:S(2)}, u32[]{:S(2)}) %all-to-all-start.2) | async-done | bytes 65568 | tf_op jit(solution)/shard_map/all_to_all | solution.py:439
  214.7 5.1 %collective-permute-start.24 = (bf16[16,16,128]{2,1,0:T(8,128)(2,1)S(1)}, bf16[16,16,128]{2,1,0:T(8,128)(2,1)S(1)}, u32[]{:S(2)}, u32[]{:S(2)}) collective-permute-start(bf16[16,16,128]{2,1,0:T(8,128)(2,1)S(1)} %all-to-all-done.2.lines), channel_id=1, source_target_pairs={{0,1},{1,0},{2,3},{3,2},{4,5},{5,4},{6,7},{7,6},{8,9},{9,8},{10,11... | collective-permute-start | bytes 196616 | tf_op jit(solution)/shard_map/ppermute | solution.py:445
  219.9 1.2 convert_bitcast_fusion
  221.8 1.6 shard_map.152
  (58 shorter events, 11.9 us)
Async XLA Ops:
  3.6 15.5 %all-to-all-start = ((bf16[16,40,256]{2,1,0:T(8,128)(2,1)}), bf16[16,40,256]{2,1,0:T(8,128)(2,1)S(1)}, u32[]{:S(2)}, u32[]{:S(2)}) async-start(bf16[16,40,256]{2,1,0:T(8,128)(2,1)} %bitcast.13), calls=%async_computation | async-start | bytes 655360 | tf_op jit(solution)/shard_map/all_to_all | solution.py:342
  19.1 0.7 copy-start.4
  28.0 8.5 %collective-permute-start.1 = (bf16[192,3072]{1,0:T(8,128)(2,1)}, bf16[192,3072]{1,0:T(8,128)(2,1)S(1)}, u32[]{:S(2)}, u32[]{:S(2)}) collective-permute-start(bf16[192,3072]{1,0:T(8,128)(2,1)} %get-tuple-element.34), channel_id=1, source_target_pairs={{0,1},{1,0},{2,3},{3,2},{4,5},{5,4},{6,7},{7,6},{8,9},{9,8},{10,11... | collective-permute-start | bytes 3538952 | tf_op jit(solution)/shard_map/ppermute | solution.py:363
  33.9 17.2 %collective-permute-start = (bf16[192,3072]{1,0:T(8,128)(2,1)}, bf16[192,3072]{1,0:T(8,128)(2,1)S(1)}, u32[]{:S(2)}, u32[]{:S(2)}) collective-permute-start(bf16[192,3072]{1,0:T(8,128)(2,1)} %get-tuple-element.32), channel_id=1, source_target_pairs={{0,1},{1,0},{2,3},{3,2},{4,5},{5,4},{6,7},{7,6},{8,9},{9,8},{10,11... | collective-permute-start | bytes 3538952 | tf_op jit(solution)/shard_map/ppermute | solution.py:364
  37.7 13.9 %copy-start.3 = (f32[192,3072]{1,0:T(8,128)S(1)}, f32[192,3072]{1,0:T(8,128)}, u32[]{:S(2)}) copy-start(f32[192,3072]{1,0:T(8,128)} %get-tuple-element.31) | copy-start | bytes 7077892
  37.7 13.9 %collective-permute-start.2 = (bf16[48,3072]{1,0:T(8,128)(2,1)S(1)}, bf16[48,3072]{1,0:T(8,128)(2,1)S(1)}, u32[]{:S(2)}, u32[]{:S(2)}) collective-permute-start(bf16[48,3072]{1,0:T(8,128)(2,1)S(1)} %add_convert_fusion.1), channel_id=1, source_target_pairs={{0,2},{1,31},{2,0},{3,5},{4,6},{5,3},{6,4},{7,9},{8,10},{9,7},{10,... | collective-permute-start | bytes 884744 | tf_op jit(solution)/shard_map/ppermute | solution.py:368
  49.1 18.2 %collective-permute-start.4 = (bf16[144,3072]{1,0:T(8,128)(2,1)S(1)}, bf16[144,3072]{1,0:T(8,128)(2,1)S(1)}, u32[]{:S(2)}, u32[]{:S(2)}) collective-permute-start(bf16[144,3072]{1,0:T(8,128)(2,1)S(1)} %add_convert_fusion), channel_id=1, source_target_pairs={{0,2},{1,31},{2,0},{3,5},{4,6},{5,3},{6,4},{7,9},{8,10},{9,7},{10,... | collective-permute-start | bytes 2654216 | tf_op jit(solution)/shard_map/ppermute | solution.py:369
  51.7 15.7 %collective-permute-start.3 = (bf16[24,3072]{1,0:T(8,128)(2,1)S(1)}, bf16[24,3072]{1,0:T(8,128)(2,1)S(1)}, u32[]{:S(2)}, u32[]{:S(2)}) collective-permute-start(bf16[24,3072]{1,0:T(8,128)(2,1)S(1)} %get-tuple-element.52), channel_id=1, source_target_pairs={{0,4},{1,29},{2,6},{3,31},{4,8},{5,1},{6,10},{7,3},{8,12},{9,5},{1... | collective-permute-start | bytes 442376 | tf_op jit(solution)/shard_map/ppermute | solution.py:385
  57.0 16.5 %collective-permute-start.8 = (bf16[24,3072]{1,0:T(8,128)(2,1)S(1)}, bf16[24,3072]{1,0:T(8,128)(2,1)S(1)}, u32[]{:S(2)}, u32[]{:S(2)}) collective-permute-start(bf16[24,3072]{1,0:T(8,128)(2,1)S(1)} %get-tuple-element.53), channel_id=1, source_target_pairs={{4,0},{29,1},{6,2},{31,3},{8,4},{1,5},{10,6},{3,7},{12,8},{5,9},{1... | collective-permute-start | bytes 442376 | tf_op jit(solution)/shard_map/ppermute | solution.py:389
  67.4 8.8 %collective-permute-start.5 = (bf16[24,3072]{1,0:T(8,128)(2,1)S(1)}, bf16[24,3072]{1,0:T(8,128)(2,1)S(1)}, u32[]{:S(2)}, u32[]{:S(2)}) collective-permute-start(bf16[24,3072]{1,0:T(8,128)(2,1)S(1)} %add_convert_fusion.7), channel_id=1, source_target_pairs={{0,4},{1,29},{2,6},{3,31},{4,8},{5,1},{6,10},{7,3},{8,12},{9,5},{1... | collective-permute-start | bytes 442376 | tf_op jit(solution)/shard_map/ppermute | solution.py:385
  73.6 10.3 %collective-permute-start.9 = (bf16[24,3072]{1,0:T(8,128)(2,1)S(1)}, bf16[24,3072]{1,0:T(8,128)(2,1)S(1)}, u32[]{:S(2)}, u32[]{:S(2)}) collective-permute-start(bf16[24,3072]{1,0:T(8,128)(2,1)S(1)} %add_convert_fusion.3), channel_id=1, source_target_pairs={{4,0},{29,1},{6,2},{31,3},{8,4},{1,5},{10,6},{3,7},{12,8},{5,9},{1... | collective-permute-start | bytes 442376 | tf_op jit(solution)/shard_map/ppermute | solution.py:389
  76.3 10.1 %collective-permute-start.6 = (bf16[24,3072]{1,0:T(8,128)(2,1)S(1)}, bf16[24,3072]{1,0:T(8,128)(2,1)S(1)}, u32[]{:S(2)}, u32[]{:S(2)}) collective-permute-start(bf16[24,3072]{1,0:T(8,128)(2,1)S(1)} %add_convert_fusion.6), channel_id=1, source_target_pairs={{0,4},{1,29},{2,6},{3,31},{4,8},{5,1},{6,10},{7,3},{8,12},{9,5},{1... | collective-permute-start | bytes 442376 | tf_op jit(solution)/shard_map/ppermute | solution.py:385
  83.9 8.6 %collective-permute-start.10 = (bf16[24,3072]{1,0:T(8,128)(2,1)S(1)}, bf16[24,3072]{1,0:T(8,128)(2,1)S(1)}, u32[]{:S(2)}, u32[]{:S(2)}) collective-permute-start(bf16[24,3072]{1,0:T(8,128)(2,1)S(1)} %add_convert_fusion.2), channel_id=1, source_target_pairs={{4,0},{29,1},{6,2},{31,3},{8,4},{1,5},{10,6},{3,7},{12,8},{5,9},{1... | collective-permute-start | bytes 442376 | tf_op jit(solution)/shard_map/ppermute | solution.py:389
  86.5 9.6 %collective-permute-start.7 = (bf16[24,3072]{1,0:T(8,128)(2,1)S(1)}, bf16[24,3072]{1,0:T(8,128)(2,1)S(1)}, u32[]{:S(2)}, u32[]{:S(2)}) collective-permute-start(bf16[24,3072]{1,0:T(8,128)(2,1)S(1)} %add_convert_fusion.5), channel_id=1, source_target_pairs={{0,4},{1,29},{2,6},{3,31},{4,8},{5,1},{6,10},{7,3},{8,12},{9,5},{1... | collective-permute-start | bytes 442376 | tf_op jit(solution)/shard_map/ppermute | solution.py:385
  96.4 11.3 %collective-permute-start.11 = (bf16[24,3200]{1,0:T(8,128)(2,1)S(1)}, bf16[24,3200]{1,0:T(8,128)(2,1)S(1)}, u32[]{:S(2)}, u32[]{:S(2)}) collective-permute-start(bf16[24,3200]{1,0:T(8,128)(2,1)S(1)} %pad_maximum_fusion.1.refs_3_), channel_id=1, source_target_pairs={{0,4},{1,29},{2,6},{3,31},{4,8},{5,1},{6,10},{7,3},{8,12},{9,5},{1... | collective-permute-start | bytes 460808 | tf_op jit(solution)/shard_map/ppermute | solution.py:404
  102.4 11.3 %collective-permute-start.15 = (bf16[24,3200]{1,0:T(8,128)(2,1)S(1)}, bf16[24,3200]{1,0:T(8,128)(2,1)S(1)}, u32[]{:S(2)}, u32[]{:S(2)}) collective-permute-start(bf16[24,3200]{1,0:T(8,128)(2,1)S(1)} %pad_maximum_fusion.1.refs_3_), channel_id=1, source_target_pairs={{4,0},{29,1},{6,2},{31,3},{8,4},{1,5},{10,6},{3,7},{12,8},{5,9},{1... | collective-permute-start | bytes 460808 | tf_op jit(solution)/shard_map/ppermute | solution.py:407
  107.7 8.6 %collective-permute-start.12 = (bf16[24,3200]{1,0:T(8,128)(2,1)S(1)}, bf16[24,3200]{1,0:T(8,128)(2,1)S(1)}, u32[]{:S(2)}, u32[]{:S(2)}) collective-permute-start(bf16[24,3200]{1,0:T(8,128)(2,1)S(1)} %collective-permute-done.11.refs_2_), channel_id=1, source_target_pairs={{0,4},{1,29},{2,6},{3,31},{4,8},{5,1},{6,10},{7,3},{8,12},{9,5},{1... | collective-permute-start | bytes 460808 | tf_op jit(solution)/shard_map/ppermute | solution.py:404
  113.6 10.2 %collective-permute-start.16 = (bf16[24,3200]{1,0:T(8,128)(2,1)S(1)}, bf16[24,3200]{1,0:T(8,128)(2,1)S(1)}, u32[]{:S(2)}, u32[]{:S(2)}) collective-permute-start(bf16[24,3200]{1,0:T(8,128)(2,1)S(1)} %collective-permute-done.15.refs_4_), channel_id=1, source_target_pairs={{4,0},{29,1},{6,2},{31,3},{8,4},{1,5},{10,6},{3,7},{12,8},{5,9},{1... | collective-permute-start | bytes 460808 | tf_op jit(solution)/shard_map/ppermute | solution.py:407
  116.3 9.8 %collective-permute-start.13 = (bf16[24,3200]{1,0:T(8,128)(2,1)S(1)}, bf16[24,3200]{1,0:T(8,128)(2,1)S(1)}, u32[]{:S(2)}, u32[]{:S(2)}) collective-permute-start(bf16[24,3200]{1,0:T(8,128)(2,1)S(1)} %collective-permute-done.12.refs_1_), channel_id=1, source_target_pairs={{0,4},{1,29},{2,6},{3,31},{4,8},{5,1},{6,10},{7,3},{8,12},{9,5},{1... | collective-permute-start | bytes 460808 | tf_op jit(solution)/shard_map/ppermute | solution.py:404
  123.9 9.7 %collective-permute-start.17 = (bf16[24,3200]{1,0:T(8,128)(2,1)S(1)}, bf16[24,3200]{1,0:T(8,128)(2,1)S(1)}, u32[]{:S(2)}, u32[]{:S(2)}) collective-permute-start(bf16[24,3200]{1,0:T(8,128)(2,1)S(1)} %collective-permute-done.16.refs_5_), channel_id=1, source_target_pairs={{4,0},{29,1},{6,2},{31,3},{8,4},{1,5},{10,6},{3,7},{12,8},{5,9},{1... | collective-permute-start | bytes 460808 | tf_op jit(solution)/shard_map/ppermute | solution.py:407
  126.2 11.6 %collective-permute-start.14 = (bf16[24,3200]{1,0:T(8,128)(2,1)S(1)}, bf16[24,3200]{1,0:T(8,128)(2,1)S(1)}, u32[]{:S(2)}, u32[]{:S(2)}) collective-permute-start(bf16[24,3200]{1,0:T(8,128)(2,1)S(1)} %collective-permute-done.13.refs_0_), channel_id=1, source_target_pairs={{0,4},{1,29},{2,6},{3,31},{4,8},{5,1},{6,10},{7,3},{8,12},{9,5},{1... | collective-permute-start | bytes 460808 | tf_op jit(solution)/shard_map/ppermute | solution.py:404
  133.7 20.3 %collective-permute-start.19 = (bf16[168,3200]{1,0:T(8,128)(2,1)S(1)}, bf16[168,3200]{1,0:T(8,128)(2,1)S(1)}, u32[]{:S(2)}, u32[]{:S(2)}) collective-permute-start(bf16[168,3200]{1,0:T(8,128)(2,1)S(1)} %shard_map.147), channel_id=1, source_target_pairs={{0,2},{1,31},{2,0},{3,5},{4,6},{5,3},{6,4},{7,9},{8,10},{9,7},{10,... | collective-permute-start | bytes 3225608 | tf_op jit(solution)/shard_map/ppermute | solution.py:411
  137.8 16.2 %collective-permute-start.18 = (bf16[24,3200]{1,0:T(8,128)(2,1)S(1)}, bf16[24,3200]{1,0:T(8,128)(2,1)S(1)}, u32[]{:S(2)}, u32[]{:S(2)}) collective-permute-start(bf16[24,3200]{1,0:T(8,128)(2,1)S(1)} %collective-permute-done.14), channel_id=1, source_target_pairs={{0,2},{1,31},{2,0},{3,5},{4,6},{5,3},{6,4},{7,9},{8,10},{9,7},{10,... | collective-permute-start | bytes 460808 | tf_op jit(solution)/shard_map/ppermute | solution.py:412
  143.2 11.0 %copy-start = (bf16[192,3200]{1,0:T(8,128)(2,1)}, bf16[192,3200]{1,0:T(8,128)(2,1)S(1)}, u32[]{:S(2)}) copy-start(bf16[192,3200]{1,0:T(8,128)(2,1)S(1)} %pad_maximum_fusion.g0) | copy-start | bytes 3686404
  143.2 16.4 %collective-permute-start.20 = (bf16[192,3200]{1,0:T(8,128)(2,1)S(1)}, bf16[192,3200]{1,0:T(8,128)(2,1)}, u32[]{:S(2)}, u32[]{:S(2)}) collective-permute-start(bf16[192,3200]{1,0:T(8,128)(2,1)S(1)} %pad_maximum_fusion.g0), channel_id=1, source_target_pairs={{0,1},{1,0},{2,3},{3,2},{4,5},{5,4},{6,7},{7,6},{8,9},{9,8},{10,11... | collective-permute-start | bytes 3686408 | tf_op jit(solution)/shard_map/ppermute | solution.py:414
  154.2 7.9 %copy-start.2 = (bf16[192,3200]{1,0:T(8,128)(2,1)}, bf16[192,3200]{1,0:T(8,128)(2,1)S(1)}, u32[]{:S(2)}) copy-start(bf16[192,3200]{1,0:T(8,128)(2,1)S(1)} %constant_dynamic-update-slice_fusion.g1) | copy-start | bytes 3686404
  154.2 7.9 %collective-permute-start.21 = (bf16[192,3200]{1,0:T(8,128)(2,1)S(1)}, bf16[192,3200]{1,0:T(8,128)(2,1)}, u32[]{:S(2)}, u32[]{:S(2)}) collective-permute-start(bf16[192,3200]{1,0:T(8,128)(2,1)S(1)} %constant_dynamic-update-slice_fusion.g1), channel_id=1, source_target_pairs={{0,1},{1,0},{2,3},{3,2},{4,5},{5,4},{6,7},{7,6},{8,9},{9,8},{10,11... | collective-permute-start | bytes 3686408 | tf_op jit(solution)/shard_map/ppermute | solution.py:416
  169.8 19.2 %all-to-all-start.1 = ((bf16[16,232,128]{2,1,0:T(8,128)(2,1)}), bf16[16,232,128]{2,1,0:T(8,128)(2,1)S(1)}, u32[]{:S(2)}, u32[]{:S(2)}) async-start(bf16[16,232,128]{2,1,0:T(8,128)(2,1)} %get-tuple-element.40.after), calls=%async_computation.1 | async-start | bytes 1900544 | tf_op jit(solution)/shard_map/all_to_all | solution.py:425
  179.8 3.1 %collective-permute-start.22 = (f32[24,128]{1,0:T(8,128)S(1)}, f32[24,128]{1,0:T(8,128)S(1)}, u32[]{:S(2)}, u32[]{:S(2)}) collective-permute-start(f32[24,128]{1,0:T(8,128)S(1)} %slice_select_fusion), channel_id=1, source_target_pairs={{0,1},{1,0},{2,3},{3,2},{4,5},{5,4},{6,7},{7,6},{8,9},{9,8},{10,11... | collective-permute-start | bytes 36872 | tf_op jit(solution)/shard_map/ppermute | solution.py:430
  183.6 4.7 %collective-permute-start.23 = (f32[12,128]{1,0:T(8,128)S(1)}, f32[12,128]{1,0:T(8,128)S(1)}, u32[]{:S(2)}, u32[]{:S(2)}) collective-permute-start(f32[12,128]{1,0:T(8,128)S(1)} %slice_select_fusion.1), channel_id=1, source_target_pairs={{0,2},{1,3},{2,0},{3,1},{4,6},{5,7},{6,4},{7,5},{8,10},{9,11},{10,... | collective-permute-start | bytes 18440 | tf_op jit(solution)/shard_map/ppermute | solution.py:432
  189.0 0.9 copy-start.1
  191.9 22.8 %all-to-all-start.2 = ((bf16[16,16,128]{2,1,0:T(8,128)(2,1)}), bf16[16,16,128]{2,1,0:T(8,128)(2,1)S(1)}, u32[]{:S(2)}, u32[]{:S(2)}) async-start(bf16[16,16,128]{2,1,0:T(8,128)(2,1)} %get-tuple-element.45.after), calls=%async_computation.2 | async-start | bytes 131072 | tf_op jit(solution)/shard_map/all_to_all | solution.py:439
  214.7 6.4 %copy-start.5 = (bf16[16,16,128]{2,1,0:T(8,128)(2,1)}, bf16[16,16,128]{2,1,0:T(8,128)(2,1)S(1)}, u32[]{:S(2)}) copy-start(bf16[16,16,128]{2,1,0:T(8,128)(2,1)S(1)} %all-to-all-done.2.lines) | copy-start | bytes 196612
  214.7 6.4 %collective-permute-start.24 = (bf16[16,16,128]{2,1,0:T(8,128)(2,1)S(1)}, bf16[16,16,128]{2,1,0:T(8,128)(2,1)S(1)}, u32[]{:S(2)}, u32[]{:S(2)}) collective-permute-start(bf16[16,16,128]{2,1,0:T(8,128)(2,1)S(1)} %all-to-all-done.2.lines), channel_id=1, source_target_pairs={{0,1},{1,0},{2,3},{3,2},{4,5},{5,4},{6,7},{7,6},{8,9},{9,8},{10,11... | collective-permute-start | bytes 196616 | tf_op jit(solution)/shard_map/ppermute | solution.py:445
  221.1 0.6 copy-start.6

commit v9 on v8

--- a/solution.py
+++ b/solution.py
@@ -406,13 +406,14 @@
         if t <= back_hops:
             left = lax.ppermute(left, "tp", bwd)
             ring[t] = left
-    parts = ring[hops + 1 :] + ring[:hops]
+    parts = ring[hops + 1 :] + ring[: hops - 1]
     (most,) = call(stack_rows, [((len(parts) * piece, block.shape[1]), BF)], *parts, limit=8 * 2**20)
     most_o = lax.ppermute(most, "tp", pair)
+    left_o = lax.ppermute(ring[hops - 1], "tp", pair)
     last_o = lax.ppermute(ring[hops], "tp", pair)
-    kept = jnp.concatenate([ring[hops], most], 0)
+    kept = jnp.concatenate([ring[hops], most, ring[hops - 1]], 0)
     kept_x = lax.ppermute(kept, "tp", swap)
-    paired = jnp.concatenate([last_o, most_o], 0)
+    paired = jnp.concatenate([last_o, most_o, left_o], 0)
     paired_x = lax.ppermute(paired, "tp", swap)
     grads = (kept, paired, kept_x, paired_x)
 

time: 225 us -> 223 us (level)
  waiting for transfers between devices: 51.1 us -> 47.4 us
    ppermute x0 -> x1, starting transfers between devices: none -> 4.57 us  [body(): left_o = lax.ppermute(ring[hops - 1], 'tp', pair)]
    ppermute x1, starting transfers between devices: 5.42 us -> 2.2 us  [body(): paired_x = lax.ppermute(paired, 'tp', swap)]
  transfers between devices with their start and end apart: 28 -> 29, of which waited for: 18 -> 16; matrix products, arithmetic and copies ran while one was open for 4% -> 4% of each run, Pallas kernels for 4% -> 4%
where the time goes in v9:
time: 223 us; the launch traced here: 222 us
  starting transfers between devices  131 us (59%)
  waiting for transfers between devices  47.4 us (21%)
  Pallas kernels  30.8 us (14%)
  other arithmetic  7.57 us (3%)
  local copies, waits for them, and re-layouts  3.44 us (2%)
    ppermute x8, starting transfers between devices, body(): right = lax.ppermute(right, 'tp', fwd)  48.9 us
    pallas_call x7, Pallas kernels, call(): pl.pallas_call(kernel, out_shape=[jax.ShapeDtypeStruct(s, d) for s, d in...  22.6 us
    ppermute x8, waiting for transfers between devices, body(): right = lax.ppermute(right, 'tp', fwd)  17.6 us
    ppermute x6, starting transfers between devices, body(): left = lax.ppermute(left, 'tp', bwd)  11.7 us
    all_to_all x1, starting transfers between devices, body(): lax.all_to_all(lines, 'tp', 0, 0, axis_index_groups=same_core, tiled=True)  11.5 us
    ppermute x1, starting transfers between devices, body(): par_a = lax.ppermute(to_a, 'tp', pair)  9.78 us
    all_to_all x1, waiting for transfers between devices, body(): lax.all_to_all(lines, 'tp', 0, 0, axis_index_groups=same_core, tiled=True)  8.85 us
    pallas_call x1, Pallas kernels, body(): pl.pallas_call(functools.partial(project, sizes), out_shape=[jax.ShapeDty...  8.17 us
  transfers between devices with their start and end apart: 29, of which 16 were waited for; matrix products, arithmetic and copies ran while one was open for 4% of the time, Pallas kernels for 4%

profile of v9, /device:TPU:1, one launch (start us, length us, event | category | flops | bytes accessed | tf_op | source)
XLA Modules:
  0.0 221.7 jit_solution(12370585678471510959)
XLA Ops:
  0.6 3.0 %shard_map.145 = (bf16[640,256]{1,0:T(8,128)(2,1)}, bf16[192,256]{1,0:T(8,128)(2,1)}) custom-call(bf16[192,128]{1,0:T(8,128)(2,1)} %tokens.1, bf16[192,128]{1,0:T(8,128)(2,1)} %cotangent.1, s32[2,192]{1,0:T(2,128)} %bitcast.14, bf16[2,192]{1,0:T(2,128)(2,1)} %bitcast.16), custom_call_target="tpu_custom_call" | custom-call | tf_op jit(solution)/shard_map/pallas_call | solution.py:30
  3.6 7.6 %all-to-all-start = ((bf16[16,40,256]{2,1,0:T(8,128)(2,1)}), bf16[16,40,256]{2,1,0:T(8,128)(2,1)S(1)}, u32[]{:S(2)}, u32[]{:S(2)}) async-start(bf16[16,40,256]{2,1,0:T(8,128)(2,1)} %bitcast.13), calls=%async_computation | async-start | bytes 655360 | tf_op jit(solution)/shard_map/all_to_all | solution.py:342
  11.9 7.2 %all-to-all-done = bf16[16,40,256]{2,1,0:T(8,128)(2,1)S(1)} async-done(((bf16[16,40,256]{2,1,0:T(8,128)(2,1)}), bf16[16,40,256]{2,1,0:T(8,128)(2,1)S(1)}, u32[]{:S(2)}, u32[]{:S(2)}) %all-to-all-start) | async-done | bytes 327712 | tf_op jit(solution)/shard_map/all_to_all | solution.py:342
  19.8 8.2 %shard_map.146 = (f32[192,3072]{1,0:T(8,128)}, f32[192,3072]{1,0:T(8,128)}, bf16[192,3072]{1,0:T(8,128)(2,1)}, bf16[192,3072]{1,0:T(8,128)(2,1)}, bf16[256,768]{...) custom-call(s32[2]{0:T(128)} %pad_add_fusion.pos, ...), custom_call_target="tpu_custom_call" | custom-call | tf_op jit(solution)/shard_map/pallas_call | solution.py:354
  28.0 5.8 %collective-permute-start.1 = (bf16[192,3072]{1,0:T(8,128)(2,1)}, bf16[192,3072]{1,0:T(8,128)(2,1)S(1)}, u32[]{:S(2)}, u32[]{:S(2)}) collective-permute-start(bf16[192,3072]{1,0:T(8,128)(2,1)} %get-tuple-element.34), channel_id=1, source_target_pairs={{0,1},{1,0},{2,3},{3,2},{4,5},{5,4},{6,7},{7,6},{8,9},{9,8},{10,11... | collective-permute-start | bytes 3538952 | tf_op jit(solution)/shard_map/ppermute | solution.py:363
  33.8 1.9 collective-permute-start
  36.5 1.1 add_convert_fusion.1
  37.6 9.8 %collective-permute-start.2 = (bf16[48,3072]{1,0:T(8,128)(2,1)S(1)}, bf16[48,3072]{1,0:T(8,128)(2,1)S(1)}, u32[]{:S(2)}, u32[]{:S(2)}) collective-permute-start(bf16[48,3072]{1,0:T(8,128)(2,1)S(1)} %add_convert_fusion.1), channel_id=1, source_target_pairs={{0,2},{1,31},{2,0},{3,5},{4,6},{5,3},{6,4},{7,9},{8,10},{9,7},{10,... | collective-permute-start | bytes 884744 | tf_op jit(solution)/shard_map/ppermute | solution.py:368
  47.4 1.6 add_convert_fusion
  49.1 1.9 collective-permute-start.4
  51.6 4.1 %collective-permute-start.3 = (bf16[24,3072]{1,0:T(8,128)(2,1)S(1)}, bf16[24,3072]{1,0:T(8,128)(2,1)S(1)}, u32[]{:S(2)}, u32[]{:S(2)}) collective-permute-start(bf16[24,3072]{1,0:T(8,128)(2,1)S(1)} %get-tuple-element.52), channel_id=1, source_target_pairs={{0,4},{1,29},{2,6},{3,31},{4,8},{5,1},{6,10},{7,3},{8,12},{9,5},{1... | collective-permute-start | bytes 442376 | tf_op jit(solution)/shard_map/ppermute | solution.py:385
  57.0 2.1 collective-permute-start.8
  59.1 8.2 %collective-permute-done.3 = bf16[24,3072]{1,0:T(8,128)(2,1)S(1)} collective-permute-done((bf16[24,3072]{1,0:T(8,128)(2,1)S(1)}, bf16[24,3072]{1,0:T(8,128)(2,1)S(1)}, u32[]{:S(2)}, u32[]{:S(2)}) %collective-permute-start.3) | collective-permute-done | bytes 147488 | tf_op jit(solution)/shard_map/ppermute | solution.py:385
  67.4 6.0 %collective-permute-start.5 = (bf16[24,3072]{1,0:T(8,128)(2,1)S(1)}, bf16[24,3072]{1,0:T(8,128)(2,1)S(1)}, u32[]{:S(2)}, u32[]{:S(2)}) collective-permute-start(bf16[24,3072]{1,0:T(8,128)(2,1)S(1)} %add_convert_fusion.7), channel_id=1, source_target_pairs={{0,4},{1,29},{2,6},{3,31},{4,8},{5,1},{6,10},{7,3},{8,12},{9,5},{1... | collective-permute-start | bytes 442376 | tf_op jit(solution)/shard_map/ppermute | solution.py:385
  73.5 1.9 collective-permute-start.9
  76.3 7.5 %collective-permute-start.6 = (bf16[24,3072]{1,0:T(8,128)(2,1)S(1)}, bf16[24,3072]{1,0:T(8,128)(2,1)S(1)}, u32[]{:S(2)}, u32[]{:S(2)}) collective-permute-start(bf16[24,3072]{1,0:T(8,128)(2,1)S(1)} %add_convert_fusion.6), channel_id=1, source_target_pairs={{0,4},{1,29},{2,6},{3,31},{4,8},{5,1},{6,10},{7,3},{8,12},{9,5},{1... | collective-permute-start | bytes 442376 | tf_op jit(solution)/shard_map/ppermute | solution.py:385
  83.9 1.9 collective-permute-start.10
  86.5 6.0 %collective-permute-start.7 = (bf16[24,3072]{1,0:T(8,128)(2,1)S(1)}, bf16[24,3072]{1,0:T(8,128)(2,1)S(1)}, u32[]{:S(2)}, u32[]{:S(2)}) collective-permute-start(bf16[24,3072]{1,0:T(8,128)(2,1)S(1)} %add_convert_fusion.5), channel_id=1, source_target_pairs={{0,4},{1,29},{2,6},{3,31},{4,8},{5,1},{6,10},{7,3},{8,12},{9,5},{1... | collective-permute-start | bytes 442376 | tf_op jit(solution)/shard_map/ppermute | solution.py:385
  92.5 3.5 %collective-permute-done.7 = bf16[24,3072]{1,0:T(8,128)(2,1)S(1)} collective-permute-done((bf16[24,3072]{1,0:T(8,128)(2,1)S(1)}, bf16[24,3072]{1,0:T(8,128)(2,1)S(1)}, u32[]{:S(2)}, u32[]{:S(2)}) %collective-permute-start.7) | collective-permute-done | bytes 147488 | tf_op jit(solution)/shard_map/ppermute | solution.py:385
  96.4 5.9 %collective-permute-start.11 = (bf16[24,3200]{1,0:T(8,128)(2,1)S(1)}, bf16[24,3200]{1,0:T(8,128)(2,1)S(1)}, u32[]{:S(2)}, u32[]{:S(2)}) collective-permute-start(bf16[24,3200]{1,0:T(8,128)(2,1)S(1)} %pad_maximum_fusion.1.refs_3_), channel_id=1, source_target_pairs={{0,4},{1,29},{2,6},{3,31},{4,8},{5,1},{6,10},{7,3},{8,12},{9,5},{1... | collective-permute-start | bytes 460808 | tf_op jit(solution)/shard_map/ppermute | solution.py:404
  102.3 1.9 collective-permute-start.15
  104.2 3.4 %collective-permute-done.11.refs_2_ = bf16[24,3200]{1,0:T(8,128)(2,1)S(1)} collective-permute-done((bf16[24,3200]{1,0:T(8,128)(2,1)S(1)}, bf16[24,3200]{1,0:T(8,128)(2,1)S(1)}, u32[]{:S(2)}, u32[]{:S(2)}) %collective-permute-start.11) | collective-permute-done | bytes 153632 | tf_op jit(solution)/shard_map/ppermute | solution.py:404
  107.7 5.9 %collective-permute-start.12 = (bf16[24,3200]{1,0:T(8,128)(2,1)S(1)}, bf16[24,3200]{1,0:T(8,128)(2,1)S(1)}, u32[]{:S(2)}, u32[]{:S(2)}) collective-permute-start(bf16[24,3200]{1,0:T(8,128)(2,1)S(1)} %collective-permute-done.11.refs_2_), channel_id=1, source_target_pairs={{0,4},{1,29},{2,6},{3,31},{4,8},{5,1},{6,10},{7,3},{8,12},{9,5},{1... | collective-permute-start | bytes 460808 | tf_op jit(solution)/shard_map/ppermute | solution.py:404
  113.6 1.9 collective-permute-start.16
  116.2 7.6 %collective-permute-start.13 = (bf16[24,3200]{1,0:T(8,128)(2,1)S(1)}, bf16[24,3200]{1,0:T(8,128)(2,1)S(1)}, u32[]{:S(2)}, u32[]{:S(2)}) collective-permute-start(bf16[24,3200]{1,0:T(8,128)(2,1)S(1)} %collective-permute-done.12.refs_1_), channel_id=1, source_target_pairs={{0,4},{1,29},{2,6},{3,31},{4,8},{5,1},{6,10},{7,3},{8,12},{9,5},{1... | collective-permute-start | bytes 460808 | tf_op jit(solution)/shard_map/ppermute | solution.py:404
  123.8 1.9 collective-permute-start.17
  126.1 5.9 %collective-permute-start.14 = (bf16[24,3200]{1,0:T(8,128)(2,1)S(1)}, bf16[24,3200]{1,0:T(8,128)(2,1)S(1)}, u32[]{:S(2)}, u32[]{:S(2)}) collective-permute-start(bf16[24,3200]{1,0:T(8,128)(2,1)S(1)} %collective-permute-done.13.refs_0_), channel_id=1, source_target_pairs={{0,4},{1,29},{2,6},{3,31},{4,8},{5,1},{6,10},{7,3},{8,12},{9,5},{1... | collective-permute-start | bytes 460808 | tf_op jit(solution)/shard_map/ppermute | solution.py:404
  132.1 1.9 collective-permute-start.19
  134.0 4.6 %collective-permute-start.20 = (bf16[24,3200]{1,0:T(8,128)(2,1)S(1)}, bf16[24,3200]{1,0:T(8,128)(2,1)S(1)}, u32[]{:S(2)}, u32[]{:S(2)}) collective-permute-start(bf16[24,3200]{1,0:T(8,128)(2,1)S(1)} %collective-permute-done.17), channel_id=1, source_target_pairs={{0,2},{1,31},{2,0},{3,5},{4,6},{5,3},{6,4},{7,9},{8,10},{9,7},{10,... | collective-permute-start | bytes 460808 | tf_op jit(solution)/shard_map/ppermute | solution.py:412
  138.6 4.3 %collective-permute-start.18 = (bf16[24,3200]{1,0:T(8,128)(2,1)S(1)}, bf16[24,3200]{1,0:T(8,128)(2,1)S(1)}, u32[]{:S(2)}, u32[]{:S(2)}) collective-permute-start(bf16[24,3200]{1,0:T(8,128)(2,1)S(1)} %collective-permute-done.14), channel_id=1, source_target_pairs={{0,2},{1,31},{2,0},{3,5},{4,6},{5,3},{6,4},{7,9},{8,10},{9,7},{10,... | collective-permute-start | bytes 460808 | tf_op jit(solution)/shard_map/ppermute | solution.py:413
  143.1 4.6 %collective-permute-start.21 = (bf16[192,3200]{1,0:T(8,128)(2,1)S(1)}, bf16[192,3200]{1,0:T(8,128)(2,1)}, u32[]{:S(2)}, u32[]{:S(2)}) collective-permute-start(bf16[192,3200]{1,0:T(8,128)(2,1)S(1)} %pad_maximum_fusion.g0), channel_id=1, source_target_pairs={{0,1},{1,0},{2,3},{3,2},{4,5},{5,4},{6,7},{7,6},{8,9},{9,8},{10,11... | collective-permute-start | bytes 3686408 | tf_op jit(solution)/shard_map/ppermute | solution.py:415
  147.6 6.2 %collective-permute-done.18 = bf16[24,3200]{1,0:T(8,128)(2,1)S(1)} collective-permute-done((bf16[24,3200]{1,0:T(8,128)(2,1)S(1)}, bf16[24,3200]{1,0:T(8,128)(2,1)S(1)}, u32[]{:S(2)}, u32[]{:S(2)}) %collective-permute-start.18) | collective-permute-done | bytes 153632 | tf_op jit(solution)/shard_map/ppermute | solution.py:413
  154.0 2.2 collective-permute-start.22
  156.3 2.7 %collective-permute-done.22.g3 = bf16[192,3200]{1,0:T(8,128)(2,1)} collective-permute-done((bf16[192,3200]{1,0:T(8,128)(2,1)S(1)}, bf16[192,3200]{1,0:T(8,128)(2,1)}, u32[]{:S(2)}, u32[]{:S(2)}) %collective-permute-start.22) | collective-permute-done | bytes 1228832 | tf_op jit(solution)/shard_map/ppermute | solution.py:417
  159.0 7.7 %shard_map.148 = (bf16[16,232,128]{2,1,0:T(8,128)(2,1)}, f32[192,128]{1,0:T(8,128)}) custom-call(s32[2]{0:T(128)} %pad_add_fusion.pos, bf16[192,3200]{1,0:T(8,128)(2,1)} %copy-done, bf16[192,3200]{1,0:T(8,128)(2,1)} %copy-done.2, bf16[192,3200]{1,0:T(8,128)(2,1)} %collective-permute-done.21.g2, bf16[192,3200]{1,0:T(8,128)(2,1)} %collective-permute-done.22.g3, ...), custom_call_target="tpu_custom_call" | custom-call | tf_op jit(solution)/shard_map/pallas_call | solution.py:30
  166.7 3.6 %all-to-all-start.1 = ((bf16[16,232,128]{2,1,0:T(8,128)(2,1)}), bf16[16,232,128]{2,1,0:T(8,128)(2,1)S(1)}, u32[]{:S(2)}, u32[]{:S(2)}) async-start(bf16[16,232,128]{2,1,0:T(8,128)(2,1)} %get-tuple-element.40.after), calls=%async_computation.1 | async-start | bytes 1900544 | tf_op jit(solution)/shard_map/all_to_all | solution.py:426
  170.4 5.6 %shard_map.149 = (bf16[3,2,128,1024]{3,2,1,0:T(8,128)(2,1)}, f32[48,128]{1,0:T(8,128)}) custom-call(bf16[192,3200]{1,0:T(8,128)(2,1)} %copy-done, bf16[192,3200]{1,0:T(8,128)(2,1)} %copy-done.2, bf16[192,3200]{1,0:T(8,128)(2,1)} %collective-permute-done.21.g2, bf16[192,3200]{1,0:T(8,128)(2,1)} %collective-permute-done.22.g3, ...), custom_call_target="tpu_custom_call" | custom-call | tf_op jit(solution)/shard_map/pallas_call | solution.py:30
  176.7 2.0 collective-permute-start.23
  180.5 3.4 %collective-permute-start.24 = (f32[12,128]{1,0:T(8,128)S(1)}, f32[12,128]{1,0:T(8,128)S(1)}, u32[]{:S(2)}, u32[]{:S(2)}) collective-permute-start(f32[12,128]{1,0:T(8,128)S(1)} %slice_select_fusion.1), channel_id=1, source_target_pairs={{0,2},{1,3},{2,0},{3,1},{4,6},{5,7},{6,4},{7,5},{8,10},{9,11},{10,... | collective-permute-start | bytes 18440 | tf_op jit(solution)/shard_map/ppermute | solution.py:433
  183.9 1.0 collective-permute-done.24
  185.5 1.5 all-to-all-done.1.home
  188.0 2.0 shard_map.150
  190.0 11.5 %all-to-all-start.2 = ((bf16[16,16,128]{2,1,0:T(8,128)(2,1)}), bf16[16,16,128]{2,1,0:T(8,128)(2,1)S(1)}, u32[]{:S(2)}, u32[]{:S(2)}) async-start(bf16[16,16,128]{2,1,0:T(8,128)(2,1)} %get-tuple-element.45.after), calls=%async_computation.2 | async-start | bytes 131072 | tf_op jit(solution)/shard_map/all_to_all | solution.py:440
  201.5 2.7 %shard_map.151 = (bf16[192,128]{1,0:T(8,128)(2,1)}, f32[2,192]{1,0:T(2,128)}) custom-call(bf16[16,232,128]{2,1,0:T(8,128)(2,1)} %copy-done.1, f32[192,128]{1,0:T(8,128)} %get-tuple-element.41.shared, s32[2,192]{1,0:T(2,128)} %bitcast.15, bf16[16,16,128]{2,1,0:T(8,128)(2,1)} %get-tuple-element.45.after), custom_call_target="tpu_custom_call" | custom-call | tf_op jit(solution)/shard_map/pallas_call | solution.py:30
  204.2 8.9 %all-to-all-done.2.lines = bf16[16,16,128]{2,1,0:T(8,128)(2,1)S(1)} async-done(((bf16[16,16,128]{2,1,0:T(8,128)(2,1)}), bf16[16,16,128]{2,1,0:T(8,128)(2,1)S(1)}, u32[]{:S(2)}, u32[]{:S(2)}) %all-to-all-start.2) | async-done | bytes 65568 | tf_op jit(solution)/shard_map/all_to_all | solution.py:440
  213.1 5.2 %collective-permute-start.25 = (bf16[16,16,128]{2,1,0:T(8,128)(2,1)S(1)}, bf16[16,16,128]{2,1,0:T(8,128)(2,1)S(1)}, u32[]{:S(2)}, u32[]{:S(2)}) collective-permute-start(bf16[16,16,128]{2,1,0:T(8,128)(2,1)S(1)} %all-to-all-done.2.lines), channel_id=1, source_target_pairs={{0,1},{1,0},{2,3},{3,2},{4,5},{5,4},{6,7},{7,6},{8,9},{9,8},{10,11... | collective-permute-start | bytes 196616 | tf_op jit(solution)/shard_map/ppermute | solution.py:446
  218.2 1.2 convert_bitcast_fusion
  220.1 1.6 shard_map.152
  (61 shorter events, 12.0 us)
Async XLA Ops:
  3.6 15.5 %all-to-all-start = ((bf16[16,40,256]{2,1,0:T(8,128)(2,1)}), bf16[16,40,256]{2,1,0:T(8,128)(2,1)S(1)}, u32[]{:S(2)}, u32[]{:S(2)}) async-start(bf16[16,40,256]{2,1,0:T(8,128)(2,1)} %bitcast.13), calls=%async_computation | async-start | bytes 655360 | tf_op jit(solution)/shard_map/all_to_all | solution.py:342
  19.1 0.7 copy-start.4
  28.0 8.5 %collective-permute-start.1 = (bf16[192,3072]{1,0:T(8,128)(2,1)}, bf16[192,3072]{1,0:T(8,128)(2,1)S(1)}, u32[]{:S(2)}, u32[]{:S(2)}) collective-permute-start(bf16[192,3072]{1,0:T(8,128)(2,1)} %get-tuple-element.34), channel_id=1, source_target_pairs={{0,1},{1,0},{2,3},{3,2},{4,5},{5,4},{6,7},{7,6},{8,9},{9,8},{10,11... | collective-permute-start | bytes 3538952 | tf_op jit(solution)/shard_map/ppermute | solution.py:363
  33.8 17.2 %collective-permute-start = (bf16[192,3072]{1,0:T(8,128)(2,1)}, bf16[192,3072]{1,0:T(8,128)(2,1)S(1)}, u32[]{:S(2)}, u32[]{:S(2)}) collective-permute-start(bf16[192,3072]{1,0:T(8,128)(2,1)} %get-tuple-element.32), channel_id=1, source_target_pairs={{0,1},{1,0},{2,3},{3,2},{4,5},{5,4},{6,7},{7,6},{8,9},{9,8},{10,11... | collective-permute-start | bytes 3538952 | tf_op jit(solution)/shard_map/ppermute | solution.py:364
  37.6 13.9 %copy-start.3 = (f32[192,3072]{1,0:T(8,128)S(1)}, f32[192,3072]{1,0:T(8,128)}, u32[]{:S(2)}) copy-start(f32[192,3072]{1,0:T(8,128)} %get-tuple-element.31) | copy-start | bytes 7077892
  37.6 13.9 %collective-permute-start.2 = (bf16[48,3072]{1,0:T(8,128)(2,1)S(1)}, bf16[48,3072]{1,0:T(8,128)(2,1)S(1)}, u32[]{:S(2)}, u32[]{:S(2)}) collective-permute-start(bf16[48,3072]{1,0:T(8,128)(2,1)S(1)} %add_convert_fusion.1), channel_id=1, source_target_pairs={{0,2},{1,31},{2,0},{3,5},{4,6},{5,3},{6,4},{7,9},{8,10},{9,7},{10,... | collective-permute-start | bytes 884744 | tf_op jit(solution)/shard_map/ppermute | solution.py:368
  49.1 18.2 %collective-permute-start.4 = (bf16[144,3072]{1,0:T(8,128)(2,1)S(1)}, bf16[144,3072]{1,0:T(8,128)(2,1)S(1)}, u32[]{:S(2)}, u32[]{:S(2)}) collective-permute-start(bf16[144,3072]{1,0:T(8,128)(2,1)S(1)} %add_convert_fusion), channel_id=1, source_target_pairs={{0,2},{1,31},{2,0},{3,5},{4,6},{5,3},{6,4},{7,9},{8,10},{9,7},{10,... | collective-permute-start | bytes 2654216 | tf_op jit(solution)/shard_map/ppermute | solution.py:369
  51.6 15.7 %collective-permute-start.3 = (bf16[24,3072]{1,0:T(8,128)(2,1)S(1)}, bf16[24,3072]{1,0:T(8,128)(2,1)S(1)}, u32[]{:S(2)}, u32[]{:S(2)}) collective-permute-start(bf16[24,3072]{1,0:T(8,128)(2,1)S(1)} %get-tuple-element.52), channel_id=1, source_target_pairs={{0,4},{1,29},{2,6},{3,31},{4,8},{5,1},{6,10},{7,3},{8,12},{9,5},{1... | collective-permute-start | bytes 442376 | tf_op jit(solution)/shard_map/ppermute | solution.py:385
  57.0 16.5 %collective-permute-start.8 = (bf16[24,3072]{1,0:T(8,128)(2,1)S(1)}, bf16[24,3072]{1,0:T(8,128)(2,1)S(1)}, u32[]{:S(2)}, u32[]{:S(2)}) collective-permute-start(bf16[24,3072]{1,0:T(8,128)(2,1)S(1)} %get-tuple-element.53), channel_id=1, source_target_pairs={{4,0},{29,1},{6,2},{31,3},{8,4},{1,5},{10,6},{3,7},{12,8},{5,9},{1... | collective-permute-start | bytes 442376 | tf_op jit(solution)/shard_map/ppermute | solution.py:389
  67.4 8.8 %collective-permute-start.5 = (bf16[24,3072]{1,0:T(8,128)(2,1)S(1)}, bf16[24,3072]{1,0:T(8,128)(2,1)S(1)}, u32[]{:S(2)}, u32[]{:S(2)}) collective-permute-start(bf16[24,3072]{1,0:T(8,128)(2,1)S(1)} %add_convert_fusion.7), channel_id=1, source_target_pairs={{0,4},{1,29},{2,6},{3,31},{4,8},{5,1},{6,10},{7,3},{8,12},{9,5},{1... | collective-permute-start | bytes 442376 | tf_op jit(solution)/shard_map/ppermute | solution.py:385
  73.5 10.3 %collective-permute-start.9 = (bf16[24,3072]{1,0:T(8,128)(2,1)S(1)}, bf16[24,3072]{1,0:T(8,128)(2,1)S(1)}, u32[]{:S(2)}, u32[]{:S(2)}) collective-permute-start(bf16[24,3072]{1,0:T(8,128)(2,1)S(1)} %add_convert_fusion.3), channel_id=1, source_target_pairs={{4,0},{29,1},{6,2},{31,3},{8,4},{1,5},{10,6},{3,7},{12,8},{5,9},{1... | collective-permute-start | bytes 442376 | tf_op jit(solution)/shard_map/ppermute | solution.py:389
  76.3 10.1 %collective-permute-start.6 = (bf16[24,3072]{1,0:T(8,128)(2,1)S(1)}, bf16[24,3072]{1,0:T(8,128)(2,1)S(1)}, u32[]{:S(2)}, u32[]{:S(2)}) collective-permute-start(bf16[24,3072]{1,0:T(8,128)(2,1)S(1)} %add_convert_fusion.6), channel_id=1, source_target_pairs={{0,4},{1,29},{2,6},{3,31},{4,8},{5,1},{6,10},{7,3},{8,12},{9,5},{1... | collective-permute-start | bytes 442376 | tf_op jit(solution)/shard_map/ppermute | solution.py:385
  83.9 8.6 %collective-permute-start.10 = (bf16[24,3072]{1,0:T(8,128)(2,1)S(1)}, bf16[24,3072]{1,0:T(8,128)(2,1)S(1)}, u32[]{:S(2)}, u32[]{:S(2)}) collective-permute-start(bf16[24,3072]{1,0:T(8,128)(2,1)S(1)} %add_convert_fusion.2), channel_id=1, source_target_pairs={{4,0},{29,1},{6,2},{31,3},{8,4},{1,5},{10,6},{3,7},{12,8},{5,9},{1... | collective-permute-start | bytes 442376 | tf_op jit(solution)/shard_map/ppermute | solution.py:389
  86.5 9.6 %collective-permute-start.7 = (bf16[24,3072]{1,0:T(8,128)(2,1)S(1)}, bf16[24,3072]{1,0:T(8,128)(2,1)S(1)}, u32[]{:S(2)}, u32[]{:S(2)}) collective-permute-start(bf16[24,3072]{1,0:T(8,128)(2,1)S(1)} %add_convert_fusion.5), channel_id=1, source_target_pairs={{0,4},{1,29},{2,6},{3,31},{4,8},{5,1},{6,10},{7,3},{8,12},{9,5},{1... | collective-permute-start | bytes 442376 | tf_op jit(solution)/shard_map/ppermute | solution.py:385
  96.4 11.3 %collective-permute-start.11 = (bf16[24,3200]{1,0:T(8,128)(2,1)S(1)}, bf16[24,3200]{1,0:T(8,128)(2,1)S(1)}, u32[]{:S(2)}, u32[]{:S(2)}) collective-permute-start(bf16[24,3200]{1,0:T(8,128)(2,1)S(1)} %pad_maximum_fusion.1.refs_3_), channel_id=1, source_target_pairs={{0,4},{1,29},{2,6},{3,31},{4,8},{5,1},{6,10},{7,3},{8,12},{9,5},{1... | collective-permute-start | bytes 460808 | tf_op jit(solution)/shard_map/ppermute | solution.py:404
  102.3 11.3 %collective-permute-start.15 = (bf16[24,3200]{1,0:T(8,128)(2,1)S(1)}, bf16[24,3200]{1,0:T(8,128)(2,1)S(1)}, u32[]{:S(2)}, u32[]{:S(2)}) collective-permute-start(bf16[24,3200]{1,0:T(8,128)(2,1)S(1)} %pad_maximum_fusion.1.refs_3_), channel_id=1, source_target_pairs={{4,0},{29,1},{6,2},{31,3},{8,4},{1,5},{10,6},{3,7},{12,8},{5,9},{1... | collective-permute-start | bytes 460808 | tf_op jit(solution)/shard_map/ppermute | solution.py:407
  107.7 8.6 %collective-permute-start.12 = (bf16[24,3200]{1,0:T(8,128)(2,1)S(1)}, bf16[24,3200]{1,0:T(8,128)(2,1)S(1)}, u32[]{:S(2)}, u32[]{:S(2)}) collective-permute-start(bf16[24,3200]{1,0:T(8,128)(2,1)S(1)} %collective-permute-done.11.refs_2_), channel_id=1, source_target_pairs={{0,4},{1,29},{2,6},{3,31},{4,8},{5,1},{6,10},{7,3},{8,12},{9,5},{1... | collective-permute-start | bytes 460808 | tf_op jit(solution)/shard_map/ppermute | solution.py:404
  113.6 10.2 %collective-permute-start.16 = (bf16[24,3200]{1,0:T(8,128)(2,1)S(1)}, bf16[24,3200]{1,0:T(8,128)(2,1)S(1)}, u32[]{:S(2)}, u32[]{:S(2)}) collective-permute-start(bf16[24,3200]{1,0:T(8,128)(2,1)S(1)} %collective-permute-done.15.refs_4_), channel_id=1, source_target_pairs={{4,0},{29,1},{6,2},{31,3},{8,4},{1,5},{10,6},{3,7},{12,8},{5,9},{1... | collective-permute-start | bytes 460808 | tf_op jit(solution)/shard_map/ppermute | solution.py:407
  116.2 9.9 %collective-permute-start.13 = (bf16[24,3200]{1,0:T(8,128)(2,1)S(1)}, bf16[24,3200]{1,0:T(8,128)(2,1)S(1)}, u32[]{:S(2)}, u32[]{:S(2)}) collective-permute-start(bf16[24,3200]{1,0:T(8,128)(2,1)S(1)} %collective-permute-done.12.refs_1_), channel_id=1, source_target_pairs={{0,4},{1,29},{2,6},{3,31},{4,8},{5,1},{6,10},{7,3},{8,12},{9,5},{1... | collective-permute-start | bytes 460808 | tf_op jit(solution)/shard_map/ppermute | solution.py:404
  123.8 10.2 %collective-permute-start.17 = (bf16[24,3200]{1,0:T(8,128)(2,1)S(1)}, bf16[24,3200]{1,0:T(8,128)(2,1)S(1)}, u32[]{:S(2)}, u32[]{:S(2)}) collective-permute-start(bf16[24,3200]{1,0:T(8,128)(2,1)S(1)} %collective-permute-done.16.refs_5_), channel_id=1, source_target_pairs={{4,0},{29,1},{6,2},{31,3},{8,4},{1,5},{10,6},{3,7},{12,8},{5,9},{1... | collective-permute-start | bytes 460808 | tf_op jit(solution)/shard_map/ppermute | solution.py:407
  126.1 12.5 %collective-permute-start.14 = (bf16[24,3200]{1,0:T(8,128)(2,1)S(1)}, bf16[24,3200]{1,0:T(8,128)(2,1)S(1)}, u32[]{:S(2)}, u32[]{:S(2)}) collective-permute-start(bf16[24,3200]{1,0:T(8,128)(2,1)S(1)} %collective-permute-done.13.refs_0_), channel_id=1, source_target_pairs={{0,4},{1,29},{2,6},{3,31},{4,8},{5,1},{6,10},{7,3},{8,12},{9,5},{1... | collective-permute-start | bytes 460808 | tf_op jit(solution)/shard_map/ppermute | solution.py:404
  132.1 21.8 %collective-permute-start.19 = (bf16[144,3200]{1,0:T(8,128)(2,1)S(1)}, bf16[144,3200]{1,0:T(8,128)(2,1)S(1)}, u32[]{:S(2)}, u32[]{:S(2)}) collective-permute-start(bf16[144,3200]{1,0:T(8,128)(2,1)S(1)} %shard_map.147), channel_id=1, source_target_pairs={{0,2},{1,31},{2,0},{3,5},{4,6},{5,3},{6,4},{7,9},{8,10},{9,7},{10,... | collective-permute-start | bytes 2764808 | tf_op jit(solution)/shard_map/ppermute | solution.py:411
  134.0 20.0 %collective-permute-start.20 = (bf16[24,3200]{1,0:T(8,128)(2,1)S(1)}, bf16[24,3200]{1,0:T(8,128)(2,1)S(1)}, u32[]{:S(2)}, u32[]{:S(2)}) collective-permute-start(bf16[24,3200]{1,0:T(8,128)(2,1)S(1)} %collective-permute-done.17), channel_id=1, source_target_pairs={{0,2},{1,31},{2,0},{3,5},{4,6},{5,3},{6,4},{7,9},{8,10},{9,7},{10,... | collective-permute-start | bytes 460808 | tf_op jit(solution)/shard_map/ppermute | solution.py:412
  138.6 15.2 %collective-permute-start.18 = (bf16[24,3200]{1,0:T(8,128)(2,1)S(1)}, bf16[24,3200]{1,0:T(8,128)(2,1)S(1)}, u32[]{:S(2)}, u32[]{:S(2)}) collective-permute-start(bf16[24,3200]{1,0:T(8,128)(2,1)S(1)} %collective-permute-done.14), channel_id=1, source_target_pairs={{0,2},{1,31},{2,0},{3,5},{4,6},{5,3},{6,4},{7,9},{8,10},{9,7},{10,... | collective-permute-start | bytes 460808 | tf_op jit(solution)/shard_map/ppermute | solution.py:413
  143.0 11.0 %copy-start = (bf16[192,3200]{1,0:T(8,128)(2,1)}, bf16[192,3200]{1,0:T(8,128)(2,1)S(1)}, u32[]{:S(2)}) copy-start(bf16[192,3200]{1,0:T(8,128)(2,1)S(1)} %pad_maximum_fusion.g0) | copy-start | bytes 3686404
  143.1 13.2 %collective-permute-start.21 = (bf16[192,3200]{1,0:T(8,128)(2,1)S(1)}, bf16[192,3200]{1,0:T(8,128)(2,1)}, u32[]{:S(2)}, u32[]{:S(2)}) collective-permute-start(bf16[192,3200]{1,0:T(8,128)(2,1)S(1)} %pad_maximum_fusion.g0), channel_id=1, source_target_pairs={{0,1},{1,0},{2,3},{3,2},{4,5},{5,4},{6,7},{7,6},{8,9},{9,8},{10,11... | collective-permute-start | bytes 3686408 | tf_op jit(solution)/shard_map/ppermute | solution.py:415
  154.0 5.0 %copy-start.2 = (bf16[192,3200]{1,0:T(8,128)(2,1)}, bf16[192,3200]{1,0:T(8,128)(2,1)S(1)}, u32[]{:S(2)}) copy-start(bf16[192,3200]{1,0:T(8,128)(2,1)S(1)} %constant_dynamic-update-slice_fusion.g1) | copy-start | bytes 3686404
  154.0 4.9 %collective-permute-start.22 = (bf16[192,3200]{1,0:T(8,128)(2,1)S(1)}, bf16[192,3200]{1,0:T(8,128)(2,1)}, u32[]{:S(2)}, u32[]{:S(2)}) collective-permute-start(bf16[192,3200]{1,0:T(8,128)(2,1)S(1)} %constant_dynamic-update-slice_fusion.g1), channel_id=1, source_target_pairs={{0,1},{1,0},{2,3},{3,2},{4,5},{5,4},{6,7},{7,6},{8,9},{9,8},{10,11... | collective-permute-start | bytes 3686408 | tf_op jit(solution)/shard_map/ppermute | solution.py:417
  166.7 20.3 %all-to-all-start.1 = ((bf16[16,232,128]{2,1,0:T(8,128)(2,1)}), bf16[16,232,128]{2,1,0:T(8,128)(2,1)S(1)}, u32[]{:S(2)}, u32[]{:S(2)}) async-start(bf16[16,232,128]{2,1,0:T(8,128)(2,1)} %get-tuple-element.40.after), calls=%async_computation.1 | async-start | bytes 1900544 | tf_op jit(solution)/shard_map/all_to_all | solution.py:426
  176.7 3.1 %collective-permute-start.23 = (f32[24,128]{1,0:T(8,128)S(1)}, f32[24,128]{1,0:T(8,128)S(1)}, u32[]{:S(2)}, u32[]{:S(2)}) collective-permute-start(f32[24,128]{1,0:T(8,128)S(1)} %slice_select_fusion), channel_id=1, source_target_pairs={{0,1},{1,0},{2,3},{3,2},{4,5},{5,4},{6,7},{7,6},{8,9},{9,8},{10,11... | collective-permute-start | bytes 36872 | tf_op jit(solution)/shard_map/ppermute | solution.py:431
  180.5 4.4 %collective-permute-start.24 = (f32[12,128]{1,0:T(8,128)S(1)}, f32[12,128]{1,0:T(8,128)S(1)}, u32[]{:S(2)}, u32[]{:S(2)}) collective-permute-start(f32[12,128]{1,0:T(8,128)S(1)} %slice_select_fusion.1), channel_id=1, source_target_pairs={{0,2},{1,3},{2,0},{3,1},{4,6},{5,7},{6,4},{7,5},{8,10},{9,11},{10,... | collective-permute-start | bytes 18440 | tf_op jit(solution)/shard_map/ppermute | solution.py:433
  187.1 0.9 copy-start.1
  190.0 23.1 %all-to-all-start.2 = ((bf16[16,16,128]{2,1,0:T(8,128)(2,1)}), bf16[16,16,128]{2,1,0:T(8,128)(2,1)S(1)}, u32[]{:S(2)}, u32[]{:S(2)}) async-start(bf16[16,16,128]{2,1,0:T(8,128)(2,1)} %get-tuple-element.45.after), calls=%async_computation.2 | async-start | bytes 131072 | tf_op jit(solution)/shard_map/all_to_all | solution.py:440
  213.1 6.4 %copy-start.5 = (bf16[16,16,128]{2,1,0:T(8,128)(2,1)}, bf16[16,16,128]{2,1,0:T(8,128)(2,1)S(1)}, u32[]{:S(2)}) copy-start(bf16[16,16,128]{2,1,0:T(8,128)(2,1)S(1)} %all-to-all-done.2.lines) | copy-start | bytes 196612
  213.1 6.4 %collective-permute-start.25 = (bf16[16,16,128]{2,1,0:T(8,128)(2,1)S(1)}, bf16[16,16,128]{2,1,0:T(8,128)(2,1)S(1)}, u32[]{:S(2)}, u32[]{:S(2)}) collective-permute-start(bf16[16,16,128]{2,1,0:T(8,128)(2,1)S(1)} %all-to-all-done.2.lines), channel_id=1, source_target_pairs={{0,1},{1,0},{2,3},{3,2},{4,5},{5,4},{6,7},{7,6},{8,9},{9,8},{10,11... | collective-permute-start | bytes 196616 | tf_op jit(solution)/shard_map/ppermute | solution.py:446
  219.5 0.6 copy-start.6
